TPU v7x, 256 devices: a 4x2x16 block of a 4x16x16 slice. The times are simulated.
256 devices in a mesh: grp: 2 (over y), ep: 32 (over z, core), tp: 4 (over x).
Axes of the slice: x: 4, y: 2, z: 16, core: 2. Of those that a mesh axis runs over, the one named last changes fastest.
The devices are a block of a 4x16x16 slice.
Arguments:
- x_in: bfloat16 [4096, 2048], P(('grp', 'ep')), parts along dimension 0, may hold values from -6 to 6
- state: float32 [4096, 96, 128], P(('grp', 'ep'), 'tp'), parts along dimension 0, may hold values from -6 to 6
- routes: int32 [4096, 2], P(('grp', 'ep')), parts along dimension 0, may hold values from 0 to 63, as said below
- w_in: bfloat16 [2048, 1536], P(None, 'tp'), may hold values from -0.125 to 0.125
- decay_rate: float32 [96, 64], P('tp'), may hold values from 0.01 to 1
- frequency: float32 [96, 64], P('tp'), may hold values from 0 to 192
- log_step: float32 [96], P('tp'), may hold values from -3 to 0
- b_in: float32 [96, 16, 128], P('tp'), may hold values from -1.5 to 1.5
- c_out: float32 [96, 16, 128], P('tp'), may hold values from -0.5 to 0.5
- skip: float32 [1536], P('tp'), may hold values from -3 to 3
- w_out: bfloat16 [1536, 2048], P('tp'), may hold values from -0.15625 to 0.15625
- gain_mix: float32 [2048], replicated, may hold values from 0.1 to 1.9
- w_group: bfloat16 [2048, 4], replicated, may hold values from -0.0625 to 0.0625
- w_expert: bfloat16 [2048, 64], replicated, may hold values from -0.0625 to 0.0625
- w_gate: bfloat16 [64, 2048, 1024], P('ep', None, 'tp'), may hold values from -0.125 to 0.125
- w_up: bfloat16 [64, 2048, 1024], P('ep', None, 'tp'), may hold values from -0.125 to 0.125
- w_down: bfloat16 [64, 1024, 2048], P('ep', 'tp'), may hold values from -3 to 3
- gain_moe: float32 [2048], replicated, may hold values from 0.1 to 1.9
Outputs:
- layer_out: bfloat16 [4096, 2048], P(('grp', 'ep')), parts along dimension 0
- new_state: float32 [4096, 96, 128], P(('grp', 'ep'), 'tp'), parts along dimension 0
There are 2 independent parts, one for each index of `grp`. A program takes and returns all parts, laid end to end along the dimension named above; an argument that names none is the same for every part. Nothing has to cross between parts.
Inputs may be any that keep to these rules, and one draw needn't show every extreme that they name: `routes`: each row names two different experts of one group of 16 consecutive expert numbers. Within the rows of one index of ep (aligned blocks of 64 rows) no expert is named by more than 4 rows, and in every block some expert is named by exactly 4 rows.
All inputs are finite; a program needn't handle non-finite values.
Results may differ from a plain program's by a relative error of at most 0.015.
Values may be sent and summed in bfloat16 or wider, within the bound.
No kernel may reach another device: no remote copies, remote signals or barrier semaphores. Data moves between devices by JAX's collectives and lax.ppermute only.
A program may use at most 64 MiB of HBM per device.

v0:
```python
import jax
import jax.numpy as jnp
from jax import lax
from jax.sharding import PartitionSpec as P

residual_scale = 8.0**0.25
norm_eps = 1e-05


def sent_to_all(x, axis):
    devices = lax.axis_size(axis)
    return lax.all_to_all(jnp.broadcast_to(x[None], (devices, *x.shape)), axis, 0, 0, tiled=True)


def taken_together(x, axis):
    everything = sent_to_all(x, axis)
    return jnp.sum(everything.astype(jnp.float32), axis=0)


def in_order(parts, dim):
    lengths = list(parts.shape[1:])
    lengths[dim] *= parts.shape[0]
    return jnp.moveaxis(parts, 0, dim).reshape(lengths)


def gather_directly(x, axis, dim):
    parts = sent_to_all(x, axis)
    return in_order(parts, dim)


def split_up(x, dim, devices):
    before, after = (x.shape[:dim], x.shape[dim + 1 :])
    return jnp.moveaxis(x.reshape(*before, devices, -1, *after), dim, 0)


def sent_and_summed(x, axis, dim):
    devices = lax.axis_size(axis)
    parts = lax.all_to_all(split_up(x, dim, devices), axis, 0, 0, tiled=True)
    return jnp.sum(parts.astype(jnp.float32), axis=0)


def normalize(values, gain):
    centre = jnp.mean(values, -1, keepdims=True)
    spread = jnp.mean(jnp.square(values - centre), -1, keepdims=True)
    return (values - centre) * lax.rsqrt(spread + norm_eps) * gain


def s5_advance(mix_input, state, decay_rate, frequency, log_step, b_in, c_out, skip):
    top_precision = lax.Precision.DEFAULT
    entries = decay_rate.shape[-1]
    group_count = decay_rate.shape[0]
    width = b_in.shape[1]
    seq_count = mix_input.shape[0]
    input_rows = mix_input.astype(jnp.float32).reshape(seq_count, group_count, width)
    step_size = jnp.exp(log_step)[:, None]
    lam_real = -decay_rate
    magnitude = jnp.exp(lam_real * step_size)
    angle_dt = frequency * step_size
    bar_real = magnitude * jnp.cos(angle_dt)
    bar_imag = magnitude * jnp.sin(angle_dt)
    minus_real = bar_real - 1.0
    modulus = lam_real * lam_real + frequency * frequency
    ratio_real = (minus_real * lam_real + bar_imag * frequency) / modulus
    ratio_imag = (bar_imag * lam_real - minus_real * frequency) / modulus
    in_real = b_in[..., :entries]
    in_imag = b_in[..., entries:]
    input_matrix_real = ratio_real[:, None, :] * in_real - ratio_imag[:, None, :] * in_imag
    input_matrix_imag = ratio_real[:, None, :] * in_imag + ratio_imag[:, None, :] * in_real
    forcing_real = jnp.einsum(
        "rxf,xfb->rxb", input_rows, input_matrix_real, precision=top_precision
    )
    forcing_imag = jnp.einsum(
        "rxf,xfb->rxb", input_rows, input_matrix_imag, precision=top_precision
    )
    old_real = state[..., :entries]
    old_imag = state[..., entries:]
    following_real = bar_real * old_real - bar_imag * old_imag + forcing_real
    following_imag = bar_real * old_imag + bar_imag * old_real + forcing_imag
    output_real = c_out[..., :entries]
    output_imag = c_out[..., entries:]
    output_matrix = jnp.einsum("lzt,zft->lzf", following_real, output_real, precision=top_precision)
    output_matrix = output_matrix - jnp.einsum(
        "lzt,zft->lzf", following_imag, output_imag, precision=top_precision
    )
    output_matrix = output_matrix + skip.reshape(group_count, width) * input_rows
    activated = jax.nn.gelu(output_matrix).reshape(seq_count, group_count * width)
    return (activated, jnp.concatenate([following_real, following_imag], axis=-1))


def route_weights(normed, routes, w_group, w_expert):
    group_total = w_group.shape[1]
    expert_total = w_expert.shape[1]
    per_group = expert_total // group_total
    group_logit = jnp.dot(normed, w_group, preferred_element_type=jnp.float32)
    group_exp = jnp.exp(group_logit)
    group_prob = group_exp / jnp.sum(group_exp, -1, keepdims=True)
    chosen = routes[:, 0] // per_group
    group_pick = jnp.sum(
        jnp.where(
            chosen[:, None] == jnp.arange(group_total, dtype=jnp.int32)[None, :], group_prob, 0.0
        ),
        -1,
    )
    expert_logit = jnp.dot(normed, w_expert, preferred_element_type=jnp.float32)
    picked = jnp.sum(
        jnp.where(
            routes[:, :, None] == jnp.arange(expert_total, dtype=jnp.int32)[None, None, :],
            expert_logit[:, None, :],
            0.0,
        ),
        -1,
    )
    pair_exp = jnp.exp(picked)
    return pair_exp / jnp.sum(pair_exp, -1, keepdims=True) * group_pick[:, None]


def per_device(
    x_in,
    state,
    routes,
    w_in,
    decay_rate,
    frequency,
    log_step,
    b_in,
    c_out,
    skip,
    w_out,
    gain_mix,
    w_group,
    w_expert,
    w_gate,
    w_up,
    w_down,
    gain_moe,
):
    top_precision = lax.Precision.DEFAULT
    seq_count = x_in.shape[0]
    model_width = x_in.shape[1]
    mix_input = jnp.dot(x_in, w_in, preferred_element_type=jnp.float32).astype(jnp.bfloat16)
    activated, new_state = s5_advance(
        mix_input, state, decay_rate, frequency, log_step, b_in, c_out, skip
    )
    partial_mix = jnp.dot(activated.astype(jnp.bfloat16), w_out, preferred_element_type=jnp.float32)
    mixed = taken_together(partial_mix.astype(jnp.bfloat16), "tp").astype(jnp.float32)
    hidden_state = normalize(residual_scale * x_in.astype(jnp.float32) + mixed, gain_mix)
    hidden_bf = hidden_state.astype(jnp.bfloat16)
    route_weight = route_weights(hidden_bf, routes, w_group, w_expert)
    expert_total = w_expert.shape[1]
    ep_count = lax.axis_size("ep")
    local_experts = w_gate.shape[0]
    capacity = max(2, 4 * seq_count // expert_total)
    total_slots = expert_total * capacity
    hits = (routes[:, :, None] == jnp.arange(expert_total, dtype=jnp.int32)[None, None, :]).astype(
        jnp.int32
    )
    tally = jnp.sum(hits, axis=1)
    prior = jnp.cumsum(tally, axis=0) - tally
    slot_in_block = jnp.sum(prior[:, None, :] * hits, axis=-1)
    target = routes * capacity + slot_in_block
    slot_ids = jnp.arange(total_slots, dtype=jnp.int32)
    matches = target[:, :, None] == slot_ids[None, None, :]
    dispatch_map = jnp.any(slot_ids[:, None, None] == target[None, :, :], axis=-1).astype(
        jnp.bfloat16
    )
    combine_map = jnp.sum(jnp.where(matches, route_weight[:, :, None], 0.0), axis=1)
    buffer = jnp.dot(dispatch_map, hidden_bf, preferred_element_type=jnp.float32).astype(
        jnp.bfloat16
    )
    buffer = buffer.reshape(ep_count, local_experts, capacity, model_width)
    column_width = model_width // lax.axis_size("tp")
    own_columns = lax.dynamic_slice_in_dim(
        buffer, lax.axis_index("tp") * column_width, column_width, 3
    )
    piece = gather_directly(
        lax.all_to_all(own_columns, "ep", split_axis=0, concat_axis=0, tiled=True), "tp", 3
    )
    gate_part = jnp.einsum("njcd,jdf->njcf", piece, w_gate, preferred_element_type=jnp.float32)
    up_part = jnp.einsum("njcd,jdf->njcf", piece, w_up, preferred_element_type=jnp.float32)
    act = (jax.nn.silu(gate_part) * up_part).astype(jnp.bfloat16)
    share = sent_and_summed(
        jnp.einsum("njcf,jfd->njcd", act, w_down, preferred_element_type=jnp.float32).astype(
            jnp.bfloat16
        ),
        "tp",
        3,
    ).astype(jnp.bfloat16)
    returned_rows = lax.all_to_all(share, "ep", split_axis=0, concat_axis=0, tiled=True)
    flat_rows = returned_rows.reshape(total_slots, returned_rows.shape[3])
    moe = jnp.dot(
        combine_map,
        lax.all_gather(flat_rows, "tp", axis=1, tiled=True).astype(jnp.float32),
        precision=top_precision,
    )
    layer_out = normalize(residual_scale * hidden_state + moe, gain_moe).astype(jnp.bfloat16)
    return (layer_out, new_state)


def solution(mesh):
    in_specs = (
        P(("grp", "ep"), None),
        P(("grp", "ep"), "tp", None),
        P(("grp", "ep"), None),
        P(None, "tp"),
        P("tp", None),
        P("tp", None),
        P("tp"),
        P("tp", None, None),
        P("tp", None, None),
        P("tp"),
        P("tp", None),
        P(),
        P(),
        P(),
        P("ep", None, "tp"),
        P("ep", None, "tp"),
        P("ep", "tp", None),
        P(),
    )
    out_specs = (P(("grp", "ep"), None), P(("grp", "ep"), "tp", None))
    return jax.shard_map(
        per_device, mesh=mesh, in_specs=in_specs, out_specs=out_specs, check_vma=False
    )
```

profile of v0, /device:TPU:40, one launch (start us, length us, event | category | flops | bytes accessed | tf_op | source)
XLA Modules:
  0.0 197.4 jit_solution(56538877208457532)
XLA Ops:
  7.2 0.8 exp.20
  8.0 1.9 convolution_convert_fusion.3
  9.9 0.1 copy.75
  10.1 0.3 fusion.60
  10.4 0.3 copy-done.14
  10.6 0.1 add_divide_fusion
  10.8 0.1 copy-done.9
  10.9 0.5 fusion.5
  11.4 1.4 fusion.6
  12.9 1.6 fusion.41
  14.4 0.4 fusion.36
  14.8 0.4 convolution_convert_fusion.2
  15.3 1.2 broadcast_in_dim.24
  16.4 4.6 %all-to-all-start = ((bf16[4,64,2048]{2,1,0:T(8,128)(2,1)}), bf16[4,64,2048]{2,1,0:T(8,128)(2,1)}, u32[]{:S(2)}, u32[]{:S(2)}) async-start(bf16[4,64,2048]{2,1,0:T(8,128)(2,1)} %broadcast_in_dim.24), calls=%async_computation | async-start | bytes 2097152 | tf_op jit(solution)/shard_map/all_to_all | solution.py:12
  21.1 0.1 reduce_window_sum.11
  21.2 0.2 select_reduce_fusion.2
  21.5 14.8 %all-to-all-done = bf16[4,64,2048]{2,1,0:T(8,128)(2,1)} async-done(((bf16[4,64,2048]{2,1,0:T(8,128)(2,1)}), bf16[4,64,2048]{2,1,0:T(8,128)(2,1)}, u32[]{:S(2)}, u32[]{:S(2)}) %all-to-all-start) | async-done | bytes 1048608 | tf_op jit(solution)/shard_map/all_to_all | solution.py:12
  36.3 1.4 convert_reduce_fusion
  37.7 1.1 fusion.59
  38.8 1.2 multiply_reduce_fusion.1
  40.0 1.1 fusion.23
  41.2 0.7 copy-done.3
  41.8 1.5 convolution_convert_fusion.1
  43.3 2.3 %reshape.109 = bf16[32,2,4,2048]{3,2,1,0:T(4,128)(2,1)} reshape(bf16[256,2048]{1,0:T(8,128)(2,1)} %convolution_convert_fusion.1) | data formatting | bytes 2097152 | tf_op jit(solution)/shard_map/reshape | solution.py:170
  45.6 1.0 constant_dynamic-slice_fusion
  46.6 46.5 %all_to_all.25 = bf16[32,2,4,512]{3,2,1,0:T(4,128)(2,1)S(1)} all-to-all(bf16[32,2,4,512]{3,2,1,0:T(4,128)(2,1)S(1)} %constant_dynamic-slice_fusion), channel_id=1, replica_groups=mesh['grp'=2,'ep'=32,'tp'=4] {'ep'}, dimensions={0} | all-to-all | bytes 524288 | tf_op jit(solution)/shard_map/all_to_all | solution.py:176
  93.3 0.1 broadcast_in_dim.34
  93.4 18.0 %all_to_all.26 = bf16[4,32,2,4,512]{4,1,3,2,0:T(8,128)(2,1)S(1)} all-to-all(bf16[4,32,2,4,512]{4,1,3,2,0:T(8,128)(2,1)S(1)} %broadcast_in_dim.34), channel_id=1, replica_groups=mesh['grp'=2,'ep'=32,'tp'=4] {'tp'}, dimensions={0} | all-to-all | bytes 2097152 | tf_op jit(solution)/shard_map/all_to_all | solution.py:12
  111.4 0.1 copy.89
  111.6 1.0 copy-done.1
  112.6 1.2 fusion.7
  113.7 3.8 %convolution_convert_fusion = bf16[2,32,4,2048]{3,1,2,0:T(8,128)(2,1)} fusion(bf16[2,256,2048]{2,1,0:T(8,128)(2,1)S(1)} %copy-done, bf16[32,2,4,2048]{3,0,2,1:T(8,128)(2,1)} %bitcast.85, bf16[2,2048,256]{2,1,0:T(8,128)(2,1)} %param.33, f32[32,2,4,256]{3,0,2,1:T(8,128)} %fusion.7), kind=kOutput, calls=%fused_computation | convolution fusion | flops 537788416 | bytes 6553600 | tf_op jit(solution)/shard_map/njcf,jfd->njcd/dot_general | solution.py:182
  117.5 1.4 copy.95
  118.8 17.5 %all_to_all.27 = bf16[4,32,2,4,512]{4,1,3,2,0:T(8,128)(2,1)} all-to-all(bf16[4,32,2,4,512]{4,1,3,2,0:T(8,128)(2,1)S(1)} %bitcast.88), channel_id=1, replica_groups=mesh['grp'=2,'ep'=32,'tp'=4] {'tp'}, dimensions={0} | all-to-all | bytes 2097152 | tf_op jit(solution)/shard_map/all_to_all | solution.py:38
  136.3 2.2 %reduce_sum.130 = bf16[32,2,4,512]{3,0,2,1:T(8,128)(2,1)} reduce(bf16[4,32,2,4,512]{4,1,3,2,0:T(8,128)(2,1)} %all_to_all.27, bf16[]{:T(256)} %constant.58.clone.1), dimensions={0}, to_apply=%region_12.13 | reduce | flops 393216 | bytes 1310722 | tf_op jit(solution)/shard_map/reduce_sum | solution.py:39
  138.5 1.2 copy.80
  139.7 26.5 %all_to_all.28 = bf16[32,2,4,512]{3,2,1,0:T(4,128)(2,1)} all-to-all(bf16[32,2,4,512]{3,2,1,0:T(4,128)(2,1)S(1)} %copy.80), channel_id=1, replica_groups=mesh['grp'=2,'ep'=32,'tp'=4] {'ep'}, dimensions={0} | all-to-all | bytes 524288 | tf_op jit(solution)/shard_map/all_to_all | solution.py:188
  166.2 1.7 reshape.112
  168.0 1.5 pad_maximum_fusion
  169.5 1.3 copy.81
  170.9 0.2 fusion.63
  171.1 0.2 select_reduce_fusion.1
  171.3 0.2 fusion.61
  171.5 0.1 select_reduce_fusion
  171.7 16.1 %all-gather.2.cloned.1.call-done = bf16[256,2048]{1,0:T(8,128)(2,1)} async-done(((bf16[256,512]{1,0:T(8,128)(2,1)}), bf16[256,2048]{1,0:T(8,128)(2,1)}) %all-gather.2.cloned.1.call-update) | async-done | bytes 1048592 | tf_op jit(solution)/shard_map/all_gather | solution.py:192
  187.8 1.7 fusion.62
  189.4 0.2 multiply_reduce_fusion
  189.7 0.8 multiply_convert_fusion
  (48 shorter events, 0.6 us)
Async XLA Ops:
  7.2 106.6 %copy-start = (bf16[2,256,2048]{2,1,0:T(8,128)(2,1)S(1)}, bf16[2,256,2048]{2,1,0:T(8,128)(2,1)}, u32[]{:S(2)}) copy-start(bf16[2,256,2048]{2,1,0:T(8,128)(2,1)} %param.34) | copy-start | bytes 6291460
  7.2 2.9 %copy-start.5 = (f32[64,24,128]{2,1,0:T(8,128)S(1)}, f32[64,24,128]{2,1,0:T(8,128)}, u32[]{:S(2)}) copy-start(f32[64,24,128]{2,1,0:T(8,128)} %param.19) | copy-start | bytes 2359300
  9.9 0.7 copy-start.14
  9.9 0.7 copy-start.15
  9.9 0.9 copy-start.9
  10.9 1.9 copy-start.17
  10.9 2.0 %copy-start.8 = (f32[24,16,128]{2,1,0:T(8,128)S(1)}, f32[24,16,128]{2,1,0:T(8,128)}, u32[]{:S(2)}) copy-start(f32[24,16,128]{2,1,0:T(8,128)} %param.26) | copy-start | bytes 589828
  12.9 2.0 %copy-start.7 = (bf16[384,2048]{1,0:T(8,128)(2,1)S(1)}, bf16[384,2048]{1,0:T(8,128)(2,1)}, u32[]{:S(2)}) copy-start(bf16[384,2048]{1,0:T(8,128)(2,1)} %param.28) | copy-start | bytes 4718596
  15.3 5.8 %copy-start.13 = (s32[64,2]{0,1:T(2,128)S(1)}, s32[64,2]{0,1:T(2,128)}, u32[]{:S(2)}) copy-start(s32[64,2]{0,1:T(2,128)} %param.20) | copy-start | bytes 1540
  16.4 19.8 %all-to-all-start = ((bf16[4,64,2048]{2,1,0:T(8,128)(2,1)}), bf16[4,64,2048]{2,1,0:T(8,128)(2,1)}, u32[]{:S(2)}, u32[]{:S(2)}) async-start(bf16[4,64,2048]{2,1,0:T(8,128)(2,1)} %broadcast_in_dim.24), calls=%async_computation | async-start | bytes 2097152 | tf_op jit(solution)/shard_map/all_to_all | solution.py:12
  21.0 19.0 %copy-start.11 = (f32[2048]{0:T(1024)S(1)}, f32[2048]{0:T(1024)}, u32[]{:S(2)}) copy-start(f32[2048]{0:T(1024)} %param.29) | copy-start | bytes 24580
  21.0 166.7 %all-gather.2.cloned.1.call-start = ((), (), s32[]{:S(2)}) async-start(), calls=%async_computation.5 | async-start | bytes 1310720 | tf_op jit(solution)/shard_map/all_gather | solution.py:192
  41.1 0.7 copy-start.3
  93.4 19.2 %copy-start.6 = (bf16[2,2048,256]{2,1,0:T(8,128)(2,1)S(1)}, bf16[2,2048,256]{2,1,0:T(8,128)(2,1)}, u32[]{:S(2)}) copy-start(bf16[2,2048,256]{2,1,0:T(8,128)(2,1)} %param.32) | copy-start | bytes 6291460
  111.6 1.0 copy-start.1
  168.0 2.9 %copy-start.4 = (bf16[64,2048]{1,0:T(8,128)(2,1)S(1)}, bf16[64,2048]{1,0:T(8,128)(2,1)}, u32[]{:S(2)}) copy-start(bf16[64,2048]{1,0:T(8,128)(2,1)} %copy-done.3) | copy-start | bytes 786436
  168.0 2.9 %copy-start.10 = (bf16[2048,64]{0,1:T(8,128)(2,1)S(1)}, bf16[2048,64]{0,1:T(8,128)(2,1)}, u32[]{:S(2)}) copy-start(bf16[2048,64]{0,1:T(8,128)(2,1)} %param.31) | copy-start | bytes 786436
  168.0 3.3 %copy-start.12 = (bf16[2048,4]{0,1:T(4,128)(2,1)S(1)}, bf16[2048,4]{0,1:T(4,128)(2,1)}, u32[]{:S(2)}) copy-start(bf16[2048,4]{0,1:T(4,128)(2,1)} %param.30) | copy-start | bytes 49156
  169.5 18.3 %copy-start.2 = (bf16[64,2048]{1,0:T(8,128)(2,1)S(1)}, bf16[64,2048]{1,0:T(8,128)(2,1)}, u32[]{:S(2)}) copy-start(bf16[64,2048]{1,0:T(8,128)(2,1)} %param.18) | copy-start | bytes 786436
  170.8 18.8 %copy-start.16 = (f32[2048]{0:T(1024)S(1)}, f32[2048]{0:T(1024)}, u32[]{:S(2)}) copy-start(f32[2048]{0:T(1024)} %param.35) | copy-start | bytes 24580
Sparse Core Ops, SparseCore 0:
  168.1 19.5 all-gather.1
where the time goes:
time: 198 us; the launch traced here: 197 us
  blocking collectives  109 us (55%)
  waiting for transfers between devices  30.9 us (16%)
  matrix products  14.6 us (7%)
  between operations  14.4 us (7%)
  local copies, waits for them, and re-layouts  13.8 us (7%)
  other arithmetic  10.5 us (5%)
  starting transfers between devices  4.58 us (2%)
    all_to_all x1, blocking collectives, per_device(): lax.all_to_all(own_columns, 'ep', split_axis=0, concat_axis=0, tiled=True)  46.5 us
    all_to_all x1, blocking collectives, per_device(): lax.all_to_all(share, 'ep', split_axis=0, concat_axis=0, tiled=True)  26.5 us
    all_to_all x1, blocking collectives, sent_to_all(): lax.all_to_all(jnp.broadcast_to(x[None], (devices, *x.shape)), axis, 0, 0...  18 us
    all_to_all x1, blocking collectives, sent_and_summed(): parts = lax.all_to_all(split_up(x, dim, devices), axis, 0, 0, tiled=True)  17.5 us
    all_gather x1, waiting for transfers between devices, per_device(): lax.all_gather(flat_rows, 'tp', axis=1, tiled=True).astype(jnp.float32)  16.1 us
    all_to_all x1, waiting for transfers between devices, sent_to_all(): lax.all_to_all(jnp.broadcast_to(x[None], (devices, *x.shape)), axis, 0, 0...  14.8 us
    all_to_all x1, starting transfers between devices, sent_to_all(): lax.all_to_all(jnp.broadcast_to(x[None], (devices, *x.shape)), axis, 0, 0...  4.58 us
  transfers between devices with their start and end apart: 2, of which 2 were waited for; matrix products, arithmetic and copies ran while one was open for 2% of the time, Pallas kernels for 0%

commit v1 on v0

v1 whole, which is shorter than its diff:
```python
import jax
import jax.numpy as jnp
from jax import lax
from jax.sharding import PartitionSpec as P

residual_scale = 8.0**0.25
norm_eps = 1e-05


def exchange(x, axis):
    return lax.all_to_all(x, axis, 0, 0, tiled=True)


def to_all(x, axis):
    return exchange(jnp.broadcast_to(x[None], (lax.axis_size(axis), *x.shape)), axis)


def normalize(values, gain, axes):
    centre = jnp.mean(values, axes, keepdims=True)
    spread = jnp.mean(jnp.square(values - centre), axes, keepdims=True)
    return (values - centre) * lax.rsqrt(spread + norm_eps) * gain


def s5_advance(mix_input, state, decay_rate, frequency, log_step, b_in, c_out, skip):
    entries = decay_rate.shape[-1]
    group_count = decay_rate.shape[0]
    width = b_in.shape[1]
    seq_count = mix_input.shape[0]
    input_rows = mix_input.astype(jnp.float32).reshape(seq_count, group_count, width)
    step_size = jnp.exp(log_step)[:, None]
    lam_real = -decay_rate
    magnitude = jnp.exp(lam_real * step_size)
    angle_dt = frequency * step_size
    bar_real = magnitude * jnp.cos(angle_dt)
    bar_imag = magnitude * jnp.sin(angle_dt)
    minus_real = bar_real - 1.0
    modulus = lam_real * lam_real + frequency * frequency
    ratio_real = (minus_real * lam_real + bar_imag * frequency) / modulus
    ratio_imag = (bar_imag * lam_real - minus_real * frequency) / modulus
    in_real = b_in[..., :entries]
    in_imag = b_in[..., entries:]
    input_matrix_real = ratio_real[:, None, :] * in_real - ratio_imag[:, None, :] * in_imag
    input_matrix_imag = ratio_real[:, None, :] * in_imag + ratio_imag[:, None, :] * in_real
    forcing_real = jnp.einsum("rxf,xfb->rxb", input_rows, input_matrix_real)
    forcing_imag = jnp.einsum("rxf,xfb->rxb", input_rows, input_matrix_imag)
    old_real = state[..., :entries]
    old_imag = state[..., entries:]
    following_real = bar_real * old_real - bar_imag * old_imag + forcing_real
    following_imag = bar_real * old_imag + bar_imag * old_real + forcing_imag
    output_matrix = jnp.einsum("lzt,zft->lzf", following_real, c_out[..., :entries])
    output_matrix = output_matrix - jnp.einsum(
        "lzt,zft->lzf", following_imag, c_out[..., entries:]
    )
    output_matrix = output_matrix + skip.reshape(group_count, width) * input_rows
    activated = jax.nn.gelu(output_matrix).reshape(seq_count, group_count * width)
    return (activated, jnp.concatenate([following_real, following_imag], axis=-1))


def route_weights(normed, routes, w_group, w_expert):
    group_total = w_group.shape[1]
    expert_total = w_expert.shape[1]
    per_group = expert_total // group_total
    group_logit = jnp.dot(normed, w_group, preferred_element_type=jnp.float32)
    group_exp = jnp.exp(group_logit)
    group_prob = group_exp / jnp.sum(group_exp, -1, keepdims=True)
    chosen = routes[:, 0] // per_group
    group_pick = jnp.sum(
        jnp.where(
            chosen[:, None] == jnp.arange(group_total, dtype=jnp.int32)[None, :], group_prob, 0.0
        ),
        -1,
    )
    expert_logit = jnp.dot(normed, w_expert, preferred_element_type=jnp.float32)
    picked = jnp.sum(
        jnp.where(
            routes[:, :, None] == jnp.arange(expert_total, dtype=jnp.int32)[None, None, :],
            expert_logit[:, None, :],
            0.0,
        ),
        -1,
    )
    pair_exp = jnp.exp(picked)
    return pair_exp / jnp.sum(pair_exp, -1, keepdims=True) * group_pick[:, None]


def slots_of(routes, expert_total, capacity):
    hits = (routes[:, :, None] == jnp.arange(expert_total, dtype=jnp.int32)[None, None, :]).astype(
        jnp.int32
    )
    tally = jnp.sum(hits, axis=1)
    prior = jnp.cumsum(tally, axis=0) - tally
    return routes * capacity + jnp.sum(prior[:, None, :] * hits, axis=-1)


def layer(
    x_in,
    state,
    routes,
    w_in,
    decay_rate,
    frequency,
    log_step,
    b_in,
    c_out,
    skip,
    w_out,
    gain_mix,
    w_group,
    w_expert,
    w_gate,
    w_up,
    w_down,
    gain_moe,
):
    seq_count, model_width = x_in.shape
    shares = lax.axis_size("tp")
    share = model_width // shares
    expert_total = w_expert.shape[1]
    ep_count = lax.axis_size("ep")
    local_experts, _, hidden = w_gate.shape
    capacity = max(2, 4 * seq_count // expert_total)
    total_slots = expert_total * capacity
    local_slots = local_experts * capacity

    target = slots_of(routes, expert_total, capacity)
    slot_ids = jnp.arange(total_slots, dtype=jnp.int32)
    dispatch_map = jnp.any(slot_ids[:, None, None] == target[None, :, :], axis=-1).astype(
        jnp.bfloat16
    )

    mix_input = jnp.dot(x_in, w_in, preferred_element_type=jnp.float32).astype(jnp.bfloat16)
    activated, new_state = s5_advance(
        mix_input, state, decay_rate, frequency, log_step, b_in, c_out, skip
    )
    activated = activated.astype(jnp.bfloat16)
    partial_mix = jnp.stack(
        [
            jnp.dot(
                activated, w_out[:, k * share : (k + 1) * share], preferred_element_type=jnp.float32
            ).astype(jnp.bfloat16)
            for k in range(shares)
        ]
    )
    mixed = jnp.sum(exchange(partial_mix, "tp").astype(jnp.float32), axis=0)
    x_wide = x_in.astype(jnp.float32)
    x_own = lax.dynamic_slice_in_dim(x_in, lax.axis_index("tp") * share, share, 1)
    x_mean = jnp.mean(x_wide, -1, keepdims=True)
    own = (residual_scale * (x_own.astype(jnp.float32) - x_mean) + mixed).astype(jnp.bfloat16)

    sent = jnp.dot(dispatch_map, own, preferred_element_type=jnp.float32).astype(jnp.bfloat16)
    rows = exchange(sent.reshape(ep_count, local_slots, share), "ep")

    here = lax.axis_index("tp")
    parts = [own] + [
        lax.ppermute(own, "tp", [(i, (i + k) % shares) for i in range(shares)])
        for k in range(1, shares)
    ]
    whole = jnp.stack(parts)[(here - jnp.arange(shares)) % shares].astype(jnp.float32)
    gain_mix = gain_mix.reshape(shares, 1, share)
    hidden_state = normalize(whole, gain_mix, (0, 2))
    hidden_bf = hidden_state.astype(jnp.bfloat16)
    hidden_rows = jnp.concatenate([hidden_bf[k] for k in range(shares)], axis=-1)
    route_weight = route_weights(hidden_rows, routes, w_group, w_expert)
    matches = target[:, :, None] == slot_ids[None, None, :]
    combine_map = jnp.sum(jnp.where(matches, route_weight[:, :, None], 0.0), axis=1)

    piece = to_all(rows.reshape(total_slots, share), "tp").astype(jnp.float32)
    piece = normalize(piece, gain_mix, (0, 2)).astype(jnp.bfloat16)
    piece = jnp.concatenate([piece[k] for k in range(shares)], axis=-1)
    expert_of = (jnp.arange(total_slots, dtype=jnp.int32) % local_slots) // capacity
    acts = []
    for j in range(local_experts):
        gate_part = jnp.dot(piece, w_gate[j], preferred_element_type=jnp.float32)
        up_part = jnp.dot(piece, w_up[j], preferred_element_type=jnp.float32)
        act = jax.nn.silu(gate_part) * up_part
        acts.append(jnp.where((expert_of == j)[:, None], act, 0.0).astype(jnp.bfloat16))
    act = jnp.concatenate(acts, axis=-1)
    down = w_down.reshape(local_experts * hidden, model_width)
    partial_out = jnp.stack(
        [
            jnp.dot(
                act, down[:, k * share : (k + 1) * share], preferred_element_type=jnp.float32
            ).astype(jnp.bfloat16)
            for k in range(shares)
        ]
    )
    summed = jnp.sum(exchange(partial_out, "tp").astype(jnp.float32), axis=0)
    returned = exchange(summed.astype(jnp.bfloat16).reshape(ep_count, local_slots, share), "ep")
    moe_own = jnp.dot(
        combine_map.astype(jnp.bfloat16),
        returned.reshape(total_slots, share),
        preferred_element_type=jnp.float32,
    )
    moe = to_all(moe_own.astype(jnp.bfloat16), "tp").astype(jnp.float32)
    out = normalize(
        residual_scale * hidden_state + moe, gain_moe.reshape(shares, 1, share), (0, 2)
    ).astype(jnp.bfloat16)
    return (jnp.concatenate([out[k] for k in range(shares)], axis=-1), new_state)


def solution(mesh):
    in_specs = (
        P(("grp", "ep"), None),
        P(("grp", "ep"), "tp", None),
        P(("grp", "ep"), None),
        P(None, "tp"),
        P("tp", None),
        P("tp", None),
        P("tp"),
        P("tp", None, None),
        P("tp", None, None),
        P("tp"),
        P("tp", None),
        P(),
        P(),
        P(),
        P("ep", None, "tp"),
        P("ep", None, "tp"),
        P("ep", "tp", None),
        P(),
    )
    out_specs = (P(("grp", "ep"), None), P(("grp", "ep"), "tp", None))
    return jax.shard_map(layer, mesh=mesh, in_specs=in_specs, out_specs=out_specs, check_vma=False)
```

time: 198 us -> 165 us (0.83)
  blocking collectives: 109 us -> 0 us
  starting transfers between devices: 4.58 us -> 51.2 us
  waiting for transfers between devices: 30.9 us -> 74.7 us
  between operations: 14.4 us -> 1.16 us
  local copies, waits for them, and re-layouts: 13.8 us -> 11.4 us
    all_to_all x4 -> x0, blocking collectives: 109 us -> none  [the longest x1 46.5 us: per_device(): lax.all_to_all(own_columns, 'ep', split_axis=0, concat_axis=0, tiled=True)]
    all_to_all x1 -> x6, waiting for transfers between devices: 14.8 us -> 62.2 us  [exchange(): return lax.all_to_all(x, axis, 0, 0, tiled=True)]
    all_to_all x1 -> x6, starting transfers between devices: 4.58 us -> 46.4 us  [exchange(): return lax.all_to_all(x, axis, 0, 0, tiled=True)]
    all_gather x1 -> x0, waiting for transfers between devices: 16.1 us -> none  [per_device(): lax.all_gather(flat_rows, 'tp', axis=1, tiled=True).astype(jnp.float32)]
    ppermute x0 -> x3, waiting for transfers between devices: none -> 12.5 us  [layer(): lax.ppermute(own, 'tp', [(i, (i + k) % shares) for i in range(shares)])]
    reshape x4 -> x0, local copies, waits for them, and re-layouts: 5.49 us -> none  [the longest x1 2.27 us: per_device(): buffer = buffer.reshape(ep_count, local_experts, capacity, model_width)]
    ppermute x0 -> x3, starting transfers between devices: none -> 4.85 us  [layer(): lax.ppermute(own, 'tp', [(i, (i + k) % shares) for i in range(shares)])]
    dot_general x10 -> x19, matrix products: 14.2 us -> 10.6 us  [the longest x1 1.69 us: s5_advance(): jnp.einsum('lzt,zft->lzf', following_imag, c_out[..., entries:])]
  transfers between devices with their start and end apart: 2 -> 9, of which waited for: 2 -> 8; matrix products, arithmetic and copies ran while one was open for 2% -> 6% of each run, Pallas kernels for 0% -> 0%
where the time goes in v1:
time: 165 us; the launch traced here: 164 us
  waiting for transfers between devices  74.7 us (45%)
  starting transfers between devices  51.2 us (31%)
  matrix products  12.9 us (8%)
  other arithmetic  12.4 us (8%)
  local copies, waits for them, and re-layouts  11.4 us (7%)
    all_to_all x6, waiting for transfers between devices, exchange(): return lax.all_to_all(x, axis, 0, 0, tiled=True)  62.2 us
    all_to_all x6, starting transfers between devices, exchange(): return lax.all_to_all(x, axis, 0, 0, tiled=True)  46.4 us
    ppermute x3, waiting for transfers between devices, layer(): lax.ppermute(own, 'tp', [(i, (i + k) % shares) for i in range(shares)])  12.5 us
    unnamed x43, local copies, waits for them, and re-layouts  6.3 us
    ppermute x3, starting transfers between devices, layer(): lax.ppermute(own, 'tp', [(i, (i + k) % shares) for i in range(shares)])  4.85 us
  transfers between devices with their start and end apart: 9, of which 8 were waited for; matrix products, arithmetic and copies ran while one was open for 6% of the time, Pallas kernels for 0%

profile of v1, /device:TPU:40, one launch (start us, length us, event | category | flops | bytes accessed | tf_op | source)
XLA Modules:
  0.0 163.8 jit_solution(11786360305772508977)
XLA Ops:
  0.7 0.8 exp.23
  1.5 0.6 copy-done
  2.1 1.3 convolution_convert_fusion.10
  5.9 1.7 %fusion.55 = bf16[64,24,16]{0,2,1:T(8,128)(2,1)S(1)} fusion(f32[24,64,16]{1,2,0:T(8,128)S(1)} %fusion.60, f32[64,24,64]{2,0,1:T(8,128)S(1)} %fusion.5, bf16[64,24,16]{0,2,1:T(8,128)(2,1)S(1)} %bitcast.107, f32[24,16,128]{2,1,0:T(8,128)} %param.26, f32[24,16]{1,0:T(8,128)S(1)} %mul.257), kind=kOutput, calls=%fused_computation.94 | convolution fusion | flops 3465216 | bytes 689664 | tf_op jit(solution)/shard_map/lzt,zft->lzf/dot_general | solution.py:51
  8.5 0.7 pad_maximum_fusion.3
  9.3 4.6 %all-to-all-start = ((bf16[4,64,512]{2,1,0:T(8,128)(2,1)}), bf16[4,64,512]{2,1,0:T(8,128)(2,1)S(1)}, u32[]{:S(2)}, u32[]{:S(2)}) async-start(bf16[4,64,512]{2,1,0:T(8,128)(2,1)} %pad_maximum_fusion.3), calls=%async_computation | async-start | bytes 524288 | tf_op jit(solution)/shard_map/all_to_all | solution.py:11
  14.5 6.1 %all-to-all-done = bf16[4,64,512]{2,1,0:T(8,128)(2,1)S(1)} async-done(((bf16[4,64,512]{2,1,0:T(8,128)(2,1)}), bf16[4,64,512]{2,1,0:T(8,128)(2,1)S(1)}, u32[]{:S(2)}, u32[]{:S(2)}) %all-to-all-start) | async-done | bytes 262176 | tf_op jit(solution)/shard_map/all_to_all | solution.py:11
  20.7 1.0 fusion.11
  21.7 24.7 %all-to-all-start.1 = ((bf16[32,8,512]{2,1,0:T(8,128)(2,1)}), bf16[32,8,512]{2,1,0:T(8,128)(2,1)S(1)}, u32[]{:S(2)}, u32[]{:S(2)}) async-start(bf16[32,8,512]{2,1,0:T(8,128)(2,1)} %fusion.11), calls=%async_computation.1 | async-start | bytes 524288 | tf_op jit(solution)/shard_map/all_to_all | solution.py:11
  46.5 21.9 %all-to-all-done.1 = bf16[32,8,512]{2,1,0:T(8,128)(2,1)S(1)} async-done(((bf16[32,8,512]{2,1,0:T(8,128)(2,1)}), bf16[32,8,512]{2,1,0:T(8,128)(2,1)S(1)}, u32[]{:S(2)}, u32[]{:S(2)}) %all-to-all-start.1) | async-done | bytes 262176 | tf_op jit(solution)/shard_map/all_to_all | solution.py:11
  68.4 1.1 broadcast_in_dim.55
  69.5 3.6 %all-to-all-start.2 = ((bf16[4,256,512]{2,1,0:T(8,128)(2,1)}), bf16[4,256,512]{2,1,0:T(8,128)(2,1)S(1)}, u32[]{:S(2)}, u32[]{:S(2)}) async-start(bf16[4,256,512]{2,1,0:T(8,128)(2,1)} %broadcast_in_dim.55), calls=%async_computation.2 | async-start | bytes 2097152 | tf_op jit(solution)/shard_map/all_to_all | solution.py:11
  73.1 0.6 fusion.79
  73.7 3.2 %collective-permute-start.2 = (bf16[64,512]{1,0:T(8,128)(2,1)S(1)}, bf16[64,512]{1,0:T(8,128)(2,1)S(1)}, u32[]{:S(2)}, u32[]{:S(2)}) collective-permute-start(bf16[64,512]{1,0:T(8,128)(2,1)S(1)} %add_convert_fusion), channel_id=1, source_target_pairs={{0,3},{1,0},{2,1},{3,2},{4,7},{5,4},{6,5},{7,6},{8,11},{9,8},{10,9... | collective-permute-start | bytes 196616 | tf_op jit(solution)/shard_map/ppermute | solution.py:155
  76.8 0.8 collective-permute-start.1
  77.6 0.9 collective-permute-start
  78.5 10.6 %collective-permute-done.2 = bf16[64,512]{1,0:T(8,128)(2,1)S(1)} collective-permute-done((bf16[64,512]{1,0:T(8,128)(2,1)S(1)}, bf16[64,512]{1,0:T(8,128)(2,1)S(1)}, u32[]{:S(2)}, u32[]{:S(2)}) %collective-permute-start.2) | collective-permute-done | bytes 65568 | tf_op jit(solution)/shard_map/ppermute | solution.py:155
  89.1 1.5 collective-permute-done.1
  91.0 0.6 gather_fusion
  92.9 1.1 copy-done.18
  94.0 0.5 fusion.23
  94.6 0.5 fusion.26
  95.1 1.0 copy-done.19
  96.2 0.5 fusion.15
  96.7 0.5 fusion.14
  97.3 1.0 copy-done.20
  99.6 1.1 pad_maximum_fusion.1
  100.7 3.6 %all-to-all-start.3 = ((bf16[4,256,512]{2,1,0:T(8,128)(2,1)}), bf16[4,256,512]{2,1,0:T(8,128)(2,1)S(1)}, u32[]{:S(2)}, u32[]{:S(2)}) async-start(bf16[4,256,512]{2,1,0:T(8,128)(2,1)} %pad_maximum_fusion.1), calls=%async_computation.3 | async-start | bytes 2097152 | tf_op jit(solution)/shard_map/all_to_all | solution.py:11
  104.6 0.6 copy-done.15
  105.4 0.7 slice_bitcast_fusion.11
  106.0 11.8 %all-to-all-done.3 = bf16[4,256,512]{2,1,0:T(8,128)(2,1)S(1)} async-done(((bf16[4,256,512]{2,1,0:T(8,128)(2,1)}), bf16[4,256,512]{2,1,0:T(8,128)(2,1)S(1)}, u32[]{:S(2)}, u32[]{:S(2)}) %all-to-all-start.3) | async-done | bytes 1048608 | tf_op jit(solution)/shard_map/all_to_all | solution.py:11
  117.8 0.9 reduce_sum.160
  118.7 5.7 %all-to-all-start.4 = ((bf16[32,8,512]{2,1,0:T(8,128)(2,1)}), bf16[32,8,512]{2,1,0:T(8,128)(2,1)}, u32[]{:S(2)}, u32[]{:S(2)}) async-start(bf16[32,8,512]{2,1,0:T(8,128)(2,1)} %bitcast.108), calls=%async_computation.4 | async-start | bytes 524288 | tf_op jit(solution)/shard_map/all_to_all | solution.py:11
  124.4 1.2 fusion.74
  125.9 1.1 fusion.84
  126.9 0.7 fusion.76
  127.6 0.8 select_reduce_fusion
  128.4 18.1 %all-to-all-done.4 = bf16[32,8,512]{2,1,0:T(8,128)(2,1)} async-done(((bf16[32,8,512]{2,1,0:T(8,128)(2,1)}), bf16[32,8,512]{2,1,0:T(8,128)(2,1)}, u32[]{:S(2)}, u32[]{:S(2)}) %all-to-all-start.4) | async-done | bytes 262176 | tf_op jit(solution)/shard_map/all_to_all | solution.py:11
  146.5 1.1 convolution_convert_fusion.9
  147.6 0.7 broadcast_in_dim.62
  148.3 4.1 %all-to-all-start.5 = ((bf16[4,64,512]{2,1,0:T(8,128)(2,1)}), bf16[4,64,512]{2,1,0:T(8,128)(2,1)}, u32[]{:S(2)}, u32[]{:S(2)}) async-start(bf16[4,64,512]{2,1,0:T(8,128)(2,1)} %broadcast_in_dim.62), calls=%async_computation.5 | async-start | bytes 524288 | tf_op jit(solution)/shard_map/all_to_all | solution.py:11
  152.4 0.7 mul.290
  153.4 1.3 copy.39
  154.8 4.3 %all-to-all-done.5 = bf16[4,64,512]{2,1,0:T(8,128)(2,1)} async-done(((bf16[4,64,512]{2,1,0:T(8,128)(2,1)}), bf16[4,64,512]{2,1,0:T(8,128)(2,1)}, u32[]{:S(2)}, u32[]{:S(2)}) %all-to-all-start.5) | async-done | bytes 262176 | tf_op jit(solution)/shard_map/all_to_all | solution.py:11
  159.1 1.3 fusion.82
  160.4 1.3 multiply_reduce_fusion
  161.8 1.3 multiply_convert_fusion
  163.1 0.7 pad_maximum_fusion.7
  (88 shorter events, 8.0 us)
Async XLA Ops:
  0.6 1.4 copy-start
  0.6 2.9 %copy-start.5 = (f32[64,24,128]{2,1,0:T(8,128)S(1)}, f32[64,24,128]{2,1,0:T(8,128)}, u32[]{:S(2)}) copy-start(f32[64,24,128]{2,1,0:T(8,128)} %param.19) | copy-start | bytes 2359300
  3.4 0.7 copy-start.11
  3.4 0.7 copy-start.12
  3.5 0.9 copy-start.9
  4.5 1.0 copy-start.17
  4.5 1.1 copy-start.8
  5.0 2.6 %copy-start.1 = (f32[64,24,64]{2,0,1:T(8,128)}, f32[64,24,64]{2,0,1:T(8,128)S(1)}, u32[]{:S(2)}) copy-start(f32[64,24,64]{2,0,1:T(8,128)S(1)} %fusion.5) | copy-start | bytes 1179652
  5.5 2.8 %copy-start.3 = (f32[64,24,64]{2,0,1:T(8,128)}, f32[64,24,64]{2,0,1:T(8,128)S(1)}, u32[]{:S(2)}) copy-start(f32[64,24,64]{2,0,1:T(8,128)S(1)} %fusion.6) | copy-start | bytes 1179652
  5.6 2.0 %copy-start.6 = (bf16[384,2048]{1,0:T(8,128)(2,1)S(1)}, bf16[384,2048]{1,0:T(8,128)(2,1)}, u32[]{:S(2)}) copy-start(bf16[384,2048]{1,0:T(8,128)(2,1)} %param.28) | copy-start | bytes 4718596
  5.9 7.9 %copy-start.7 = (bf16[64,2048]{1,0:T(8,128)(2,1)S(1)}, bf16[64,2048]{1,0:T(8,128)(2,1)}, u32[]{:S(2)}) copy-start(bf16[64,2048]{1,0:T(8,128)(2,1)} %param.18) | copy-start | bytes 786436
  7.6 6.4 %copy-start.10 = (s32[64,2]{0,1:T(2,128)S(1)}, s32[64,2]{0,1:T(2,128)}, u32[]{:S(2)}) copy-start(s32[64,2]{0,1:T(2,128)} %param.20) | copy-start | bytes 1540
  8.1 38.4 %copy-start.14 = (f32[2048]{0:T(1024)S(1)}, f32[2048]{0:T(1024)}, u32[]{:S(2)}) copy-start(f32[2048]{0:T(1024)} %param.29) | copy-start | bytes 24580
  9.3 11.3 %all-to-all-start = ((bf16[4,64,512]{2,1,0:T(8,128)(2,1)}), bf16[4,64,512]{2,1,0:T(8,128)(2,1)S(1)}, u32[]{:S(2)}, u32[]{:S(2)}) async-start(bf16[4,64,512]{2,1,0:T(8,128)(2,1)} %pad_maximum_fusion.3), calls=%async_computation | async-start | bytes 524288 | tf_op jit(solution)/shard_map/all_to_all | solution.py:11
  14.4 55.1 %copy-start.13 = (s32[64,2]{0,1:T(2,128)}, s32[64,2]{0,1:T(2,128)S(1)}, u32[]{:S(2)}) copy-start(s32[64,2]{0,1:T(2,128)S(1)} %multiply_add_fusion.1) | copy-start | bytes 1540
  21.7 46.7 %all-to-all-start.1 = ((bf16[32,8,512]{2,1,0:T(8,128)(2,1)}), bf16[32,8,512]{2,1,0:T(8,128)(2,1)S(1)}, u32[]{:S(2)}, u32[]{:S(2)}) async-start(bf16[32,8,512]{2,1,0:T(8,128)(2,1)} %fusion.11), calls=%async_computation.1 | async-start | bytes 524288 | tf_op jit(solution)/shard_map/all_to_all | solution.py:11
  69.5 22.3 %all-to-all-start.2 = ((bf16[4,256,512]{2,1,0:T(8,128)(2,1)}), bf16[4,256,512]{2,1,0:T(8,128)(2,1)S(1)}, u32[]{:S(2)}, u32[]{:S(2)}) async-start(bf16[4,256,512]{2,1,0:T(8,128)(2,1)} %broadcast_in_dim.55), calls=%async_computation.2 | async-start | bytes 2097152 | tf_op jit(solution)/shard_map/all_to_all | solution.py:11
  73.7 15.4 %collective-permute-start.2 = (bf16[64,512]{1,0:T(8,128)(2,1)S(1)}, bf16[64,512]{1,0:T(8,128)(2,1)S(1)}, u32[]{:S(2)}, u32[]{:S(2)}) collective-permute-start(bf16[64,512]{1,0:T(8,128)(2,1)S(1)} %add_convert_fusion), channel_id=1, source_target_pairs={{0,3},{1,0},{2,1},{3,2},{4,7},{5,4},{6,5},{7,6},{8,11},{9,8},{10,9... | collective-permute-start | bytes 196616 | tf_op jit(solution)/shard_map/ppermute | solution.py:155
  76.8 13.8 %collective-permute-start.1 = (bf16[64,512]{1,0:T(8,128)(2,1)S(1)}, bf16[64,512]{1,0:T(8,128)(2,1)S(1)}, u32[]{:S(2)}, u32[]{:S(2)}) collective-permute-start(bf16[64,512]{1,0:T(8,128)(2,1)S(1)} %add_convert_fusion), channel_id=1, source_target_pairs={{0,2},{1,3},{2,0},{3,1},{4,6},{5,7},{6,4},{7,5},{8,10},{9,11},{10,... | collective-permute-start | bytes 196616 | tf_op jit(solution)/shard_map/ppermute | solution.py:155
  77.6 13.4 %collective-permute-start = (bf16[64,512]{1,0:T(8,128)(2,1)S(1)}, bf16[64,512]{1,0:T(8,128)(2,1)S(1)}, u32[]{:S(2)}, u32[]{:S(2)}) collective-permute-start(bf16[64,512]{1,0:T(8,128)(2,1)S(1)} %add_convert_fusion), channel_id=1, source_target_pairs={{0,1},{1,2},{2,3},{3,0},{4,5},{5,6},{6,7},{7,4},{8,9},{9,10},{10,1... | collective-permute-start | bytes 196616 | tf_op jit(solution)/shard_map/ppermute | solution.py:155
  92.4 1.6 copy-start.18
  94.6 1.6 copy-start.19
  96.7 1.6 copy-start.20
  100.7 17.0 %all-to-all-start.3 = ((bf16[4,256,512]{2,1,0:T(8,128)(2,1)}), bf16[4,256,512]{2,1,0:T(8,128)(2,1)S(1)}, u32[]{:S(2)}, u32[]{:S(2)}) async-start(bf16[4,256,512]{2,1,0:T(8,128)(2,1)} %pad_maximum_fusion.1), calls=%async_computation.3 | async-start | bytes 2097152 | tf_op jit(solution)/shard_map/all_to_all | solution.py:11
  104.6 0.6 copy-start.15
  118.7 34.5 %copy-start.2 = (f32[64,24,64]{2,0,1:T(8,128)S(1)}, f32[64,24,64]{2,0,1:T(8,128)}, u32[]{:S(2)}) copy-start(f32[64,24,64]{2,0,1:T(8,128)} %copy-done.1) | copy-start | bytes 1179652
  118.7 34.5 %copy-start.4 = (f32[64,24,64]{2,0,1:T(8,128)S(1)}, f32[64,24,64]{2,0,1:T(8,128)}, u32[]{:S(2)}) copy-start(f32[64,24,64]{2,0,1:T(8,128)} %copy-done.3) | copy-start | bytes 1179652
  118.7 27.8 %all-to-all-start.4 = ((bf16[32,8,512]{2,1,0:T(8,128)(2,1)}), bf16[32,8,512]{2,1,0:T(8,128)(2,1)}, u32[]{:S(2)}, u32[]{:S(2)}) async-start(bf16[32,8,512]{2,1,0:T(8,128)(2,1)} %bitcast.108), calls=%async_computation.4 | async-start | bytes 524288 | tf_op jit(solution)/shard_map/all_to_all | solution.py:11
  148.3 10.8 %all-to-all-start.5 = ((bf16[4,64,512]{2,1,0:T(8,128)(2,1)}), bf16[4,64,512]{2,1,0:T(8,128)(2,1)}, u32[]{:S(2)}, u32[]{:S(2)}) async-start(bf16[4,64,512]{2,1,0:T(8,128)(2,1)} %broadcast_in_dim.62), calls=%async_computation.5 | async-start | bytes 524288 | tf_op jit(solution)/shard_map/all_to_all | solution.py:11
  152.4 6.7 %copy-start.16 = (f32[64]{0:T(128)S(1)}, f32[64]{0:T(128)}, u32[]{:S(2)}) copy-start(f32[64]{0:T(128)} %copy-done.15) | copy-start | bytes 772

commit v2 on v1

--- a/solution.py
+++ b/solution.py
@@ -1,6 +1,8 @@
 import jax
 import jax.numpy as jnp
 from jax import lax
+from jax.experimental import pallas as pl
+from jax.experimental.pallas import tpu as pltpu
 from jax.sharding import PartitionSpec as P
 
 residual_scale = 8.0**0.25
@@ -11,8 +13,12 @@
     return lax.all_to_all(x, axis, 0, 0, tiled=True)
 
 
-def to_all(x, axis):
-    return exchange(jnp.broadcast_to(x[None], (lax.axis_size(axis), *x.shape)), axis)
+def shifted(pieces, axis):
+    size = lax.axis_size(axis)
+    return [pieces[0]] + [
+        lax.ppermute(pieces[k], axis, [(i, (i + k) % size) for i in range(size)])
+        for k in range(1, size)
+    ]
 
 
 def normalize(values, gain, axes):
@@ -56,11 +62,10 @@
     return (activated, jnp.concatenate([following_real, following_imag], axis=-1))
 
 
-def route_weights(normed, routes, w_group, w_expert):
-    group_total = w_group.shape[1]
-    expert_total = w_expert.shape[1]
+def route_weights(logits, routes, group_total):
+    expert_total = logits.shape[1] - group_total
     per_group = expert_total // group_total
-    group_logit = jnp.dot(normed, w_group, preferred_element_type=jnp.float32)
+    group_logit = logits[:, :group_total]
     group_exp = jnp.exp(group_logit)
     group_prob = group_exp / jnp.sum(group_exp, -1, keepdims=True)
     chosen = routes[:, 0] // per_group
@@ -70,7 +75,7 @@
         ),
         -1,
     )
-    expert_logit = jnp.dot(normed, w_expert, preferred_element_type=jnp.float32)
+    expert_logit = logits[:, group_total:]
     picked = jnp.sum(
         jnp.where(
             routes[:, :, None] == jnp.arange(expert_total, dtype=jnp.int32)[None, None, :],
@@ -90,6 +95,124 @@
     tally = jnp.sum(hits, axis=1)
     prior = jnp.cumsum(tally, axis=0) - tally
     return routes * capacity + jnp.sum(prior[:, None, :] * hits, axis=-1)
+
+
+def experts(here, pieces, gain, w_gate, w_up, w_down, capacity):
+    slots, share = pieces[0].shape
+    shares = len(pieces)
+    local_experts, width, hidden = w_gate.shape
+    chunk = 32
+
+    def kernel(here_ref, *refs):
+        piece_refs = refs[:shares]
+        gain_ref, gate_ref, up_ref, down_ref = refs[shares : shares + 4]
+        out_refs = refs[shares + 4 : 2 * shares + 4]
+        row_ref, act_ref, gate_near, up_near, down_near, sems = refs[2 * shares + 4 :]
+        t = here_ref[0]
+        copies = []
+        for j in range(local_experts):
+            copies.append(pltpu.make_async_copy(gate_ref.at[j], gate_near.at[j], sems.at[2 * j]))
+            copies.append(pltpu.make_async_copy(up_ref.at[j], up_near.at[j], sems.at[2 * j + 1]))
+        copies.append(pltpu.make_async_copy(down_ref, down_near, sems.at[2 * local_experts]))
+        for copy in copies:
+            copy.start()
+        froms = [lax.rem(t + shares - k, shares) for k in range(shares)]
+
+        def norm_rows(i, carry):
+            rows = pl.ds(pl.multiple_of(i * chunk, chunk), chunk)
+            values = [r[rows, :].astype(jnp.float32) for r in piece_refs]
+            total = values[0]
+            for v in values[1:]:
+                total = total + v
+            centre = jnp.sum(total, -1, keepdims=True) / width
+            values = [v - centre for v in values]
+            total = values[0] * values[0]
+            for v in values[1:]:
+                total = total + v * v
+            scale = lax.rsqrt(jnp.sum(total, -1, keepdims=True) / width + norm_eps)
+            for k, v in enumerate(values):
+                columns = pl.ds(pl.multiple_of(froms[k] * share, share), share)
+                row_ref[rows, columns] = (v * scale * gain_ref[froms[k]]).astype(jnp.bfloat16)
+            return carry
+
+        lax.fori_loop(0, slots // chunk, norm_rows, 0)
+        slot = lax.broadcasted_iota(jnp.int32, (slots, hidden), 0)
+        expert_of = lax.rem(slot, local_experts * capacity) // capacity
+        for j in range(local_experts):
+            rows = row_ref[...]
+            copies[2 * j].wait()
+            gate_part = jnp.dot(rows, gate_near[j], preferred_element_type=jnp.float32)
+            copies[2 * j + 1].wait()
+            up_part = jnp.dot(rows, up_near[j], preferred_element_type=jnp.float32)
+            act = gate_part * jax.nn.sigmoid(gate_part) * up_part
+            act_ref[:, j * hidden : (j + 1) * hidden] = jnp.where(
+                expert_of == j, act, 0.0
+            ).astype(jnp.bfloat16)
+        copies[-1].wait()
+        for k in (1, shares - 1, *range(2, shares - 1), 0):
+            to = lax.rem(t + k, shares)
+            columns = pl.ds(pl.multiple_of(to * share, share), share)
+            out_refs[k][...] = jnp.dot(
+                act_ref[...], down_near[:, columns], preferred_element_type=jnp.float32
+            ).astype(jnp.bfloat16)
+
+    vmem = pl.BlockSpec(memory_space=pltpu.VMEM)
+    return pl.pallas_call(
+        kernel,
+        in_specs=[pl.BlockSpec(memory_space=pltpu.SMEM)]
+        + [vmem] * (shares + 1)
+        + [pl.BlockSpec(memory_space=pltpu.HBM)] * 3,
+        out_specs=[vmem] * shares,
+        out_shape=[jax.ShapeDtypeStruct((slots, share), jnp.bfloat16)] * shares,
+        scratch_shapes=[
+            pltpu.VMEM((slots, width), jnp.bfloat16),
+            pltpu.VMEM((slots, local_experts * hidden), jnp.bfloat16),
+            pltpu.VMEM(w_gate.shape, w_gate.dtype),
+            pltpu.VMEM(w_up.shape, w_up.dtype),
+            pltpu.VMEM(w_down.shape, w_down.dtype),
+            pltpu.SemaphoreType.DMA((2 * local_experts + 1,)),
+        ],
+        compiler_params=pltpu.CompilerParams(vmem_limit_bytes=24 * 1024 * 1024),
+        name="experts",
+    )(here, *pieces, gain, w_gate, w_up, w_down)
+
+
+def finish(here, hidden, pieces, gain):
+    rows, share = pieces[0].shape
+    shares = len(pieces)
+    width = shares * share
+
+    def kernel(here_ref, hidden_ref, *refs):
+        piece_refs = refs[:shares]
+        gain_ref, out_ref = refs[shares:]
+        t = here_ref[0]
+        froms = [lax.rem(t + shares - k, shares) for k in range(shares)]
+        values = [
+            residual_scale * hidden_ref[k] + piece_refs[k][...].astype(jnp.float32)
+            for k in range(shares)
+        ]
+        total = values[0]
+        for v in values[1:]:
+            total = total + v
+        centre = jnp.sum(total, -1, keepdims=True) / width
+        values = [v - centre for v in values]
+        total = values[0] * values[0]
+        for v in values[1:]:
+            total = total + v * v
+        scale = lax.rsqrt(jnp.sum(total, -1, keepdims=True) / width + norm_eps)
+        for k, v in enumerate(values):
+            columns = pl.ds(pl.multiple_of(froms[k] * share, share), share)
+            out_ref[:, columns] = (v * scale * gain_ref[froms[k]]).astype(jnp.bfloat16)
+
+    vmem = pl.BlockSpec(memory_space=pltpu.VMEM)
+    return pl.pallas_call(
+        kernel,
+        in_specs=[pl.BlockSpec(memory_space=pltpu.SMEM)] + [vmem] * (shares + 2),
+        out_specs=vmem,
+        out_shape=jax.ShapeDtypeStruct((rows, width), jnp.bfloat16),
+        compiler_params=pltpu.CompilerParams(vmem_limit_bytes=8 * 1024 * 1024),
+        name="finish",
+    )(here, hidden, *pieces, gain)
 
 
 def layer(
@@ -121,6 +244,8 @@
     capacity = max(2, 4 * seq_count // expert_total)
     total_slots = expert_total * capacity
     local_slots = local_experts * capacity
+    here = lax.axis_index("tp")
+    here_array = here.astype(jnp.int32).reshape(1)
 
     target = slots_of(routes, expert_total, capacity)
     slot_ids = jnp.arange(total_slots, dtype=jnp.int32)
@@ -132,70 +257,50 @@
     activated, new_state = s5_advance(
         mix_input, state, decay_rate, frequency, log_step, b_in, c_out, skip
     )
-    activated = activated.astype(jnp.bfloat16)
-    partial_mix = jnp.stack(
-        [
-            jnp.dot(
-                activated, w_out[:, k * share : (k + 1) * share], preferred_element_type=jnp.float32
-            ).astype(jnp.bfloat16)
-            for k in range(shares)
-        ]
-    )
-    mixed = jnp.sum(exchange(partial_mix, "tp").astype(jnp.float32), axis=0)
-    x_wide = x_in.astype(jnp.float32)
-    x_own = lax.dynamic_slice_in_dim(x_in, lax.axis_index("tp") * share, share, 1)
-    x_mean = jnp.mean(x_wide, -1, keepdims=True)
-    own = (residual_scale * (x_own.astype(jnp.float32) - x_mean) + mixed).astype(jnp.bfloat16)
+    partial_mix = jnp.dot(
+        activated.astype(jnp.bfloat16), w_out, preferred_element_type=jnp.float32
+    ).astype(jnp.bfloat16)
+
+    def own_columns(values, k):
+        return lax.dynamic_slice_in_dim(values, ((here + k) % shares) * share, share, 1)
+
+    arrived = shifted([own_columns(partial_mix, k) for k in range(shares)], "tp")
+    mixed = sum(a.astype(jnp.float32) for a in arrived)
+    x_mean = jnp.mean(x_in.astype(jnp.float32), -1, keepdims=True)
+    x_own = own_columns(x_in, 0).astype(jnp.float32)
+    own = (residual_scale * (x_own - x_mean) + mixed).astype(jnp.bfloat16)
 
     sent = jnp.dot(dispatch_map, own, preferred_element_type=jnp.float32).astype(jnp.bfloat16)
     rows = exchange(sent.reshape(ep_count, local_slots, share), "ep")
 
-    here = lax.axis_index("tp")
-    parts = [own] + [
-        lax.ppermute(own, "tp", [(i, (i + k) % shares) for i in range(shares)])
-        for k in range(1, shares)
-    ]
-    whole = jnp.stack(parts)[(here - jnp.arange(shares)) % shares].astype(jnp.float32)
+    parts = shifted([own] * shares, "tp")
+    whole = jnp.stack(parts).astype(jnp.float32)
+    order = (here - jnp.arange(shares)) % shares
     gain_mix = gain_mix.reshape(shares, 1, share)
-    hidden_state = normalize(whole, gain_mix, (0, 2))
+    hidden_state = normalize(whole, gain_mix[order], (0, 2))
     hidden_bf = hidden_state.astype(jnp.bfloat16)
-    hidden_rows = jnp.concatenate([hidden_bf[k] for k in range(shares)], axis=-1)
-    route_weight = route_weights(hidden_rows, routes, w_group, w_expert)
+    w_router = jnp.concatenate([w_group, w_expert], axis=-1).reshape(shares, share, -1)[order]
+    logits = jnp.einsum("krd,kde->re", hidden_bf, w_router, preferred_element_type=jnp.float32)
+    route_weight = route_weights(logits, routes, w_group.shape[1])
     matches = target[:, :, None] == slot_ids[None, None, :]
     combine_map = jnp.sum(jnp.where(matches, route_weight[:, :, None], 0.0), axis=1)
 
-    piece = to_all(rows.reshape(total_slots, share), "tp").astype(jnp.float32)
-    piece = normalize(piece, gain_mix, (0, 2)).astype(jnp.bfloat16)
-    piece = jnp.concatenate([piece[k] for k in range(shares)], axis=-1)
-    expert_of = (jnp.arange(total_slots, dtype=jnp.int32) % local_slots) // capacity
-    acts = []
-    for j in range(local_experts):
-        gate_part = jnp.dot(piece, w_gate[j], preferred_element_type=jnp.float32)
-        up_part = jnp.dot(piece, w_up[j], preferred_element_type=jnp.float32)
-        act = jax.nn.silu(gate_part) * up_part
-        acts.append(jnp.where((expert_of == j)[:, None], act, 0.0).astype(jnp.bfloat16))
-    act = jnp.concatenate(acts, axis=-1)
-    down = w_down.reshape(local_experts * hidden, model_width)
-    partial_out = jnp.stack(
-        [
-            jnp.dot(
-                act, down[:, k * share : (k + 1) * share], preferred_element_type=jnp.float32
-            ).astype(jnp.bfloat16)
-            for k in range(shares)
-        ]
-    )
-    summed = jnp.sum(exchange(partial_out, "tp").astype(jnp.float32), axis=0)
-    returned = exchange(summed.astype(jnp.bfloat16).reshape(ep_count, local_slots, share), "ep")
+    rows = rows.reshape(total_slots, share)
+    pieces = shifted([rows] * shares, "tp")
+    w_down = w_down.reshape(local_experts * hidden, model_width)
+    weights = [pltpu.with_memory_space_constraint(w, pltpu.HBM) for w in (w_gate, w_up, w_down)]
+    outs = experts(here_array, pieces, gain_mix, *weights, capacity)
+    arrived = shifted(outs, "tp")
+    summed = sum(a.astype(jnp.float32) for a in arrived).astype(jnp.bfloat16)
+    returned = exchange(summed.reshape(ep_count, local_slots, share), "ep")
     moe_own = jnp.dot(
         combine_map.astype(jnp.bfloat16),
         returned.reshape(total_slots, share),
         preferred_element_type=jnp.float32,
-    )
-    moe = to_all(moe_own.astype(jnp.bfloat16), "tp").astype(jnp.float32)
-    out = normalize(
-        residual_scale * hidden_state + moe, gain_moe.reshape(shares, 1, share), (0, 2)
     ).astype(jnp.bfloat16)
-    return (jnp.concatenate([out[k] for k in range(shares)], axis=-1), new_state)
+    moe = shifted([moe_own] * shares, "tp")
+    out = finish(here_array, hidden_state, moe, gain_moe.reshape(shares, 1, share))
+    return (out, new_state)
 
 
 def solution(mesh):

time: 165 us -> 143 us (0.87)
  waiting for transfers between devices: 74.7 us -> 58.1 us
  matrix products: 12.9 us -> 6.3 us
  Pallas kernels: 0 us -> 6.39 us
  other arithmetic: 12.4 us -> 9.68 us
  starting transfers between devices: 51.2 us -> 49 us
    all_to_all x6 -> x2, waiting for transfers between devices: 62.2 us -> 36.9 us  [exchange(): return lax.all_to_all(x, axis, 0, 0, tiled=True)]
    all_to_all x6 -> x2, starting transfers between devices: 46.4 us -> 29.5 us  [exchange(): return lax.all_to_all(x, axis, 0, 0, tiled=True)]
    ppermute x3 -> x15, starting transfers between devices: 4.85 us -> 19.5 us  [shifted(): lax.ppermute(pieces[k], axis, [(i, (i + k) % size) for i in range(size)])]
    ppermute x3 -> x15, waiting for transfers between devices: 12.5 us -> 21.1 us  [shifted(): lax.ppermute(pieces[k], axis, [(i, (i + k) % size) for i in range(size)])]
    pallas_call x0 -> x2, Pallas kernels: none -> 6.39 us  [the longest x1 5.43 us: experts(): pl.pallas_call(kernel, in_specs=[pl.BlockSpec(memory_space=pltpu.SMEM)] +...]
    dot_general x14 -> x2, matrix products: 6.56 us -> 0.63 us  [the longest x1 0.41 us: layer(): jnp.dot(activated.astype(jnp.bfloat16), w_out, preferred_element_type=jnp...]
    reshape x0 -> x3, local copies, waits for them, and re-layouts: none -> 3.54 us  [the longest x2 3.53 us: layer(): jnp.concatenate([w_group, w_expert], axis=-1).reshape(shares, share, -1)]
    unnamed x43 -> x49, local copies, waits for them, and re-layouts: 6.3 us -> 2.98 us
  transfers between devices with their start and end apart: 9 -> 17, of which waited for: 8 -> 9; matrix products, arithmetic and copies ran while one was open for 6% -> 12% of each run, Pallas kernels for 0% -> 0%
where the time goes in v2:
time: 143 us; the launch traced here: 142 us
  waiting for transfers between devices  58.1 us (41%)
  starting transfers between devices  49 us (34%)
  local copies, waits for them, and re-layouts  11.5 us (8%)
  other arithmetic  9.68 us (7%)
  Pallas kernels  6.39 us (4%)
  matrix products  6.3 us (4%)
    all_to_all x2, waiting for transfers between devices, exchange(): return lax.all_to_all(x, axis, 0, 0, tiled=True)  36.9 us
    all_to_all x2, starting transfers between devices, exchange(): return lax.all_to_all(x, axis, 0, 0, tiled=True)  29.5 us
    ppermute x15, waiting for transfers between devices, shifted(): lax.ppermute(pieces[k], axis, [(i, (i + k) % size) for i in range(size)])  21.1 us
    ppermute x15, starting transfers between devices, shifted(): lax.ppermute(pieces[k], axis, [(i, (i + k) % size) for i in range(size)])  19.5 us
    pallas_call x1, Pallas kernels, experts(): pl.pallas_call(kernel, in_specs=[pl.BlockSpec(memory_space=pltpu.SMEM)] +...  5.43 us
    reshape x2, local copies, waits for them, and re-layouts, layer(): jnp.concatenate([w_group, w_expert], axis=-1).reshape(shares, share, -1)  3.53 us
    unnamed x49, local copies, waits for them, and re-layouts  2.98 us
  transfers between devices with their start and end apart: 17, of which 9 were waited for; matrix products, arithmetic and copies ran while one was open for 12% of the time, Pallas kernels for 0%

profile of v2, /device:TPU:40, one launch (start us, length us, event | category | flops | bytes accessed | tf_op | source)
XLA Modules:
  0.0 142.1 jit_solution(13833480539701557994)
XLA Ops:
  0.7 0.8 exp.16
  1.5 1.9 %convolution_convert_fusion.3 = bf16[64,384]{1,0:T(8,128)(2,1)S(1)} fusion(bf16[64,2048]{1,0:T(8,128)(2,1)} %param.18, bf16[2048,384]{1,0:T(8,128)(2,1)} %param.21), kind=kOutput, calls=%fused_computation.13 | convolution fusion | flops 100687872 | bytes 1884160 | tf_op jit(solution)/shard_map/dot_general | solution.py:256
  3.8 0.4 copy-done.16
  4.5 0.5 fusion
  5.0 0.5 fusion.1
  6.2 1.4 fusion.19
  7.6 0.4 convolution_convert_fusion
  8.1 0.7 copy-done.7
  8.8 1.7 %collective-permute-start = (bf16[64,512]{1,0:T(8,128)(2,1)S(1)}, bf16[64,512]{1,0:T(8,128)(2,1)S(1)}, u32[]{:S(2)}, u32[]{:S(2)}) collective-permute-start(bf16[64,512]{1,0:T(8,128)(2,1)S(1)} %get-tuple-element.20), channel_id=1, source_target_pairs={{0,1},{1,2},{2,3},{3,0},{4,5},{5,6},{6,7},{7,4},{8,9},{9,10},{10,1... | collective-permute-start | bytes 196616 | tf_op jit(solution)/shard_map/ppermute | solution.py:19
  10.5 1.7 %collective-permute-start.2 = (bf16[64,512]{1,0:T(8,128)(2,1)S(1)}, bf16[64,512]{1,0:T(8,128)(2,1)S(1)}, u32[]{:S(2)}, u32[]{:S(2)}) collective-permute-start(bf16[64,512]{1,0:T(8,128)(2,1)S(1)} %get-tuple-element.21), channel_id=1, source_target_pairs={{0,3},{1,0},{2,1},{3,2},{4,7},{5,4},{6,5},{7,6},{8,11},{9,8},{10,9... | collective-permute-start | bytes 196616 | tf_op jit(solution)/shard_map/ppermute | solution.py:19
  12.2 2.0 %collective-permute-start.1 = (bf16[64,512]{1,0:T(8,128)(2,1)S(1)}, bf16[64,512]{1,0:T(8,128)(2,1)S(1)}, u32[]{:S(2)}, u32[]{:S(2)}) collective-permute-start(bf16[64,512]{1,0:T(8,128)(2,1)S(1)} %get-tuple-element.22), channel_id=1, source_target_pairs={{0,2},{1,3},{2,0},{3,1},{4,6},{5,7},{6,4},{7,5},{8,10},{9,11},{10,... | collective-permute-start | bytes 196616 | tf_op jit(solution)/shard_map/ppermute | solution.py:19
  14.9 3.1 %collective-permute-done.1 = bf16[64,512]{1,0:T(8,128)(2,1)S(1)} collective-permute-done((bf16[64,512]{1,0:T(8,128)(2,1)S(1)}, bf16[64,512]{1,0:T(8,128)(2,1)S(1)}, u32[]{:S(2)}, u32[]{:S(2)}) %collective-permute-start.1) | collective-permute-done | bytes 65568 | tf_op jit(solution)/shard_map/ppermute | solution.py:19
  18.0 0.9 add_convert_fusion.1
  18.9 1.0 fusion.2
  19.9 24.7 %all-to-all-start = ((bf16[32,8,512]{2,1,0:T(8,128)(2,1)}), bf16[32,8,512]{2,1,0:T(8,128)(2,1)S(1)}, u32[]{:S(2)}, u32[]{:S(2)}) async-start(bf16[32,8,512]{2,1,0:T(8,128)(2,1)} %fusion.2), calls=%async_computation | async-start | bytes 524288 | tf_op jit(solution)/shard_map/all_to_all | solution.py:13
  44.6 0.6 fusion.42
  45.2 0.8 pad_maximum_fusion.1
  46.0 1.9 %collective-permute-start.5 = (bf16[64,512]{1,0:T(8,128)(2,1)S(1)}, bf16[64,512]{1,0:T(8,128)(2,1)S(1)}, u32[]{:S(2)}, u32[]{:S(2)}) collective-permute-start(bf16[64,512]{1,0:T(8,128)(2,1)S(1)} %add_convert_fusion.1), channel_id=1, source_target_pairs={{0,3},{1,0},{2,1},{3,2},{4,7},{5,4},{6,5},{7,6},{8,11},{9,8},{10,9... | collective-permute-start | bytes 196616 | tf_op jit(solution)/shard_map/ppermute | solution.py:19
  47.9 0.6 collective-permute-start.4
  48.6 1.0 collective-permute-start.3
  49.6 17.0 %all-to-all-done = bf16[32,8,512]{2,1,0:T(8,128)(2,1)S(1)} async-done(((bf16[32,8,512]{2,1,0:T(8,128)(2,1)}), bf16[32,8,512]{2,1,0:T(8,128)(2,1)S(1)}, u32[]{:S(2)}, u32[]{:S(2)}) %all-to-all-start) | async-done | bytes 262176 | tf_op jit(solution)/shard_map/all_to_all | solution.py:13
  66.6 1.9 %collective-permute-start.8 = (bf16[256,512]{1,0:T(8,128)(2,1)S(1)}, bf16[256,512]{1,0:T(8,128)(2,1)S(1)}, u32[]{:S(2)}, u32[]{:S(2)}) collective-permute-start(bf16[256,512]{1,0:T(8,128)(2,1)S(1)} %bitcast.54), channel_id=1, source_target_pairs={{0,3},{1,0},{2,1},{3,2},{4,7},{5,4},{6,5},{7,6},{8,11},{9,8},{10,9... | collective-permute-start | bytes 786440 | tf_op jit(solution)/shard_map/ppermute | solution.py:19
  68.5 0.5 collective-permute-start.7
  69.0 1.3 collective-permute-start.6
  70.4 0.6 pad_clamp_fusion
  71.0 1.8 %reshape.163 = bf16[4,512,68]{1,0,2:T(4,128)(2,1)} reshape(bf16[2048,68]{0,1:T(8,128)(2,1)} %pad_maximum_fusion.1) | data formatting | bytes 557056 | tf_op jit(solution)/shard_map/reshape | solution.py:282
  72.8 1.7 %copy.47 = bf16[4,512,68]{1,2,0:T(8,128)(2,1)} copy(bf16[4,512,68]{1,0,2:T(4,128)(2,1)} %reshape.163) | data formatting | bytes 557056 | tf_op jit(solution)/shard_map/reshape | solution.py:282
  74.5 1.3 gather_fusion
  75.8 2.4 %gather_fusion.1 = bf16[4,512,68]{1,2,0:T(8,128)(2,1)} fusion(bf16[4,512,68]{1,2,0:T(8,128)(2,1)} %copy.47, s32[1024]{0:T(1024)} %pad_clamp_fusion), kind=kCustom, calls=%fused_computation.1 | custom fusion | bytes 557072 | tf_op jit(solution)/shard_map/gather | solution.py:282
  78.1 1.0 convert_reduce_fusion
  79.2 0.6 collective-permute-done.8.refs_3_
  79.8 3.7 %collective-permute-done.6.refs_1_ = bf16[256,512]{1,0:T(8,128)(2,1)S(1)} collective-permute-done((bf16[256,512]{1,0:T(8,128)(2,1)S(1)}, bf16[256,512]{1,0:T(8,128)(2,1)S(1)}, u32[]{:S(2)}, u32[]{:S(2)}) %collective-permute-start.6) | collective-permute-done | bytes 262176 | tf_op jit(solution)/shard_map/ppermute | solution.py:19
  83.5 5.4 %experts.1 = (bf16[256,512]{1,0:T(8,128)(2,1)S(1)}, bf16[256,512]{1,0:T(8,128)(2,1)S(1)}, bf16[256,512]{1,0:T(8,128)(2,1)S(1)}, bf16[256,512]{1,0:T(8,128)(2,1)S(1)}) custom-call(s32[1]{0:T(128)} %bitcast.here_ref, bf16[256,512]{1,0:T(8,128)(2,1)S(1)} %bitcast.57, bf16[256,512]{1,0:T(8,128)(2,1)S(1)} %collective-permute-done.6.refs_1_, ...), custom_call_target="tpu_custom_call" | custom-call | tf_op jit(solution)/shard_map/experts/pallas_call | solution.py:160
  89.1 2.0 %collective-permute-start.10 = (bf16[256,512]{1,0:T(8,128)(2,1)S(1)}, bf16[256,512]{1,0:T(8,128)(2,1)S(1)}, u32[]{:S(2)}, u32[]{:S(2)}) collective-permute-start(bf16[256,512]{1,0:T(8,128)(2,1)S(1)} %get-tuple-element.8), channel_id=1, source_target_pairs={{0,2},{1,3},{2,0},{3,1},{4,6},{5,7},{6,4},{7,5},{8,10},{9,11},{10,... | collective-permute-start | bytes 786440 | tf_op jit(solution)/shard_map/ppermute | solution.py:19
  91.1 1.2 collective-permute-start.11
  92.3 1.1 fusion.7
  93.4 10.7 %collective-permute-done.9 = bf16[256,512]{1,0:T(8,128)(2,1)S(1)} collective-permute-done((bf16[256,512]{1,0:T(8,128)(2,1)S(1)}, bf16[256,512]{1,0:T(8,128)(2,1)S(1)}, u32[]{:S(2)}, u32[]{:S(2)}) %collective-permute-start.9) | collective-permute-done | bytes 262176 | tf_op jit(solution)/shard_map/ppermute | solution.py:19
  104.1 0.6 collective-permute-done.11
  104.7 0.8 fusion.9
  105.6 4.8 %all-to-all-start.1 = ((bf16[32,8,512]{2,1,0:T(8,128)(2,1)}), bf16[32,8,512]{2,1,0:T(8,128)(2,1)S(1)}, u32[]{:S(2)}, u32[]{:S(2)}) async-start(bf16[32,8,512]{2,1,0:T(8,128)(2,1)} %fusion.9), calls=%async_computation.1 | async-start | bytes 524288 | tf_op jit(solution)/shard_map/all_to_all | solution.py:13
  110.4 1.0 fusion.8.hidden_ref
  112.4 19.9 %all-to-all-done.1 = bf16[32,8,512]{2,1,0:T(8,128)(2,1)S(1)} async-done(((bf16[32,8,512]{2,1,0:T(8,128)(2,1)}), bf16[32,8,512]{2,1,0:T(8,128)(2,1)S(1)}, u32[]{:S(2)}, u32[]{:S(2)}) %all-to-all-start.1) | async-done | bytes 262176 | tf_op jit(solution)/shard_map/all_to_all | solution.py:13
  132.5 2.5 %collective-permute-start.14 = (bf16[64,512]{1,0:T(8,128)(2,1)S(1)}, bf16[64,512]{1,0:T(8,128)(2,1)S(1)}, u32[]{:S(2)}, u32[]{:S(2)}) collective-permute-start(bf16[64,512]{1,0:T(8,128)(2,1)S(1)} %convolution_convert_fusion.2.refs_0_), channel_id=1, source_target_pairs={{0,3},{1,0},{2,1},{3,2},{4,7},{5,4},{6,5},{7,6},{8,11},{9,8},{10,9... | collective-permute-start | bytes 196616 | tf_op jit(solution)/shard_map/ppermute | solution.py:19
  134.9 1.0 collective-permute-start.12
  135.9 1.4 pad_maximum_fusion
  137.4 1.3 copy.48
  138.7 2.1 %collective-permute-done.13.refs_2_ = bf16[64,512]{1,0:T(8,128)(2,1)S(1)} collective-permute-done((bf16[64,512]{1,0:T(8,128)(2,1)S(1)}, bf16[64,512]{1,0:T(8,128)(2,1)S(1)}, u32[]{:S(2)}, u32[]{:S(2)}) %collective-permute-start.13) | collective-permute-done | bytes 65568 | tf_op jit(solution)/shard_map/ppermute | solution.py:19
  141.1 1.0 finish.1
  (84 shorter events, 3.6 us)
Async XLA Ops:
  0.6 7.0 %copy-start = (bf16[384,2048]{1,0:T(8,128)(2,1)S(1)}, bf16[384,2048]{1,0:T(8,128)(2,1)}, u32[]{:S(2)}) copy-start(bf16[384,2048]{1,0:T(8,128)(2,1)} %param.28) | copy-start | bytes 4718596
  0.6 2.8 %copy-start.4 = (f32[64,24,128]{2,1,0:T(8,128)S(1)}, f32[64,24,128]{2,1,0:T(8,128)}, u32[]{:S(2)}) copy-start(f32[64,24,128]{2,1,0:T(8,128)} %param.19) | copy-start | bytes 2359300
  3.5 0.7 copy-start.16
  3.5 0.7 copy-start.17
  3.5 0.9 copy-start.9
  5.0 0.7 copy-start.22
  5.0 0.9 copy-start.8
  5.6 2.0 %copy-start.3 = (f32[64,24,64]{2,0,1:T(8,128)}, f32[64,24,64]{2,0,1:T(8,128)S(1)}, u32[]{:S(2)}) copy-start(f32[64,24,64]{2,0,1:T(8,128)S(1)} %fusion.1) | copy-start | bytes 1179652
  6.2 8.0 %copy-start.6 = (bf16[64,2048]{1,0:T(8,128)(2,1)S(1)}, bf16[64,2048]{1,0:T(8,128)(2,1)}, u32[]{:S(2)}) copy-start(bf16[64,2048]{1,0:T(8,128)(2,1)} %param.18) | copy-start | bytes 786436
  7.6 6.8 %copy-start.14 = (s32[64,2]{0,1:T(2,128)S(1)}, s32[64,2]{0,1:T(2,128)}, u32[]{:S(2)}) copy-start(s32[64,2]{0,1:T(2,128)} %param.20) | copy-start | bytes 1540
  8.0 0.7 copy-start.7
  8.8 36.5 %copy-start.11 = (bf16[2048,64]{0,1:T(8,128)(2,1)S(1)}, bf16[2048,64]{0,1:T(8,128)(2,1)}, u32[]{:S(2)}) copy-start(bf16[2048,64]{0,1:T(8,128)(2,1)} %param.31) | copy-start | bytes 786436
  8.8 36.5 %copy-start.13 = (bf16[2048,4]{0,1:T(4,128)(2,1)S(1)}, bf16[2048,4]{0,1:T(4,128)(2,1)}, u32[]{:S(2)}) copy-start(bf16[2048,4]{0,1:T(4,128)(2,1)} %param.30) | copy-start | bytes 49156
  8.8 62.2 %copy-start.1 = (f32[2048]{0:T(1024)S(1)}, f32[2048]{0:T(1024)}, u32[]{:S(2)}) copy-start(f32[2048]{0:T(1024)} %param.29) | copy-start | bytes 24580
  8.8 6.1 %collective-permute-start = (bf16[64,512]{1,0:T(8,128)(2,1)S(1)}, bf16[64,512]{1,0:T(8,128)(2,1)S(1)}, u32[]{:S(2)}, u32[]{:S(2)}) collective-permute-start(bf16[64,512]{1,0:T(8,128)(2,1)S(1)} %get-tuple-element.20), channel_id=1, source_target_pairs={{0,1},{1,2},{2,3},{3,0},{4,5},{5,6},{6,7},{7,4},{8,9},{9,10},{10,1... | collective-permute-start | bytes 196616 | tf_op jit(solution)/shard_map/ppermute | solution.py:19
  10.5 4.4 %collective-permute-start.2 = (bf16[64,512]{1,0:T(8,128)(2,1)S(1)}, bf16[64,512]{1,0:T(8,128)(2,1)S(1)}, u32[]{:S(2)}, u32[]{:S(2)}) collective-permute-start(bf16[64,512]{1,0:T(8,128)(2,1)S(1)} %get-tuple-element.21), channel_id=1, source_target_pairs={{0,3},{1,0},{2,1},{3,2},{4,7},{5,4},{6,5},{7,6},{8,11},{9,8},{10,9... | collective-permute-start | bytes 196616 | tf_op jit(solution)/shard_map/ppermute | solution.py:19
  12.2 5.8 %collective-permute-start.1 = (bf16[64,512]{1,0:T(8,128)(2,1)S(1)}, bf16[64,512]{1,0:T(8,128)(2,1)S(1)}, u32[]{:S(2)}, u32[]{:S(2)}) collective-permute-start(bf16[64,512]{1,0:T(8,128)(2,1)S(1)} %get-tuple-element.22), channel_id=1, source_target_pairs={{0,2},{1,3},{2,0},{3,1},{4,6},{5,7},{6,4},{7,5},{8,10},{9,11},{10,... | collective-permute-start | bytes 196616 | tf_op jit(solution)/shard_map/ppermute | solution.py:19
  14.7 54.3 %copy-start.18 = (s32[64,2]{0,1:T(2,128)}, s32[64,2]{0,1:T(2,128)S(1)}, u32[]{:S(2)}) copy-start(s32[64,2]{0,1:T(2,128)S(1)} %multiply_add_fusion.1) | copy-start | bytes 1540
  19.9 46.7 %all-to-all-start = ((bf16[32,8,512]{2,1,0:T(8,128)(2,1)}), bf16[32,8,512]{2,1,0:T(8,128)(2,1)S(1)}, u32[]{:S(2)}, u32[]{:S(2)}) async-start(bf16[32,8,512]{2,1,0:T(8,128)(2,1)} %fusion.2), calls=%async_computation | async-start | bytes 524288 | tf_op jit(solution)/shard_map/all_to_all | solution.py:13
  46.0 23.0 %collective-permute-start.5 = (bf16[64,512]{1,0:T(8,128)(2,1)S(1)}, bf16[64,512]{1,0:T(8,128)(2,1)S(1)}, u32[]{:S(2)}, u32[]{:S(2)}) collective-permute-start(bf16[64,512]{1,0:T(8,128)(2,1)S(1)} %add_convert_fusion.1), channel_id=1, source_target_pairs={{0,3},{1,0},{2,1},{3,2},{4,7},{5,4},{6,5},{7,6},{8,11},{9,8},{10,9... | collective-permute-start | bytes 196616 | tf_op jit(solution)/shard_map/ppermute | solution.py:19
  47.9 30.2 %collective-permute-start.4 = (bf16[64,512]{1,0:T(8,128)(2,1)S(1)}, bf16[64,512]{1,0:T(8,128)(2,1)}, u32[]{:S(2)}, u32[]{:S(2)}) collective-permute-start(bf16[64,512]{1,0:T(8,128)(2,1)S(1)} %add_convert_fusion.1), channel_id=1, source_target_pairs={{0,2},{1,3},{2,0},{3,1},{4,6},{5,7},{6,4},{7,5},{8,10},{9,11},{10,... | collective-permute-start | bytes 196616 | tf_op jit(solution)/shard_map/ppermute | solution.py:19
  48.6 29.6 %collective-permute-start.3 = (bf16[64,512]{1,0:T(8,128)(2,1)S(1)}, bf16[64,512]{1,0:T(8,128)(2,1)}, u32[]{:S(2)}, u32[]{:S(2)}) collective-permute-start(bf16[64,512]{1,0:T(8,128)(2,1)S(1)} %add_convert_fusion.1), channel_id=1, source_target_pairs={{0,1},{1,2},{2,3},{3,0},{4,5},{5,6},{6,7},{7,4},{8,9},{9,10},{10,1... | collective-permute-start | bytes 196616 | tf_op jit(solution)/shard_map/ppermute | solution.py:19
  66.6 13.2 %collective-permute-start.8 = (bf16[256,512]{1,0:T(8,128)(2,1)S(1)}, bf16[256,512]{1,0:T(8,128)(2,1)S(1)}, u32[]{:S(2)}, u32[]{:S(2)}) collective-permute-start(bf16[256,512]{1,0:T(8,128)(2,1)S(1)} %bitcast.54), channel_id=1, source_target_pairs={{0,3},{1,0},{2,1},{3,2},{4,7},{5,4},{6,5},{7,6},{8,11},{9,8},{10,9... | collective-permute-start | bytes 786440 | tf_op jit(solution)/shard_map/ppermute | solution.py:19
  68.5 11.3 %collective-permute-start.7 = (bf16[256,512]{1,0:T(8,128)(2,1)S(1)}, bf16[256,512]{1,0:T(8,128)(2,1)S(1)}, u32[]{:S(2)}, u32[]{:S(2)}) collective-permute-start(bf16[256,512]{1,0:T(8,128)(2,1)S(1)} %bitcast.55), channel_id=1, source_target_pairs={{0,2},{1,3},{2,0},{3,1},{4,6},{5,7},{6,4},{7,5},{8,10},{9,11},{10,... | collective-permute-start | bytes 786440 | tf_op jit(solution)/shard_map/ppermute | solution.py:19
  69.0 23.3 %copy-start.10 = (bf16[64,512]{1,0:T(8,128)(2,1)}, bf16[64,512]{1,0:T(8,128)(2,1)S(1)}, u32[]{:S(2)}) copy-start(bf16[64,512]{1,0:T(8,128)(2,1)S(1)} %collective-permute-done.5) | copy-start | bytes 196612
  69.0 14.4 %collective-permute-start.6 = (bf16[256,512]{1,0:T(8,128)(2,1)S(1)}, bf16[256,512]{1,0:T(8,128)(2,1)S(1)}, u32[]{:S(2)}, u32[]{:S(2)}) collective-permute-start(bf16[256,512]{1,0:T(8,128)(2,1)S(1)} %bitcast.56), channel_id=1, source_target_pairs={{0,1},{1,2},{2,3},{3,0},{4,5},{5,6},{6,7},{7,4},{8,9},{9,10},{10,1... | collective-permute-start | bytes 786440 | tf_op jit(solution)/shard_map/ppermute | solution.py:19
  79.1 13.1 %copy-start.20 = (f32[64]{0:T(128)}, f32[64]{0:T(128)S(1)}, u32[]{:S(2)}) copy-start(f32[64]{0:T(128)S(1)} %broadcast_multiply_fusion) | copy-start | bytes 772
  88.9 21.4 %copy-start.12 = (f32[4,512]{1,0:T(4,128)S(1)}, f32[4,512]{1,0:T(4,128)}, u32[]{:S(2)}) copy-start(f32[4,512]{1,0:T(4,128)} %gather_fusion) | copy-start | bytes 24580
  88.9 22.5 %copy-start.5 = (bf16[4,512,68]{1,2,0:T(8,128)(2,1)S(1)}, bf16[4,512,68]{1,2,0:T(8,128)(2,1)}, u32[]{:S(2)}) copy-start(bf16[4,512,68]{1,2,0:T(8,128)(2,1)} %gather_fusion.1) | copy-start | bytes 835588
  88.9 15.2 %collective-permute-start.9 = (bf16[256,512]{1,0:T(8,128)(2,1)S(1)}, bf16[256,512]{1,0:T(8,128)(2,1)S(1)}, u32[]{:S(2)}, u32[]{:S(2)}) collective-permute-start(bf16[256,512]{1,0:T(8,128)(2,1)S(1)} %get-tuple-element.7), channel_id=1, source_target_pairs={{0,1},{1,2},{2,3},{3,0},{4,5},{5,6},{6,7},{7,4},{8,9},{9,10},{10,1... | collective-permute-start | bytes 786440 | tf_op jit(solution)/shard_map/ppermute | solution.py:19
  89.1 15.0 %collective-permute-start.10 = (bf16[256,512]{1,0:T(8,128)(2,1)S(1)}, bf16[256,512]{1,0:T(8,128)(2,1)S(1)}, u32[]{:S(2)}, u32[]{:S(2)}) collective-permute-start(bf16[256,512]{1,0:T(8,128)(2,1)S(1)} %get-tuple-element.8), channel_id=1, source_target_pairs={{0,2},{1,3},{2,0},{3,1},{4,6},{5,7},{6,4},{7,5},{8,10},{9,11},{10,... | collective-permute-start | bytes 786440 | tf_op jit(solution)/shard_map/ppermute | solution.py:19
  91.1 13.6 %collective-permute-start.11 = (bf16[256,512]{1,0:T(8,128)(2,1)S(1)}, bf16[256,512]{1,0:T(8,128)(2,1)S(1)}, u32[]{:S(2)}, u32[]{:S(2)}) collective-permute-start(bf16[256,512]{1,0:T(8,128)(2,1)S(1)} %get-tuple-element.9), channel_id=1, source_target_pairs={{0,3},{1,0},{2,1},{3,2},{4,7},{5,4},{6,5},{7,6},{8,11},{9,8},{10,9... | collective-permute-start | bytes 786440 | tf_op jit(solution)/shard_map/ppermute | solution.py:19
  93.4 17.0 %copy-start.21 = (f32[64]{0:T(128)S(1)}, f32[64]{0:T(128)}, u32[]{:S(2)}) copy-start(f32[64]{0:T(128)} %copy-done.20) | copy-start | bytes 772
  104.7 7.0 %copy-start.15 = (s32[64,2]{0,1:T(2,128)S(1)}, s32[64,2]{0,1:T(2,128)}, u32[]{:S(2)}) copy-start(s32[64,2]{0,1:T(2,128)} %param.20) | copy-start | bytes 1540
  104.7 7.3 %copy-start.23 = (s32[64]{0:T(128)S(1)}, s32[64]{0:T(128)}, u32[]{:S(2)}) copy-start(s32[64]{0:T(128)} %fusion.42) | copy-start | bytes 772
  104.7 7.5 %copy-start.19 = (s32[64,2]{0,1:T(2,128)S(1)}, s32[64,2]{0,1:T(2,128)}, u32[]{:S(2)}) copy-start(s32[64,2]{0,1:T(2,128)} %copy-done.18) | copy-start | bytes 1540
  105.6 26.7 %all-to-all-start.1 = ((bf16[32,8,512]{2,1,0:T(8,128)(2,1)}), bf16[32,8,512]{2,1,0:T(8,128)(2,1)S(1)}, u32[]{:S(2)}, u32[]{:S(2)}) async-start(bf16[32,8,512]{2,1,0:T(8,128)(2,1)} %fusion.9), calls=%async_computation.1 | async-start | bytes 524288 | tf_op jit(solution)/shard_map/all_to_all | solution.py:13
  132.5 8.6 %copy-start.2 = (f32[2048]{0:T(1024)S(1)}, f32[2048]{0:T(1024)}, u32[]{:S(2)}) copy-start(f32[2048]{0:T(1024)} %param.35) | copy-start | bytes 24580
  132.5 6.2 %collective-permute-start.14 = (bf16[64,512]{1,0:T(8,128)(2,1)S(1)}, bf16[64,512]{1,0:T(8,128)(2,1)S(1)}, u32[]{:S(2)}, u32[]{:S(2)}) collective-permute-start(bf16[64,512]{1,0:T(8,128)(2,1)S(1)} %convolution_convert_fusion.2.refs_0_), channel_id=1, source_target_pairs={{0,3},{1,0},{2,1},{3,2},{4,7},{5,4},{6,5},{7,6},{8,11},{9,8},{10,9... | collective-permute-start | bytes 196616 | tf_op jit(solution)/shard_map/ppermute | solution.py:19
  134.9 5.9 %collective-permute-start.13 = (bf16[64,512]{1,0:T(8,128)(2,1)S(1)}, bf16[64,512]{1,0:T(8,128)(2,1)S(1)}, u32[]{:S(2)}, u32[]{:S(2)}) collective-permute-start(bf16[64,512]{1,0:T(8,128)(2,1)S(1)} %convolution_convert_fusion.2.refs_0_), channel_id=1, source_target_pairs={{0,2},{1,3},{2,0},{3,1},{4,6},{5,7},{6,4},{7,5},{8,10},{9,11},{10,... | collective-permute-start | bytes 196616 | tf_op jit(solution)/shard_map/ppermute | solution.py:19
  134.9 6.2 %collective-permute-start.12 = (bf16[64,512]{1,0:T(8,128)(2,1)S(1)}, bf16[64,512]{1,0:T(8,128)(2,1)S(1)}, u32[]{:S(2)}, u32[]{:S(2)}) collective-permute-start(bf16[64,512]{1,0:T(8,128)(2,1)S(1)} %convolution_convert_fusion.2.refs_0_), channel_id=1, source_target_pairs={{0,1},{1,2},{2,3},{3,0},{4,5},{5,6},{6,7},{7,4},{8,9},{9,10},{10,1... | collective-permute-start | bytes 196616 | tf_op jit(solution)/shard_map/ppermute | solution.py:19

commit v3 on v2

v3 whole, which is shorter than its diff:
```python
import jax
import jax.numpy as jnp
from jax import lax
from jax.experimental import pallas as pl
from jax.experimental.pallas import tpu as pltpu
from jax.sharding import PartitionSpec as P

residual_scale = 8.0**0.25
norm_eps = 1e-05


def exchange(x, axis):
    return lax.all_to_all(x, axis, 0, 0, tiled=True)


def shifted(pieces, axis):
    size = lax.axis_size(axis)
    return [pieces[0]] + [
        lax.ppermute(pieces[k], axis, [(i, (i + k) % size) for i in range(size)])
        for k in range(1, size)
    ]


def normalize(values, gain, axes):
    centre = jnp.mean(values, axes, keepdims=True)
    spread = jnp.mean(jnp.square(values - centre), axes, keepdims=True)
    return (values - centre) * lax.rsqrt(spread + norm_eps) * gain


def route_weights(logits, routes, group_total):
    expert_total = logits.shape[1] - group_total
    per_group = expert_total // group_total
    group_logit = logits[:, :group_total]
    group_exp = jnp.exp(group_logit)
    group_prob = group_exp / jnp.sum(group_exp, -1, keepdims=True)
    chosen = routes[:, 0] // per_group
    group_pick = jnp.sum(
        jnp.where(
            chosen[:, None] == jnp.arange(group_total, dtype=jnp.int32)[None, :], group_prob, 0.0
        ),
        -1,
    )
    expert_logit = logits[:, group_total:]
    picked = jnp.sum(
        jnp.where(
            routes[:, :, None] == jnp.arange(expert_total, dtype=jnp.int32)[None, None, :],
            expert_logit[:, None, :],
            0.0,
        ),
        -1,
    )
    pair_exp = jnp.exp(picked)
    return pair_exp / jnp.sum(pair_exp, -1, keepdims=True) * group_pick[:, None]


def slots_of(routes, expert_total, capacity):
    hits = (routes[:, :, None] == jnp.arange(expert_total, dtype=jnp.int32)[None, None, :]).astype(
        jnp.int32
    )
    tally = jnp.sum(hits, axis=1)
    prior = jnp.cumsum(tally, axis=0) - tally
    return routes * capacity + jnp.sum(prior[:, None, :] * hits, axis=-1)


def ring_places(here_ref, shares):
    t = here_ref[0]
    froms = [lax.rem(t + shares - k, shares) for k in range(shares)]
    tos = [lax.rem(t + k, shares) for k in range(shares)]
    return froms, tos


def columns_of(place, share):
    return pl.ds(pl.multiple_of(place * share, share), share)


def near(ref):
    return pltpu.VMEM(ref.shape, ref.dtype)


def mixer(here, x_in, state, w_in, decay_rate, frequency, log_step, b_in, c_out, skip, w_out):
    seq_count, width = x_in.shape
    channels = w_in.shape[1]
    groups, entries = decay_rate.shape
    per_group = b_in.shape[1]
    lanes = 2 * entries
    shares = lax.axis_size("tp")
    share = width // shares
    together = lanes // per_group
    cut = 4
    arrays = (decay_rate, frequency, log_step, x_in, w_in, b_in, state, c_out, skip, w_out)

    def kernel(here_ref, *refs):
        far = refs[: len(arrays)]
        base_ref = refs[len(arrays)]
        part_refs = refs[len(arrays) + 1 : len(arrays) + shares]
        new_far = refs[len(arrays) + shares]
        rest = refs[len(arrays) + shares + 1 :]
        close = rest[: len(arrays)]
        decay_ref, freq_ref, log_ref, x_ref, w_in_ref, b_ref, state_ref, c_ref, skip_ref, w_out_ref = close
        new_ref, in_ref, out_ref, act_ref, sems = rest[len(arrays) :]
        _, tos = ring_places(here_ref, shares)
        piece = width // cut
        copies = {}
        for i, (a, b) in enumerate(zip(far, close)):
            if i == 4:
                for q in range(cut):
                    rows = slice(q * piece, (q + 1) * piece)
                    copies[i, q] = pltpu.make_async_copy(
                        a.at[rows], b.at[rows], sems.at[len(arrays) + q]
                    )
            else:
                copies[i] = pltpu.make_async_copy(a, b, sems.at[i])
        for copy in copies.values():
            copy.start()

        lane = lax.broadcasted_iota(jnp.int32, (1, lanes), 1)
        sign = jnp.where(lane < entries, -1.0, 1.0)
        for i in (0, 1, 2):
            copies[i].wait()
        eye = lax.broadcasted_iota(jnp.int32, (groups, groups), 0) == lax.broadcasted_iota(
            jnp.int32, (groups, groups), 1
        )
        log_column = jnp.sum(jnp.where(eye, log_ref[...], 0.0), -1, keepdims=True)
        step_size = jnp.exp(log_column)
        lam_real = -decay_ref[...]
        freq = freq_ref[...]
        magnitude = jnp.exp(lam_real * step_size)
        angle = freq * step_size
        bar_real = magnitude * jnp.cos(angle)
        bar_imag = magnitude * jnp.sin(angle)
        minus_real = bar_real - 1.0
        modulus = lam_real * lam_real + freq * freq
        ratio_real = (minus_real * lam_real + bar_imag * freq) / modulus
        ratio_imag = (bar_imag * lam_real - minus_real * freq) / modulus

        def twice(v):
            return jnp.concatenate([v, v], axis=-1)

        bar_real = twice(bar_real)
        bar_imag = twice(bar_imag) * sign
        ratio_real = twice(ratio_real)
        ratio_imag = twice(ratio_imag) * sign

        copies[3].wait()
        x_wide = x_ref[...].astype(jnp.float32)
        x_mean = jnp.sum(x_wide, -1, keepdims=True) / width
        x_own = x_ref[:, columns_of(here_ref[0], share)].astype(jnp.float32)
        base_ref[...] = residual_scale * (x_own - x_mean)
        copies[5].wait()
        for g in range(groups):
            b = b_ref[g]
            in_ref[g * per_group : (g + 1) * per_group, :] = (
                ratio_real[g : g + 1] * b + ratio_imag[g : g + 1] * pltpu.roll(b, entries, 1)
            ).astype(jnp.bfloat16)
        copies[7].wait()
        for g in range(groups):
            out_ref[g * per_group : (g + 1) * per_group, :] = (c_ref[g] * -sign).astype(jnp.bfloat16)
        mix = None
        for q in range(cut):
            copies[4, q].wait()
            rows = slice(q * piece, (q + 1) * piece)
            term = jnp.dot(x_ref[:, rows], w_in_ref[rows, :], preferred_element_type=jnp.float32)
            mix = term if mix is None else mix + term
        mix = mix.astype(jnp.bfloat16).astype(jnp.float32)
        copies[6].wait()
        copies[8].wait()
        old = state_ref.reshape(seq_count * groups, lanes)
        new = new_ref.reshape(seq_count * groups, lanes)
        lane_group = lane // per_group
        for j in range(groups // together):
            span = slice(j * lanes, (j + 1) * lanes)
            inputs = mix[:, span]
            spread = jnp.concatenate(
                [jnp.where(lane_group == g, inputs, 0.0) for g in range(together)], axis=0
            ).astype(jnp.bfloat16)
            forcing = jnp.dot(spread, in_ref[span, :], preferred_element_type=jnp.float32)
            held = []
            for g in range(together):
                at = j * together + g
                rows = pl.ds(at, seq_count, stride=groups)
                h = old[rows, :]
                h = (
                    bar_real[at : at + 1] * h
                    + bar_imag[at : at + 1] * pltpu.roll(h, entries, 1)
                    + forcing[g * seq_count : (g + 1) * seq_count]
                )
                new[rows, :] = h
                held.append(h.astype(jnp.bfloat16))
            read = lax.dot_general(
                jnp.concatenate(held, axis=0),
                out_ref[span, :],
                (((1,), (1,)), ((), ())),
                preferred_element_type=jnp.float32,
            )
            value = skip_ref[:, span] * inputs
            for g in range(together):
                value = value + jnp.where(
                    lane_group == g, read[g * seq_count : (g + 1) * seq_count], 0.0
                )
            act_ref[:, span] = jax.nn.gelu(value).astype(jnp.bfloat16)
        send = pltpu.make_async_copy(new_ref, new_far, sems.at[len(arrays) + cut])
        send.start()
        copies[9].wait()
        for k in range(shares):
            part = jnp.dot(
                act_ref[...],
                w_out_ref[:, columns_of(tos[k], share)],
                preferred_element_type=jnp.float32,
            ).astype(jnp.bfloat16)
            if k == 0:
                base_ref[...] += part.astype(jnp.float32)
            else:
                part_refs[k - 1][...] = part
        send.wait()

    vmem = pl.BlockSpec(memory_space=pltpu.VMEM)
    hbm = pl.BlockSpec(memory_space=pltpu.HBM)
    return pl.pallas_call(
        kernel,
        in_specs=[pl.BlockSpec(memory_space=pltpu.SMEM)] + [hbm] * len(arrays),
        out_specs=[vmem] * shares + [hbm],
        out_shape=[jax.ShapeDtypeStruct((seq_count, share), jnp.float32)]
        + [jax.ShapeDtypeStruct((seq_count, share), jnp.bfloat16)] * (shares - 1)
        + [jax.ShapeDtypeStruct(state.shape, state.dtype)],
        scratch_shapes=[near(a) for a in arrays]
        + [
            near(state),
            pltpu.VMEM((channels, lanes), jnp.bfloat16),
            pltpu.VMEM((channels, lanes), jnp.bfloat16),
            pltpu.VMEM((seq_count, channels), jnp.bfloat16),
            pltpu.SemaphoreType.DMA((len(arrays) + cut + 1,)),
        ],
        compiler_params=pltpu.CompilerParams(vmem_limit_bytes=16 * 1024 * 1024),
        name="mixer",
    )(here, *[pltpu.with_memory_space_constraint(a, pltpu.HBM) for a in arrays])


def place_rows(base, arrived, target, total_slots):
    seq_count, share = base.shape

    def kernel(base_ref, target_ref, *refs):
        own_ref, sent_ref = refs[-2:]
        own = base_ref[...]
        for r in refs[:-2]:
            own = own + r[...].astype(jnp.float32)
        own = own.astype(jnp.bfloat16)
        own_ref[...] = own
        slot = lax.broadcasted_iota(jnp.int32, (total_slots, seq_count), 0)
        hit = slot == target_ref[0:1, :]
        for k in range(1, target_ref.shape[0]):
            hit = hit | (slot == target_ref[k : k + 1, :])
        chosen = jnp.where(hit, 1.0, 0.0).astype(jnp.bfloat16)
        sent_ref[...] = jnp.dot(chosen, own, preferred_element_type=jnp.float32).astype(jnp.bfloat16)

    vmem = pl.BlockSpec(memory_space=pltpu.VMEM)
    return pl.pallas_call(
        kernel,
        in_specs=[vmem] * (2 + len(arrived)),
        out_specs=[vmem] * 2,
        out_shape=[
            jax.ShapeDtypeStruct((seq_count, share), jnp.bfloat16),
            jax.ShapeDtypeStruct((total_slots, share), jnp.bfloat16),
        ],
        compiler_params=pltpu.CompilerParams(vmem_limit_bytes=8 * 1024 * 1024),
        name="place_rows",
    )(base, target.T, *arrived)


def fetch(*weights):
    count = len(weights)

    def kernel(*refs):
        copies = [
            pltpu.make_async_copy(refs[i], refs[count + i], refs[-1].at[i]) for i in range(count)
        ]
        for copy in copies:
            copy.start()
        for copy in copies:
            copy.wait()

    return pl.pallas_call(
        kernel,
        in_specs=[pl.BlockSpec(memory_space=pltpu.HBM)] * count,
        out_specs=[pl.BlockSpec(memory_space=pltpu.VMEM)] * count,
        out_shape=[pltpu.VMEM(w.shape, w.dtype) for w in weights],
        scratch_shapes=[pltpu.SemaphoreType.DMA((count,))],
        compiler_params=pltpu.CompilerParams(vmem_limit_bytes=1024 * 1024),
        name="fetch",
    )(*[pltpu.with_memory_space_constraint(w, pltpu.HBM) for w in weights])


def swap_halves(first, second):
    half = first.shape[1] // 2
    low = lax.broadcasted_iota(jnp.int32, first.shape, 1) < half
    return (
        jnp.where(low, first, pltpu.roll(second, half, 1)),
        jnp.where(low, pltpu.roll(first, half, 1), second),
    )


def experts(here, pieces, gain, w_gate, w_up, w_down):
    slots, share = pieces[0].shape
    shares = len(pieces)
    local_experts, width, hidden = w_gate.shape
    tile = 8
    chunk = 4 * tile
    kept = slots // local_experts

    def kernel(here_ref, *refs):
        piece_refs = refs[:shares]
        gain_ref, gate_ref, up_ref, down_ref = refs[shares : shares + 4]
        out_refs = refs[shares + 4 : 2 * shares + 4]
        row_ref, act_ref = refs[2 * shares + 4 :]
        froms, tos = ring_places(here_ref, shares)

        def norm_rows(i, carry):
            rows = pl.ds(pl.multiple_of(i * chunk, chunk), chunk)
            values = [r[rows, :].astype(jnp.float32) for r in piece_refs]
            total = values[0]
            for v in values[1:]:
                total = total + v
            centre = jnp.sum(total, -1, keepdims=True) / width
            values = [v - centre for v in values]
            total = values[0] * values[0]
            for v in values[1:]:
                total = total + v * v
            scale = lax.rsqrt(jnp.sum(total, -1, keepdims=True) / width + norm_eps)
            rows = pl.ds(pl.multiple_of(i * (chunk // 2), chunk // 2), chunk // 2)
            for k, v in enumerate(values):
                v = (v * scale * gain_ref[froms[k]]).reshape(2, 2, tile, share)
                for j, part in enumerate(swap_halves(v[:, 0], v[:, 1])):
                    row_ref[j, rows, columns_of(froms[k], share)] = part.reshape(
                        chunk // 2, share
                    ).astype(jnp.bfloat16)
            return carry

        lax.fori_loop(0, slots // chunk, norm_rows, 0)
        for j in range(local_experts):
            rows = row_ref[j]
            gate_part = jnp.dot(rows, gate_ref[j], preferred_element_type=jnp.float32)
            up_part = jnp.dot(rows, up_ref[j], preferred_element_type=jnp.float32)
            act_ref[j] = (gate_part * jax.nn.sigmoid(gate_part) * up_part).astype(jnp.bfloat16)
        for k in (1, shares - 1, *range(2, shares - 1), 0):
            outs = [
                jnp.dot(
                    act_ref[j],
                    down_ref[j, :, columns_of(tos[k], share)],
                    preferred_element_type=jnp.float32,
                ).reshape(kept // tile, tile, share)
                for j in range(local_experts)
            ]
            both = jnp.stack(swap_halves(*outs), axis=1).reshape(slots, share)
            out_refs[k][...] = both.astype(jnp.bfloat16)

    vmem = pl.BlockSpec(memory_space=pltpu.VMEM)
    return pl.pallas_call(
        kernel,
        in_specs=[pl.BlockSpec(memory_space=pltpu.SMEM)] + [vmem] * (shares + 4),
        out_specs=[vmem] * shares,
        out_shape=[jax.ShapeDtypeStruct((slots, share), jnp.bfloat16)] * shares,
        scratch_shapes=[
            pltpu.VMEM((local_experts, kept, width), jnp.bfloat16),
            pltpu.VMEM((local_experts, kept, hidden), jnp.bfloat16),
        ],
        compiler_params=pltpu.CompilerParams(vmem_limit_bytes=24 * 1024 * 1024),
        name="experts",
    )(here, *pieces, gain, w_gate, w_up, w_down)


def finish(here, hidden, pieces, gain):
    rows, share = pieces[0].shape
    shares = len(pieces)
    width = shares * share

    def kernel(here_ref, hidden_ref, *refs):
        piece_refs = refs[:shares]
        gain_ref, out_ref = refs[shares:]
        froms, _ = ring_places(here_ref, shares)
        values = [
            residual_scale * hidden_ref[k] + piece_refs[k][...].astype(jnp.float32)
            for k in range(shares)
        ]
        total = values[0]
        for v in values[1:]:
            total = total + v
        centre = jnp.sum(total, -1, keepdims=True) / width
        values = [v - centre for v in values]
        total = values[0] * values[0]
        for v in values[1:]:
            total = total + v * v
        scale = lax.rsqrt(jnp.sum(total, -1, keepdims=True) / width + norm_eps)
        for k, v in enumerate(values):
            out_ref[:, columns_of(froms[k], share)] = (v * scale * gain_ref[froms[k]]).astype(jnp.bfloat16)

    vmem = pl.BlockSpec(memory_space=pltpu.VMEM)
    return pl.pallas_call(
        kernel,
        in_specs=[pl.BlockSpec(memory_space=pltpu.SMEM)] + [vmem] * (shares + 2),
        out_specs=vmem,
        out_shape=jax.ShapeDtypeStruct((rows, width), jnp.bfloat16),
        compiler_params=pltpu.CompilerParams(vmem_limit_bytes=8 * 1024 * 1024),
        name="finish",
    )(here, hidden, *pieces, gain)


def layer(
    x_in,
    state,
    routes,
    w_in,
    decay_rate,
    frequency,
    log_step,
    b_in,
    c_out,
    skip,
    w_out,
    gain_mix,
    w_group,
    w_expert,
    w_gate,
    w_up,
    w_down,
    gain_moe,
):
    seq_count, model_width = x_in.shape
    shares = lax.axis_size("tp")
    share = model_width // shares
    expert_total = w_expert.shape[1]
    ep_count = lax.axis_size("ep")
    local_experts = w_gate.shape[0]
    capacity = max(2, 4 * seq_count // expert_total)
    total_slots = expert_total * capacity
    local_slots = local_experts * capacity
    here = lax.axis_index("tp")
    here_array = here.astype(jnp.int32).reshape(1)

    target = slots_of(routes, expert_total, capacity)
    slot_ids = jnp.arange(total_slots, dtype=jnp.int32)

    base, *parts, new_state = mixer(
        here_array,
        x_in,
        state,
        w_in,
        decay_rate,
        frequency,
        log_step.reshape(1, -1),
        b_in,
        c_out,
        skip.reshape(1, -1),
        w_out,
    )
    arrived = shifted([base, *parts], "tp")
    own, sent = place_rows(base, arrived[1:], target, total_slots)
    rows = exchange(sent.reshape(ep_count, local_slots, share), "ep")

    parts = shifted([own] * shares, "tp")
    whole = jnp.stack(parts).astype(jnp.float32)
    order = (here - jnp.arange(shares)) % shares
    gain_mix = gain_mix.reshape(shares, 1, share)
    hidden_state = normalize(whole, gain_mix[order], (0, 2))
    hidden_bf = hidden_state.astype(jnp.bfloat16)
    w_router = jnp.concatenate([w_group, w_expert], axis=-1).reshape(shares, share, -1)[order]
    logits = jnp.einsum("krd,kde->re", hidden_bf, w_router, preferred_element_type=jnp.float32)
    route_weight = route_weights(logits, routes, w_group.shape[1])
    matches = target[:, :, None] == slot_ids[None, None, :]
    combine_map = jnp.sum(jnp.where(matches, route_weight[:, :, None], 0.0), axis=1)

    rows = rows.reshape(total_slots, share)
    pieces = shifted([rows] * shares, "tp")
    weights = fetch(w_gate, w_up, w_down)
    outs = experts(here_array, pieces, gain_mix, *weights)
    arrived = shifted(outs, "tp")
    summed = sum(a.astype(jnp.float32) for a in arrived).astype(jnp.bfloat16)
    returned = exchange(summed.reshape(ep_count, local_slots, share), "ep")
    moe_own = jnp.dot(
        combine_map.astype(jnp.bfloat16),
        returned.reshape(total_slots, share),
        preferred_element_type=jnp.float32,
    ).astype(jnp.bfloat16)
    moe = shifted([moe_own] * shares, "tp")
    out = finish(here_array, hidden_state, moe, gain_moe.reshape(shares, 1, share))
    return (out, new_state)


def solution(mesh):
    in_specs = (
        P(("grp", "ep"), None),
        P(("grp", "ep"), "tp", None),
        P(("grp", "ep"), None),
        P(None, "tp"),
        P("tp", None),
        P("tp", None),
        P("tp"),
        P("tp", None, None),
        P("tp", None, None),
        P("tp"),
        P("tp", None),
        P(),
        P(),
        P(),
        P("ep", None, "tp"),
        P("ep", None, "tp"),
        P("ep", "tp", None),
        P(),
    )
    out_specs = (P(("grp", "ep"), None), P(("grp", "ep"), "tp", None))
    return jax.shard_map(layer, mesh=mesh, in_specs=in_specs, out_specs=out_specs, check_vma=False)
```

time: 143 us -> 135 us (0.944)
  local copies, waits for them, and re-layouts: 11.5 us -> 2.66 us
  waiting for transfers between devices: 58.1 us -> 65.9 us
  other arithmetic: 9.68 us -> 2.48 us
  matrix products: 6.3 us -> 0.38 us
  Pallas kernels: 6.39 us -> 11.8 us
  starting transfers between devices: 49 us -> 50.5 us
    pallas_call x0 -> x3, Pallas kernels: none -> 7.76 us  [the longest x1 3.93 us: mixer(): pl.pallas_call(kernel, in_specs=[pl.BlockSpec(memory_space=pltpu.SMEM)] +...]
    dot_general x7 -> x0, matrix products: 5.93 us -> none  [the longest x1 1.85 us: layer(): jnp.dot(x_in, w_in, preferred_element_type=jnp.float32).astype(jnp.bfloat16)]
    ppermute x15, waiting for transfers between devices: 21.1 us -> 26.9 us  [shifted(): lax.ppermute(pieces[k], axis, [(i, (i + k) % size) for i in range(size)])]
    reshape x2, local copies, waits for them, and re-layouts: 3.53 us -> 0.19 us  [layer(): jnp.concatenate([w_group, w_expert], axis=-1).reshape(shares, share, -1)]
    unnamed x49 -> x10, local copies, waits for them, and re-layouts: 2.98 us -> 0.02 us
    pallas_call x1, Pallas kernels: 5.43 us -> 3.04 us  [experts(): pl.pallas_call(kernel, in_specs=[pl.BlockSpec(memory_space=pltpu.SMEM)] +...]
    all_to_all x2, waiting for transfers between devices: 36.9 us -> 39.1 us  [exchange(): return lax.all_to_all(x, axis, 0, 0, tiled=True)]
    gather x1, local copies, waits for them, and re-layouts: 2.35 us -> 0.56 us  [layer(): jnp.concatenate([w_group, w_expert], axis=-1).reshape(shares, share, -1)]
  transfers between devices with their start and end apart: 17 -> 17, of which waited for: 9 -> 10; matrix products, arithmetic and copies ran while one was open for 12% -> 2% of each run, Pallas kernels for 0% -> 2%
where the time goes in v3:
time: 135 us
  waiting for transfers between devices  65.9 us (49%)
  starting transfers between devices  50.5 us (37%)
  Pallas kernels  11.8 us (9%)
  local copies, waits for them, and re-layouts  2.66 us (2%)
  other arithmetic  2.48 us (2%)
    all_to_all x2, waiting for transfers between devices, exchange(): return lax.all_to_all(x, axis, 0, 0, tiled=True)  39.1 us
    all_to_all x2, starting transfers between devices, exchange(): return lax.all_to_all(x, axis, 0, 0, tiled=True)  29.5 us
    ppermute x15, waiting for transfers between devices, shifted(): lax.ppermute(pieces[k], axis, [(i, (i + k) % size) for i in range(size)])  26.9 us
    ppermute x15, starting transfers between devices, shifted(): lax.ppermute(pieces[k], axis, [(i, (i + k) % size) for i in range(size)])  21 us
    pallas_call x1, Pallas kernels, mixer(): pl.pallas_call(kernel, in_specs=[pl.BlockSpec(memory_space=pltpu.SMEM)] +...  3.93 us
    pallas_call x1, Pallas kernels, experts(): pl.pallas_call(kernel, in_specs=[pl.BlockSpec(memory_space=pltpu.SMEM)] +...  3.04 us
    pallas_call x1, Pallas kernels, fetch(): pl.pallas_call(kernel, in_specs=[pl.BlockSpec(memory_space=pltpu.HBM)] *...  2.89 us
  transfers between devices with their start and end apart: 17, of which 10 were waited for; matrix products, arithmetic and copies ran while one was open for 2% of the time, Pallas kernels for 2%

profile of v3, /device:TPU:40, one launch (start us, length us, event | category | flops | bytes accessed | tf_op | source)
XLA Modules:
  0.0 134.6 jit_solution(13140382177236324383)
XLA Ops:
  0.6 1.2 reshape.145.refs_8_
  1.9 3.9 %mixer.1 = (f32[64,512]{1,0:T(8,128)S(1)}, bf16[64,512]{1,0:T(8,128)(2,1)S(1)}, bf16[64,512]{1,0:T(8,128)(2,1)S(1)}, bf16[64,512]{1,0:T(8,128)(2,1)S(1)}, f32[64,24,128]{2,1,0:T(8,128)}) custom-call(s32[1]{0:T(128)} %bitcast.here_ref, f32[24,64]{1,0:T(8,128)} %refs_0_.2, f32[24,64]{1,0:T(8,128)} %refs_1_.2, f32[1,24]{1,0:T(1,128)} %bitcast.45, ...), custom_call_target="tpu_custom_call" | custom-call | tf_op jit(solution)/shard_map/mixer/pallas_call | solution.py:218
  5.8 1.7 %collective-permute-start = (bf16[64,512]{1,0:T(8,128)(2,1)S(1)}, bf16[64,512]{1,0:T(8,128)(2,1)S(1)}, u32[]{:S(2)}, u32[]{:S(2)}) collective-permute-start(bf16[64,512]{1,0:T(8,128)(2,1)S(1)} %get-tuple-element.17), channel_id=1, source_target_pairs={{0,1},{1,2},{2,3},{3,0},{4,5},{5,6},{6,7},{7,4},{8,9},{9,10},{10,1... | collective-permute-start | bytes 196616 | tf_op jit(solution)/shard_map/ppermute | solution.py:19
  7.6 3.0 %collective-permute-start.1 = (bf16[64,512]{1,0:T(8,128)(2,1)S(1)}, bf16[64,512]{1,0:T(8,128)(2,1)S(1)}, u32[]{:S(2)}, u32[]{:S(2)}) collective-permute-start(bf16[64,512]{1,0:T(8,128)(2,1)S(1)} %get-tuple-element.18), channel_id=1, source_target_pairs={{0,2},{1,3},{2,0},{3,1},{4,6},{5,7},{6,4},{7,5},{8,10},{9,11},{10,... | collective-permute-start | bytes 196616 | tf_op jit(solution)/shard_map/ppermute | solution.py:19
  10.6 1.3 collective-permute-start.2
  12.0 0.1 reduce_window_sum.11
  12.1 0.2 select_reduce_fusion.2
  12.3 1.6 %collective-permute-done.1.refs_1_ = bf16[64,512]{1,0:T(8,128)(2,1)S(1)} collective-permute-done((bf16[64,512]{1,0:T(8,128)(2,1)S(1)}, bf16[64,512]{1,0:T(8,128)(2,1)S(1)}, u32[]{:S(2)}, u32[]{:S(2)}) %collective-permute-start.1) | collective-permute-done | bytes 65568 | tf_op jit(solution)/shard_map/ppermute | solution.py:19
  13.9 1.0 collective-permute-done.2.refs_2_
  14.8 0.9 place_rows.1
  15.8 24.7 %all-to-all-start = ((bf16[32,8,512]{2,1,0:T(8,128)(2,1)}), bf16[32,8,512]{2,1,0:T(8,128)(2,1)S(1)}, u32[]{:S(2)}, u32[]{:S(2)}) async-start(bf16[32,8,512]{2,1,0:T(8,128)(2,1)} %bitcast.10), calls=%async_computation | async-start | bytes 524288 | tf_op jit(solution)/shard_map/all_to_all | solution.py:13
  40.6 2.6 %collective-permute-start.5 = (bf16[64,512]{1,0:T(8,128)(2,1)S(1)}, bf16[64,512]{1,0:T(8,128)(2,1)S(1)}, u32[]{:S(2)}, u32[]{:S(2)}) collective-permute-start(bf16[64,512]{1,0:T(8,128)(2,1)S(1)} %get-tuple-element.20), channel_id=1, source_target_pairs={{0,3},{1,0},{2,1},{3,2},{4,7},{5,4},{6,5},{7,6},{8,11},{9,8},{10,9... | collective-permute-start | bytes 196616 | tf_op jit(solution)/shard_map/ppermute | solution.py:19
  43.3 0.1 collective-permute-start.4
  43.4 0.9 collective-permute-start.3
  44.3 18.2 %all-to-all-done = bf16[32,8,512]{2,1,0:T(8,128)(2,1)S(1)} async-done(((bf16[32,8,512]{2,1,0:T(8,128)(2,1)}), bf16[32,8,512]{2,1,0:T(8,128)(2,1)S(1)}, u32[]{:S(2)}, u32[]{:S(2)}) %all-to-all-start) | async-done | bytes 262176 | tf_op jit(solution)/shard_map/all_to_all | solution.py:13
  62.5 0.3 collective-permute-start.6
  62.8 3.7 %collective-permute-start.7 = (bf16[256,512]{1,0:T(8,128)(2,1)S(1)}, bf16[256,512]{1,0:T(8,128)(2,1)S(1)}, u32[]{:S(2)}, u32[]{:S(2)}) collective-permute-start(bf16[256,512]{1,0:T(8,128)(2,1)S(1)} %bitcast.27), channel_id=1, source_target_pairs={{0,2},{1,3},{2,0},{3,1},{4,6},{5,7},{6,4},{7,5},{8,10},{9,11},{10,... | collective-permute-start | bytes 786440 | tf_op jit(solution)/shard_map/ppermute | solution.py:19
  66.5 0.2 collective-permute-start.8
  66.7 0.1 reshape.147
  66.9 0.6 gather_fusion
  67.5 0.6 gather_fusion.1
  68.0 2.9 %fetch.1 = (bf16[2,2048,256]{2,1,0:T(8,128)(2,1)S(1)}, bf16[2,2048,256]{2,1,0:T(8,128)(2,1)S(1)}, bf16[2,256,2048]{2,1,0:T(8,128)(2,1)S(1)}) custom-call(bf16[2,2048,256]{2,1,0:T(8,128)(2,1)} %refs_0_.3, bf16[2,2048,256]{2,1,0:T(8,128)(2,1)} %refs_1_.3, bf16[2,256,2048]{2,1,0:T(8,128)(2,1)} %refs_2_.1), custom_call_target="tpu_custom_call" | custom-call | tf_op jit(solution)/shard_map/fetch/pallas_call | solution.py:281
  70.9 0.1 convert_reduce_fusion
  71.1 1.1 collective-permute-done.6.refs_1_
  72.2 6.0 %collective-permute-done.7.refs_2_ = bf16[256,512]{1,0:T(8,128)(2,1)S(1)} collective-permute-done((bf16[256,512]{1,0:T(8,128)(2,1)S(1)}, bf16[256,512]{1,0:T(8,128)(2,1)S(1)}, u32[]{:S(2)}, u32[]{:S(2)}) %collective-permute-start.7) | collective-permute-done | bytes 262176 | tf_op jit(solution)/shard_map/ppermute | solution.py:19
  78.2 3.0 %experts.1 = (bf16[256,512]{1,0:T(8,128)(2,1)S(1)}, bf16[256,512]{1,0:T(8,128)(2,1)S(1)}, bf16[256,512]{1,0:T(8,128)(2,1)S(1)}, bf16[256,512]{1,0:T(8,128)(2,1)S(1)}) custom-call(s32[1]{0:T(128)} %bitcast.here_ref, bf16[256,512]{1,0:T(8,128)(2,1)S(1)} %bitcast.29, bf16[256,512]{1,0:T(8,128)(2,1)S(1)} %collective-permute-done.6.refs_1_, ...), custom_call_target="tpu_custom_call" | custom-call | tf_op jit(solution)/shard_map/experts/pallas_call | solution.py:356
  81.3 2.6 %collective-permute-start.11 = (bf16[256,512]{1,0:T(8,128)(2,1)S(1)}, bf16[256,512]{1,0:T(8,128)(2,1)S(1)}, u32[]{:S(2)}, u32[]{:S(2)}) collective-permute-start(bf16[256,512]{1,0:T(8,128)(2,1)S(1)} %get-tuple-element.28), channel_id=1, source_target_pairs={{0,3},{1,0},{2,1},{3,2},{4,7},{5,4},{6,5},{7,6},{8,11},{9,8},{10,9... | collective-permute-start | bytes 786440 | tf_op jit(solution)/shard_map/ppermute | solution.py:19
  83.9 0.3 collective-permute-start.10
  84.2 0.9 collective-permute-start.9
  85.1 0.2 fusion.2
  85.3 9.9 %collective-permute-done.11 = bf16[256,512]{1,0:T(8,128)(2,1)S(1)} collective-permute-done((bf16[256,512]{1,0:T(8,128)(2,1)S(1)}, bf16[256,512]{1,0:T(8,128)(2,1)S(1)}, u32[]{:S(2)}, u32[]{:S(2)}) %collective-permute-start.11) | collective-permute-done | bytes 262176 | tf_op jit(solution)/shard_map/ppermute | solution.py:19
  95.3 3.4 %collective-permute-done.9 = bf16[256,512]{1,0:T(8,128)(2,1)S(1)} collective-permute-done((bf16[256,512]{1,0:T(8,128)(2,1)S(1)}, bf16[256,512]{1,0:T(8,128)(2,1)S(1)}, u32[]{:S(2)}, u32[]{:S(2)}) %collective-permute-start.9) | collective-permute-done | bytes 262176 | tf_op jit(solution)/shard_map/ppermute | solution.py:19
  98.7 0.8 fusion.4
  99.5 4.8 %all-to-all-start.1 = ((bf16[32,8,512]{2,1,0:T(8,128)(2,1)}), bf16[32,8,512]{2,1,0:T(8,128)(2,1)S(1)}, u32[]{:S(2)}, u32[]{:S(2)}) async-start(bf16[32,8,512]{2,1,0:T(8,128)(2,1)} %fusion.4), calls=%async_computation.1 | async-start | bytes 524288 | tf_op jit(solution)/shard_map/all_to_all | solution.py:13
  104.3 0.2 fusion.3.hidden_ref
  104.5 0.2 convolution_bitcast_fusion
  104.8 0.2 select_reduce_fusion.1
  105.0 0.1 fusion.8
  105.1 0.2 select_reduce_fusion.3
  105.3 0.1 select_reduce_fusion
  105.4 20.8 %all-to-all-done.1 = bf16[32,8,512]{2,1,0:T(8,128)(2,1)S(1)} async-done(((bf16[32,8,512]{2,1,0:T(8,128)(2,1)}), bf16[32,8,512]{2,1,0:T(8,128)(2,1)S(1)}, u32[]{:S(2)}, u32[]{:S(2)}) %all-to-all-start.1) | async-done | bytes 262176 | tf_op jit(solution)/shard_map/all_to_all | solution.py:13
  126.3 0.2 convolution_convert_fusion.refs_0_
  126.4 0.1 collective-permute-start.12
  126.6 2.3 %collective-permute-start.13 = (bf16[64,512]{1,0:T(8,128)(2,1)S(1)}, bf16[64,512]{1,0:T(8,128)(2,1)S(1)}, u32[]{:S(2)}, u32[]{:S(2)}) collective-permute-start(bf16[64,512]{1,0:T(8,128)(2,1)S(1)} %convolution_convert_fusion.refs_0_), channel_id=1, source_target_pairs={{0,2},{1,3},{2,0},{3,1},{4,6},{5,7},{6,4},{7,5},{8,10},{9,11},{10,... | collective-permute-start | bytes 196616 | tf_op jit(solution)/shard_map/ppermute | solution.py:19
  128.9 0.9 collective-permute-start.14
  129.8 2.9 %collective-permute-done.12.refs_1_ = bf16[64,512]{1,0:T(8,128)(2,1)S(1)} collective-permute-done((bf16[64,512]{1,0:T(8,128)(2,1)S(1)}, bf16[64,512]{1,0:T(8,128)(2,1)S(1)}, u32[]{:S(2)}, u32[]{:S(2)}) %collective-permute-start.12) | collective-permute-done | bytes 65568 | tf_op jit(solution)/shard_map/ppermute | solution.py:19
  132.7 0.9 collective-permute-done.14.refs_3_
  133.6 1.0 finish.1
  (31 shorter events, 0.4 us)
Async XLA Ops:
  1.9 10.0 %copy-start.4 = (s32[64,2]{0,1:T(2,128)S(1)}, s32[64,2]{0,1:T(2,128)}, u32[]{:S(2)}) copy-start(s32[64,2]{0,1:T(2,128)} %param.20) | copy-start | bytes 1540
  1.9 38.7 %copy-start.2 = (bf16[2048,64]{0,1:T(8,128)(2,1)S(1)}, bf16[2048,64]{0,1:T(8,128)(2,1)}, u32[]{:S(2)}) copy-start(bf16[2048,64]{0,1:T(8,128)(2,1)} %param.31) | copy-start | bytes 786436
  1.9 38.7 %copy-start.3 = (bf16[2048,4]{0,1:T(4,128)(2,1)S(1)}, bf16[2048,4]{0,1:T(4,128)(2,1)}, u32[]{:S(2)}) copy-start(bf16[2048,4]{0,1:T(4,128)(2,1)} %param.30) | copy-start | bytes 49156
  1.9 64.8 %copy-start = (f32[2048]{0:T(1024)S(1)}, f32[2048]{0:T(1024)}, u32[]{:S(2)}) copy-start(f32[2048]{0:T(1024)} %param.29) | copy-start | bytes 24580
  5.8 6.4 %collective-permute-start = (bf16[64,512]{1,0:T(8,128)(2,1)S(1)}, bf16[64,512]{1,0:T(8,128)(2,1)S(1)}, u32[]{:S(2)}, u32[]{:S(2)}) collective-permute-start(bf16[64,512]{1,0:T(8,128)(2,1)S(1)} %get-tuple-element.17), channel_id=1, source_target_pairs={{0,1},{1,2},{2,3},{3,0},{4,5},{5,6},{6,7},{7,4},{8,9},{9,10},{10,1... | collective-permute-start | bytes 196616 | tf_op jit(solution)/shard_map/ppermute | solution.py:19
  7.6 6.3 %collective-permute-start.1 = (bf16[64,512]{1,0:T(8,128)(2,1)S(1)}, bf16[64,512]{1,0:T(8,128)(2,1)S(1)}, u32[]{:S(2)}, u32[]{:S(2)}) collective-permute-start(bf16[64,512]{1,0:T(8,128)(2,1)S(1)} %get-tuple-element.18), channel_id=1, source_target_pairs={{0,2},{1,3},{2,0},{3,1},{4,6},{5,7},{6,4},{7,5},{8,10},{9,11},{10,... | collective-permute-start | bytes 196616 | tf_op jit(solution)/shard_map/ppermute | solution.py:19
  10.6 4.3 %collective-permute-start.2 = (bf16[64,512]{1,0:T(8,128)(2,1)S(1)}, bf16[64,512]{1,0:T(8,128)(2,1)S(1)}, u32[]{:S(2)}, u32[]{:S(2)}) collective-permute-start(bf16[64,512]{1,0:T(8,128)(2,1)S(1)} %get-tuple-element.19), channel_id=1, source_target_pairs={{0,3},{1,0},{2,1},{3,2},{4,7},{5,4},{6,5},{7,6},{8,11},{9,8},{10,9... | collective-permute-start | bytes 196616 | tf_op jit(solution)/shard_map/ppermute | solution.py:19
  15.8 46.7 %all-to-all-start = ((bf16[32,8,512]{2,1,0:T(8,128)(2,1)}), bf16[32,8,512]{2,1,0:T(8,128)(2,1)S(1)}, u32[]{:S(2)}, u32[]{:S(2)}) async-start(bf16[32,8,512]{2,1,0:T(8,128)(2,1)} %bitcast.10), calls=%async_computation | async-start | bytes 524288 | tf_op jit(solution)/shard_map/all_to_all | solution.py:13
  40.6 25.9 %collective-permute-start.5 = (bf16[64,512]{1,0:T(8,128)(2,1)S(1)}, bf16[64,512]{1,0:T(8,128)(2,1)S(1)}, u32[]{:S(2)}, u32[]{:S(2)}) collective-permute-start(bf16[64,512]{1,0:T(8,128)(2,1)S(1)} %get-tuple-element.20), channel_id=1, source_target_pairs={{0,3},{1,0},{2,1},{3,2},{4,7},{5,4},{6,5},{7,6},{8,11},{9,8},{10,9... | collective-permute-start | bytes 196616 | tf_op jit(solution)/shard_map/ppermute | solution.py:19
  43.3 27.6 %collective-permute-start.4 = (bf16[64,512]{1,0:T(8,128)(2,1)S(1)}, bf16[64,512]{1,0:T(8,128)(2,1)S(1)}, u32[]{:S(2)}, u32[]{:S(2)}) collective-permute-start(bf16[64,512]{1,0:T(8,128)(2,1)S(1)} %get-tuple-element.20), channel_id=1, source_target_pairs={{0,2},{1,3},{2,0},{3,1},{4,6},{5,7},{6,4},{7,5},{8,10},{9,11},{10,... | collective-permute-start | bytes 196616 | tf_op jit(solution)/shard_map/ppermute | solution.py:19
  43.4 27.5 %collective-permute-start.3 = (bf16[64,512]{1,0:T(8,128)(2,1)S(1)}, bf16[64,512]{1,0:T(8,128)(2,1)S(1)}, u32[]{:S(2)}, u32[]{:S(2)}) collective-permute-start(bf16[64,512]{1,0:T(8,128)(2,1)S(1)} %get-tuple-element.20), channel_id=1, source_target_pairs={{0,1},{1,2},{2,3},{3,0},{4,5},{5,6},{6,7},{7,4},{8,9},{9,10},{10,1... | collective-permute-start | bytes 196616 | tf_op jit(solution)/shard_map/ppermute | solution.py:19
  62.5 9.7 %collective-permute-start.6 = (bf16[256,512]{1,0:T(8,128)(2,1)S(1)}, bf16[256,512]{1,0:T(8,128)(2,1)S(1)}, u32[]{:S(2)}, u32[]{:S(2)}) collective-permute-start(bf16[256,512]{1,0:T(8,128)(2,1)S(1)} %bitcast.26), channel_id=1, source_target_pairs={{0,1},{1,2},{2,3},{3,0},{4,5},{5,6},{6,7},{7,4},{8,9},{9,10},{10,1... | collective-permute-start | bytes 786440 | tf_op jit(solution)/shard_map/ppermute | solution.py:19
  62.8 15.4 %collective-permute-start.7 = (bf16[256,512]{1,0:T(8,128)(2,1)S(1)}, bf16[256,512]{1,0:T(8,128)(2,1)S(1)}, u32[]{:S(2)}, u32[]{:S(2)}) collective-permute-start(bf16[256,512]{1,0:T(8,128)(2,1)S(1)} %bitcast.27), channel_id=1, source_target_pairs={{0,2},{1,3},{2,0},{3,1},{4,6},{5,7},{6,4},{7,5},{8,10},{9,11},{10,... | collective-permute-start | bytes 786440 | tf_op jit(solution)/shard_map/ppermute | solution.py:19
  66.5 11.7 %collective-permute-start.8 = (bf16[256,512]{1,0:T(8,128)(2,1)S(1)}, bf16[256,512]{1,0:T(8,128)(2,1)S(1)}, u32[]{:S(2)}, u32[]{:S(2)}) collective-permute-start(bf16[256,512]{1,0:T(8,128)(2,1)S(1)} %bitcast.28), channel_id=1, source_target_pairs={{0,3},{1,0},{2,1},{3,2},{4,7},{5,4},{6,5},{7,6},{8,11},{9,8},{10,9... | collective-permute-start | bytes 786440 | tf_op jit(solution)/shard_map/ppermute | solution.py:19
  81.3 14.0 %collective-permute-start.11 = (bf16[256,512]{1,0:T(8,128)(2,1)S(1)}, bf16[256,512]{1,0:T(8,128)(2,1)S(1)}, u32[]{:S(2)}, u32[]{:S(2)}) collective-permute-start(bf16[256,512]{1,0:T(8,128)(2,1)S(1)} %get-tuple-element.28), channel_id=1, source_target_pairs={{0,3},{1,0},{2,1},{3,2},{4,7},{5,4},{6,5},{7,6},{8,11},{9,8},{10,9... | collective-permute-start | bytes 786440 | tf_op jit(solution)/shard_map/ppermute | solution.py:19
  83.9 11.4 %collective-permute-start.10 = (bf16[256,512]{1,0:T(8,128)(2,1)S(1)}, bf16[256,512]{1,0:T(8,128)(2,1)S(1)}, u32[]{:S(2)}, u32[]{:S(2)}) collective-permute-start(bf16[256,512]{1,0:T(8,128)(2,1)S(1)} %get-tuple-element.27), channel_id=1, source_target_pairs={{0,2},{1,3},{2,0},{3,1},{4,6},{5,7},{6,4},{7,5},{8,10},{9,11},{10,... | collective-permute-start | bytes 786440 | tf_op jit(solution)/shard_map/ppermute | solution.py:19
  84.2 49.4 %copy-start.1 = (f32[2048]{0:T(1024)S(1)}, f32[2048]{0:T(1024)}, u32[]{:S(2)}) copy-start(f32[2048]{0:T(1024)} %param.35) | copy-start | bytes 24580
  84.2 14.5 %collective-permute-start.9 = (bf16[256,512]{1,0:T(8,128)(2,1)S(1)}, bf16[256,512]{1,0:T(8,128)(2,1)S(1)}, u32[]{:S(2)}, u32[]{:S(2)}) collective-permute-start(bf16[256,512]{1,0:T(8,128)(2,1)S(1)} %get-tuple-element.26), channel_id=1, source_target_pairs={{0,1},{1,2},{2,3},{3,0},{4,5},{5,6},{6,7},{7,4},{8,9},{9,10},{10,1... | collective-permute-start | bytes 786440 | tf_op jit(solution)/shard_map/ppermute | solution.py:19
  99.5 26.7 %all-to-all-start.1 = ((bf16[32,8,512]{2,1,0:T(8,128)(2,1)}), bf16[32,8,512]{2,1,0:T(8,128)(2,1)S(1)}, u32[]{:S(2)}, u32[]{:S(2)}) async-start(bf16[32,8,512]{2,1,0:T(8,128)(2,1)} %fusion.4), calls=%async_computation.1 | async-start | bytes 524288 | tf_op jit(solution)/shard_map/all_to_all | solution.py:13
  126.4 6.3 %collective-permute-start.12 = (bf16[64,512]{1,0:T(8,128)(2,1)S(1)}, bf16[64,512]{1,0:T(8,128)(2,1)S(1)}, u32[]{:S(2)}, u32[]{:S(2)}) collective-permute-start(bf16[64,512]{1,0:T(8,128)(2,1)S(1)} %convolution_convert_fusion.refs_0_), channel_id=1, source_target_pairs={{0,1},{1,2},{2,3},{3,0},{4,5},{5,6},{6,7},{7,4},{8,9},{9,10},{10,1... | collective-permute-start | bytes 196616 | tf_op jit(solution)/shard_map/ppermute | solution.py:19
  126.6 6.2 %collective-permute-start.13 = (bf16[64,512]{1,0:T(8,128)(2,1)S(1)}, bf16[64,512]{1,0:T(8,128)(2,1)S(1)}, u32[]{:S(2)}, u32[]{:S(2)}) collective-permute-start(bf16[64,512]{1,0:T(8,128)(2,1)S(1)} %convolution_convert_fusion.refs_0_), channel_id=1, source_target_pairs={{0,2},{1,3},{2,0},{3,1},{4,6},{5,7},{6,4},{7,5},{8,10},{9,11},{10,... | collective-permute-start | bytes 196616 | tf_op jit(solution)/shard_map/ppermute | solution.py:19
  128.9 4.7 %collective-permute-start.14 = (bf16[64,512]{1,0:T(8,128)(2,1)S(1)}, bf16[64,512]{1,0:T(8,128)(2,1)S(1)}, u32[]{:S(2)}, u32[]{:S(2)}) collective-permute-start(bf16[64,512]{1,0:T(8,128)(2,1)S(1)} %convolution_convert_fusion.refs_0_), channel_id=1, source_target_pairs={{0,3},{1,0},{2,1},{3,2},{4,7},{5,4},{6,5},{7,6},{8,11},{9,8},{10,9... | collective-permute-start | bytes 196616 | tf_op jit(solution)/shard_map/ppermute | solution.py:19

commit v4 on v3

--- a/solution.py
+++ b/solution.py
@@ -192,7 +192,7 @@
                 (((1,), (1,)), ((), ())),
                 preferred_element_type=jnp.float32,
             )
-            value = skip_ref[:, span] * inputs
+            value = skip_ref[span] * inputs
             for g in range(together):
                 value = value + jnp.where(
                     lane_group == g, read[g * seq_count : (g + 1) * seq_count], 0.0
@@ -365,6 +365,29 @@
         compiler_params=pltpu.CompilerParams(vmem_limit_bytes=24 * 1024 * 1024),
         name="experts",
     )(here, *pieces, gain, w_gate, w_up, w_down)
+
+
+def add_up(halves):
+    rows, share = halves[0][0].shape
+    count = len(halves[0])
+
+    def kernel(*refs):
+        for h in range(len(halves)):
+            group = refs[h * count : (h + 1) * count]
+            total = group[0][...].astype(jnp.float32)
+            for r in group[1:]:
+                total = total + r[...].astype(jnp.float32)
+            refs[-1][h * rows : (h + 1) * rows, :] = total.astype(jnp.bfloat16)
+
+    vmem = pl.BlockSpec(memory_space=pltpu.VMEM)
+    return pl.pallas_call(
+        kernel,
+        in_specs=[vmem] * (count * len(halves)),
+        out_specs=vmem,
+        out_shape=jax.ShapeDtypeStruct((rows * len(halves), share), jnp.bfloat16),
+        compiler_params=pltpu.CompilerParams(vmem_limit_bytes=8 * 1024 * 1024),
+        name="add_up",
+    )(*[r for half in halves for r in half])
 
 
 def finish(here, hidden, pieces, gain):
@@ -448,7 +471,7 @@
         log_step.reshape(1, -1),
         b_in,
         c_out,
-        skip.reshape(1, -1),
+        skip,
         w_out,
     )
     arrived = shifted([base, *parts], "tp")
@@ -467,12 +490,17 @@
     matches = target[:, :, None] == slot_ids[None, None, :]
     combine_map = jnp.sum(jnp.where(matches, route_weight[:, :, None], 0.0), axis=1)
 
-    rows = rows.reshape(total_slots, share)
-    pieces = shifted([rows] * shares, "tp")
     weights = fetch(w_gate, w_up, w_down)
-    outs = experts(here_array, pieces, gain_mix, *weights)
-    arrived = shifted(outs, "tp")
-    summed = sum(a.astype(jnp.float32) for a in arrived).astype(jnp.bfloat16)
+    half = ep_count // 2
+    gathered = []
+    for h in range(2):
+        rows_half = rows[h * half : (h + 1) * half].reshape(half * local_slots, share)
+        gathered.append(shifted([rows_half] * shares, "tp"))
+    arrived = []
+    for h in range(2):
+        outs = experts(here_array, gathered[h], gain_mix, *weights)
+        arrived.append(shifted(outs, "tp"))
+    summed = add_up(arrived)
     returned = exchange(summed.reshape(ep_count, local_slots, share), "ep")
     moe_own = jnp.dot(
         combine_map.astype(jnp.bfloat16),

time: 135 us -> 132 us (0.978)
  waiting for transfers between devices: 65.9 us -> 44.9 us
  starting transfers between devices: 50.5 us -> 62.3 us
  local copies, waits for them, and re-layouts: 2.66 us -> 7.27 us
  Pallas kernels: 11.8 us -> 14.1 us
    ppermute x15 -> x21, waiting for transfers between devices: 26.9 us -> 12.9 us  [shifted(): lax.ppermute(pieces[k], axis, [(i, (i + k) % size) for i in range(size)])]
    ppermute x15 -> x21, starting transfers between devices: 21 us -> 32.8 us  [shifted(): lax.ppermute(pieces[k], axis, [(i, (i + k) % size) for i in range(size)])]
    all_to_all x2, waiting for transfers between devices: 39.1 us -> 32 us  [exchange(): return lax.all_to_all(x, axis, 0, 0, tiled=True)]
    unnamed x10 -> x18, local copies, waits for them, and re-layouts: 0.02 us -> 5.85 us
    pallas_call x1 -> x2, Pallas kernels: 3.04 us -> 4.51 us  [experts(): pl.pallas_call(kernel, in_specs=[pl.BlockSpec(memory_space=pltpu.SMEM)] +...]
  transfers between devices with their start and end apart: 17 -> 23, of which waited for: 10 -> 10; matrix products, arithmetic and copies ran while one was open for 2% -> 2% of each run, Pallas kernels for 2% -> 6%
where the time goes in v4:
time: 132 us; the launch traced here: 131 us
  starting transfers between devices  62.3 us (47%)
  waiting for transfers between devices  44.9 us (34%)
  Pallas kernels  14.1 us (11%)
  local copies, waits for them, and re-layouts  7.27 us (6%)
  other arithmetic  1.64 us (1%)
    ppermute x21, starting transfers between devices, shifted(): lax.ppermute(pieces[k], axis, [(i, (i + k) % size) for i in range(size)])  32.8 us
    all_to_all x2, waiting for transfers between devices, exchange(): return lax.all_to_all(x, axis, 0, 0, tiled=True)  32 us
    all_to_all x2, starting transfers between devices, exchange(): return lax.all_to_all(x, axis, 0, 0, tiled=True)  29.5 us
    ppermute x21, waiting for transfers between devices, shifted(): lax.ppermute(pieces[k], axis, [(i, (i + k) % size) for i in range(size)])  12.9 us
    unnamed x18, local copies, waits for them, and re-layouts  5.85 us
    pallas_call x2, Pallas kernels, experts(): pl.pallas_call(kernel, in_specs=[pl.BlockSpec(memory_space=pltpu.SMEM)] +...  4.51 us
    pallas_call x1, Pallas kernels, mixer(): pl.pallas_call(kernel, in_specs=[pl.BlockSpec(memory_space=pltpu.SMEM)] +...  3.93 us
    pallas_call x1, Pallas kernels, fetch(): pl.pallas_call(kernel, in_specs=[pl.BlockSpec(memory_space=pltpu.HBM)] *...  2.89 us
  transfers between devices with their start and end apart: 23, of which 10 were waited for; matrix products, arithmetic and copies ran while one was open for 2% of the time, Pallas kernels for 6%

profile of v4, /device:TPU:40, one launch (start us, length us, event | category | flops | bytes accessed | tf_op | source)
XLA Modules:
  0.0 131.5 jit_solution(460888612135054579)
XLA Ops:
  0.7 3.9 %mixer.1 = (f32[64,512]{1,0:T(8,128)S(1)}, bf16[64,512]{1,0:T(8,128)(2,1)S(1)}, bf16[64,512]{1,0:T(8,128)(2,1)S(1)}, bf16[64,512]{1,0:T(8,128)(2,1)S(1)}, f32[64,24,128]{2,1,0:T(8,128)}) custom-call(s32[1]{0:T(128)} %bitcast.here_ref, f32[24,64]{1,0:T(8,128)} %refs_0_.2, f32[24,64]{1,0:T(8,128)} %refs_1_.2, f32[1,24]{1,0:T(1,128)} %bitcast.44, ...), custom_call_target="tpu_custom_call" | custom-call | tf_op jit(solution)/shard_map/mixer/pallas_call | solution.py:218
  4.6 1.7 %collective-permute-start = (bf16[64,512]{1,0:T(8,128)(2,1)S(1)}, bf16[64,512]{1,0:T(8,128)(2,1)S(1)}, u32[]{:S(2)}, u32[]{:S(2)}) collective-permute-start(bf16[64,512]{1,0:T(8,128)(2,1)S(1)} %get-tuple-element.21), channel_id=1, source_target_pairs={{0,1},{1,2},{2,3},{3,0},{4,5},{5,6},{6,7},{7,4},{8,9},{9,10},{10,1... | collective-permute-start | bytes 196616 | tf_op jit(solution)/shard_map/ppermute | solution.py:19
  6.4 3.0 %collective-permute-start.1 = (bf16[64,512]{1,0:T(8,128)(2,1)S(1)}, bf16[64,512]{1,0:T(8,128)(2,1)S(1)}, u32[]{:S(2)}, u32[]{:S(2)}) collective-permute-start(bf16[64,512]{1,0:T(8,128)(2,1)S(1)} %get-tuple-element.22), channel_id=1, source_target_pairs={{0,2},{1,3},{2,0},{3,1},{4,6},{5,7},{6,4},{7,5},{8,10},{9,11},{10,... | collective-permute-start | bytes 196616 | tf_op jit(solution)/shard_map/ppermute | solution.py:19
  9.4 1.3 collective-permute-start.2
  10.9 0.2 select_reduce_fusion.2
  11.1 1.6 %collective-permute-done.1.refs_1_ = bf16[64,512]{1,0:T(8,128)(2,1)S(1)} collective-permute-done((bf16[64,512]{1,0:T(8,128)(2,1)S(1)}, bf16[64,512]{1,0:T(8,128)(2,1)S(1)}, u32[]{:S(2)}, u32[]{:S(2)}) %collective-permute-start.1) | collective-permute-done | bytes 65568 | tf_op jit(solution)/shard_map/ppermute | solution.py:19
  12.6 1.0 collective-permute-done.2.refs_2_
  13.6 0.9 place_rows.1
  14.6 24.7 %all-to-all-start = ((bf16[32,8,512]{2,1,0:T(8,128)(2,1)}), bf16[32,8,512]{2,1,0:T(8,128)(2,1)S(1)}, u32[]{:S(2)}, u32[]{:S(2)}) async-start(bf16[32,8,512]{2,1,0:T(8,128)(2,1)} %bitcast.10), calls=%async_computation | async-start | bytes 524288 | tf_op jit(solution)/shard_map/all_to_all | solution.py:13
  39.7 2.6 %collective-permute-start.5 = (bf16[64,512]{1,0:T(8,128)(2,1)S(1)}, bf16[64,512]{1,0:T(8,128)(2,1)S(1)}, u32[]{:S(2)}, u32[]{:S(2)}) collective-permute-start(bf16[64,512]{1,0:T(8,128)(2,1)S(1)} %get-tuple-element.24), channel_id=1, source_target_pairs={{0,3},{1,0},{2,1},{3,2},{4,7},{5,4},{6,5},{7,6},{8,11},{9,8},{10,9... | collective-permute-start | bytes 196616 | tf_op jit(solution)/shard_map/ppermute | solution.py:19
  42.3 1.0 collective-permute-start.3
  43.3 0.6 gather_fusion
  43.9 0.6 gather_fusion.1
  44.4 2.9 %fetch.1 = (bf16[2,2048,256]{2,1,0:T(8,128)(2,1)S(1)}, bf16[2,2048,256]{2,1,0:T(8,128)(2,1)S(1)}, bf16[2,256,2048]{2,1,0:T(8,128)(2,1)S(1)}) custom-call(bf16[2,2048,256]{2,1,0:T(8,128)(2,1)} %refs_0_.3, bf16[2,2048,256]{2,1,0:T(8,128)(2,1)} %refs_1_.3, bf16[2,256,2048]{2,1,0:T(8,128)(2,1)} %refs_2_.1), custom_call_target="tpu_custom_call" | custom-call | tf_op jit(solution)/shard_map/fetch/pallas_call | solution.py:281
  47.4 1.3 %copy-done = bf16[2,2048,256]{2,1,0:T(8,128)(2,1)} copy-done((bf16[2,2048,256]{2,1,0:T(8,128)(2,1)}, bf16[2,2048,256]{2,1,0:T(8,128)(2,1)S(1)}, u32[]{:S(2)}) %copy-start) | copy-done | bytes 2097176
  48.7 1.3 %copy-done.2 = bf16[2,256,2048]{2,1,0:T(8,128)(2,1)} copy-done((bf16[2,256,2048]{2,1,0:T(8,128)(2,1)}, bf16[2,256,2048]{2,1,0:T(8,128)(2,1)S(1)}, u32[]{:S(2)}) %copy-start.2) | copy-done | bytes 2097176
  50.2 11.2 %all-to-all-done = bf16[32,8,512]{2,1,0:T(8,128)(2,1)S(1)} async-done(((bf16[32,8,512]{2,1,0:T(8,128)(2,1)}), bf16[32,8,512]{2,1,0:T(8,128)(2,1)S(1)}, u32[]{:S(2)}, u32[]{:S(2)}) %all-to-all-start) | async-done | bytes 262176 | tf_op jit(solution)/shard_map/all_to_all | solution.py:13
  61.3 0.4 collective-permute-start.6
  61.7 3.7 %collective-permute-start.7 = (bf16[128,512]{1,0:T(8,128)(2,1)S(1)}, bf16[128,512]{1,0:T(8,128)(2,1)S(1)}, u32[]{:S(2)}, u32[]{:S(2)}) collective-permute-start(bf16[128,512]{1,0:T(8,128)(2,1)S(1)} %get-tuple-element.39.refs_0_), channel_id=1, source_target_pairs={{0,2},{1,3},{2,0},{3,1},{4,6},{5,7},{6,4},{7,5},{8,10},{9,11},{10,... | collective-permute-start | bytes 393224 | tf_op jit(solution)/shard_map/ppermute | solution.py:19
  65.6 1.9 %collective-permute-start.12 = (bf16[128,512]{1,0:T(8,128)(2,1)S(1)}, bf16[128,512]{1,0:T(8,128)(2,1)S(1)}, u32[]{:S(2)}, u32[]{:S(2)}) collective-permute-start(bf16[128,512]{1,0:T(8,128)(2,1)S(1)} %get-tuple-element.38.refs_0_), channel_id=1, source_target_pairs={{0,1},{1,2},{2,3},{3,0},{4,5},{5,6},{6,7},{7,4},{8,9},{9,10},{10,1... | collective-permute-start | bytes 393224 | tf_op jit(solution)/shard_map/ppermute | solution.py:19
  67.4 0.2 collective-permute-start.13
  67.6 0.7 collective-permute-done.6.refs_1_
  68.3 2.0 %collective-permute-start.14 = (bf16[128,512]{1,0:T(8,128)(2,1)S(1)}, bf16[128,512]{1,0:T(8,128)(2,1)S(1)}, u32[]{:S(2)}, u32[]{:S(2)}) collective-permute-start(bf16[128,512]{1,0:T(8,128)(2,1)S(1)} %get-tuple-element.38.refs_0_), channel_id=1, source_target_pairs={{0,3},{1,0},{2,1},{3,2},{4,7},{5,4},{6,5},{7,6},{8,11},{9,8},{10,9... | collective-permute-start | bytes 393224 | tf_op jit(solution)/shard_map/ppermute | solution.py:19
  70.3 2.2 %collective-permute-done.7.refs_2_ = bf16[128,512]{1,0:T(8,128)(2,1)S(1)} collective-permute-done((bf16[128,512]{1,0:T(8,128)(2,1)S(1)}, bf16[128,512]{1,0:T(8,128)(2,1)S(1)}, u32[]{:S(2)}, u32[]{:S(2)}) %collective-permute-start.7) | collective-permute-done | bytes 131104 | tf_op jit(solution)/shard_map/ppermute | solution.py:19
  72.6 1.6 %copy-done.1 = bf16[2,2048,256]{2,1,0:T(8,128)(2,1)S(1)} copy-done((bf16[2,2048,256]{2,1,0:T(8,128)(2,1)S(1)}, bf16[2,2048,256]{2,1,0:T(8,128)(2,1)}, u32[]{:S(2)}) %copy-start.1) | copy-done | bytes 2097176
  74.2 1.6 %copy-done.3 = bf16[2,256,2048]{2,1,0:T(8,128)(2,1)S(1)} copy-done((bf16[2,256,2048]{2,1,0:T(8,128)(2,1)S(1)}, bf16[2,256,2048]{2,1,0:T(8,128)(2,1)}, u32[]{:S(2)}) %copy-start.3) | copy-done | bytes 2097176
  75.8 2.2 %experts.2 = (bf16[128,512]{1,0:T(8,128)(2,1)S(1)}, bf16[128,512]{1,0:T(8,128)(2,1)S(1)}, bf16[128,512]{1,0:T(8,128)(2,1)S(1)}, bf16[128,512]{1,0:T(8,128)(2,1)S(1)}) custom-call(s32[1]{0:T(128)} %bitcast.here_ref, bf16[128,512]{1,0:T(8,128)(2,1)S(1)} %get-tuple-element.39.refs_0_, bf16[128,512]{1,0:T(8,128)(2,1)S(1)} %collective-permute-done.6.refs_1_, ...), custom_call_target="tpu_custom_call" | custom-call | tf_op jit(solution)/shard_map/experts/pallas_call | solution.py:356
  78.0 2.2 %collective-permute-start.9 = (bf16[128,512]{1,0:T(8,128)(2,1)S(1)}, bf16[128,512]{1,0:T(8,128)(2,1)S(1)}, u32[]{:S(2)}, u32[]{:S(2)}) collective-permute-start(bf16[128,512]{1,0:T(8,128)(2,1)S(1)} %get-tuple-element.30), channel_id=1, source_target_pairs={{0,1},{1,2},{2,3},{3,0},{4,5},{5,6},{6,7},{7,4},{8,9},{9,10},{10,1... | collective-permute-start | bytes 393224 | tf_op jit(solution)/shard_map/ppermute | solution.py:19
  80.3 0.2 fusion.2
  80.5 2.8 %collective-permute-start.10 = (bf16[128,512]{1,0:T(8,128)(2,1)S(1)}, bf16[128,512]{1,0:T(8,128)(2,1)S(1)}, u32[]{:S(2)}, u32[]{:S(2)}) collective-permute-start(bf16[128,512]{1,0:T(8,128)(2,1)S(1)} %get-tuple-element.31), channel_id=1, source_target_pairs={{0,2},{1,3},{2,0},{3,1},{4,6},{5,7},{6,4},{7,5},{8,10},{9,11},{10,... | collective-permute-start | bytes 393224 | tf_op jit(solution)/shard_map/ppermute | solution.py:19
  83.3 2.3 %experts.3 = (bf16[128,512]{1,0:T(8,128)(2,1)S(1)}, bf16[128,512]{1,0:T(8,128)(2,1)S(1)}, bf16[128,512]{1,0:T(8,128)(2,1)S(1)}, bf16[128,512]{1,0:T(8,128)(2,1)S(1)}) custom-call(s32[1]{0:T(128)} %bitcast.here_ref, bf16[128,512]{1,0:T(8,128)(2,1)S(1)} %get-tuple-element.38.refs_0_, bf16[128,512]{1,0:T(8,128)(2,1)S(1)} %collective-permute-done.12.refs_1_, ...), custom_call_target="tpu_custom_call" | custom-call | tf_op jit(solution)/shard_map/experts/pallas_call | solution.py:356
  85.6 2.1 %collective-permute-start.15 = (bf16[128,512]{1,0:T(8,128)(2,1)S(1)}, bf16[128,512]{1,0:T(8,128)(2,1)S(1)}, u32[]{:S(2)}, u32[]{:S(2)}) collective-permute-start(bf16[128,512]{1,0:T(8,128)(2,1)S(1)} %get-tuple-element.34), channel_id=1, source_target_pairs={{0,1},{1,2},{2,3},{3,0},{4,5},{5,6},{6,7},{7,4},{8,9},{9,10},{10,1... | collective-permute-start | bytes 393224 | tf_op jit(solution)/shard_map/ppermute | solution.py:19
  87.7 0.8 collective-permute-start.16
  88.6 2.0 %collective-permute-start.17 = (bf16[128,512]{1,0:T(8,128)(2,1)S(1)}, bf16[128,512]{1,0:T(8,128)(2,1)S(1)}, u32[]{:S(2)}, u32[]{:S(2)}) collective-permute-start(bf16[128,512]{1,0:T(8,128)(2,1)S(1)} %get-tuple-element.36), channel_id=1, source_target_pairs={{0,3},{1,0},{2,1},{3,2},{4,7},{5,4},{6,5},{7,6},{8,11},{9,8},{10,9... | collective-permute-start | bytes 393224 | tf_op jit(solution)/shard_map/ppermute | solution.py:19
  90.6 3.8 %collective-permute-done.15.refs_5_ = bf16[128,512]{1,0:T(8,128)(2,1)S(1)} collective-permute-done((bf16[128,512]{1,0:T(8,128)(2,1)S(1)}, bf16[128,512]{1,0:T(8,128)(2,1)S(1)}, u32[]{:S(2)}, u32[]{:S(2)}) %collective-permute-start.15) | collective-permute-done | bytes 131104 | tf_op jit(solution)/shard_map/ppermute | solution.py:19
  94.4 0.8 add_up.1
  95.2 4.8 %all-to-all-start.1 = ((bf16[32,8,512]{2,1,0:T(8,128)(2,1)}), bf16[32,8,512]{2,1,0:T(8,128)(2,1)S(1)}, u32[]{:S(2)}, u32[]{:S(2)}) async-start(bf16[32,8,512]{2,1,0:T(8,128)(2,1)} %bitcast.14), calls=%async_computation.1 | async-start | bytes 524288 | tf_op jit(solution)/shard_map/all_to_all | solution.py:13
  100.2 0.2 convolution_bitcast_fusion
  100.5 0.2 select_reduce_fusion.1
  100.8 0.2 select_reduce_fusion.3
  101.1 20.8 %all-to-all-done.1 = bf16[32,8,512]{2,1,0:T(8,128)(2,1)S(1)} async-done(((bf16[32,8,512]{2,1,0:T(8,128)(2,1)}), bf16[32,8,512]{2,1,0:T(8,128)(2,1)S(1)}, u32[]{:S(2)}, u32[]{:S(2)}) %all-to-all-start.1) | async-done | bytes 262176 | tf_op jit(solution)/shard_map/all_to_all | solution.py:13
  122.1 1.5 %collective-permute-start.18 = (bf16[64,512]{1,0:T(8,128)(2,1)S(1)}, bf16[64,512]{1,0:T(8,128)(2,1)S(1)}, u32[]{:S(2)}, u32[]{:S(2)}) collective-permute-start(bf16[64,512]{1,0:T(8,128)(2,1)S(1)} %convolution_convert_fusion.refs_0_), channel_id=1, source_target_pairs={{0,1},{1,2},{2,3},{3,0},{4,5},{5,6},{6,7},{7,4},{8,9},{9,10},{10,1... | collective-permute-start | bytes 196616 | tf_op jit(solution)/shard_map/ppermute | solution.py:19
  123.7 2.6 %collective-permute-start.19 = (bf16[64,512]{1,0:T(8,128)(2,1)S(1)}, bf16[64,512]{1,0:T(8,128)(2,1)S(1)}, u32[]{:S(2)}, u32[]{:S(2)}) collective-permute-start(bf16[64,512]{1,0:T(8,128)(2,1)S(1)} %convolution_convert_fusion.refs_0_), channel_id=1, source_target_pairs={{0,2},{1,3},{2,0},{3,1},{4,6},{5,7},{6,4},{7,5},{8,10},{9,11},{10,... | collective-permute-start | bytes 196616 | tf_op jit(solution)/shard_map/ppermute | solution.py:19
  126.2 0.7 collective-permute-start.20
  126.9 0.9 collective-permute-done.18.refs_1_
  127.9 1.6 %collective-permute-done.19.refs_2_ = bf16[64,512]{1,0:T(8,128)(2,1)S(1)} collective-permute-done((bf16[64,512]{1,0:T(8,128)(2,1)S(1)}, bf16[64,512]{1,0:T(8,128)(2,1)S(1)}, u32[]{:S(2)}, u32[]{:S(2)}) %collective-permute-start.19) | collective-permute-done | bytes 65568 | tf_op jit(solution)/shard_map/ppermute | solution.py:19
  129.4 1.0 collective-permute-done.20.refs_3_
  130.5 1.0 finish.1
  (52 shorter events, 1.5 us)
Async XLA Ops:
  0.6 10.0 %copy-start.8 = (s32[64,2]{0,1:T(2,128)S(1)}, s32[64,2]{0,1:T(2,128)}, u32[]{:S(2)}) copy-start(s32[64,2]{0,1:T(2,128)} %param.20) | copy-start | bytes 1540
  0.6 38.7 %copy-start.4 = (f32[2048]{0:T(1024)S(1)}, f32[2048]{0:T(1024)}, u32[]{:S(2)}) copy-start(f32[2048]{0:T(1024)} %param.29) | copy-start | bytes 24580
  0.7 38.7 %copy-start.6 = (bf16[2048,64]{0,1:T(8,128)(2,1)S(1)}, bf16[2048,64]{0,1:T(8,128)(2,1)}, u32[]{:S(2)}) copy-start(bf16[2048,64]{0,1:T(8,128)(2,1)} %param.31) | copy-start | bytes 786436
  0.7 38.7 %copy-start.7 = (bf16[2048,4]{0,1:T(4,128)(2,1)S(1)}, bf16[2048,4]{0,1:T(4,128)(2,1)}, u32[]{:S(2)}) copy-start(bf16[2048,4]{0,1:T(4,128)(2,1)} %param.30) | copy-start | bytes 49156
  4.6 6.4 %collective-permute-start = (bf16[64,512]{1,0:T(8,128)(2,1)S(1)}, bf16[64,512]{1,0:T(8,128)(2,1)S(1)}, u32[]{:S(2)}, u32[]{:S(2)}) collective-permute-start(bf16[64,512]{1,0:T(8,128)(2,1)S(1)} %get-tuple-element.21), channel_id=1, source_target_pairs={{0,1},{1,2},{2,3},{3,0},{4,5},{5,6},{6,7},{7,4},{8,9},{9,10},{10,1... | collective-permute-start | bytes 196616 | tf_op jit(solution)/shard_map/ppermute | solution.py:19
  6.4 6.3 %collective-permute-start.1 = (bf16[64,512]{1,0:T(8,128)(2,1)S(1)}, bf16[64,512]{1,0:T(8,128)(2,1)S(1)}, u32[]{:S(2)}, u32[]{:S(2)}) collective-permute-start(bf16[64,512]{1,0:T(8,128)(2,1)S(1)} %get-tuple-element.22), channel_id=1, source_target_pairs={{0,2},{1,3},{2,0},{3,1},{4,6},{5,7},{6,4},{7,5},{8,10},{9,11},{10,... | collective-permute-start | bytes 196616 | tf_op jit(solution)/shard_map/ppermute | solution.py:19
  9.4 4.3 %collective-permute-start.2 = (bf16[64,512]{1,0:T(8,128)(2,1)S(1)}, bf16[64,512]{1,0:T(8,128)(2,1)S(1)}, u32[]{:S(2)}, u32[]{:S(2)}) collective-permute-start(bf16[64,512]{1,0:T(8,128)(2,1)S(1)} %get-tuple-element.23), channel_id=1, source_target_pairs={{0,3},{1,0},{2,1},{3,2},{4,7},{5,4},{6,5},{7,6},{8,11},{9,8},{10,9... | collective-permute-start | bytes 196616 | tf_op jit(solution)/shard_map/ppermute | solution.py:19
  14.6 46.7 %all-to-all-start = ((bf16[32,8,512]{2,1,0:T(8,128)(2,1)}), bf16[32,8,512]{2,1,0:T(8,128)(2,1)S(1)}, u32[]{:S(2)}, u32[]{:S(2)}) async-start(bf16[32,8,512]{2,1,0:T(8,128)(2,1)} %bitcast.10), calls=%async_computation | async-start | bytes 524288 | tf_op jit(solution)/shard_map/all_to_all | solution.py:13
  39.7 10.3 %collective-permute-start.5 = (bf16[64,512]{1,0:T(8,128)(2,1)S(1)}, bf16[64,512]{1,0:T(8,128)(2,1)S(1)}, u32[]{:S(2)}, u32[]{:S(2)}) collective-permute-start(bf16[64,512]{1,0:T(8,128)(2,1)S(1)} %get-tuple-element.24), channel_id=1, source_target_pairs={{0,3},{1,0},{2,1},{3,2},{4,7},{5,4},{6,5},{7,6},{8,11},{9,8},{10,9... | collective-permute-start | bytes 196616 | tf_op jit(solution)/shard_map/ppermute | solution.py:19
  42.3 7.7 %collective-permute-start.4 = (bf16[64,512]{1,0:T(8,128)(2,1)S(1)}, bf16[64,512]{1,0:T(8,128)(2,1)S(1)}, u32[]{:S(2)}, u32[]{:S(2)}) collective-permute-start(bf16[64,512]{1,0:T(8,128)(2,1)S(1)} %get-tuple-element.24), channel_id=1, source_target_pairs={{0,2},{1,3},{2,0},{3,1},{4,6},{5,7},{6,4},{7,5},{8,10},{9,11},{10,... | collective-permute-start | bytes 196616 | tf_op jit(solution)/shard_map/ppermute | solution.py:19
  42.3 7.7 %collective-permute-start.3 = (bf16[64,512]{1,0:T(8,128)(2,1)S(1)}, bf16[64,512]{1,0:T(8,128)(2,1)S(1)}, u32[]{:S(2)}, u32[]{:S(2)}) collective-permute-start(bf16[64,512]{1,0:T(8,128)(2,1)S(1)} %get-tuple-element.24), channel_id=1, source_target_pairs={{0,1},{1,2},{2,3},{3,0},{4,5},{5,6},{6,7},{7,4},{8,9},{9,10},{10,1... | collective-permute-start | bytes 196616 | tf_op jit(solution)/shard_map/ppermute | solution.py:19
  47.3 1.3 %copy-start = (bf16[2,2048,256]{2,1,0:T(8,128)(2,1)}, bf16[2,2048,256]{2,1,0:T(8,128)(2,1)S(1)}, u32[]{:S(2)}) copy-start(bf16[2,2048,256]{2,1,0:T(8,128)(2,1)S(1)} %get-tuple-element.27.refs_6_) | copy-start | bytes 6291460
  48.7 1.3 %copy-start.2 = (bf16[2,256,2048]{2,1,0:T(8,128)(2,1)}, bf16[2,256,2048]{2,1,0:T(8,128)(2,1)S(1)}, u32[]{:S(2)}) copy-start(bf16[2,256,2048]{2,1,0:T(8,128)(2,1)S(1)} %get-tuple-element.28.refs_7_) | copy-start | bytes 6291460
  61.3 7.0 %collective-permute-start.6 = (bf16[128,512]{1,0:T(8,128)(2,1)S(1)}, bf16[128,512]{1,0:T(8,128)(2,1)S(1)}, u32[]{:S(2)}, u32[]{:S(2)}) collective-permute-start(bf16[128,512]{1,0:T(8,128)(2,1)S(1)} %get-tuple-element.39.refs_0_), channel_id=1, source_target_pairs={{0,1},{1,2},{2,3},{3,0},{4,5},{5,6},{6,7},{7,4},{8,9},{9,10},{10,1... | collective-permute-start | bytes 393224 | tf_op jit(solution)/shard_map/ppermute | solution.py:19
  61.7 10.8 %collective-permute-start.7 = (bf16[128,512]{1,0:T(8,128)(2,1)S(1)}, bf16[128,512]{1,0:T(8,128)(2,1)S(1)}, u32[]{:S(2)}, u32[]{:S(2)}) collective-permute-start(bf16[128,512]{1,0:T(8,128)(2,1)S(1)} %get-tuple-element.39.refs_0_), channel_id=1, source_target_pairs={{0,2},{1,3},{2,0},{3,1},{4,6},{5,7},{6,4},{7,5},{8,10},{9,11},{10,... | collective-permute-start | bytes 393224 | tf_op jit(solution)/shard_map/ppermute | solution.py:19
  65.4 7.2 %collective-permute-start.8 = (bf16[128,512]{1,0:T(8,128)(2,1)S(1)}, bf16[128,512]{1,0:T(8,128)(2,1)S(1)}, u32[]{:S(2)}, u32[]{:S(2)}) collective-permute-start(bf16[128,512]{1,0:T(8,128)(2,1)S(1)} %get-tuple-element.39.refs_0_), channel_id=1, source_target_pairs={{0,3},{1,0},{2,1},{3,2},{4,7},{5,4},{6,5},{7,6},{8,11},{9,8},{10,9... | collective-permute-start | bytes 393224 | tf_op jit(solution)/shard_map/ppermute | solution.py:19
  65.6 17.7 %collective-permute-start.12 = (bf16[128,512]{1,0:T(8,128)(2,1)S(1)}, bf16[128,512]{1,0:T(8,128)(2,1)S(1)}, u32[]{:S(2)}, u32[]{:S(2)}) collective-permute-start(bf16[128,512]{1,0:T(8,128)(2,1)S(1)} %get-tuple-element.38.refs_0_), channel_id=1, source_target_pairs={{0,1},{1,2},{2,3},{3,0},{4,5},{5,6},{6,7},{7,4},{8,9},{9,10},{10,1... | collective-permute-start | bytes 393224 | tf_op jit(solution)/shard_map/ppermute | solution.py:19
  67.4 15.9 %collective-permute-start.13 = (bf16[128,512]{1,0:T(8,128)(2,1)S(1)}, bf16[128,512]{1,0:T(8,128)(2,1)S(1)}, u32[]{:S(2)}, u32[]{:S(2)}) collective-permute-start(bf16[128,512]{1,0:T(8,128)(2,1)S(1)} %get-tuple-element.38.refs_0_), channel_id=1, source_target_pairs={{0,2},{1,3},{2,0},{3,1},{4,6},{5,7},{6,4},{7,5},{8,10},{9,11},{10,... | collective-permute-start | bytes 393224 | tf_op jit(solution)/shard_map/ppermute | solution.py:19
  68.3 15.0 %collective-permute-start.14 = (bf16[128,512]{1,0:T(8,128)(2,1)S(1)}, bf16[128,512]{1,0:T(8,128)(2,1)S(1)}, u32[]{:S(2)}, u32[]{:S(2)}) collective-permute-start(bf16[128,512]{1,0:T(8,128)(2,1)S(1)} %get-tuple-element.38.refs_0_), channel_id=1, source_target_pairs={{0,3},{1,0},{2,1},{3,2},{4,7},{5,4},{6,5},{7,6},{8,11},{9,8},{10,9... | collective-permute-start | bytes 393224 | tf_op jit(solution)/shard_map/ppermute | solution.py:19
  72.6 1.6 %copy-start.1 = (bf16[2,2048,256]{2,1,0:T(8,128)(2,1)S(1)}, bf16[2,2048,256]{2,1,0:T(8,128)(2,1)}, u32[]{:S(2)}) copy-start(bf16[2,2048,256]{2,1,0:T(8,128)(2,1)} %copy-done) | copy-start | bytes 6291460
  74.2 1.6 %copy-start.3 = (bf16[2,256,2048]{2,1,0:T(8,128)(2,1)S(1)}, bf16[2,256,2048]{2,1,0:T(8,128)(2,1)}, u32[]{:S(2)}) copy-start(bf16[2,256,2048]{2,1,0:T(8,128)(2,1)} %copy-done.2) | copy-start | bytes 6291460
  78.0 10.5 %collective-permute-start.9 = (bf16[128,512]{1,0:T(8,128)(2,1)S(1)}, bf16[128,512]{1,0:T(8,128)(2,1)S(1)}, u32[]{:S(2)}, u32[]{:S(2)}) collective-permute-start(bf16[128,512]{1,0:T(8,128)(2,1)S(1)} %get-tuple-element.30), channel_id=1, source_target_pairs={{0,1},{1,2},{2,3},{3,0},{4,5},{5,6},{6,7},{7,4},{8,9},{9,10},{10,1... | collective-permute-start | bytes 393224 | tf_op jit(solution)/shard_map/ppermute | solution.py:19
  80.5 10.1 %collective-permute-start.10 = (bf16[128,512]{1,0:T(8,128)(2,1)S(1)}, bf16[128,512]{1,0:T(8,128)(2,1)S(1)}, u32[]{:S(2)}, u32[]{:S(2)}) collective-permute-start(bf16[128,512]{1,0:T(8,128)(2,1)S(1)} %get-tuple-element.31), channel_id=1, source_target_pairs={{0,2},{1,3},{2,0},{3,1},{4,6},{5,7},{6,4},{7,5},{8,10},{9,11},{10,... | collective-permute-start | bytes 393224 | tf_op jit(solution)/shard_map/ppermute | solution.py:19
  83.3 7.2 %collective-permute-start.11 = (bf16[128,512]{1,0:T(8,128)(2,1)S(1)}, bf16[128,512]{1,0:T(8,128)(2,1)S(1)}, u32[]{:S(2)}, u32[]{:S(2)}) collective-permute-start(bf16[128,512]{1,0:T(8,128)(2,1)S(1)} %get-tuple-element.32), channel_id=1, source_target_pairs={{0,3},{1,0},{2,1},{3,2},{4,7},{5,4},{6,5},{7,6},{8,11},{9,8},{10,9... | collective-permute-start | bytes 393224 | tf_op jit(solution)/shard_map/ppermute | solution.py:19
  85.6 44.9 %copy-start.5 = (f32[2048]{0:T(1024)S(1)}, f32[2048]{0:T(1024)}, u32[]{:S(2)}) copy-start(f32[2048]{0:T(1024)} %param.35) | copy-start | bytes 24580
  85.6 8.8 %collective-permute-start.15 = (bf16[128,512]{1,0:T(8,128)(2,1)S(1)}, bf16[128,512]{1,0:T(8,128)(2,1)S(1)}, u32[]{:S(2)}, u32[]{:S(2)}) collective-permute-start(bf16[128,512]{1,0:T(8,128)(2,1)S(1)} %get-tuple-element.34), channel_id=1, source_target_pairs={{0,1},{1,2},{2,3},{3,0},{4,5},{5,6},{6,7},{7,4},{8,9},{9,10},{10,1... | collective-permute-start | bytes 393224 | tf_op jit(solution)/shard_map/ppermute | solution.py:19
  87.7 6.6 %collective-permute-start.16 = (bf16[128,512]{1,0:T(8,128)(2,1)S(1)}, bf16[128,512]{1,0:T(8,128)(2,1)S(1)}, u32[]{:S(2)}, u32[]{:S(2)}) collective-permute-start(bf16[128,512]{1,0:T(8,128)(2,1)S(1)} %get-tuple-element.35), channel_id=1, source_target_pairs={{0,2},{1,3},{2,0},{3,1},{4,6},{5,7},{6,4},{7,5},{8,10},{9,11},{10,... | collective-permute-start | bytes 393224 | tf_op jit(solution)/shard_map/ppermute | solution.py:19
  88.6 5.8 %collective-permute-start.17 = (bf16[128,512]{1,0:T(8,128)(2,1)S(1)}, bf16[128,512]{1,0:T(8,128)(2,1)S(1)}, u32[]{:S(2)}, u32[]{:S(2)}) collective-permute-start(bf16[128,512]{1,0:T(8,128)(2,1)S(1)} %get-tuple-element.36), channel_id=1, source_target_pairs={{0,3},{1,0},{2,1},{3,2},{4,7},{5,4},{6,5},{7,6},{8,11},{9,8},{10,9... | collective-permute-start | bytes 393224 | tf_op jit(solution)/shard_map/ppermute | solution.py:19
  95.2 26.7 %all-to-all-start.1 = ((bf16[32,8,512]{2,1,0:T(8,128)(2,1)}), bf16[32,8,512]{2,1,0:T(8,128)(2,1)S(1)}, u32[]{:S(2)}, u32[]{:S(2)}) async-start(bf16[32,8,512]{2,1,0:T(8,128)(2,1)} %bitcast.14), calls=%async_computation.1 | async-start | bytes 524288 | tf_op jit(solution)/shard_map/all_to_all | solution.py:13
  122.1 5.7 %collective-permute-start.18 = (bf16[64,512]{1,0:T(8,128)(2,1)S(1)}, bf16[64,512]{1,0:T(8,128)(2,1)S(1)}, u32[]{:S(2)}, u32[]{:S(2)}) collective-permute-start(bf16[64,512]{1,0:T(8,128)(2,1)S(1)} %convolution_convert_fusion.refs_0_), channel_id=1, source_target_pairs={{0,1},{1,2},{2,3},{3,0},{4,5},{5,6},{6,7},{7,4},{8,9},{9,10},{10,1... | collective-permute-start | bytes 196616 | tf_op jit(solution)/shard_map/ppermute | solution.py:19
  123.7 5.8 %collective-permute-start.19 = (bf16[64,512]{1,0:T(8,128)(2,1)S(1)}, bf16[64,512]{1,0:T(8,128)(2,1)S(1)}, u32[]{:S(2)}, u32[]{:S(2)}) collective-permute-start(bf16[64,512]{1,0:T(8,128)(2,1)S(1)} %convolution_convert_fusion.refs_0_), channel_id=1, source_target_pairs={{0,2},{1,3},{2,0},{3,1},{4,6},{5,7},{6,4},{7,5},{8,10},{9,11},{10,... | collective-permute-start | bytes 196616 | tf_op jit(solution)/shard_map/ppermute | solution.py:19
  126.2 4.3 %collective-permute-start.20 = (bf16[64,512]{1,0:T(8,128)(2,1)S(1)}, bf16[64,512]{1,0:T(8,128)(2,1)S(1)}, u32[]{:S(2)}, u32[]{:S(2)}) collective-permute-start(bf16[64,512]{1,0:T(8,128)(2,1)S(1)} %convolution_convert_fusion.refs_0_), channel_id=1, source_target_pairs={{0,3},{1,0},{2,1},{3,2},{4,7},{5,4},{6,5},{7,6},{8,11},{9,8},{10,9... | collective-permute-start | bytes 196616 | tf_op jit(solution)/shard_map/ppermute | solution.py:19

commit v5 on v4

--- a/solution.py
+++ b/solution.py
@@ -87,7 +87,7 @@
     share = width // shares
     together = lanes // per_group
     cut = 4
-    arrays = (decay_rate, frequency, log_step, x_in, w_in, b_in, state, c_out, skip, w_out)
+    arrays = (decay_rate, frequency, log_step, x_in, w_in, b_in, c_out, skip, state, w_out)
 
     def kernel(here_ref, *refs):
         far = refs[: len(arrays)]
@@ -96,7 +96,7 @@
         new_far = refs[len(arrays) + shares]
         rest = refs[len(arrays) + shares + 1 :]
         close = rest[: len(arrays)]
-        decay_ref, freq_ref, log_ref, x_ref, w_in_ref, b_ref, state_ref, c_ref, skip_ref, w_out_ref = close
+        decay_ref, freq_ref, log_ref, x_ref, w_in_ref, b_ref, c_ref, skip_ref, state_ref, w_out_ref = close
         new_ref, in_ref, out_ref, act_ref, sems = rest[len(arrays) :]
         _, tos = ring_places(here_ref, shares)
         piece = width // cut
@@ -142,19 +142,6 @@
         ratio_imag = twice(ratio_imag) * sign
 
         copies[3].wait()
-        x_wide = x_ref[...].astype(jnp.float32)
-        x_mean = jnp.sum(x_wide, -1, keepdims=True) / width
-        x_own = x_ref[:, columns_of(here_ref[0], share)].astype(jnp.float32)
-        base_ref[...] = residual_scale * (x_own - x_mean)
-        copies[5].wait()
-        for g in range(groups):
-            b = b_ref[g]
-            in_ref[g * per_group : (g + 1) * per_group, :] = (
-                ratio_real[g : g + 1] * b + ratio_imag[g : g + 1] * pltpu.roll(b, entries, 1)
-            ).astype(jnp.bfloat16)
-        copies[7].wait()
-        for g in range(groups):
-            out_ref[g * per_group : (g + 1) * per_group, :] = (c_ref[g] * -sign).astype(jnp.bfloat16)
         mix = None
         for q in range(cut):
             copies[4, q].wait()
@@ -162,7 +149,20 @@
             term = jnp.dot(x_ref[:, rows], w_in_ref[rows, :], preferred_element_type=jnp.float32)
             mix = term if mix is None else mix + term
         mix = mix.astype(jnp.bfloat16).astype(jnp.float32)
+        copies[5].wait()
+        for g in range(groups):
+            b = b_ref[g]
+            in_ref[g * per_group : (g + 1) * per_group, :] = (
+                ratio_real[g : g + 1] * b + ratio_imag[g : g + 1] * pltpu.roll(b, entries, 1)
+            ).astype(jnp.bfloat16)
         copies[6].wait()
+        for g in range(groups):
+            out_ref[g * per_group : (g + 1) * per_group, :] = (c_ref[g] * -sign).astype(jnp.bfloat16)
+        x_wide = x_ref[...].astype(jnp.float32)
+        x_mean = jnp.sum(x_wide, -1, keepdims=True) / width
+        x_own = x_ref[:, columns_of(here_ref[0], share)].astype(jnp.float32)
+        base_ref[...] = residual_scale * (x_own - x_mean)
+        copies[7].wait()
         copies[8].wait()
         old = state_ref.reshape(seq_count * groups, lanes)
         new = new_ref.reshape(seq_count * groups, lanes)
@@ -237,29 +237,44 @@
 
 def place_rows(base, arrived, target, total_slots):
     seq_count, share = base.shape
+    cut = 4
+    piece = total_slots // cut
 
     def kernel(base_ref, target_ref, *refs):
-        own_ref, sent_ref = refs[-2:]
+        own_ref, sent_far, sent_ref, sems = refs[-4:]
         own = base_ref[...]
-        for r in refs[:-2]:
+        for r in refs[:-4]:
             own = own + r[...].astype(jnp.float32)
         own = own.astype(jnp.bfloat16)
+        copies = []
+        for q in range(cut):
+            rows = slice(q * piece, (q + 1) * piece)
+            slot = lax.broadcasted_iota(jnp.int32, (piece, seq_count), 0) + q * piece
+            hit = slot == target_ref[0:1, :]
+            for k in range(1, target_ref.shape[0]):
+                hit = hit | (slot == target_ref[k : k + 1, :])
+            chosen = jnp.where(hit, 1.0, 0.0).astype(jnp.bfloat16)
+            sent_ref[rows, :] = jnp.dot(chosen, own, preferred_element_type=jnp.float32).astype(
+                jnp.bfloat16
+            )
+            copies.append(pltpu.make_async_copy(sent_ref.at[rows], sent_far.at[rows], sems.at[q]))
+            copies[-1].start()
         own_ref[...] = own
-        slot = lax.broadcasted_iota(jnp.int32, (total_slots, seq_count), 0)
-        hit = slot == target_ref[0:1, :]
-        for k in range(1, target_ref.shape[0]):
-            hit = hit | (slot == target_ref[k : k + 1, :])
-        chosen = jnp.where(hit, 1.0, 0.0).astype(jnp.bfloat16)
-        sent_ref[...] = jnp.dot(chosen, own, preferred_element_type=jnp.float32).astype(jnp.bfloat16)
+        for copy in copies:
+            copy.wait()
 
     vmem = pl.BlockSpec(memory_space=pltpu.VMEM)
     return pl.pallas_call(
         kernel,
         in_specs=[vmem] * (2 + len(arrived)),
-        out_specs=[vmem] * 2,
+        out_specs=[vmem, pl.BlockSpec(memory_space=pltpu.HBM)],
         out_shape=[
             jax.ShapeDtypeStruct((seq_count, share), jnp.bfloat16),
             jax.ShapeDtypeStruct((total_slots, share), jnp.bfloat16),
+        ],
+        scratch_shapes=[
+            pltpu.VMEM((total_slots, share), jnp.bfloat16),
+            pltpu.SemaphoreType.DMA((cut,)),
         ],
         compiler_params=pltpu.CompilerParams(vmem_limit_bytes=8 * 1024 * 1024),
         name="place_rows",
@@ -394,33 +409,48 @@
     rows, share = pieces[0].shape
     shares = len(pieces)
     width = shares * share
+    cut = 4
+    piece = rows // cut
 
     def kernel(here_ref, hidden_ref, *refs):
         piece_refs = refs[:shares]
-        gain_ref, out_ref = refs[shares:]
+        gain_ref, out_far, out_ref, sems = refs[shares:]
         froms, _ = ring_places(here_ref, shares)
-        values = [
-            residual_scale * hidden_ref[k] + piece_refs[k][...].astype(jnp.float32)
-            for k in range(shares)
-        ]
-        total = values[0]
-        for v in values[1:]:
-            total = total + v
-        centre = jnp.sum(total, -1, keepdims=True) / width
-        values = [v - centre for v in values]
-        total = values[0] * values[0]
-        for v in values[1:]:
-            total = total + v * v
-        scale = lax.rsqrt(jnp.sum(total, -1, keepdims=True) / width + norm_eps)
-        for k, v in enumerate(values):
-            out_ref[:, columns_of(froms[k], share)] = (v * scale * gain_ref[froms[k]]).astype(jnp.bfloat16)
+        copies = []
+        for q in range(cut):
+            some = slice(q * piece, (q + 1) * piece)
+            values = [
+                residual_scale * hidden_ref[k, some] + piece_refs[k][some].astype(jnp.float32)
+                for k in range(shares)
+            ]
+            total = values[0]
+            for v in values[1:]:
+                total = total + v
+            centre = jnp.sum(total, -1, keepdims=True) / width
+            values = [v - centre for v in values]
+            total = values[0] * values[0]
+            for v in values[1:]:
+                total = total + v * v
+            scale = lax.rsqrt(jnp.sum(total, -1, keepdims=True) / width + norm_eps)
+            for k, v in enumerate(values):
+                out_ref[some, columns_of(froms[k], share)] = (v * scale * gain_ref[froms[k]]).astype(
+                    jnp.bfloat16
+                )
+            copies.append(pltpu.make_async_copy(out_ref.at[some], out_far.at[some], sems.at[q]))
+            copies[-1].start()
+        for copy in copies:
+            copy.wait()
 
     vmem = pl.BlockSpec(memory_space=pltpu.VMEM)
     return pl.pallas_call(
         kernel,
         in_specs=[pl.BlockSpec(memory_space=pltpu.SMEM)] + [vmem] * (shares + 2),
-        out_specs=vmem,
+        out_specs=pl.BlockSpec(memory_space=pltpu.HBM),
         out_shape=jax.ShapeDtypeStruct((rows, width), jnp.bfloat16),
+        scratch_shapes=[
+            pltpu.VMEM((rows, width), jnp.bfloat16),
+            pltpu.SemaphoreType.DMA((cut,)),
+        ],
         compiler_params=pltpu.CompilerParams(vmem_limit_bytes=8 * 1024 * 1024),
         name="finish",
     )(here, hidden, *pieces, gain)

time: 132 us -> 132 us (level)
  no operation moved by 1% of the time
where the time goes in v5:
time: 132 us; the launch traced here: 131 us
  starting transfers between devices  62.3 us (47%)
  waiting for transfers between devices  44.9 us (34%)
  Pallas kernels  13.6 us (10%)
  local copies, waits for them, and re-layouts  7.27 us (6%)
  other arithmetic  1.64 us (1%)
    ppermute x21, starting transfers between devices, shifted(): lax.ppermute(pieces[k], axis, [(i, (i + k) % size) for i in range(size)])  32.8 us
    all_to_all x2, waiting for transfers between devices, exchange(): return lax.all_to_all(x, axis, 0, 0, tiled=True)  32 us
    all_to_all x2, starting transfers between devices, exchange(): return lax.all_to_all(x, axis, 0, 0, tiled=True)  29.5 us
    ppermute x21, waiting for transfers between devices, shifted(): lax.ppermute(pieces[k], axis, [(i, (i + k) % size) for i in range(size)])  12.9 us
    unnamed x18, local copies, waits for them, and re-layouts  5.85 us
    pallas_call x2, Pallas kernels, experts(): pl.pallas_call(kernel, in_specs=[pl.BlockSpec(memory_space=pltpu.SMEM)] +...  4.51 us
    pallas_call x1, Pallas kernels, mixer(): pl.pallas_call(kernel, in_specs=[pl.BlockSpec(memory_space=pltpu.SMEM)] +...  3.56 us
    pallas_call x1, Pallas kernels, fetch(): pl.pallas_call(kernel, in_specs=[pl.BlockSpec(memory_space=pltpu.HBM)] *...  2.89 us
  transfers between devices with their start and end apart: 23, of which 10 were waited for; matrix products, arithmetic and copies ran while one was open for 2% of the time, Pallas kernels for 6%

profile of v5, /device:TPU:40, one launch (start us, length us, event | category | flops | bytes accessed | tf_op | source)
XLA Modules:
  0.0 131.2 jit_solution(8858126496535170957)
XLA Ops:
  0.7 3.6 %mixer.1 = (f32[64,512]{1,0:T(8,128)S(1)}, bf16[64,512]{1,0:T(8,128)(2,1)S(1)}, bf16[64,512]{1,0:T(8,128)(2,1)S(1)}, bf16[64,512]{1,0:T(8,128)(2,1)S(1)}, f32[64,24,128]{2,1,0:T(8,128)}) custom-call(s32[1]{0:T(128)} %bitcast.here_ref, f32[24,64]{1,0:T(8,128)} %refs_0_.2, f32[24,64]{1,0:T(8,128)} %refs_1_.2, f32[1,24]{1,0:T(1,128)} %bitcast.44, ...), custom_call_target="tpu_custom_call" | custom-call | tf_op jit(solution)/shard_map/mixer/pallas_call | solution.py:218
  4.2 1.7 %collective-permute-start = (bf16[64,512]{1,0:T(8,128)(2,1)S(1)}, bf16[64,512]{1,0:T(8,128)(2,1)S(1)}, u32[]{:S(2)}, u32[]{:S(2)}) collective-permute-start(bf16[64,512]{1,0:T(8,128)(2,1)S(1)} %get-tuple-element.21), channel_id=1, source_target_pairs={{0,1},{1,2},{2,3},{3,0},{4,5},{5,6},{6,7},{7,4},{8,9},{9,10},{10,1... | collective-permute-start | bytes 196616 | tf_op jit(solution)/shard_map/ppermute | solution.py:19
  6.0 3.0 %collective-permute-start.1 = (bf16[64,512]{1,0:T(8,128)(2,1)S(1)}, bf16[64,512]{1,0:T(8,128)(2,1)S(1)}, u32[]{:S(2)}, u32[]{:S(2)}) collective-permute-start(bf16[64,512]{1,0:T(8,128)(2,1)S(1)} %get-tuple-element.22), channel_id=1, source_target_pairs={{0,2},{1,3},{2,0},{3,1},{4,6},{5,7},{6,4},{7,5},{8,10},{9,11},{10,... | collective-permute-start | bytes 196616 | tf_op jit(solution)/shard_map/ppermute | solution.py:19
  9.0 1.3 collective-permute-start.2
  10.5 0.2 select_reduce_fusion.2
  10.7 1.6 %collective-permute-done.1.refs_1_ = bf16[64,512]{1,0:T(8,128)(2,1)S(1)} collective-permute-done((bf16[64,512]{1,0:T(8,128)(2,1)S(1)}, bf16[64,512]{1,0:T(8,128)(2,1)S(1)}, u32[]{:S(2)}, u32[]{:S(2)}) %collective-permute-start.1) | collective-permute-done | bytes 65568 | tf_op jit(solution)/shard_map/ppermute | solution.py:19
  12.3 1.0 collective-permute-done.2.refs_2_
  13.3 0.9 place_rows.1
  14.2 24.8 %all-to-all-start = ((bf16[32,8,512]{2,1,0:T(8,128)(2,1)}), bf16[32,8,512]{2,1,0:T(8,128)(2,1)S(1)}, u32[]{:S(2)}, u32[]{:S(2)}) async-start(bf16[32,8,512]{2,1,0:T(8,128)(2,1)} %bitcast.10), calls=%async_computation | async-start | bytes 524288 | tf_op jit(solution)/shard_map/all_to_all | solution.py:13
  39.3 2.6 %collective-permute-start.5 = (bf16[64,512]{1,0:T(8,128)(2,1)S(1)}, bf16[64,512]{1,0:T(8,128)(2,1)S(1)}, u32[]{:S(2)}, u32[]{:S(2)}) collective-permute-start(bf16[64,512]{1,0:T(8,128)(2,1)S(1)} %get-tuple-element.24), channel_id=1, source_target_pairs={{0,3},{1,0},{2,1},{3,2},{4,7},{5,4},{6,5},{7,6},{8,11},{9,8},{10,9... | collective-permute-start | bytes 196616 | tf_op jit(solution)/shard_map/ppermute | solution.py:19
  41.9 1.0 collective-permute-start.3
  42.9 0.6 gather_fusion
  43.5 0.6 gather_fusion.1
  44.1 2.9 %fetch.1 = (bf16[2,2048,256]{2,1,0:T(8,128)(2,1)S(1)}, bf16[2,2048,256]{2,1,0:T(8,128)(2,1)S(1)}, bf16[2,256,2048]{2,1,0:T(8,128)(2,1)S(1)}) custom-call(bf16[2,2048,256]{2,1,0:T(8,128)(2,1)} %refs_0_.3, bf16[2,2048,256]{2,1,0:T(8,128)(2,1)} %refs_1_.3, bf16[2,256,2048]{2,1,0:T(8,128)(2,1)} %refs_2_.1), custom_call_target="tpu_custom_call" | custom-call | tf_op jit(solution)/shard_map/fetch/pallas_call | solution.py:296
  47.0 1.3 %copy-done = bf16[2,2048,256]{2,1,0:T(8,128)(2,1)} copy-done((bf16[2,2048,256]{2,1,0:T(8,128)(2,1)}, bf16[2,2048,256]{2,1,0:T(8,128)(2,1)S(1)}, u32[]{:S(2)}) %copy-start) | copy-done | bytes 2097176
  48.3 1.3 %copy-done.2 = bf16[2,256,2048]{2,1,0:T(8,128)(2,1)} copy-done((bf16[2,256,2048]{2,1,0:T(8,128)(2,1)}, bf16[2,256,2048]{2,1,0:T(8,128)(2,1)S(1)}, u32[]{:S(2)}) %copy-start.2) | copy-done | bytes 2097176
  49.8 11.2 %all-to-all-done = bf16[32,8,512]{2,1,0:T(8,128)(2,1)S(1)} async-done(((bf16[32,8,512]{2,1,0:T(8,128)(2,1)}), bf16[32,8,512]{2,1,0:T(8,128)(2,1)S(1)}, u32[]{:S(2)}, u32[]{:S(2)}) %all-to-all-start) | async-done | bytes 262176 | tf_op jit(solution)/shard_map/all_to_all | solution.py:13
  60.9 0.4 collective-permute-start.6
  61.4 3.7 %collective-permute-start.7 = (bf16[128,512]{1,0:T(8,128)(2,1)S(1)}, bf16[128,512]{1,0:T(8,128)(2,1)S(1)}, u32[]{:S(2)}, u32[]{:S(2)}) collective-permute-start(bf16[128,512]{1,0:T(8,128)(2,1)S(1)} %get-tuple-element.39.refs_0_), channel_id=1, source_target_pairs={{0,2},{1,3},{2,0},{3,1},{4,6},{5,7},{6,4},{7,5},{8,10},{9,11},{10,... | collective-permute-start | bytes 393224 | tf_op jit(solution)/shard_map/ppermute | solution.py:19
  65.0 0.2 collective-permute-start.8
  65.2 1.9 %collective-permute-start.12 = (bf16[128,512]{1,0:T(8,128)(2,1)S(1)}, bf16[128,512]{1,0:T(8,128)(2,1)S(1)}, u32[]{:S(2)}, u32[]{:S(2)}) collective-permute-start(bf16[128,512]{1,0:T(8,128)(2,1)S(1)} %get-tuple-element.38.refs_0_), channel_id=1, source_target_pairs={{0,1},{1,2},{2,3},{3,0},{4,5},{5,6},{6,7},{7,4},{8,9},{9,10},{10,1... | collective-permute-start | bytes 393224 | tf_op jit(solution)/shard_map/ppermute | solution.py:19
  67.2 0.7 collective-permute-done.6.refs_1_
  67.9 2.0 %collective-permute-start.14 = (bf16[128,512]{1,0:T(8,128)(2,1)S(1)}, bf16[128,512]{1,0:T(8,128)(2,1)S(1)}, u32[]{:S(2)}, u32[]{:S(2)}) collective-permute-start(bf16[128,512]{1,0:T(8,128)(2,1)S(1)} %get-tuple-element.38.refs_0_), channel_id=1, source_target_pairs={{0,3},{1,0},{2,1},{3,2},{4,7},{5,4},{6,5},{7,6},{8,11},{9,8},{10,9... | collective-permute-start | bytes 393224 | tf_op jit(solution)/shard_map/ppermute | solution.py:19
  69.9 2.2 %collective-permute-done.7.refs_2_ = bf16[128,512]{1,0:T(8,128)(2,1)S(1)} collective-permute-done((bf16[128,512]{1,0:T(8,128)(2,1)S(1)}, bf16[128,512]{1,0:T(8,128)(2,1)S(1)}, u32[]{:S(2)}, u32[]{:S(2)}) %collective-permute-start.7) | collective-permute-done | bytes 131104 | tf_op jit(solution)/shard_map/ppermute | solution.py:19
  72.2 1.6 %copy-done.1 = bf16[2,2048,256]{2,1,0:T(8,128)(2,1)S(1)} copy-done((bf16[2,2048,256]{2,1,0:T(8,128)(2,1)S(1)}, bf16[2,2048,256]{2,1,0:T(8,128)(2,1)}, u32[]{:S(2)}) %copy-start.1) | copy-done | bytes 2097176
  73.8 1.6 %copy-done.3 = bf16[2,256,2048]{2,1,0:T(8,128)(2,1)S(1)} copy-done((bf16[2,256,2048]{2,1,0:T(8,128)(2,1)S(1)}, bf16[2,256,2048]{2,1,0:T(8,128)(2,1)}, u32[]{:S(2)}) %copy-start.3) | copy-done | bytes 2097176
  75.4 2.2 %experts.2 = (bf16[128,512]{1,0:T(8,128)(2,1)S(1)}, bf16[128,512]{1,0:T(8,128)(2,1)S(1)}, bf16[128,512]{1,0:T(8,128)(2,1)S(1)}, bf16[128,512]{1,0:T(8,128)(2,1)S(1)}) custom-call(s32[1]{0:T(128)} %bitcast.here_ref, bf16[128,512]{1,0:T(8,128)(2,1)S(1)} %get-tuple-element.39.refs_0_, bf16[128,512]{1,0:T(8,128)(2,1)S(1)} %collective-permute-done.6.refs_1_, ...), custom_call_target="tpu_custom_call" | custom-call | tf_op jit(solution)/shard_map/experts/pallas_call | solution.py:371
  77.6 2.2 %collective-permute-start.9 = (bf16[128,512]{1,0:T(8,128)(2,1)S(1)}, bf16[128,512]{1,0:T(8,128)(2,1)S(1)}, u32[]{:S(2)}, u32[]{:S(2)}) collective-permute-start(bf16[128,512]{1,0:T(8,128)(2,1)S(1)} %get-tuple-element.30), channel_id=1, source_target_pairs={{0,1},{1,2},{2,3},{3,0},{4,5},{5,6},{6,7},{7,4},{8,9},{9,10},{10,1... | collective-permute-start | bytes 393224 | tf_op jit(solution)/shard_map/ppermute | solution.py:19
  79.9 0.2 fusion.2
  80.1 2.8 %collective-permute-start.10 = (bf16[128,512]{1,0:T(8,128)(2,1)S(1)}, bf16[128,512]{1,0:T(8,128)(2,1)S(1)}, u32[]{:S(2)}, u32[]{:S(2)}) collective-permute-start(bf16[128,512]{1,0:T(8,128)(2,1)S(1)} %get-tuple-element.31), channel_id=1, source_target_pairs={{0,2},{1,3},{2,0},{3,1},{4,6},{5,7},{6,4},{7,5},{8,10},{9,11},{10,... | collective-permute-start | bytes 393224 | tf_op jit(solution)/shard_map/ppermute | solution.py:19
  83.0 2.3 %experts.3 = (bf16[128,512]{1,0:T(8,128)(2,1)S(1)}, bf16[128,512]{1,0:T(8,128)(2,1)S(1)}, bf16[128,512]{1,0:T(8,128)(2,1)S(1)}, bf16[128,512]{1,0:T(8,128)(2,1)S(1)}) custom-call(s32[1]{0:T(128)} %bitcast.here_ref, bf16[128,512]{1,0:T(8,128)(2,1)S(1)} %get-tuple-element.38.refs_0_, bf16[128,512]{1,0:T(8,128)(2,1)S(1)} %collective-permute-done.12.refs_1_, ...), custom_call_target="tpu_custom_call" | custom-call | tf_op jit(solution)/shard_map/experts/pallas_call | solution.py:371
  85.2 2.1 %collective-permute-start.15 = (bf16[128,512]{1,0:T(8,128)(2,1)S(1)}, bf16[128,512]{1,0:T(8,128)(2,1)S(1)}, u32[]{:S(2)}, u32[]{:S(2)}) collective-permute-start(bf16[128,512]{1,0:T(8,128)(2,1)S(1)} %get-tuple-element.34), channel_id=1, source_target_pairs={{0,1},{1,2},{2,3},{3,0},{4,5},{5,6},{6,7},{7,4},{8,9},{9,10},{10,1... | collective-permute-start | bytes 393224 | tf_op jit(solution)/shard_map/ppermute | solution.py:19
  87.3 0.8 collective-permute-start.16
  88.2 2.0 %collective-permute-start.17 = (bf16[128,512]{1,0:T(8,128)(2,1)S(1)}, bf16[128,512]{1,0:T(8,128)(2,1)S(1)}, u32[]{:S(2)}, u32[]{:S(2)}) collective-permute-start(bf16[128,512]{1,0:T(8,128)(2,1)S(1)} %get-tuple-element.36), channel_id=1, source_target_pairs={{0,3},{1,0},{2,1},{3,2},{4,7},{5,4},{6,5},{7,6},{8,11},{9,8},{10,9... | collective-permute-start | bytes 393224 | tf_op jit(solution)/shard_map/ppermute | solution.py:19
  90.2 3.8 %collective-permute-done.15.refs_5_ = bf16[128,512]{1,0:T(8,128)(2,1)S(1)} collective-permute-done((bf16[128,512]{1,0:T(8,128)(2,1)S(1)}, bf16[128,512]{1,0:T(8,128)(2,1)S(1)}, u32[]{:S(2)}, u32[]{:S(2)}) %collective-permute-start.15) | collective-permute-done | bytes 131104 | tf_op jit(solution)/shard_map/ppermute | solution.py:19
  94.0 0.8 add_up.1
  94.8 4.8 %all-to-all-start.1 = ((bf16[32,8,512]{2,1,0:T(8,128)(2,1)}), bf16[32,8,512]{2,1,0:T(8,128)(2,1)S(1)}, u32[]{:S(2)}, u32[]{:S(2)}) async-start(bf16[32,8,512]{2,1,0:T(8,128)(2,1)} %bitcast.14), calls=%async_computation.1 | async-start | bytes 524288 | tf_op jit(solution)/shard_map/all_to_all | solution.py:13
  99.8 0.2 convolution_bitcast_fusion
  100.1 0.2 select_reduce_fusion.1
  100.4 0.2 select_reduce_fusion.3
  100.7 20.8 %all-to-all-done.1 = bf16[32,8,512]{2,1,0:T(8,128)(2,1)S(1)} async-done(((bf16[32,8,512]{2,1,0:T(8,128)(2,1)}), bf16[32,8,512]{2,1,0:T(8,128)(2,1)S(1)}, u32[]{:S(2)}, u32[]{:S(2)}) %all-to-all-start.1) | async-done | bytes 262176 | tf_op jit(solution)/shard_map/all_to_all | solution.py:13
  121.7 1.5 %collective-permute-start.18 = (bf16[64,512]{1,0:T(8,128)(2,1)S(1)}, bf16[64,512]{1,0:T(8,128)(2,1)S(1)}, u32[]{:S(2)}, u32[]{:S(2)}) collective-permute-start(bf16[64,512]{1,0:T(8,128)(2,1)S(1)} %convolution_convert_fusion.refs_0_), channel_id=1, source_target_pairs={{0,1},{1,2},{2,3},{3,0},{4,5},{5,6},{6,7},{7,4},{8,9},{9,10},{10,1... | collective-permute-start | bytes 196616 | tf_op jit(solution)/shard_map/ppermute | solution.py:19
  123.3 2.6 %collective-permute-start.19 = (bf16[64,512]{1,0:T(8,128)(2,1)S(1)}, bf16[64,512]{1,0:T(8,128)(2,1)S(1)}, u32[]{:S(2)}, u32[]{:S(2)}) collective-permute-start(bf16[64,512]{1,0:T(8,128)(2,1)S(1)} %convolution_convert_fusion.refs_0_), channel_id=1, source_target_pairs={{0,2},{1,3},{2,0},{3,1},{4,6},{5,7},{6,4},{7,5},{8,10},{9,11},{10,... | collective-permute-start | bytes 196616 | tf_op jit(solution)/shard_map/ppermute | solution.py:19
  125.8 0.7 collective-permute-start.20
  126.5 0.9 collective-permute-done.18.refs_1_
  127.5 1.6 %collective-permute-done.19.refs_2_ = bf16[64,512]{1,0:T(8,128)(2,1)S(1)} collective-permute-done((bf16[64,512]{1,0:T(8,128)(2,1)S(1)}, bf16[64,512]{1,0:T(8,128)(2,1)S(1)}, u32[]{:S(2)}, u32[]{:S(2)}) %collective-permute-start.19) | collective-permute-done | bytes 65568 | tf_op jit(solution)/shard_map/ppermute | solution.py:19
  129.0 1.0 collective-permute-done.20.refs_3_
  130.1 0.9 finish.1
  (52 shorter events, 1.5 us)
Async XLA Ops:
  0.6 9.6 %copy-start.8 = (s32[64,2]{0,1:T(2,128)S(1)}, s32[64,2]{0,1:T(2,128)}, u32[]{:S(2)}) copy-start(s32[64,2]{0,1:T(2,128)} %param.20) | copy-start | bytes 1540
  0.6 38.3 %copy-start.4 = (f32[2048]{0:T(1024)S(1)}, f32[2048]{0:T(1024)}, u32[]{:S(2)}) copy-start(f32[2048]{0:T(1024)} %param.29) | copy-start | bytes 24580
  0.7 38.3 %copy-start.6 = (bf16[2048,64]{0,1:T(8,128)(2,1)S(1)}, bf16[2048,64]{0,1:T(8,128)(2,1)}, u32[]{:S(2)}) copy-start(bf16[2048,64]{0,1:T(8,128)(2,1)} %param.31) | copy-start | bytes 786436
  0.7 38.3 %copy-start.7 = (bf16[2048,4]{0,1:T(4,128)(2,1)S(1)}, bf16[2048,4]{0,1:T(4,128)(2,1)}, u32[]{:S(2)}) copy-start(bf16[2048,4]{0,1:T(4,128)(2,1)} %param.30) | copy-start | bytes 49156
  4.2 6.4 %collective-permute-start = (bf16[64,512]{1,0:T(8,128)(2,1)S(1)}, bf16[64,512]{1,0:T(8,128)(2,1)S(1)}, u32[]{:S(2)}, u32[]{:S(2)}) collective-permute-start(bf16[64,512]{1,0:T(8,128)(2,1)S(1)} %get-tuple-element.21), channel_id=1, source_target_pairs={{0,1},{1,2},{2,3},{3,0},{4,5},{5,6},{6,7},{7,4},{8,9},{9,10},{10,1... | collective-permute-start | bytes 196616 | tf_op jit(solution)/shard_map/ppermute | solution.py:19
  6.0 6.3 %collective-permute-start.1 = (bf16[64,512]{1,0:T(8,128)(2,1)S(1)}, bf16[64,512]{1,0:T(8,128)(2,1)S(1)}, u32[]{:S(2)}, u32[]{:S(2)}) collective-permute-start(bf16[64,512]{1,0:T(8,128)(2,1)S(1)} %get-tuple-element.22), channel_id=1, source_target_pairs={{0,2},{1,3},{2,0},{3,1},{4,6},{5,7},{6,4},{7,5},{8,10},{9,11},{10,... | collective-permute-start | bytes 196616 | tf_op jit(solution)/shard_map/ppermute | solution.py:19
  9.0 4.3 %collective-permute-start.2 = (bf16[64,512]{1,0:T(8,128)(2,1)S(1)}, bf16[64,512]{1,0:T(8,128)(2,1)S(1)}, u32[]{:S(2)}, u32[]{:S(2)}) collective-permute-start(bf16[64,512]{1,0:T(8,128)(2,1)S(1)} %get-tuple-element.23), channel_id=1, source_target_pairs={{0,3},{1,0},{2,1},{3,2},{4,7},{5,4},{6,5},{7,6},{8,11},{9,8},{10,9... | collective-permute-start | bytes 196616 | tf_op jit(solution)/shard_map/ppermute | solution.py:19
  14.2 46.8 %all-to-all-start = ((bf16[32,8,512]{2,1,0:T(8,128)(2,1)}), bf16[32,8,512]{2,1,0:T(8,128)(2,1)S(1)}, u32[]{:S(2)}, u32[]{:S(2)}) async-start(bf16[32,8,512]{2,1,0:T(8,128)(2,1)} %bitcast.10), calls=%async_computation | async-start | bytes 524288 | tf_op jit(solution)/shard_map/all_to_all | solution.py:13
  39.3 10.3 %collective-permute-start.5 = (bf16[64,512]{1,0:T(8,128)(2,1)S(1)}, bf16[64,512]{1,0:T(8,128)(2,1)S(1)}, u32[]{:S(2)}, u32[]{:S(2)}) collective-permute-start(bf16[64,512]{1,0:T(8,128)(2,1)S(1)} %get-tuple-element.24), channel_id=1, source_target_pairs={{0,3},{1,0},{2,1},{3,2},{4,7},{5,4},{6,5},{7,6},{8,11},{9,8},{10,9... | collective-permute-start | bytes 196616 | tf_op jit(solution)/shard_map/ppermute | solution.py:19
  41.9 7.7 %collective-permute-start.4 = (bf16[64,512]{1,0:T(8,128)(2,1)S(1)}, bf16[64,512]{1,0:T(8,128)(2,1)S(1)}, u32[]{:S(2)}, u32[]{:S(2)}) collective-permute-start(bf16[64,512]{1,0:T(8,128)(2,1)S(1)} %get-tuple-element.24), channel_id=1, source_target_pairs={{0,2},{1,3},{2,0},{3,1},{4,6},{5,7},{6,4},{7,5},{8,10},{9,11},{10,... | collective-permute-start | bytes 196616 | tf_op jit(solution)/shard_map/ppermute | solution.py:19
  41.9 7.7 %collective-permute-start.3 = (bf16[64,512]{1,0:T(8,128)(2,1)S(1)}, bf16[64,512]{1,0:T(8,128)(2,1)S(1)}, u32[]{:S(2)}, u32[]{:S(2)}) collective-permute-start(bf16[64,512]{1,0:T(8,128)(2,1)S(1)} %get-tuple-element.24), channel_id=1, source_target_pairs={{0,1},{1,2},{2,3},{3,0},{4,5},{5,6},{6,7},{7,4},{8,9},{9,10},{10,1... | collective-permute-start | bytes 196616 | tf_op jit(solution)/shard_map/ppermute | solution.py:19
  47.0 1.3 %copy-start = (bf16[2,2048,256]{2,1,0:T(8,128)(2,1)}, bf16[2,2048,256]{2,1,0:T(8,128)(2,1)S(1)}, u32[]{:S(2)}) copy-start(bf16[2,2048,256]{2,1,0:T(8,128)(2,1)S(1)} %get-tuple-element.27.refs_6_) | copy-start | bytes 6291460
  48.3 1.3 %copy-start.2 = (bf16[2,256,2048]{2,1,0:T(8,128)(2,1)}, bf16[2,256,2048]{2,1,0:T(8,128)(2,1)S(1)}, u32[]{:S(2)}) copy-start(bf16[2,256,2048]{2,1,0:T(8,128)(2,1)S(1)} %get-tuple-element.28.refs_7_) | copy-start | bytes 6291460
  60.9 7.0 %collective-permute-start.6 = (bf16[128,512]{1,0:T(8,128)(2,1)S(1)}, bf16[128,512]{1,0:T(8,128)(2,1)S(1)}, u32[]{:S(2)}, u32[]{:S(2)}) collective-permute-start(bf16[128,512]{1,0:T(8,128)(2,1)S(1)} %get-tuple-element.39.refs_0_), channel_id=1, source_target_pairs={{0,1},{1,2},{2,3},{3,0},{4,5},{5,6},{6,7},{7,4},{8,9},{9,10},{10,1... | collective-permute-start | bytes 393224 | tf_op jit(solution)/shard_map/ppermute | solution.py:19
  61.4 10.8 %collective-permute-start.7 = (bf16[128,512]{1,0:T(8,128)(2,1)S(1)}, bf16[128,512]{1,0:T(8,128)(2,1)S(1)}, u32[]{:S(2)}, u32[]{:S(2)}) collective-permute-start(bf16[128,512]{1,0:T(8,128)(2,1)S(1)} %get-tuple-element.39.refs_0_), channel_id=1, source_target_pairs={{0,2},{1,3},{2,0},{3,1},{4,6},{5,7},{6,4},{7,5},{8,10},{9,11},{10,... | collective-permute-start | bytes 393224 | tf_op jit(solution)/shard_map/ppermute | solution.py:19
  65.0 7.2 %collective-permute-start.8 = (bf16[128,512]{1,0:T(8,128)(2,1)S(1)}, bf16[128,512]{1,0:T(8,128)(2,1)S(1)}, u32[]{:S(2)}, u32[]{:S(2)}) collective-permute-start(bf16[128,512]{1,0:T(8,128)(2,1)S(1)} %get-tuple-element.39.refs_0_), channel_id=1, source_target_pairs={{0,3},{1,0},{2,1},{3,2},{4,7},{5,4},{6,5},{7,6},{8,11},{9,8},{10,9... | collective-permute-start | bytes 393224 | tf_op jit(solution)/shard_map/ppermute | solution.py:19
  65.2 17.7 %collective-permute-start.12 = (bf16[128,512]{1,0:T(8,128)(2,1)S(1)}, bf16[128,512]{1,0:T(8,128)(2,1)S(1)}, u32[]{:S(2)}, u32[]{:S(2)}) collective-permute-start(bf16[128,512]{1,0:T(8,128)(2,1)S(1)} %get-tuple-element.38.refs_0_), channel_id=1, source_target_pairs={{0,1},{1,2},{2,3},{3,0},{4,5},{5,6},{6,7},{7,4},{8,9},{9,10},{10,1... | collective-permute-start | bytes 393224 | tf_op jit(solution)/shard_map/ppermute | solution.py:19
  67.1 15.9 %collective-permute-start.13 = (bf16[128,512]{1,0:T(8,128)(2,1)S(1)}, bf16[128,512]{1,0:T(8,128)(2,1)S(1)}, u32[]{:S(2)}, u32[]{:S(2)}) collective-permute-start(bf16[128,512]{1,0:T(8,128)(2,1)S(1)} %get-tuple-element.38.refs_0_), channel_id=1, source_target_pairs={{0,2},{1,3},{2,0},{3,1},{4,6},{5,7},{6,4},{7,5},{8,10},{9,11},{10,... | collective-permute-start | bytes 393224 | tf_op jit(solution)/shard_map/ppermute | solution.py:19
  67.9 15.1 %collective-permute-start.14 = (bf16[128,512]{1,0:T(8,128)(2,1)S(1)}, bf16[128,512]{1,0:T(8,128)(2,1)S(1)}, u32[]{:S(2)}, u32[]{:S(2)}) collective-permute-start(bf16[128,512]{1,0:T(8,128)(2,1)S(1)} %get-tuple-element.38.refs_0_), channel_id=1, source_target_pairs={{0,3},{1,0},{2,1},{3,2},{4,7},{5,4},{6,5},{7,6},{8,11},{9,8},{10,9... | collective-permute-start | bytes 393224 | tf_op jit(solution)/shard_map/ppermute | solution.py:19
  72.2 1.6 %copy-start.1 = (bf16[2,2048,256]{2,1,0:T(8,128)(2,1)S(1)}, bf16[2,2048,256]{2,1,0:T(8,128)(2,1)}, u32[]{:S(2)}) copy-start(bf16[2,2048,256]{2,1,0:T(8,128)(2,1)} %copy-done) | copy-start | bytes 6291460
  73.8 1.6 %copy-start.3 = (bf16[2,256,2048]{2,1,0:T(8,128)(2,1)S(1)}, bf16[2,256,2048]{2,1,0:T(8,128)(2,1)}, u32[]{:S(2)}) copy-start(bf16[2,256,2048]{2,1,0:T(8,128)(2,1)} %copy-done.2) | copy-start | bytes 6291460
  77.6 10.5 %collective-permute-start.9 = (bf16[128,512]{1,0:T(8,128)(2,1)S(1)}, bf16[128,512]{1,0:T(8,128)(2,1)S(1)}, u32[]{:S(2)}, u32[]{:S(2)}) collective-permute-start(bf16[128,512]{1,0:T(8,128)(2,1)S(1)} %get-tuple-element.30), channel_id=1, source_target_pairs={{0,1},{1,2},{2,3},{3,0},{4,5},{5,6},{6,7},{7,4},{8,9},{9,10},{10,1... | collective-permute-start | bytes 393224 | tf_op jit(solution)/shard_map/ppermute | solution.py:19
  80.1 10.1 %collective-permute-start.10 = (bf16[128,512]{1,0:T(8,128)(2,1)S(1)}, bf16[128,512]{1,0:T(8,128)(2,1)S(1)}, u32[]{:S(2)}, u32[]{:S(2)}) collective-permute-start(bf16[128,512]{1,0:T(8,128)(2,1)S(1)} %get-tuple-element.31), channel_id=1, source_target_pairs={{0,2},{1,3},{2,0},{3,1},{4,6},{5,7},{6,4},{7,5},{8,10},{9,11},{10,... | collective-permute-start | bytes 393224 | tf_op jit(solution)/shard_map/ppermute | solution.py:19
  82.9 7.2 %collective-permute-start.11 = (bf16[128,512]{1,0:T(8,128)(2,1)S(1)}, bf16[128,512]{1,0:T(8,128)(2,1)S(1)}, u32[]{:S(2)}, u32[]{:S(2)}) collective-permute-start(bf16[128,512]{1,0:T(8,128)(2,1)S(1)} %get-tuple-element.32), channel_id=1, source_target_pairs={{0,3},{1,0},{2,1},{3,2},{4,7},{5,4},{6,5},{7,6},{8,11},{9,8},{10,9... | collective-permute-start | bytes 393224 | tf_op jit(solution)/shard_map/ppermute | solution.py:19
  85.2 44.9 %copy-start.5 = (f32[2048]{0:T(1024)S(1)}, f32[2048]{0:T(1024)}, u32[]{:S(2)}) copy-start(f32[2048]{0:T(1024)} %param.35) | copy-start | bytes 24580
  85.2 8.7 %collective-permute-start.15 = (bf16[128,512]{1,0:T(8,128)(2,1)S(1)}, bf16[128,512]{1,0:T(8,128)(2,1)S(1)}, u32[]{:S(2)}, u32[]{:S(2)}) collective-permute-start(bf16[128,512]{1,0:T(8,128)(2,1)S(1)} %get-tuple-element.34), channel_id=1, source_target_pairs={{0,1},{1,2},{2,3},{3,0},{4,5},{5,6},{6,7},{7,4},{8,9},{9,10},{10,1... | collective-permute-start | bytes 393224 | tf_op jit(solution)/shard_map/ppermute | solution.py:19
  87.3 6.6 %collective-permute-start.16 = (bf16[128,512]{1,0:T(8,128)(2,1)S(1)}, bf16[128,512]{1,0:T(8,128)(2,1)S(1)}, u32[]{:S(2)}, u32[]{:S(2)}) collective-permute-start(bf16[128,512]{1,0:T(8,128)(2,1)S(1)} %get-tuple-element.35), channel_id=1, source_target_pairs={{0,2},{1,3},{2,0},{3,1},{4,6},{5,7},{6,4},{7,5},{8,10},{9,11},{10,... | collective-permute-start | bytes 393224 | tf_op jit(solution)/shard_map/ppermute | solution.py:19
  88.2 5.8 %collective-permute-start.17 = (bf16[128,512]{1,0:T(8,128)(2,1)S(1)}, bf16[128,512]{1,0:T(8,128)(2,1)S(1)}, u32[]{:S(2)}, u32[]{:S(2)}) collective-permute-start(bf16[128,512]{1,0:T(8,128)(2,1)S(1)} %get-tuple-element.36), channel_id=1, source_target_pairs={{0,3},{1,0},{2,1},{3,2},{4,7},{5,4},{6,5},{7,6},{8,11},{9,8},{10,9... | collective-permute-start | bytes 393224 | tf_op jit(solution)/shard_map/ppermute | solution.py:19
  94.8 26.7 %all-to-all-start.1 = ((bf16[32,8,512]{2,1,0:T(8,128)(2,1)}), bf16[32,8,512]{2,1,0:T(8,128)(2,1)S(1)}, u32[]{:S(2)}, u32[]{:S(2)}) async-start(bf16[32,8,512]{2,1,0:T(8,128)(2,1)} %bitcast.14), calls=%async_computation.1 | async-start | bytes 524288 | tf_op jit(solution)/shard_map/all_to_all | solution.py:13
  121.7 5.7 %collective-permute-start.18 = (bf16[64,512]{1,0:T(8,128)(2,1)S(1)}, bf16[64,512]{1,0:T(8,128)(2,1)S(1)}, u32[]{:S(2)}, u32[]{:S(2)}) collective-permute-start(bf16[64,512]{1,0:T(8,128)(2,1)S(1)} %convolution_convert_fusion.refs_0_), channel_id=1, source_target_pairs={{0,1},{1,2},{2,3},{3,0},{4,5},{5,6},{6,7},{7,4},{8,9},{9,10},{10,1... | collective-permute-start | bytes 196616 | tf_op jit(solution)/shard_map/ppermute | solution.py:19
  123.3 5.8 %collective-permute-start.19 = (bf16[64,512]{1,0:T(8,128)(2,1)S(1)}, bf16[64,512]{1,0:T(8,128)(2,1)S(1)}, u32[]{:S(2)}, u32[]{:S(2)}) collective-permute-start(bf16[64,512]{1,0:T(8,128)(2,1)S(1)} %convolution_convert_fusion.refs_0_), channel_id=1, source_target_pairs={{0,2},{1,3},{2,0},{3,1},{4,6},{5,7},{6,4},{7,5},{8,10},{9,11},{10,... | collective-permute-start | bytes 196616 | tf_op jit(solution)/shard_map/ppermute | solution.py:19
  125.8 4.3 %collective-permute-start.20 = (bf16[64,512]{1,0:T(8,128)(2,1)S(1)}, bf16[64,512]{1,0:T(8,128)(2,1)S(1)}, u32[]{:S(2)}, u32[]{:S(2)}) collective-permute-start(bf16[64,512]{1,0:T(8,128)(2,1)S(1)} %convolution_convert_fusion.refs_0_), channel_id=1, source_target_pairs={{0,3},{1,0},{2,1},{3,2},{4,7},{5,4},{6,5},{7,6},{8,11},{9,8},{10,9... | collective-permute-start | bytes 196616 | tf_op jit(solution)/shard_map/ppermute | solution.py:19

commit v6 on v5

--- a/solution.py
+++ b/solution.py
@@ -281,12 +281,13 @@
     )(base, target.T, *arrived)
 
 
-def fetch(*weights):
+def fetch(which, *weights):
     count = len(weights)
 
     def kernel(*refs):
         copies = [
-            pltpu.make_async_copy(refs[i], refs[count + i], refs[-1].at[i]) for i in range(count)
+            pltpu.make_async_copy(refs[i].at[which], refs[count + i], refs[-1].at[i])
+            for i in range(count)
         ]
         for copy in copies:
             copy.start()
@@ -297,7 +298,7 @@
         kernel,
         in_specs=[pl.BlockSpec(memory_space=pltpu.HBM)] * count,
         out_specs=[pl.BlockSpec(memory_space=pltpu.VMEM)] * count,
-        out_shape=[pltpu.VMEM(w.shape, w.dtype) for w in weights],
+        out_shape=[pltpu.VMEM(w.shape[1:], w.dtype) for w in weights],
         scratch_shapes=[pltpu.SemaphoreType.DMA((count,))],
         compiler_params=pltpu.CompilerParams(vmem_limit_bytes=1024 * 1024),
         name="fetch",
@@ -313,19 +314,64 @@
     )
 
 
-def experts(here, pieces, gain, w_gate, w_up, w_down):
+def by_expert(rows):
+    slots, share = rows.shape
+    tile = 8
+
+    def kernel(rows_ref, *out_refs):
+        tiles = rows_ref[...].astype(jnp.float32).reshape(slots // (2 * tile), 2, tile, share)
+        for out_ref, part in zip(out_refs, swap_halves(tiles[:, 0], tiles[:, 1])):
+            out_ref[...] = part.reshape(slots // 2, share).astype(jnp.bfloat16)
+
+    vmem = pl.BlockSpec(memory_space=pltpu.VMEM)
+    return pl.pallas_call(
+        kernel,
+        in_specs=[vmem],
+        out_specs=[vmem] * 2,
+        out_shape=[jax.ShapeDtypeStruct((slots // 2, share), jnp.bfloat16)] * 2,
+        compiler_params=pltpu.CompilerParams(vmem_limit_bytes=8 * 1024 * 1024),
+        name="by_expert",
+    )(rows)
+
+
+def add_up(arrived):
+    rows, share = arrived[0][0].shape
+    count = len(arrived[0])
+    tile = 8
+
+    def kernel(*refs):
+        totals = []
+        for h in range(2):
+            group = refs[h * count : (h + 1) * count]
+            total = group[0][...].astype(jnp.float32)
+            for r in group[1:]:
+                total = total + r[...].astype(jnp.float32)
+            totals.append(total.reshape(rows // tile, tile, share))
+        both = jnp.stack(swap_halves(*totals), axis=1).reshape(2 * rows, share)
+        refs[-1][...] = both.astype(jnp.bfloat16)
+
+    vmem = pl.BlockSpec(memory_space=pltpu.VMEM)
+    return pl.pallas_call(
+        kernel,
+        in_specs=[vmem] * (2 * count),
+        out_specs=vmem,
+        out_shape=jax.ShapeDtypeStruct((2 * rows, share), jnp.bfloat16),
+        compiler_params=pltpu.CompilerParams(vmem_limit_bytes=8 * 1024 * 1024),
+        name="add_up",
+    )(*arrived[0], *arrived[1])
+
+
+def expert(here, pieces, gain, w_gate, w_up, w_down):
     slots, share = pieces[0].shape
     shares = len(pieces)
-    local_experts, width, hidden = w_gate.shape
-    tile = 8
-    chunk = 4 * tile
-    kept = slots // local_experts
+    width = w_gate.shape[0]
+    chunk = 32
 
     def kernel(here_ref, *refs):
         piece_refs = refs[:shares]
         gain_ref, gate_ref, up_ref, down_ref = refs[shares : shares + 4]
         out_refs = refs[shares + 4 : 2 * shares + 4]
-        row_ref, act_ref = refs[2 * shares + 4 :]
+        row_ref = refs[-1]
         froms, tos = ring_places(here_ref, shares)
 
         def norm_rows(i, carry):
@@ -340,32 +386,21 @@
             for v in values[1:]:
                 total = total + v * v
             scale = lax.rsqrt(jnp.sum(total, -1, keepdims=True) / width + norm_eps)
-            rows = pl.ds(pl.multiple_of(i * (chunk // 2), chunk // 2), chunk // 2)
             for k, v in enumerate(values):
-                v = (v * scale * gain_ref[froms[k]]).reshape(2, 2, tile, share)
-                for j, part in enumerate(swap_halves(v[:, 0], v[:, 1])):
-                    row_ref[j, rows, columns_of(froms[k], share)] = part.reshape(
-                        chunk // 2, share
-                    ).astype(jnp.bfloat16)
+                row_ref[rows, columns_of(froms[k], share)] = (
+                    v * scale * gain_ref[froms[k]]
+                ).astype(jnp.bfloat16)
             return carry
 
         lax.fori_loop(0, slots // chunk, norm_rows, 0)
-        for j in range(local_experts):
-            rows = row_ref[j]
-            gate_part = jnp.dot(rows, gate_ref[j], preferred_element_type=jnp.float32)
-            up_part = jnp.dot(rows, up_ref[j], preferred_element_type=jnp.float32)
-            act_ref[j] = (gate_part * jax.nn.sigmoid(gate_part) * up_part).astype(jnp.bfloat16)
-        for k in (1, shares - 1, *range(2, shares - 1), 0):
-            outs = [
-                jnp.dot(
-                    act_ref[j],
-                    down_ref[j, :, columns_of(tos[k], share)],
-                    preferred_element_type=jnp.float32,
-                ).reshape(kept // tile, tile, share)
-                for j in range(local_experts)
-            ]
-            both = jnp.stack(swap_halves(*outs), axis=1).reshape(slots, share)
-            out_refs[k][...] = both.astype(jnp.bfloat16)
+        rows = row_ref[...]
+        gate_part = jnp.dot(rows, gate_ref[...], preferred_element_type=jnp.float32)
+        up_part = jnp.dot(rows, up_ref[...], preferred_element_type=jnp.float32)
+        act = (gate_part * jax.nn.sigmoid(gate_part) * up_part).astype(jnp.bfloat16)
+        for k in range(shares):
+            out_refs[k][...] = jnp.dot(
+                act, down_ref[:, columns_of(tos[k], share)], preferred_element_type=jnp.float32
+            ).astype(jnp.bfloat16)
 
     vmem = pl.BlockSpec(memory_space=pltpu.VMEM)
     return pl.pallas_call(
@@ -373,36 +408,10 @@
         in_specs=[pl.BlockSpec(memory_space=pltpu.SMEM)] + [vmem] * (shares + 4),
         out_specs=[vmem] * shares,
         out_shape=[jax.ShapeDtypeStruct((slots, share), jnp.bfloat16)] * shares,
-        scratch_shapes=[
-            pltpu.VMEM((local_experts, kept, width), jnp.bfloat16),
-            pltpu.VMEM((local_experts, kept, hidden), jnp.bfloat16),
-        ],
-        compiler_params=pltpu.CompilerParams(vmem_limit_bytes=24 * 1024 * 1024),
-        name="experts",
+        scratch_shapes=[pltpu.VMEM((slots, width), jnp.bfloat16)],
+        compiler_params=pltpu.CompilerParams(vmem_limit_bytes=16 * 1024 * 1024),
+        name="expert",
     )(here, *pieces, gain, w_gate, w_up, w_down)
-
-
-def add_up(halves):
-    rows, share = halves[0][0].shape
-    count = len(halves[0])
-
-    def kernel(*refs):
-        for h in range(len(halves)):
-            group = refs[h * count : (h + 1) * count]
-            total = group[0][...].astype(jnp.float32)
-            for r in group[1:]:
-                total = total + r[...].astype(jnp.float32)
-            refs[-1][h * rows : (h + 1) * rows, :] = total.astype(jnp.bfloat16)
-
-    vmem = pl.BlockSpec(memory_space=pltpu.VMEM)
-    return pl.pallas_call(
-        kernel,
-        in_specs=[vmem] * (count * len(halves)),
-        out_specs=vmem,
-        out_shape=jax.ShapeDtypeStruct((rows * len(halves), share), jnp.bfloat16),
-        compiler_params=pltpu.CompilerParams(vmem_limit_bytes=8 * 1024 * 1024),
-        name="add_up",
-    )(*[r for half in halves for r in half])
 
 
 def finish(here, hidden, pieces, gain):
@@ -520,15 +529,14 @@
     matches = target[:, :, None] == slot_ids[None, None, :]
     combine_map = jnp.sum(jnp.where(matches, route_weight[:, :, None], 0.0), axis=1)
 
-    weights = fetch(w_gate, w_up, w_down)
-    half = ep_count // 2
+    rows = by_expert(rows.reshape(total_slots, share))
     gathered = []
-    for h in range(2):
-        rows_half = rows[h * half : (h + 1) * half].reshape(half * local_slots, share)
-        gathered.append(shifted([rows_half] * shares, "tp"))
+    for j in range(local_experts):
+        gathered.append(shifted([rows[j]] * shares, "tp"))
     arrived = []
-    for h in range(2):
-        outs = experts(here_array, gathered[h], gain_mix, *weights)
+    for j in range(local_experts):
+        weights = fetch(j, w_gate, w_up, w_down)
+        outs = expert(here_array, gathered[j], gain_mix, *weights)
         arrived.append(shifted(outs, "tp"))
     summed = add_up(arrived)
     returned = exchange(summed.reshape(ep_count, local_slots, share), "ep")

time: 132 us -> 140 us (1.061)
  waiting for transfers between devices: 44.9 us -> 35.8 us
  starting transfers between devices: 62.3 us -> 69.9 us
  local copies, waits for them, and re-layouts: 7.27 us -> 13.1 us
  other arithmetic: 1.64 us -> 5.99 us
    all_to_all x2, waiting for transfers between devices: 32 us -> 20 us  [exchange(): return lax.all_to_all(x, axis, 0, 0, tiled=True)]
    all_to_all x2, starting transfers between devices: 29.5 us -> 37.1 us  [exchange(): return lax.all_to_all(x, axis, 0, 0, tiled=True)]
    reshape x2, local copies, waits for them, and re-layouts: 0.19 us -> 3.56 us  [layer(): jnp.concatenate([w_group, w_expert], axis=-1).reshape(shares, share, -1)]
    ppermute x21, waiting for transfers between devices: 12.9 us -> 15.8 us  [shifted(): lax.ppermute(pieces[k], axis, [(i, (i + k) % size) for i in range(size)])]
    gather x1, local copies, waits for them, and re-layouts: 0.56 us -> 2.24 us  [layer(): jnp.concatenate([w_group, w_expert], axis=-1).reshape(shares, share, -1)]
    concatenate x1, other arithmetic: 0.08 us -> 1.73 us  [layer(): jnp.concatenate([w_group, w_expert], axis=-1).reshape(shares, share, -1)]
    pallas_call x3 -> x4, Pallas kernels: 5.35 us -> 4.13 us  [the longest x2 3.18 us: expert(): pl.pallas_call(kernel, in_specs=[pl.BlockSpec(memory_space=pltpu.SMEM)] +...]
    pallas_call x1 -> x2, Pallas kernels: 2.89 us -> 3.79 us  [fetch(): pl.pallas_call(kernel, in_specs=[pl.BlockSpec(memory_space=pltpu.HBM)] *...]
  transfers between devices with their start and end apart: 23 -> 23, of which waited for: 10 -> 13; matrix products, arithmetic and copies ran while one was open for 2% -> 9% of each run, Pallas kernels for 6% -> 5%
where the time goes in v6:
time: 140 us; the launch traced here: 139 us
  starting transfers between devices  69.9 us (50%)
  waiting for transfers between devices  35.8 us (26%)
  Pallas kernels  13.3 us (10%)
  local copies, waits for them, and re-layouts  13.1 us (9%)
  other arithmetic  5.99 us (4%)
    all_to_all x2, starting transfers between devices, exchange(): return lax.all_to_all(x, axis, 0, 0, tiled=True)  37.1 us
    ppermute x21, starting transfers between devices, shifted(): lax.ppermute(pieces[k], axis, [(i, (i + k) % size) for i in range(size)])  32.8 us
    all_to_all x2, waiting for transfers between devices, exchange(): return lax.all_to_all(x, axis, 0, 0, tiled=True)  20 us
    ppermute x21, waiting for transfers between devices, shifted(): lax.ppermute(pieces[k], axis, [(i, (i + k) % size) for i in range(size)])  15.8 us
    unnamed x22, local copies, waits for them, and re-layouts  6.63 us
    pallas_call x2, Pallas kernels, fetch(): pl.pallas_call(kernel, in_specs=[pl.BlockSpec(memory_space=pltpu.HBM)] *...  3.79 us
    reshape x2, local copies, waits for them, and re-layouts, layer(): jnp.concatenate([w_group, w_expert], axis=-1).reshape(shares, share, -1)  3.56 us
    pallas_call x1, Pallas kernels, mixer(): pl.pallas_call(kernel, in_specs=[pl.BlockSpec(memory_space=pltpu.SMEM)] +...  3.51 us
  transfers between devices with their start and end apart: 23, of which 13 were waited for; matrix products, arithmetic and copies ran while one was open for 9% of the time, Pallas kernels for 5%

profile of v6, /device:TPU:40, one launch (start us, length us, event | category | flops | bytes accessed | tf_op | source)
XLA Modules:
  0.0 139.5 jit_solution(6403109509355102684)
XLA Ops:
  0.6 3.5 %mixer.1 = (f32[64,512]{1,0:T(8,128)S(1)}, bf16[64,512]{1,0:T(8,128)(2,1)S(1)}, bf16[64,512]{1,0:T(8,128)(2,1)S(1)}, bf16[64,512]{1,0:T(8,128)(2,1)S(1)}, f32[64,24,128]{2,1,0:T(8,128)}) custom-call(s32[1]{0:T(128)} %bitcast.here_ref, f32[24,64]{1,0:T(8,128)} %refs_0_.3, f32[24,64]{1,0:T(8,128)} %refs_1_.3, f32[1,24]{1,0:T(1,128)} %bitcast.33, ...), custom_call_target="tpu_custom_call" | custom-call | tf_op jit(solution)/shard_map/mixer/pallas_call | solution.py:218
  4.2 1.7 %collective-permute-start = (bf16[64,512]{1,0:T(8,128)(2,1)S(1)}, bf16[64,512]{1,0:T(8,128)(2,1)S(1)}, u32[]{:S(2)}, u32[]{:S(2)}) collective-permute-start(bf16[64,512]{1,0:T(8,128)(2,1)S(1)} %get-tuple-element.26), channel_id=1, source_target_pairs={{0,1},{1,2},{2,3},{3,0},{4,5},{5,6},{6,7},{7,4},{8,9},{9,10},{10,1... | collective-permute-start | bytes 196616 | tf_op jit(solution)/shard_map/ppermute | solution.py:19
  5.9 3.0 %collective-permute-start.1 = (bf16[64,512]{1,0:T(8,128)(2,1)S(1)}, bf16[64,512]{1,0:T(8,128)(2,1)S(1)}, u32[]{:S(2)}, u32[]{:S(2)}) collective-permute-start(bf16[64,512]{1,0:T(8,128)(2,1)S(1)} %get-tuple-element.27), channel_id=1, source_target_pairs={{0,2},{1,3},{2,0},{3,1},{4,6},{5,7},{6,4},{7,5},{8,10},{9,11},{10,... | collective-permute-start | bytes 196616 | tf_op jit(solution)/shard_map/ppermute | solution.py:19
  8.9 1.3 collective-permute-start.2
  10.6 1.6 %collective-permute-done.1.refs_1_ = bf16[64,512]{1,0:T(8,128)(2,1)S(1)} collective-permute-done((bf16[64,512]{1,0:T(8,128)(2,1)S(1)}, bf16[64,512]{1,0:T(8,128)(2,1)S(1)}, u32[]{:S(2)}, u32[]{:S(2)}) %collective-permute-start.1) | collective-permute-done | bytes 65568 | tf_op jit(solution)/shard_map/ppermute | solution.py:19
  12.2 1.0 collective-permute-done.2.refs_2_
  13.2 0.9 place_rows.1
  14.1 24.8 %all-to-all-start = ((bf16[32,8,512]{2,1,0:T(8,128)(2,1)}), bf16[32,8,512]{2,1,0:T(8,128)(2,1)S(1)}, u32[]{:S(2)}, u32[]{:S(2)}) async-start(bf16[32,8,512]{2,1,0:T(8,128)(2,1)} %bitcast.10), calls=%async_computation | async-start | bytes 524288 | tf_op jit(solution)/shard_map/all_to_all | solution.py:13
  38.9 1.9 %fetch.2 = (bf16[2048,256]{1,0:T(8,128)(2,1)S(1)}, bf16[2048,256]{1,0:T(8,128)(2,1)S(1)}, bf16[256,2048]{1,0:T(8,128)(2,1)S(1)}) custom-call(bf16[2,2048,256]{2,1,0:T(8,128)(2,1)} %refs_0_.5, bf16[2,2048,256]{2,1,0:T(8,128)(2,1)} %refs_1_.5, bf16[2,256,2048]{2,1,0:T(8,128)(2,1)} %refs_2_.3), custom_call_target="tpu_custom_call" | custom-call | tf_op jit(solution)/shard_map/fetch/pallas_call | solution.py:297
  40.8 1.0 copy-done
  41.7 1.0 copy-done.2
  42.7 1.0 copy-done.4
  43.7 1.9 %fetch.3 = (bf16[2048,256]{1,0:T(8,128)(2,1)S(1)}, bf16[2048,256]{1,0:T(8,128)(2,1)S(1)}, bf16[256,2048]{1,0:T(8,128)(2,1)S(1)}) custom-call(bf16[2,2048,256]{2,1,0:T(8,128)(2,1)} %refs_0_.5, bf16[2,2048,256]{2,1,0:T(8,128)(2,1)} %refs_1_.5, bf16[2,256,2048]{2,1,0:T(8,128)(2,1)} %refs_2_.3), custom_call_target="tpu_custom_call" | custom-call | tf_op jit(solution)/shard_map/fetch/pallas_call | solution.py:297
  45.6 1.7 %pad_maximum_fusion = bf16[2048,68]{0,1:T(8,128)(2,1)} fusion(bf16[2048,64]{0,1:T(8,128)(2,1)} %param.31, bf16[2048,4]{0,1:T(4,128)(2,1)S(1)} %copy-done.9), kind=kLoop, calls=%fused_computation.10 | loop fusion | flops 557056 | bytes 557056 | tf_op jit(solution)/shard_map/concatenate | solution.py:526
  47.4 1.8 %reshape.143 = bf16[4,512,68]{1,0,2:T(4,128)(2,1)} reshape(bf16[2048,68]{0,1:T(8,128)(2,1)} %pad_maximum_fusion) | data formatting | bytes 557056 | tf_op jit(solution)/shard_map/reshape | solution.py:526
  49.2 1.7 %copy.27 = bf16[4,512,68]{1,2,0:T(8,128)(2,1)} copy(bf16[4,512,68]{1,0,2:T(4,128)(2,1)} %reshape.143) | data formatting | bytes 557056 | tf_op jit(solution)/shard_map/reshape | solution.py:526
  51.0 2.6 %collective-permute-start.5 = (bf16[64,512]{1,0:T(8,128)(2,1)S(1)}, bf16[64,512]{1,0:T(8,128)(2,1)}, u32[]{:S(2)}, u32[]{:S(2)}) collective-permute-start(bf16[64,512]{1,0:T(8,128)(2,1)S(1)} %get-tuple-element.29), channel_id=1, source_target_pairs={{0,3},{1,0},{2,1},{3,2},{4,7},{5,4},{6,5},{7,6},{8,11},{9,8},{10,9... | collective-permute-start | bytes 196616 | tf_op jit(solution)/shard_map/ppermute | solution.py:19
  53.6 1.0 collective-permute-start.3
  55.2 2.2 %gather_fusion.1 = bf16[4,512,68]{1,2,0:T(8,128)(2,1)} fusion(bf16[4,512,68]{1,2,0:T(8,128)(2,1)} %copy.27, s32[1024]{0:T(1024)S(1)} %pad_clamp_fusion), kind=kCustom, calls=%fused_computation.1 | custom fusion | bytes 557072 | tf_op jit(solution)/shard_map/gather | solution.py:526
  57.4 2.1 %collective-permute-done.4 = bf16[64,512]{1,0:T(8,128)(2,1)} collective-permute-done((bf16[64,512]{1,0:T(8,128)(2,1)S(1)}, bf16[64,512]{1,0:T(8,128)(2,1)}, u32[]{:S(2)}, u32[]{:S(2)}) %collective-permute-start.4) | collective-permute-done | bytes 65568 | tf_op jit(solution)/shard_map/ppermute | solution.py:19
  59.9 1.0 convert_reduce_fusion
  61.4 3.7 %collective-permute-start.7 = (bf16[128,512]{1,0:T(8,128)(2,1)S(1)}, bf16[128,512]{1,0:T(8,128)(2,1)S(1)}, u32[]{:S(2)}, u32[]{:S(2)}) collective-permute-start(bf16[128,512]{1,0:T(8,128)(2,1)S(1)} %get-tuple-element.31.refs_0_), channel_id=1, source_target_pairs={{0,2},{1,3},{2,0},{3,1},{4,6},{5,7},{6,4},{7,5},{8,10},{9,11},{10,... | collective-permute-start | bytes 393224 | tf_op jit(solution)/shard_map/ppermute | solution.py:19
  65.4 1.7 %collective-permute-start.12 = (bf16[128,512]{1,0:T(8,128)(2,1)S(1)}, bf16[128,512]{1,0:T(8,128)(2,1)S(1)}, u32[]{:S(2)}, u32[]{:S(2)}) collective-permute-start(bf16[128,512]{1,0:T(8,128)(2,1)S(1)} %get-tuple-element.39.refs_0_), channel_id=1, source_target_pairs={{0,1},{1,2},{2,3},{3,0},{4,5},{5,6},{6,7},{7,4},{8,9},{9,10},{10,1... | collective-permute-start | bytes 393224 | tf_op jit(solution)/shard_map/ppermute | solution.py:19
  67.9 2.0 %collective-permute-start.14 = (bf16[128,512]{1,0:T(8,128)(2,1)S(1)}, bf16[128,512]{1,0:T(8,128)(2,1)S(1)}, u32[]{:S(2)}, u32[]{:S(2)}) collective-permute-start(bf16[128,512]{1,0:T(8,128)(2,1)S(1)} %get-tuple-element.39.refs_0_), channel_id=1, source_target_pairs={{0,3},{1,0},{2,1},{3,2},{4,7},{5,4},{6,5},{7,6},{8,11},{9,8},{10,9... | collective-permute-start | bytes 393224 | tf_op jit(solution)/shard_map/ppermute | solution.py:19
  69.9 2.2 %collective-permute-done.7.refs_2_ = bf16[128,512]{1,0:T(8,128)(2,1)S(1)} collective-permute-done((bf16[128,512]{1,0:T(8,128)(2,1)S(1)}, bf16[128,512]{1,0:T(8,128)(2,1)S(1)}, u32[]{:S(2)}, u32[]{:S(2)}) %collective-permute-start.7) | collective-permute-done | bytes 131104 | tf_op jit(solution)/shard_map/ppermute | solution.py:19
  72.2 1.2 copy-done.1
  73.4 1.2 copy-done.3
  74.6 1.2 copy-done.5
  75.9 1.6 %expert.2 = (bf16[128,512]{1,0:T(8,128)(2,1)S(1)}, bf16[128,512]{1,0:T(8,128)(2,1)S(1)}, bf16[128,512]{1,0:T(8,128)(2,1)S(1)}, bf16[128,512]{1,0:T(8,128)(2,1)S(1)}) custom-call(s32[1]{0:T(128)} %bitcast.here_ref, bf16[128,512]{1,0:T(8,128)(2,1)S(1)} %get-tuple-element.31.refs_0_, bf16[128,512]{1,0:T(8,128)(2,1)S(1)} %collective-permute-done.6.refs_1_, ...), custom_call_target="tpu_custom_call" | custom-call | tf_op jit(solution)/shard_map/expert/pallas_call | solution.py:406
  77.4 2.3 %collective-permute-start.9 = (bf16[128,512]{1,0:T(8,128)(2,1)S(1)}, bf16[128,512]{1,0:T(8,128)(2,1)S(1)}, u32[]{:S(2)}, u32[]{:S(2)}) collective-permute-start(bf16[128,512]{1,0:T(8,128)(2,1)S(1)} %get-tuple-element.36), channel_id=1, source_target_pairs={{0,1},{1,2},{2,3},{3,0},{4,5},{5,6},{6,7},{7,4},{8,9},{9,10},{10,1... | collective-permute-start | bytes 393224 | tf_op jit(solution)/shard_map/ppermute | solution.py:19
  79.8 1.1 fusion.2
  80.9 2.9 %collective-permute-start.10 = (bf16[128,512]{1,0:T(8,128)(2,1)S(1)}, bf16[128,512]{1,0:T(8,128)(2,1)S(1)}, u32[]{:S(2)}, u32[]{:S(2)}) collective-permute-start(bf16[128,512]{1,0:T(8,128)(2,1)S(1)} %get-tuple-element.37), channel_id=1, source_target_pairs={{0,2},{1,3},{2,0},{3,1},{4,6},{5,7},{6,4},{7,5},{8,10},{9,11},{10,... | collective-permute-start | bytes 393224 | tf_op jit(solution)/shard_map/ppermute | solution.py:19
  83.9 1.6 %expert.3 = (bf16[128,512]{1,0:T(8,128)(2,1)S(1)}, bf16[128,512]{1,0:T(8,128)(2,1)S(1)}, bf16[128,512]{1,0:T(8,128)(2,1)S(1)}, bf16[128,512]{1,0:T(8,128)(2,1)S(1)}) custom-call(s32[1]{0:T(128)} %bitcast.here_ref, bf16[128,512]{1,0:T(8,128)(2,1)S(1)} %get-tuple-element.39.refs_0_, bf16[128,512]{1,0:T(8,128)(2,1)S(1)} %collective-permute-done.12.refs_1_, ...), custom_call_target="tpu_custom_call" | custom-call | tf_op jit(solution)/shard_map/expert/pallas_call | solution.py:406
  85.5 2.1 %collective-permute-start.15 = (bf16[128,512]{1,0:T(8,128)(2,1)S(1)}, bf16[128,512]{1,0:T(8,128)(2,1)S(1)}, u32[]{:S(2)}, u32[]{:S(2)}) collective-permute-start(bf16[128,512]{1,0:T(8,128)(2,1)S(1)} %get-tuple-element.44), channel_id=1, source_target_pairs={{0,1},{1,2},{2,3},{3,0},{4,5},{5,6},{6,7},{7,4},{8,9},{9,10},{10,1... | collective-permute-start | bytes 393224 | tf_op jit(solution)/shard_map/ppermute | solution.py:19
  87.6 0.7 collective-permute-start.16
  88.4 2.1 %collective-permute-start.17 = (bf16[128,512]{1,0:T(8,128)(2,1)S(1)}, bf16[128,512]{1,0:T(8,128)(2,1)S(1)}, u32[]{:S(2)}, u32[]{:S(2)}) collective-permute-start(bf16[128,512]{1,0:T(8,128)(2,1)S(1)} %get-tuple-element.46), channel_id=1, source_target_pairs={{0,3},{1,0},{2,1},{3,2},{4,7},{5,4},{6,5},{7,6},{8,11},{9,8},{10,9... | collective-permute-start | bytes 393224 | tf_op jit(solution)/shard_map/ppermute | solution.py:19
  90.5 1.9 %collective-permute-done.15.refs_5_ = bf16[128,512]{1,0:T(8,128)(2,1)S(1)} collective-permute-done((bf16[128,512]{1,0:T(8,128)(2,1)S(1)}, bf16[128,512]{1,0:T(8,128)(2,1)S(1)}, u32[]{:S(2)}, u32[]{:S(2)}) %collective-permute-start.15) | collective-permute-done | bytes 131104 | tf_op jit(solution)/shard_map/ppermute | solution.py:19
  92.4 1.7 %collective-permute-done.16.refs_6_ = bf16[128,512]{1,0:T(8,128)(2,1)S(1)} collective-permute-done((bf16[128,512]{1,0:T(8,128)(2,1)S(1)}, bf16[128,512]{1,0:T(8,128)(2,1)S(1)}, u32[]{:S(2)}, u32[]{:S(2)}) %collective-permute-start.16) | collective-permute-done | bytes 131104 | tf_op jit(solution)/shard_map/ppermute | solution.py:19
  94.5 0.9 add_up.1
  95.3 12.4 %all-to-all-start.1 = ((bf16[32,8,512]{2,1,0:T(8,128)(2,1)}), bf16[32,8,512]{2,1,0:T(8,128)(2,1)S(1)}, u32[]{:S(2)}, u32[]{:S(2)}) async-start(bf16[32,8,512]{2,1,0:T(8,128)(2,1)} %bitcast.13), calls=%async_computation.1 | async-start | bytes 524288 | tf_op jit(solution)/shard_map/all_to_all | solution.py:13
  107.7 1.0 fusion.3.hidden_ref
  109.7 20.0 %all-to-all-done.1 = bf16[32,8,512]{2,1,0:T(8,128)(2,1)S(1)} async-done(((bf16[32,8,512]{2,1,0:T(8,128)(2,1)}), bf16[32,8,512]{2,1,0:T(8,128)(2,1)S(1)}, u32[]{:S(2)}, u32[]{:S(2)}) %all-to-all-start.1) | async-done | bytes 262176 | tf_op jit(solution)/shard_map/all_to_all | solution.py:13
  129.9 1.3 collective-permute-start.18
  131.2 2.9 %collective-permute-start.19 = (bf16[64,512]{1,0:T(8,128)(2,1)S(1)}, bf16[64,512]{1,0:T(8,128)(2,1)S(1)}, u32[]{:S(2)}, u32[]{:S(2)}) collective-permute-start(bf16[64,512]{1,0:T(8,128)(2,1)S(1)} %convolution_convert_fusion.refs_0_), channel_id=1, source_target_pairs={{0,2},{1,3},{2,0},{3,1},{4,6},{5,7},{6,4},{7,5},{8,10},{9,11},{10,... | collective-permute-start | bytes 196616 | tf_op jit(solution)/shard_map/ppermute | solution.py:19
  134.4 1.5 %collective-permute-done.18.refs_1_ = bf16[64,512]{1,0:T(8,128)(2,1)S(1)} collective-permute-done((bf16[64,512]{1,0:T(8,128)(2,1)S(1)}, bf16[64,512]{1,0:T(8,128)(2,1)S(1)}, u32[]{:S(2)}, u32[]{:S(2)}) %collective-permute-start.18) | collective-permute-done | bytes 65568 | tf_op jit(solution)/shard_map/ppermute | solution.py:19
  136.0 1.5 %collective-permute-done.19.refs_2_ = bf16[64,512]{1,0:T(8,128)(2,1)S(1)} collective-permute-done((bf16[64,512]{1,0:T(8,128)(2,1)S(1)}, bf16[64,512]{1,0:T(8,128)(2,1)S(1)}, u32[]{:S(2)}, u32[]{:S(2)}) %collective-permute-start.19) | collective-permute-done | bytes 65568 | tf_op jit(solution)/shard_map/ppermute | solution.py:19
  137.4 1.0 collective-permute-done.20.refs_3_
  138.4 0.9 finish.1
  (57 shorter events, 4.8 us)
Async XLA Ops:
  0.6 9.6 %copy-start.10 = (s32[64,2]{0,1:T(2,128)S(1)}, s32[64,2]{0,1:T(2,128)}, u32[]{:S(2)}) copy-start(s32[64,2]{0,1:T(2,128)} %param.20) | copy-start | bytes 1540
  4.2 6.4 %collective-permute-start = (bf16[64,512]{1,0:T(8,128)(2,1)S(1)}, bf16[64,512]{1,0:T(8,128)(2,1)S(1)}, u32[]{:S(2)}, u32[]{:S(2)}) collective-permute-start(bf16[64,512]{1,0:T(8,128)(2,1)S(1)} %get-tuple-element.26), channel_id=1, source_target_pairs={{0,1},{1,2},{2,3},{3,0},{4,5},{5,6},{6,7},{7,4},{8,9},{9,10},{10,1... | collective-permute-start | bytes 196616 | tf_op jit(solution)/shard_map/ppermute | solution.py:19
  5.9 6.3 %collective-permute-start.1 = (bf16[64,512]{1,0:T(8,128)(2,1)S(1)}, bf16[64,512]{1,0:T(8,128)(2,1)S(1)}, u32[]{:S(2)}, u32[]{:S(2)}) collective-permute-start(bf16[64,512]{1,0:T(8,128)(2,1)S(1)} %get-tuple-element.27), channel_id=1, source_target_pairs={{0,2},{1,3},{2,0},{3,1},{4,6},{5,7},{6,4},{7,5},{8,10},{9,11},{10,... | collective-permute-start | bytes 196616 | tf_op jit(solution)/shard_map/ppermute | solution.py:19
  8.9 4.3 %collective-permute-start.2 = (bf16[64,512]{1,0:T(8,128)(2,1)S(1)}, bf16[64,512]{1,0:T(8,128)(2,1)S(1)}, u32[]{:S(2)}, u32[]{:S(2)}) collective-permute-start(bf16[64,512]{1,0:T(8,128)(2,1)S(1)} %get-tuple-element.28), channel_id=1, source_target_pairs={{0,3},{1,0},{2,1},{3,2},{4,7},{5,4},{6,5},{7,6},{8,11},{9,8},{10,9... | collective-permute-start | bytes 196616 | tf_op jit(solution)/shard_map/ppermute | solution.py:19
  14.1 46.8 %all-to-all-start = ((bf16[32,8,512]{2,1,0:T(8,128)(2,1)}), bf16[32,8,512]{2,1,0:T(8,128)(2,1)S(1)}, u32[]{:S(2)}, u32[]{:S(2)}) async-start(bf16[32,8,512]{2,1,0:T(8,128)(2,1)} %bitcast.10), calls=%async_computation | async-start | bytes 524288 | tf_op jit(solution)/shard_map/all_to_all | solution.py:13
  40.7 1.0 copy-start
  41.7 1.0 copy-start.2
  42.7 1.0 copy-start.4
  43.7 1.9 %copy-start.6 = (f32[2048]{0:T(1024)S(1)}, f32[2048]{0:T(1024)}, u32[]{:S(2)}) copy-start(f32[2048]{0:T(1024)} %param.29) | copy-start | bytes 24580
  43.7 1.9 %copy-start.9 = (bf16[2048,4]{0,1:T(4,128)(2,1)S(1)}, bf16[2048,4]{0,1:T(4,128)(2,1)}, u32[]{:S(2)}) copy-start(bf16[2048,4]{0,1:T(4,128)(2,1)} %param.30) | copy-start | bytes 49156
  51.0 6.4 %collective-permute-start.5 = (bf16[64,512]{1,0:T(8,128)(2,1)S(1)}, bf16[64,512]{1,0:T(8,128)(2,1)}, u32[]{:S(2)}, u32[]{:S(2)}) collective-permute-start(bf16[64,512]{1,0:T(8,128)(2,1)S(1)} %get-tuple-element.29), channel_id=1, source_target_pairs={{0,3},{1,0},{2,1},{3,2},{4,7},{5,4},{6,5},{7,6},{8,11},{9,8},{10,9... | collective-permute-start | bytes 196616 | tf_op jit(solution)/shard_map/ppermute | solution.py:19
  53.6 5.9 %collective-permute-start.4 = (bf16[64,512]{1,0:T(8,128)(2,1)S(1)}, bf16[64,512]{1,0:T(8,128)(2,1)}, u32[]{:S(2)}, u32[]{:S(2)}) collective-permute-start(bf16[64,512]{1,0:T(8,128)(2,1)S(1)} %get-tuple-element.29), channel_id=1, source_target_pairs={{0,2},{1,3},{2,0},{3,1},{4,6},{5,7},{6,4},{7,5},{8,10},{9,11},{10,... | collective-permute-start | bytes 196616 | tf_op jit(solution)/shard_map/ppermute | solution.py:19
  53.6 6.3 %collective-permute-start.3 = (bf16[64,512]{1,0:T(8,128)(2,1)S(1)}, bf16[64,512]{1,0:T(8,128)(2,1)}, u32[]{:S(2)}, u32[]{:S(2)}) collective-permute-start(bf16[64,512]{1,0:T(8,128)(2,1)S(1)} %get-tuple-element.29), channel_id=1, source_target_pairs={{0,1},{1,2},{2,3},{3,0},{4,5},{5,6},{6,7},{7,4},{8,9},{9,10},{10,1... | collective-permute-start | bytes 196616 | tf_op jit(solution)/shard_map/ppermute | solution.py:19
  61.0 6.9 %collective-permute-start.6 = (bf16[128,512]{1,0:T(8,128)(2,1)S(1)}, bf16[128,512]{1,0:T(8,128)(2,1)S(1)}, u32[]{:S(2)}, u32[]{:S(2)}) collective-permute-start(bf16[128,512]{1,0:T(8,128)(2,1)S(1)} %get-tuple-element.31.refs_0_), channel_id=1, source_target_pairs={{0,1},{1,2},{2,3},{3,0},{4,5},{5,6},{6,7},{7,4},{8,9},{9,10},{10,1... | collective-permute-start | bytes 393224 | tf_op jit(solution)/shard_map/ppermute | solution.py:19
  61.4 10.8 %collective-permute-start.7 = (bf16[128,512]{1,0:T(8,128)(2,1)S(1)}, bf16[128,512]{1,0:T(8,128)(2,1)S(1)}, u32[]{:S(2)}, u32[]{:S(2)}) collective-permute-start(bf16[128,512]{1,0:T(8,128)(2,1)S(1)} %get-tuple-element.31.refs_0_), channel_id=1, source_target_pairs={{0,2},{1,3},{2,0},{3,1},{4,6},{5,7},{6,4},{7,5},{8,10},{9,11},{10,... | collective-permute-start | bytes 393224 | tf_op jit(solution)/shard_map/ppermute | solution.py:19
  65.0 7.2 %collective-permute-start.8 = (bf16[128,512]{1,0:T(8,128)(2,1)S(1)}, bf16[128,512]{1,0:T(8,128)(2,1)S(1)}, u32[]{:S(2)}, u32[]{:S(2)}) collective-permute-start(bf16[128,512]{1,0:T(8,128)(2,1)S(1)} %get-tuple-element.31.refs_0_), channel_id=1, source_target_pairs={{0,3},{1,0},{2,1},{3,2},{4,7},{5,4},{6,5},{7,6},{8,11},{9,8},{10,9... | collective-permute-start | bytes 393224 | tf_op jit(solution)/shard_map/ppermute | solution.py:19
  65.4 18.5 %collective-permute-start.12 = (bf16[128,512]{1,0:T(8,128)(2,1)S(1)}, bf16[128,512]{1,0:T(8,128)(2,1)S(1)}, u32[]{:S(2)}, u32[]{:S(2)}) collective-permute-start(bf16[128,512]{1,0:T(8,128)(2,1)S(1)} %get-tuple-element.39.refs_0_), channel_id=1, source_target_pairs={{0,1},{1,2},{2,3},{3,0},{4,5},{5,6},{6,7},{7,4},{8,9},{9,10},{10,1... | collective-permute-start | bytes 393224 | tf_op jit(solution)/shard_map/ppermute | solution.py:19
  67.0 16.8 %collective-permute-start.13 = (bf16[128,512]{1,0:T(8,128)(2,1)S(1)}, bf16[128,512]{1,0:T(8,128)(2,1)S(1)}, u32[]{:S(2)}, u32[]{:S(2)}) collective-permute-start(bf16[128,512]{1,0:T(8,128)(2,1)S(1)} %get-tuple-element.39.refs_0_), channel_id=1, source_target_pairs={{0,2},{1,3},{2,0},{3,1},{4,6},{5,7},{6,4},{7,5},{8,10},{9,11},{10,... | collective-permute-start | bytes 393224 | tf_op jit(solution)/shard_map/ppermute | solution.py:19
  67.9 16.0 %collective-permute-start.14 = (bf16[128,512]{1,0:T(8,128)(2,1)S(1)}, bf16[128,512]{1,0:T(8,128)(2,1)S(1)}, u32[]{:S(2)}, u32[]{:S(2)}) collective-permute-start(bf16[128,512]{1,0:T(8,128)(2,1)S(1)} %get-tuple-element.39.refs_0_), channel_id=1, source_target_pairs={{0,3},{1,0},{2,1},{3,2},{4,7},{5,4},{6,5},{7,6},{8,11},{9,8},{10,9... | collective-permute-start | bytes 393224 | tf_op jit(solution)/shard_map/ppermute | solution.py:19
  72.2 1.2 copy-start.1
  73.4 1.2 copy-start.3
  74.6 1.2 copy-start.5
  77.4 10.9 %collective-permute-start.9 = (bf16[128,512]{1,0:T(8,128)(2,1)S(1)}, bf16[128,512]{1,0:T(8,128)(2,1)S(1)}, u32[]{:S(2)}, u32[]{:S(2)}) collective-permute-start(bf16[128,512]{1,0:T(8,128)(2,1)S(1)} %get-tuple-element.36), channel_id=1, source_target_pairs={{0,1},{1,2},{2,3},{3,0},{4,5},{5,6},{6,7},{7,4},{8,9},{9,10},{10,1... | collective-permute-start | bytes 393224 | tf_op jit(solution)/shard_map/ppermute | solution.py:19
  80.9 9.5 %collective-permute-start.10 = (bf16[128,512]{1,0:T(8,128)(2,1)S(1)}, bf16[128,512]{1,0:T(8,128)(2,1)S(1)}, u32[]{:S(2)}, u32[]{:S(2)}) collective-permute-start(bf16[128,512]{1,0:T(8,128)(2,1)S(1)} %get-tuple-element.37), channel_id=1, source_target_pairs={{0,2},{1,3},{2,0},{3,1},{4,6},{5,7},{6,4},{7,5},{8,10},{9,11},{10,... | collective-permute-start | bytes 393224 | tf_op jit(solution)/shard_map/ppermute | solution.py:19
  83.9 6.6 %collective-permute-start.11 = (bf16[128,512]{1,0:T(8,128)(2,1)S(1)}, bf16[128,512]{1,0:T(8,128)(2,1)S(1)}, u32[]{:S(2)}, u32[]{:S(2)}) collective-permute-start(bf16[128,512]{1,0:T(8,128)(2,1)S(1)} %get-tuple-element.38), channel_id=1, source_target_pairs={{0,3},{1,0},{2,1},{3,2},{4,7},{5,4},{6,5},{7,6},{8,11},{9,8},{10,9... | collective-permute-start | bytes 393224 | tf_op jit(solution)/shard_map/ppermute | solution.py:19
  85.5 23.3 %copy-start.8 = (bf16[4,512,68]{1,2,0:T(8,128)(2,1)S(1)}, bf16[4,512,68]{1,2,0:T(8,128)(2,1)}, u32[]{:S(2)}) copy-start(bf16[4,512,68]{1,2,0:T(8,128)(2,1)} %gather_fusion.1) | copy-start | bytes 835588
  85.5 52.9 %copy-start.7 = (f32[2048]{0:T(1024)S(1)}, f32[2048]{0:T(1024)}, u32[]{:S(2)}) copy-start(f32[2048]{0:T(1024)} %param.35) | copy-start | bytes 24580
  85.5 6.8 %collective-permute-start.15 = (bf16[128,512]{1,0:T(8,128)(2,1)S(1)}, bf16[128,512]{1,0:T(8,128)(2,1)S(1)}, u32[]{:S(2)}, u32[]{:S(2)}) collective-permute-start(bf16[128,512]{1,0:T(8,128)(2,1)S(1)} %get-tuple-element.44), channel_id=1, source_target_pairs={{0,1},{1,2},{2,3},{3,0},{4,5},{5,6},{6,7},{7,4},{8,9},{9,10},{10,1... | collective-permute-start | bytes 393224 | tf_op jit(solution)/shard_map/ppermute | solution.py:19
  87.6 6.5 %collective-permute-start.16 = (bf16[128,512]{1,0:T(8,128)(2,1)S(1)}, bf16[128,512]{1,0:T(8,128)(2,1)S(1)}, u32[]{:S(2)}, u32[]{:S(2)}) collective-permute-start(bf16[128,512]{1,0:T(8,128)(2,1)S(1)} %get-tuple-element.45), channel_id=1, source_target_pairs={{0,2},{1,3},{2,0},{3,1},{4,6},{5,7},{6,4},{7,5},{8,10},{9,11},{10,... | collective-permute-start | bytes 393224 | tf_op jit(solution)/shard_map/ppermute | solution.py:19
  88.4 6.1 %collective-permute-start.17 = (bf16[128,512]{1,0:T(8,128)(2,1)S(1)}, bf16[128,512]{1,0:T(8,128)(2,1)S(1)}, u32[]{:S(2)}, u32[]{:S(2)}) collective-permute-start(bf16[128,512]{1,0:T(8,128)(2,1)S(1)} %get-tuple-element.46), channel_id=1, source_target_pairs={{0,3},{1,0},{2,1},{3,2},{4,7},{5,4},{6,5},{7,6},{8,11},{9,8},{10,9... | collective-permute-start | bytes 393224 | tf_op jit(solution)/shard_map/ppermute | solution.py:19
  95.3 34.4 %all-to-all-start.1 = ((bf16[32,8,512]{2,1,0:T(8,128)(2,1)}), bf16[32,8,512]{2,1,0:T(8,128)(2,1)S(1)}, u32[]{:S(2)}, u32[]{:S(2)}) async-start(bf16[32,8,512]{2,1,0:T(8,128)(2,1)} %bitcast.13), calls=%async_computation.1 | async-start | bytes 524288 | tf_op jit(solution)/shard_map/all_to_all | solution.py:13
  129.9 6.1 %collective-permute-start.18 = (bf16[64,512]{1,0:T(8,128)(2,1)S(1)}, bf16[64,512]{1,0:T(8,128)(2,1)S(1)}, u32[]{:S(2)}, u32[]{:S(2)}) collective-permute-start(bf16[64,512]{1,0:T(8,128)(2,1)S(1)} %convolution_convert_fusion.refs_0_), channel_id=1, source_target_pairs={{0,1},{1,2},{2,3},{3,0},{4,5},{5,6},{6,7},{7,4},{8,9},{9,10},{10,1... | collective-permute-start | bytes 196616 | tf_op jit(solution)/shard_map/ppermute | solution.py:19
  131.2 6.2 %collective-permute-start.19 = (bf16[64,512]{1,0:T(8,128)(2,1)S(1)}, bf16[64,512]{1,0:T(8,128)(2,1)S(1)}, u32[]{:S(2)}, u32[]{:S(2)}) collective-permute-start(bf16[64,512]{1,0:T(8,128)(2,1)S(1)} %convolution_convert_fusion.refs_0_), channel_id=1, source_target_pairs={{0,2},{1,3},{2,0},{3,1},{4,6},{5,7},{6,4},{7,5},{8,10},{9,11},{10,... | collective-permute-start | bytes 196616 | tf_op jit(solution)/shard_map/ppermute | solution.py:19
  134.1 4.3 %collective-permute-start.20 = (bf16[64,512]{1,0:T(8,128)(2,1)S(1)}, bf16[64,512]{1,0:T(8,128)(2,1)S(1)}, u32[]{:S(2)}, u32[]{:S(2)}) collective-permute-start(bf16[64,512]{1,0:T(8,128)(2,1)S(1)} %convolution_convert_fusion.refs_0_), channel_id=1, source_target_pairs={{0,3},{1,0},{2,1},{3,2},{4,7},{5,4},{6,5},{7,6},{8,11},{9,8},{10,9... | collective-permute-start | bytes 196616 | tf_op jit(solution)/shard_map/ppermute | solution.py:19

commit v7 on v6

--- a/solution.py
+++ b/solution.py
@@ -53,15 +53,6 @@
     return pair_exp / jnp.sum(pair_exp, -1, keepdims=True) * group_pick[:, None]
 
 
-def slots_of(routes, expert_total, capacity):
-    hits = (routes[:, :, None] == jnp.arange(expert_total, dtype=jnp.int32)[None, None, :]).astype(
-        jnp.int32
-    )
-    tally = jnp.sum(hits, axis=1)
-    prior = jnp.cumsum(tally, axis=0) - tally
-    return routes * capacity + jnp.sum(prior[:, None, :] * hits, axis=-1)
-
-
 def ring_places(here_ref, shares):
     t = here_ref[0]
     froms = [lax.rem(t + shares - k, shares) for k in range(shares)]
@@ -77,7 +68,22 @@
     return pltpu.VMEM(ref.shape, ref.dtype)
 
 
-def mixer(here, x_in, state, w_in, decay_rate, frequency, log_step, b_in, c_out, skip, w_out):
+def mixer(
+    here,
+    routes,
+    expert_total,
+    capacity,
+    x_in,
+    state,
+    w_in,
+    decay_rate,
+    frequency,
+    log_step,
+    b_in,
+    c_out,
+    skip,
+    w_out,
+):
     seq_count, width = x_in.shape
     channels = w_in.shape[1]
     groups, entries = decay_rate.shape
@@ -87,16 +93,17 @@
     share = width // shares
     together = lanes // per_group
     cut = 4
-    arrays = (decay_rate, frequency, log_step, x_in, w_in, b_in, c_out, skip, state, w_out)
+    arrays = (decay_rate, frequency, log_step, x_in, w_in, b_in, c_out, skip, state, w_out, routes)
+    picks = routes.shape[0]
 
     def kernel(here_ref, *refs):
         far = refs[: len(arrays)]
         base_ref = refs[len(arrays)]
         part_refs = refs[len(arrays) + 1 : len(arrays) + shares]
-        new_far = refs[len(arrays) + shares]
-        rest = refs[len(arrays) + shares + 1 :]
+        new_far, target_ref = refs[len(arrays) + shares : len(arrays) + shares + 2]
+        rest = refs[len(arrays) + shares + 2 :]
         close = rest[: len(arrays)]
-        decay_ref, freq_ref, log_ref, x_ref, w_in_ref, b_ref, c_ref, skip_ref, state_ref, w_out_ref = close
+        decay_ref, freq_ref, log_ref, x_ref, w_in_ref, b_ref, c_ref, skip_ref, state_ref, w_out_ref, routes_ref = close
         new_ref, in_ref, out_ref, act_ref, sems = rest[len(arrays) :]
         _, tos = ring_places(here_ref, shares)
         piece = width // cut
@@ -113,6 +120,20 @@
         for copy in copies.values():
             copy.start()
 
+        copies[10].wait()
+        named = lax.broadcasted_iota(jnp.int32, (expert_total, seq_count), 0)
+        hits = [jnp.where(named == routes_ref[k : k + 1, :], 1.0, 0.0) for k in range(picks)]
+        earlier = lax.broadcasted_iota(jnp.int32, (seq_count, seq_count), 0) < (
+            lax.broadcasted_iota(jnp.int32, (seq_count, seq_count), 1)
+        )
+        before = jnp.dot(
+            sum(hits).astype(jnp.bfloat16),
+            jnp.where(earlier, 1.0, 0.0).astype(jnp.bfloat16),
+            preferred_element_type=jnp.float32,
+        )
+        for k in range(picks):
+            place = jnp.sum(hits[k] * before, axis=0, keepdims=True)
+            target_ref[k : k + 1, :] = routes_ref[k : k + 1, :] * capacity + place.astype(jnp.int32)
         lane = lax.broadcasted_iota(jnp.int32, (1, lanes), 1)
         sign = jnp.where(lane < entries, -1.0, 1.0)
         for i in (0, 1, 2):
@@ -218,10 +239,13 @@
     return pl.pallas_call(
         kernel,
         in_specs=[pl.BlockSpec(memory_space=pltpu.SMEM)] + [hbm] * len(arrays),
-        out_specs=[vmem] * shares + [hbm],
+        out_specs=[vmem] * shares + [hbm, vmem],
         out_shape=[jax.ShapeDtypeStruct((seq_count, share), jnp.float32)]
         + [jax.ShapeDtypeStruct((seq_count, share), jnp.bfloat16)] * (shares - 1)
-        + [jax.ShapeDtypeStruct(state.shape, state.dtype)],
+        + [
+            jax.ShapeDtypeStruct(state.shape, state.dtype),
+            jax.ShapeDtypeStruct(routes.shape, jnp.int32),
+        ],
         scratch_shapes=[near(a) for a in arrays]
         + [
             near(state),
@@ -237,56 +261,45 @@
 
 def place_rows(base, arrived, target, total_slots):
     seq_count, share = base.shape
-    cut = 4
-    piece = total_slots // cut
 
     def kernel(base_ref, target_ref, *refs):
-        own_ref, sent_far, sent_ref, sems = refs[-4:]
+        own_ref, sent_ref = refs[-2:]
         own = base_ref[...]
-        for r in refs[:-4]:
+        for r in refs[:-2]:
             own = own + r[...].astype(jnp.float32)
         own = own.astype(jnp.bfloat16)
-        copies = []
-        for q in range(cut):
-            rows = slice(q * piece, (q + 1) * piece)
-            slot = lax.broadcasted_iota(jnp.int32, (piece, seq_count), 0) + q * piece
-            hit = slot == target_ref[0:1, :]
-            for k in range(1, target_ref.shape[0]):
-                hit = hit | (slot == target_ref[k : k + 1, :])
-            chosen = jnp.where(hit, 1.0, 0.0).astype(jnp.bfloat16)
-            sent_ref[rows, :] = jnp.dot(chosen, own, preferred_element_type=jnp.float32).astype(
-                jnp.bfloat16
-            )
-            copies.append(pltpu.make_async_copy(sent_ref.at[rows], sent_far.at[rows], sems.at[q]))
-            copies[-1].start()
         own_ref[...] = own
-        for copy in copies:
-            copy.wait()
+        slot = lax.broadcasted_iota(jnp.int32, (total_slots, seq_count), 0)
+        hit = slot == target_ref[0:1, :]
+        for k in range(1, target_ref.shape[0]):
+            hit = hit | (slot == target_ref[k : k + 1, :])
+        chosen = jnp.where(hit, 1.0, 0.0).astype(jnp.bfloat16)
+        sent_ref[...] = jnp.dot(chosen, own, preferred_element_type=jnp.float32).astype(jnp.bfloat16)
 
     vmem = pl.BlockSpec(memory_space=pltpu.VMEM)
     return pl.pallas_call(
         kernel,
         in_specs=[vmem] * (2 + len(arrived)),
-        out_specs=[vmem, pl.BlockSpec(memory_space=pltpu.HBM)],
+        out_specs=[vmem] * 2,
         out_shape=[
             jax.ShapeDtypeStruct((seq_count, share), jnp.bfloat16),
             jax.ShapeDtypeStruct((total_slots, share), jnp.bfloat16),
         ],
-        scratch_shapes=[
-            pltpu.VMEM((total_slots, share), jnp.bfloat16),
-            pltpu.SemaphoreType.DMA((cut,)),
-        ],
         compiler_params=pltpu.CompilerParams(vmem_limit_bytes=8 * 1024 * 1024),
         name="place_rows",
-    )(base, target.T, *arrived)
-
-
-def fetch(which, *weights):
+    )(base, target, *arrived)
+
+
+def fetch(*weights):
     count = len(weights)
+    local_experts = weights[0].shape[0]
 
     def kernel(*refs):
         copies = [
-            pltpu.make_async_copy(refs[i].at[which], refs[count + i], refs[-1].at[i])
+            pltpu.make_async_copy(
+                refs[i].at[j], refs[count + j * count + i], refs[-1].at[j * count + i]
+            )
+            for j in range(local_experts)
             for i in range(count)
         ]
         for copy in copies:
@@ -294,15 +307,16 @@
         for copy in copies:
             copy.wait()
 
-    return pl.pallas_call(
+    out = pl.pallas_call(
         kernel,
         in_specs=[pl.BlockSpec(memory_space=pltpu.HBM)] * count,
-        out_specs=[pl.BlockSpec(memory_space=pltpu.VMEM)] * count,
-        out_shape=[pltpu.VMEM(w.shape[1:], w.dtype) for w in weights],
-        scratch_shapes=[pltpu.SemaphoreType.DMA((count,))],
+        out_specs=[pl.BlockSpec(memory_space=pltpu.VMEM)] * (count * local_experts),
+        out_shape=[pltpu.VMEM(w.shape[1:], w.dtype) for w in weights] * local_experts,
+        scratch_shapes=[pltpu.SemaphoreType.DMA((count * local_experts,))],
         compiler_params=pltpu.CompilerParams(vmem_limit_bytes=1024 * 1024),
         name="fetch",
     )(*[pltpu.with_memory_space_constraint(w, pltpu.HBM) for w in weights])
+    return [out[j * count : (j + 1) * count] for j in range(local_experts)]
 
 
 def swap_halves(first, second):
@@ -497,11 +511,11 @@
     here = lax.axis_index("tp")
     here_array = here.astype(jnp.int32).reshape(1)
 
-    target = slots_of(routes, expert_total, capacity)
-    slot_ids = jnp.arange(total_slots, dtype=jnp.int32)
-
-    base, *parts, new_state = mixer(
+    base, *parts, new_state, target = mixer(
         here_array,
+        routes.T,
+        expert_total,
+        capacity,
         x_in,
         state,
         w_in,
@@ -514,32 +528,37 @@
         w_out,
     )
     arrived = shifted([base, *parts], "tp")
+    weights = fetch(w_gate, w_up, w_down)
     own, sent = place_rows(base, arrived[1:], target, total_slots)
     rows = exchange(sent.reshape(ep_count, local_slots, share), "ep")
 
-    parts = shifted([own] * shares, "tp")
-    whole = jnp.stack(parts).astype(jnp.float32)
-    order = (here - jnp.arange(shares)) % shares
-    gain_mix = gain_mix.reshape(shares, 1, share)
-    hidden_state = normalize(whole, gain_mix[order], (0, 2))
-    hidden_bf = hidden_state.astype(jnp.bfloat16)
-    w_router = jnp.concatenate([w_group, w_expert], axis=-1).reshape(shares, share, -1)[order]
-    logits = jnp.einsum("krd,kde->re", hidden_bf, w_router, preferred_element_type=jnp.float32)
-    route_weight = route_weights(logits, routes, w_group.shape[1])
-    matches = target[:, :, None] == slot_ids[None, None, :]
-    combine_map = jnp.sum(jnp.where(matches, route_weight[:, :, None], 0.0), axis=1)
-
+    gains = gain_mix.reshape(shares, 1, share)
     rows = by_expert(rows.reshape(total_slots, share))
     gathered = []
     for j in range(local_experts):
         gathered.append(shifted([rows[j]] * shares, "tp"))
     arrived = []
     for j in range(local_experts):
-        weights = fetch(j, w_gate, w_up, w_down)
-        outs = expert(here_array, gathered[j], gain_mix, *weights)
+        outs = expert(here_array, gathered[j], gains, *weights[j])
         arrived.append(shifted(outs, "tp"))
     summed = add_up(arrived)
+    summed, own, target, routes, gain_mix, w_group, w_expert = lax.optimization_barrier(
+        (summed, own, target, routes, gain_mix, w_group, w_expert)
+    )
     returned = exchange(summed.reshape(ep_count, local_slots, share), "ep")
+
+    parts = shifted([own] * shares, "tp")
+    whole = jnp.stack(parts).astype(jnp.float32)
+    order = (here - jnp.arange(shares)) % shares
+    hidden_state = normalize(whole, gain_mix.reshape(shares, 1, share)[order], (0, 2))
+    hidden_bf = hidden_state.astype(jnp.bfloat16)
+    w_router = jnp.concatenate([w_group, w_expert], axis=-1).reshape(shares, share, -1)[order]
+    logits = jnp.einsum("krd,kde->re", hidden_bf, w_router, preferred_element_type=jnp.float32)
+    route_weight = route_weights(logits, routes, w_group.shape[1])
+    slot_ids = jnp.arange(total_slots, dtype=jnp.int32)
+    matches = target.T[:, :, None] == slot_ids[None, None, :]
+    combine_map = jnp.sum(jnp.where(matches, route_weight[:, :, None], 0.0), axis=1)
+
     moe_own = jnp.dot(
         combine_map.astype(jnp.bfloat16),
         returned.reshape(total_slots, share),

time: 140 us -> 132 us (0.943)
  blocking collectives: 0 us -> 46.5 us
  starting transfers between devices: 69.9 us -> 37.4 us
  local copies, waits for them, and re-layouts: 13.1 us -> 1.43 us
  waiting for transfers between devices: 35.8 us -> 30.2 us
  other arithmetic: 5.99 us -> 1.29 us
    all_to_all x0 -> x1, blocking collectives: none -> 46.5 us  [exchange(): return lax.all_to_all(x, axis, 0, 0, tiled=True)]
    all_to_all x2 -> x1, starting transfers between devices: 37.1 us -> 4.79 us  [exchange(): return lax.all_to_all(x, axis, 0, 0, tiled=True)]
    unnamed x22 -> x10, local copies, waits for them, and re-layouts: 6.63 us -> 0.03 us
    ppermute x21, waiting for transfers between devices: 15.8 us -> 9.84 us  [shifted(): lax.ppermute(pieces[k], axis, [(i, (i + k) % size) for i in range(size)])]
    reshape x2, local copies, waits for them, and re-layouts: 3.56 us -> 0.19 us  [layer(): jnp.concatenate([w_group, w_expert], axis=-1).reshape(shares, share, -1)]
    gather x1, local copies, waits for them, and re-layouts: 2.24 us -> 0.57 us  [layer(): jnp.concatenate([w_group, w_expert], axis=-1).reshape(shares, share, -1)]
    concatenate x1, other arithmetic: 1.73 us -> 0.08 us  [layer(): jnp.concatenate([w_group, w_expert], axis=-1).reshape(shares, share, -1)]
    pallas_call x2 -> x1, Pallas kernels: 3.79 us -> 2.85 us  [fetch(): pl.pallas_call(kernel, in_specs=[pl.BlockSpec(memory_space=pltpu.HBM)] *...]
  transfers between devices with their start and end apart: 23 -> 22, of which waited for: 13 -> 6; matrix products, arithmetic and copies ran while one was open for 9% -> 2% of each run, Pallas kernels for 5% -> 5%
where the time goes in v7:
time: 132 us; the launch traced here: 131 us
  blocking collectives  46.5 us (35%)
  starting transfers between devices  37.4 us (28%)
  waiting for transfers between devices  30.2 us (23%)
  Pallas kernels  13 us (10%)
  local copies, waits for them, and re-layouts  1.43 us (1%)
    all_to_all x1, blocking collectives, exchange(): return lax.all_to_all(x, axis, 0, 0, tiled=True)  46.5 us
    ppermute x21, starting transfers between devices, shifted(): lax.ppermute(pieces[k], axis, [(i, (i + k) % size) for i in range(size)])  32.6 us
    all_to_all x1, waiting for transfers between devices, exchange(): return lax.all_to_all(x, axis, 0, 0, tiled=True)  20.4 us
    ppermute x21, waiting for transfers between devices, shifted(): lax.ppermute(pieces[k], axis, [(i, (i + k) % size) for i in range(size)])  9.84 us
    pallas_call x1, Pallas kernels, mixer(): pl.pallas_call(kernel, in_specs=[pl.BlockSpec(memory_space=pltpu.SMEM)] +...  4.8 us
    all_to_all x1, starting transfers between devices, exchange(): return lax.all_to_all(x, axis, 0, 0, tiled=True)  4.79 us
    pallas_call x2, Pallas kernels, expert(): pl.pallas_call(kernel, in_specs=[pl.BlockSpec(memory_space=pltpu.SMEM)] +...  3.21 us
    pallas_call x1, Pallas kernels, fetch(): pl.pallas_call(kernel, in_specs=[pl.BlockSpec(memory_space=pltpu.HBM)] *...  2.85 us
  transfers between devices with their start and end apart: 22, of which 6 were waited for; matrix products, arithmetic and copies ran while one was open for 2% of the time, Pallas kernels for 5%

profile of v7, /device:TPU:40, one launch (start us, length us, event | category | flops | bytes accessed | tf_op | source)
XLA Modules:
  0.0 131.3 jit_solution(7059194113917997946)
XLA Ops:
  0.6 4.8 %mixer.1 = (f32[64,512]{1,0:T(8,128)S(1)}, bf16[64,512]{1,0:T(8,128)(2,1)S(1)}, bf16[64,512]{1,0:T(8,128)(2,1)S(1)}, bf16[64,512]{1,0:T(8,128)(2,1)S(1)}, f32[64,24,128]{2,1,0:T(8,128)}, /*index=5*/s32[2,64]{1,0:T(2,128)S(1)}) custom-call(s32[1]{0:T(128)} %bitcast.here_ref, f32[24,64]{1,0:T(8,128)} %refs_0_.2, f32[24,64]{1,0:T(8,128)} %refs_1_.2, ...), custom_call_target="tpu_custom_call" | custom-call | tf_op jit(solution)/shard_map/mixer/pallas_call | solution.py:239
  5.4 1.7 %collective-permute-start = (bf16[64,512]{1,0:T(8,128)(2,1)S(1)}, bf16[64,512]{1,0:T(8,128)(2,1)S(1)}, u32[]{:S(2)}, u32[]{:S(2)}) collective-permute-start(bf16[64,512]{1,0:T(8,128)(2,1)S(1)} %get-tuple-element.35), channel_id=1, source_target_pairs={{0,1},{1,2},{2,3},{3,0},{4,5},{5,6},{6,7},{7,4},{8,9},{9,10},{10,1... | collective-permute-start | bytes 196616 | tf_op jit(solution)/shard_map/ppermute | solution.py:19
  7.2 3.0 %collective-permute-start.1 = (bf16[64,512]{1,0:T(8,128)(2,1)S(1)}, bf16[64,512]{1,0:T(8,128)(2,1)S(1)}, u32[]{:S(2)}, u32[]{:S(2)}) collective-permute-start(bf16[64,512]{1,0:T(8,128)(2,1)S(1)} %get-tuple-element.36), channel_id=1, source_target_pairs={{0,2},{1,3},{2,0},{3,1},{4,6},{5,7},{6,4},{7,5},{8,10},{9,11},{10,... | collective-permute-start | bytes 196616 | tf_op jit(solution)/shard_map/ppermute | solution.py:19
  10.2 1.3 collective-permute-start.2
  11.5 2.0 %collective-permute-done.1.refs_1_ = bf16[64,512]{1,0:T(8,128)(2,1)S(1)} collective-permute-done((bf16[64,512]{1,0:T(8,128)(2,1)S(1)}, bf16[64,512]{1,0:T(8,128)(2,1)S(1)}, u32[]{:S(2)}, u32[]{:S(2)}) %collective-permute-start.1) | collective-permute-done | bytes 65568 | tf_op jit(solution)/shard_map/ppermute | solution.py:19
  13.5 1.0 collective-permute-done.2.refs_2_
  14.4 0.2 place_rows.1
  14.7 46.5 %all_to_all.10 = bf16[32,8,512]{2,1,0:T(8,128)(2,1)S(1)} all-to-all(bf16[32,8,512]{2,1,0:T(8,128)(2,1)S(1)} %bitcast.30), channel_id=1, replica_groups=mesh['grp'=2,'ep'=32,'tp'=4] {'ep'}, dimensions={0} | all-to-all | bytes 524288 | tf_op jit(solution)/shard_map/all_to_all | solution.py:13
  61.3 1.6 %collective-permute-start.10 = (bf16[128,512]{1,0:T(8,128)(2,1)S(1)}, bf16[128,512]{1,0:T(8,128)(2,1)S(1)}, u32[]{:S(2)}, u32[]{:S(2)}) collective-permute-start(bf16[128,512]{1,0:T(8,128)(2,1)S(1)} %get-tuple-element.47.refs_0_), channel_id=1, source_target_pairs={{0,2},{1,3},{2,0},{3,1},{4,6},{5,7},{6,4},{7,5},{8,10},{9,11},{10,... | collective-permute-start | bytes 393224 | tf_op jit(solution)/shard_map/ppermute | solution.py:19
  63.0 1.5 %collective-permute-start.11 = (bf16[128,512]{1,0:T(8,128)(2,1)S(1)}, bf16[128,512]{1,0:T(8,128)(2,1)S(1)}, u32[]{:S(2)}, u32[]{:S(2)}) collective-permute-start(bf16[128,512]{1,0:T(8,128)(2,1)S(1)} %get-tuple-element.47.refs_0_), channel_id=1, source_target_pairs={{0,3},{1,0},{2,1},{3,2},{4,7},{5,4},{6,5},{7,6},{8,11},{9,8},{10,9... | collective-permute-start | bytes 393224 | tf_op jit(solution)/shard_map/ppermute | solution.py:19
  64.4 0.6 collective-permute-start.9
  65.0 2.9 %fetch.1 = (bf16[2048,256]{1,0:T(8,128)(2,1)S(1)}, bf16[2048,256]{1,0:T(8,128)(2,1)S(1)}, bf16[256,2048]{1,0:T(8,128)(2,1)S(1)}, bf16[2048,256]{1,0:T(8,128)(2,1...) custom-call(bf16[2,2048,256]{2,1,0:T(8,128)(2,1)} %refs_0_.3, bf16[2,2048,256]{2,1,0:T(8,128)(2,1)} %refs_1_.3, ...), custom_call_target="tpu_custom_call" | custom-call | tf_op jit(solution)/shard_map/fetch/pallas_call | solution.py:310
  67.8 2.0 %collective-permute-start.3 = (bf16[128,512]{1,0:T(8,128)(2,1)S(1)}, bf16[128,512]{1,0:T(8,128)(2,1)S(1)}, u32[]{:S(2)}, u32[]{:S(2)}) collective-permute-start(bf16[128,512]{1,0:T(8,128)(2,1)S(1)} %get-tuple-element.39.refs_0_), channel_id=1, source_target_pairs={{0,1},{1,2},{2,3},{3,0},{4,5},{5,6},{6,7},{7,4},{8,9},{9,10},{10,1... | collective-permute-start | bytes 393224 | tf_op jit(solution)/shard_map/ppermute | solution.py:19
  69.8 2.3 %collective-permute-start.4 = (bf16[128,512]{1,0:T(8,128)(2,1)S(1)}, bf16[128,512]{1,0:T(8,128)(2,1)S(1)}, u32[]{:S(2)}, u32[]{:S(2)}) collective-permute-start(bf16[128,512]{1,0:T(8,128)(2,1)S(1)} %get-tuple-element.39.refs_0_), channel_id=1, source_target_pairs={{0,2},{1,3},{2,0},{3,1},{4,6},{5,7},{6,4},{7,5},{8,10},{9,11},{10,... | collective-permute-start | bytes 393224 | tf_op jit(solution)/shard_map/ppermute | solution.py:19
  72.1 0.5 collective-permute-start.5
  72.7 1.6 %expert.3 = (bf16[128,512]{1,0:T(8,128)(2,1)S(1)}, bf16[128,512]{1,0:T(8,128)(2,1)S(1)}, bf16[128,512]{1,0:T(8,128)(2,1)S(1)}, bf16[128,512]{1,0:T(8,128)(2,1)S(1)}) custom-call(s32[1]{0:T(128)} %bitcast.here_ref, bf16[128,512]{1,0:T(8,128)(2,1)S(1)} %get-tuple-element.47.refs_0_, bf16[128,512]{1,0:T(8,128)(2,1)S(1)} %collective-permute-done.9.refs_1_, ...), custom_call_target="tpu_custom_call" | custom-call | tf_op jit(solution)/shard_map/expert/pallas_call | solution.py:420
  74.3 1.6 %collective-permute-start.12 = (bf16[128,512]{1,0:T(8,128)(2,1)S(1)}, bf16[128,512]{1,0:T(8,128)(2,1)S(1)}, u32[]{:S(2)}, u32[]{:S(2)}) collective-permute-start(bf16[128,512]{1,0:T(8,128)(2,1)S(1)} %get-tuple-element.52), channel_id=1, source_target_pairs={{0,1},{1,2},{2,3},{3,0},{4,5},{5,6},{6,7},{7,4},{8,9},{9,10},{10,1... | collective-permute-start | bytes 393224 | tf_op jit(solution)/shard_map/ppermute | solution.py:19
  75.9 1.3 collective-permute-start.13
  77.1 1.6 %collective-permute-start.14 = (bf16[128,512]{1,0:T(8,128)(2,1)S(1)}, bf16[128,512]{1,0:T(8,128)(2,1)S(1)}, u32[]{:S(2)}, u32[]{:S(2)}) collective-permute-start(bf16[128,512]{1,0:T(8,128)(2,1)S(1)} %get-tuple-element.54), channel_id=1, source_target_pairs={{0,3},{1,0},{2,1},{3,2},{4,7},{5,4},{6,5},{7,6},{8,11},{9,8},{10,9... | collective-permute-start | bytes 393224 | tf_op jit(solution)/shard_map/ppermute | solution.py:19
  78.7 1.6 %expert.2 = (bf16[128,512]{1,0:T(8,128)(2,1)S(1)}, bf16[128,512]{1,0:T(8,128)(2,1)S(1)}, bf16[128,512]{1,0:T(8,128)(2,1)S(1)}, bf16[128,512]{1,0:T(8,128)(2,1)S(1)}) custom-call(s32[1]{0:T(128)} %bitcast.here_ref, bf16[128,512]{1,0:T(8,128)(2,1)S(1)} %get-tuple-element.39.refs_0_, bf16[128,512]{1,0:T(8,128)(2,1)S(1)} %collective-permute-done.3.refs_1_, ...), custom_call_target="tpu_custom_call" | custom-call | tf_op jit(solution)/shard_map/expert/pallas_call | solution.py:420
  80.3 0.6 collective-permute-start.6
  80.9 2.2 %collective-permute-start.7 = (bf16[128,512]{1,0:T(8,128)(2,1)S(1)}, bf16[128,512]{1,0:T(8,128)(2,1)S(1)}, u32[]{:S(2)}, u32[]{:S(2)}) collective-permute-start(bf16[128,512]{1,0:T(8,128)(2,1)S(1)} %get-tuple-element.45), channel_id=1, source_target_pairs={{0,2},{1,3},{2,0},{3,1},{4,6},{5,7},{6,4},{7,5},{8,10},{9,11},{10,... | collective-permute-start | bytes 393224 | tf_op jit(solution)/shard_map/ppermute | solution.py:19
  83.2 1.8 %collective-permute-start.8 = (bf16[128,512]{1,0:T(8,128)(2,1)S(1)}, bf16[128,512]{1,0:T(8,128)(2,1)S(1)}, u32[]{:S(2)}, u32[]{:S(2)}) collective-permute-start(bf16[128,512]{1,0:T(8,128)(2,1)S(1)} %get-tuple-element.46), channel_id=1, source_target_pairs={{0,3},{1,0},{2,1},{3,2},{4,7},{5,4},{6,5},{7,6},{8,11},{9,8},{10,9... | collective-permute-start | bytes 393224 | tf_op jit(solution)/shard_map/ppermute | solution.py:19
  85.0 3.9 %collective-permute-done.6.refs_1_ = bf16[128,512]{1,0:T(8,128)(2,1)S(1)} collective-permute-done((bf16[128,512]{1,0:T(8,128)(2,1)S(1)}, bf16[128,512]{1,0:T(8,128)(2,1)S(1)}, u32[]{:S(2)}, u32[]{:S(2)}) %collective-permute-start.6) | collective-permute-done | bytes 131104 | tf_op jit(solution)/shard_map/ppermute | solution.py:19
  88.9 0.9 add_up.1
  89.8 1.3 collective-permute-start.15
  91.0 2.9 %collective-permute-start.16 = (bf16[64,512]{1,0:T(8,128)(2,1)S(1)}, bf16[64,512]{1,0:T(8,128)(2,1)S(1)}, u32[]{:S(2)}, u32[]{:S(2)}) collective-permute-start(bf16[64,512]{1,0:T(8,128)(2,1)S(1)} %get-tuple-element.56), channel_id=1, source_target_pairs={{0,2},{1,3},{2,0},{3,1},{4,6},{5,7},{6,4},{7,5},{8,10},{9,11},{10,... | collective-permute-start | bytes 196616 | tf_op jit(solution)/shard_map/ppermute | solution.py:19
  93.9 0.4 collective-permute-start.17
  94.4 0.1 reshape.140
  94.6 0.6 gather_fusion.1
  95.2 0.6 gather_fusion
  95.7 4.8 %all-to-all-start.1 = ((bf16[32,8,512]{2,1,0:T(8,128)(2,1)}), bf16[32,8,512]{2,1,0:T(8,128)(2,1)S(1)}, u32[]{:S(2)}, u32[]{:S(2)}) async-start(bf16[32,8,512]{2,1,0:T(8,128)(2,1)} %bitcast.14), calls=%async_computation.1 | async-start | bytes 524288 | tf_op jit(solution)/shard_map/all_to_all | solution.py:13
  100.6 0.1 convert_reduce_fusion
  100.7 0.2 fusion.2
  101.0 0.2 fusion.3.hidden_ref
  101.1 0.2 convolution_bitcast_fusion
  101.4 0.2 select_reduce_fusion.1
  101.6 0.1 fusion.7
  101.8 0.2 select_reduce_fusion.2
  102.0 0.1 select_reduce_fusion
  102.1 20.4 %all-to-all-done.1 = bf16[32,8,512]{2,1,0:T(8,128)(2,1)S(1)} async-done(((bf16[32,8,512]{2,1,0:T(8,128)(2,1)}), bf16[32,8,512]{2,1,0:T(8,128)(2,1)S(1)}, u32[]{:S(2)}, u32[]{:S(2)}) %all-to-all-start.1) | async-done | bytes 262176 | tf_op jit(solution)/shard_map/all_to_all | solution.py:13
  122.5 0.2 convolution_convert_fusion.refs_0_
  122.7 1.8 %collective-permute-start.18 = (bf16[64,512]{1,0:T(8,128)(2,1)S(1)}, bf16[64,512]{1,0:T(8,128)(2,1)S(1)}, u32[]{:S(2)}, u32[]{:S(2)}) collective-permute-start(bf16[64,512]{1,0:T(8,128)(2,1)S(1)} %convolution_convert_fusion.refs_0_), channel_id=1, source_target_pairs={{0,1},{1,2},{2,3},{3,0},{4,5},{5,6},{6,7},{7,4},{8,9},{9,10},{10,1... | collective-permute-start | bytes 196616 | tf_op jit(solution)/shard_map/ppermute | solution.py:19
  124.4 0.7 collective-permute-start.19
  125.1 2.2 %collective-permute-start.20 = (bf16[64,512]{1,0:T(8,128)(2,1)S(1)}, bf16[64,512]{1,0:T(8,128)(2,1)S(1)}, u32[]{:S(2)}, u32[]{:S(2)}) collective-permute-start(bf16[64,512]{1,0:T(8,128)(2,1)S(1)} %convolution_convert_fusion.refs_0_), channel_id=1, source_target_pairs={{0,3},{1,0},{2,1},{3,2},{4,7},{5,4},{6,5},{7,6},{8,11},{9,8},{10,9... | collective-permute-start | bytes 196616 | tf_op jit(solution)/shard_map/ppermute | solution.py:19
  127.3 1.5 %collective-permute-done.18.refs_1_ = bf16[64,512]{1,0:T(8,128)(2,1)S(1)} collective-permute-done((bf16[64,512]{1,0:T(8,128)(2,1)S(1)}, bf16[64,512]{1,0:T(8,128)(2,1)S(1)}, u32[]{:S(2)}, u32[]{:S(2)}) %collective-permute-start.18) | collective-permute-done | bytes 65568 | tf_op jit(solution)/shard_map/ppermute | solution.py:19
  128.7 1.5 %collective-permute-done.19.refs_2_ = bf16[64,512]{1,0:T(8,128)(2,1)S(1)} collective-permute-done((bf16[64,512]{1,0:T(8,128)(2,1)S(1)}, bf16[64,512]{1,0:T(8,128)(2,1)S(1)}, u32[]{:S(2)}, u32[]{:S(2)}) %collective-permute-start.19) | collective-permute-done | bytes 65568 | tf_op jit(solution)/shard_map/ppermute | solution.py:19
  130.2 0.9 finish.1
  (38 shorter events, 0.5 us)
Async XLA Ops:
  5.4 6.0 %collective-permute-start = (bf16[64,512]{1,0:T(8,128)(2,1)S(1)}, bf16[64,512]{1,0:T(8,128)(2,1)S(1)}, u32[]{:S(2)}, u32[]{:S(2)}) collective-permute-start(bf16[64,512]{1,0:T(8,128)(2,1)S(1)} %get-tuple-element.35), channel_id=1, source_target_pairs={{0,1},{1,2},{2,3},{3,0},{4,5},{5,6},{6,7},{7,4},{8,9},{9,10},{10,1... | collective-permute-start | bytes 196616 | tf_op jit(solution)/shard_map/ppermute | solution.py:19
  7.2 6.3 %collective-permute-start.1 = (bf16[64,512]{1,0:T(8,128)(2,1)S(1)}, bf16[64,512]{1,0:T(8,128)(2,1)S(1)}, u32[]{:S(2)}, u32[]{:S(2)}) collective-permute-start(bf16[64,512]{1,0:T(8,128)(2,1)S(1)} %get-tuple-element.36), channel_id=1, source_target_pairs={{0,2},{1,3},{2,0},{3,1},{4,6},{5,7},{6,4},{7,5},{8,10},{9,11},{10,... | collective-permute-start | bytes 196616 | tf_op jit(solution)/shard_map/ppermute | solution.py:19
  10.2 4.3 %collective-permute-start.2 = (bf16[64,512]{1,0:T(8,128)(2,1)S(1)}, bf16[64,512]{1,0:T(8,128)(2,1)S(1)}, u32[]{:S(2)}, u32[]{:S(2)}) collective-permute-start(bf16[64,512]{1,0:T(8,128)(2,1)S(1)} %get-tuple-element.37), channel_id=1, source_target_pairs={{0,3},{1,0},{2,1},{3,2},{4,7},{5,4},{6,5},{7,6},{8,11},{9,8},{10,9... | collective-permute-start | bytes 196616 | tf_op jit(solution)/shard_map/ppermute | solution.py:19
  61.3 11.3 %copy-start = (f32[2048]{0:T(1024)S(1)}, f32[2048]{0:T(1024)}, u32[]{:S(2)}) copy-start(f32[2048]{0:T(1024)} %param.29) | copy-start | bytes 24580
  61.3 10.8 %collective-permute-start.10 = (bf16[128,512]{1,0:T(8,128)(2,1)S(1)}, bf16[128,512]{1,0:T(8,128)(2,1)S(1)}, u32[]{:S(2)}, u32[]{:S(2)}) collective-permute-start(bf16[128,512]{1,0:T(8,128)(2,1)S(1)} %get-tuple-element.47.refs_0_), channel_id=1, source_target_pairs={{0,2},{1,3},{2,0},{3,1},{4,6},{5,7},{6,4},{7,5},{8,10},{9,11},{10,... | collective-permute-start | bytes 393224 | tf_op jit(solution)/shard_map/ppermute | solution.py:19
  63.0 9.7 %collective-permute-start.11 = (bf16[128,512]{1,0:T(8,128)(2,1)S(1)}, bf16[128,512]{1,0:T(8,128)(2,1)S(1)}, u32[]{:S(2)}, u32[]{:S(2)}) collective-permute-start(bf16[128,512]{1,0:T(8,128)(2,1)S(1)} %get-tuple-element.47.refs_0_), channel_id=1, source_target_pairs={{0,3},{1,0},{2,1},{3,2},{4,7},{5,4},{6,5},{7,6},{8,11},{9,8},{10,9... | collective-permute-start | bytes 393224 | tf_op jit(solution)/shard_map/ppermute | solution.py:19
  64.4 8.2 %collective-permute-start.9 = (bf16[128,512]{1,0:T(8,128)(2,1)S(1)}, bf16[128,512]{1,0:T(8,128)(2,1)S(1)}, u32[]{:S(2)}, u32[]{:S(2)}) collective-permute-start(bf16[128,512]{1,0:T(8,128)(2,1)S(1)} %get-tuple-element.47.refs_0_), channel_id=1, source_target_pairs={{0,1},{1,2},{2,3},{3,0},{4,5},{5,6},{6,7},{7,4},{8,9},{9,10},{10,1... | collective-permute-start | bytes 393224 | tf_op jit(solution)/shard_map/ppermute | solution.py:19
  67.8 9.3 %collective-permute-start.3 = (bf16[128,512]{1,0:T(8,128)(2,1)S(1)}, bf16[128,512]{1,0:T(8,128)(2,1)S(1)}, u32[]{:S(2)}, u32[]{:S(2)}) collective-permute-start(bf16[128,512]{1,0:T(8,128)(2,1)S(1)} %get-tuple-element.39.refs_0_), channel_id=1, source_target_pairs={{0,1},{1,2},{2,3},{3,0},{4,5},{5,6},{6,7},{7,4},{8,9},{9,10},{10,1... | collective-permute-start | bytes 393224 | tf_op jit(solution)/shard_map/ppermute | solution.py:19
  69.8 8.9 %collective-permute-start.4 = (bf16[128,512]{1,0:T(8,128)(2,1)S(1)}, bf16[128,512]{1,0:T(8,128)(2,1)S(1)}, u32[]{:S(2)}, u32[]{:S(2)}) collective-permute-start(bf16[128,512]{1,0:T(8,128)(2,1)S(1)} %get-tuple-element.39.refs_0_), channel_id=1, source_target_pairs={{0,2},{1,3},{2,0},{3,1},{4,6},{5,7},{6,4},{7,5},{8,10},{9,11},{10,... | collective-permute-start | bytes 393224 | tf_op jit(solution)/shard_map/ppermute | solution.py:19
  72.1 6.6 %collective-permute-start.5 = (bf16[128,512]{1,0:T(8,128)(2,1)S(1)}, bf16[128,512]{1,0:T(8,128)(2,1)S(1)}, u32[]{:S(2)}, u32[]{:S(2)}) collective-permute-start(bf16[128,512]{1,0:T(8,128)(2,1)S(1)} %get-tuple-element.39.refs_0_), channel_id=1, source_target_pairs={{0,3},{1,0},{2,1},{3,2},{4,7},{5,4},{6,5},{7,6},{8,11},{9,8},{10,9... | collective-permute-start | bytes 393224 | tf_op jit(solution)/shard_map/ppermute | solution.py:19
  74.3 8.9 %collective-permute-start.12 = (bf16[128,512]{1,0:T(8,128)(2,1)S(1)}, bf16[128,512]{1,0:T(8,128)(2,1)S(1)}, u32[]{:S(2)}, u32[]{:S(2)}) collective-permute-start(bf16[128,512]{1,0:T(8,128)(2,1)S(1)} %get-tuple-element.52), channel_id=1, source_target_pairs={{0,1},{1,2},{2,3},{3,0},{4,5},{5,6},{6,7},{7,4},{8,9},{9,10},{10,1... | collective-permute-start | bytes 393224 | tf_op jit(solution)/shard_map/ppermute | solution.py:19
  75.9 9.1 %collective-permute-start.13 = (bf16[128,512]{1,0:T(8,128)(2,1)S(1)}, bf16[128,512]{1,0:T(8,128)(2,1)S(1)}, u32[]{:S(2)}, u32[]{:S(2)}) collective-permute-start(bf16[128,512]{1,0:T(8,128)(2,1)S(1)} %get-tuple-element.53), channel_id=1, source_target_pairs={{0,2},{1,3},{2,0},{3,1},{4,6},{5,7},{6,4},{7,5},{8,10},{9,11},{10,... | collective-permute-start | bytes 393224 | tf_op jit(solution)/shard_map/ppermute | solution.py:19
  77.1 7.9 %collective-permute-start.14 = (bf16[128,512]{1,0:T(8,128)(2,1)S(1)}, bf16[128,512]{1,0:T(8,128)(2,1)S(1)}, u32[]{:S(2)}, u32[]{:S(2)}) collective-permute-start(bf16[128,512]{1,0:T(8,128)(2,1)S(1)} %get-tuple-element.54), channel_id=1, source_target_pairs={{0,3},{1,0},{2,1},{3,2},{4,7},{5,4},{6,5},{7,6},{8,11},{9,8},{10,9... | collective-permute-start | bytes 393224 | tf_op jit(solution)/shard_map/ppermute | solution.py:19
  78.7 15.6 %copy-start.2 = (bf16[2048,64]{0,1:T(8,128)(2,1)S(1)}, bf16[2048,64]{0,1:T(8,128)(2,1)}, u32[]{:S(2)}) copy-start(bf16[2048,64]{0,1:T(8,128)(2,1)} %param.31) | copy-start | bytes 786436
  78.7 15.6 %copy-start.3 = (bf16[2048,4]{0,1:T(4,128)(2,1)S(1)}, bf16[2048,4]{0,1:T(4,128)(2,1)}, u32[]{:S(2)}) copy-start(bf16[2048,4]{0,1:T(4,128)(2,1)} %param.30) | copy-start | bytes 49156
  78.7 15.6 %copy-start.4 = (s32[64,2]{0,1:T(2,128)S(1)}, s32[64,2]{0,1:T(2,128)}, u32[]{:S(2)}) copy-start(s32[64,2]{0,1:T(2,128)} %param.20) | copy-start | bytes 1540
  80.3 8.5 %collective-permute-start.6 = (bf16[128,512]{1,0:T(8,128)(2,1)S(1)}, bf16[128,512]{1,0:T(8,128)(2,1)S(1)}, u32[]{:S(2)}, u32[]{:S(2)}) collective-permute-start(bf16[128,512]{1,0:T(8,128)(2,1)S(1)} %get-tuple-element.44), channel_id=1, source_target_pairs={{0,1},{1,2},{2,3},{3,0},{4,5},{5,6},{6,7},{7,4},{8,9},{9,10},{10,1... | collective-permute-start | bytes 393224 | tf_op jit(solution)/shard_map/ppermute | solution.py:19
  80.9 7.9 %collective-permute-start.7 = (bf16[128,512]{1,0:T(8,128)(2,1)S(1)}, bf16[128,512]{1,0:T(8,128)(2,1)S(1)}, u32[]{:S(2)}, u32[]{:S(2)}) collective-permute-start(bf16[128,512]{1,0:T(8,128)(2,1)S(1)} %get-tuple-element.45), channel_id=1, source_target_pairs={{0,2},{1,3},{2,0},{3,1},{4,6},{5,7},{6,4},{7,5},{8,10},{9,11},{10,... | collective-permute-start | bytes 393224 | tf_op jit(solution)/shard_map/ppermute | solution.py:19
  83.2 5.7 %collective-permute-start.8 = (bf16[128,512]{1,0:T(8,128)(2,1)S(1)}, bf16[128,512]{1,0:T(8,128)(2,1)S(1)}, u32[]{:S(2)}, u32[]{:S(2)}) collective-permute-start(bf16[128,512]{1,0:T(8,128)(2,1)S(1)} %get-tuple-element.46), channel_id=1, source_target_pairs={{0,3},{1,0},{2,1},{3,2},{4,7},{5,4},{6,5},{7,6},{8,11},{9,8},{10,9... | collective-permute-start | bytes 393224 | tf_op jit(solution)/shard_map/ppermute | solution.py:19
  89.8 10.8 %collective-permute-start.15 = (bf16[64,512]{1,0:T(8,128)(2,1)S(1)}, bf16[64,512]{1,0:T(8,128)(2,1)S(1)}, u32[]{:S(2)}, u32[]{:S(2)}) collective-permute-start(bf16[64,512]{1,0:T(8,128)(2,1)S(1)} %get-tuple-element.56), channel_id=1, source_target_pairs={{0,1},{1,2},{2,3},{3,0},{4,5},{5,6},{6,7},{7,4},{8,9},{9,10},{10,1... | collective-permute-start | bytes 196616 | tf_op jit(solution)/shard_map/ppermute | solution.py:19
  91.0 9.5 %collective-permute-start.16 = (bf16[64,512]{1,0:T(8,128)(2,1)S(1)}, bf16[64,512]{1,0:T(8,128)(2,1)S(1)}, u32[]{:S(2)}, u32[]{:S(2)}) collective-permute-start(bf16[64,512]{1,0:T(8,128)(2,1)S(1)} %get-tuple-element.56), channel_id=1, source_target_pairs={{0,2},{1,3},{2,0},{3,1},{4,6},{5,7},{6,4},{7,5},{8,10},{9,11},{10,... | collective-permute-start | bytes 196616 | tf_op jit(solution)/shard_map/ppermute | solution.py:19
  93.9 6.7 %collective-permute-start.17 = (bf16[64,512]{1,0:T(8,128)(2,1)S(1)}, bf16[64,512]{1,0:T(8,128)(2,1)S(1)}, u32[]{:S(2)}, u32[]{:S(2)}) collective-permute-start(bf16[64,512]{1,0:T(8,128)(2,1)S(1)} %get-tuple-element.56), channel_id=1, source_target_pairs={{0,3},{1,0},{2,1},{3,2},{4,7},{5,4},{6,5},{7,6},{8,11},{9,8},{10,9... | collective-permute-start | bytes 196616 | tf_op jit(solution)/shard_map/ppermute | solution.py:19
  94.6 35.6 %copy-start.1 = (f32[2048]{0:T(1024)S(1)}, f32[2048]{0:T(1024)}, u32[]{:S(2)}) copy-start(f32[2048]{0:T(1024)} %param.35) | copy-start | bytes 24580
  95.7 26.8 %all-to-all-start.1 = ((bf16[32,8,512]{2,1,0:T(8,128)(2,1)}), bf16[32,8,512]{2,1,0:T(8,128)(2,1)S(1)}, u32[]{:S(2)}, u32[]{:S(2)}) async-start(bf16[32,8,512]{2,1,0:T(8,128)(2,1)} %bitcast.14), calls=%async_computation.1 | async-start | bytes 524288 | tf_op jit(solution)/shard_map/all_to_all | solution.py:13
  122.7 6.1 %collective-permute-start.18 = (bf16[64,512]{1,0:T(8,128)(2,1)S(1)}, bf16[64,512]{1,0:T(8,128)(2,1)S(1)}, u32[]{:S(2)}, u32[]{:S(2)}) collective-permute-start(bf16[64,512]{1,0:T(8,128)(2,1)S(1)} %convolution_convert_fusion.refs_0_), channel_id=1, source_target_pairs={{0,1},{1,2},{2,3},{3,0},{4,5},{5,6},{6,7},{7,4},{8,9},{9,10},{10,1... | collective-permute-start | bytes 196616 | tf_op jit(solution)/shard_map/ppermute | solution.py:19
  124.4 5.8 %collective-permute-start.19 = (bf16[64,512]{1,0:T(8,128)(2,1)S(1)}, bf16[64,512]{1,0:T(8,128)(2,1)S(1)}, u32[]{:S(2)}, u32[]{:S(2)}) collective-permute-start(bf16[64,512]{1,0:T(8,128)(2,1)S(1)} %convolution_convert_fusion.refs_0_), channel_id=1, source_target_pairs={{0,2},{1,3},{2,0},{3,1},{4,6},{5,7},{6,4},{7,5},{8,10},{9,11},{10,... | collective-permute-start | bytes 196616 | tf_op jit(solution)/shard_map/ppermute | solution.py:19
  125.1 5.1 %collective-permute-start.20 = (bf16[64,512]{1,0:T(8,128)(2,1)S(1)}, bf16[64,512]{1,0:T(8,128)(2,1)S(1)}, u32[]{:S(2)}, u32[]{:S(2)}) collective-permute-start(bf16[64,512]{1,0:T(8,128)(2,1)S(1)} %convolution_convert_fusion.refs_0_), channel_id=1, source_target_pairs={{0,3},{1,0},{2,1},{3,2},{4,7},{5,4},{6,5},{7,6},{8,11},{9,8},{10,9... | collective-permute-start | bytes 196616 | tf_op jit(solution)/shard_map/ppermute | solution.py:19

commit v8 on v6

--- a/solution.py
+++ b/solution.py
@@ -93,11 +93,11 @@
         far = refs[: len(arrays)]
         base_ref = refs[len(arrays)]
         part_refs = refs[len(arrays) + 1 : len(arrays) + shares]
-        new_far = refs[len(arrays) + shares]
+        new_ref = refs[len(arrays) + shares]
         rest = refs[len(arrays) + shares + 1 :]
         close = rest[: len(arrays)]
         decay_ref, freq_ref, log_ref, x_ref, w_in_ref, b_ref, c_ref, skip_ref, state_ref, w_out_ref = close
-        new_ref, in_ref, out_ref, act_ref, sems = rest[len(arrays) :]
+        in_ref, out_ref, act_ref, sems = rest[len(arrays) :]
         _, tos = ring_places(here_ref, shares)
         piece = width // cut
         copies = {}
@@ -107,6 +107,12 @@
                     rows = slice(q * piece, (q + 1) * piece)
                     copies[i, q] = pltpu.make_async_copy(
                         a.at[rows], b.at[rows], sems.at[len(arrays) + q]
+                    )
+            elif i == 9:
+                for k in range(shares):
+                    columns = columns_of(tos[k], share)
+                    copies[i, k] = pltpu.make_async_copy(
+                        a.at[:, columns], b.at[:, columns], sems.at[len(arrays) + cut + k]
                     )
             else:
                 copies[i] = pltpu.make_async_copy(a, b, sems.at[i])
@@ -198,10 +204,8 @@
                     lane_group == g, read[g * seq_count : (g + 1) * seq_count], 0.0
                 )
             act_ref[:, span] = jax.nn.gelu(value).astype(jnp.bfloat16)
-        send = pltpu.make_async_copy(new_ref, new_far, sems.at[len(arrays) + cut])
-        send.start()
-        copies[9].wait()
         for k in range(shares):
+            copies[9, k].wait()
             part = jnp.dot(
                 act_ref[...],
                 w_out_ref[:, columns_of(tos[k], share)],
@@ -211,24 +215,22 @@
                 base_ref[...] += part.astype(jnp.float32)
             else:
                 part_refs[k - 1][...] = part
-        send.wait()
 
     vmem = pl.BlockSpec(memory_space=pltpu.VMEM)
     hbm = pl.BlockSpec(memory_space=pltpu.HBM)
     return pl.pallas_call(
         kernel,
         in_specs=[pl.BlockSpec(memory_space=pltpu.SMEM)] + [hbm] * len(arrays),
-        out_specs=[vmem] * shares + [hbm],
+        out_specs=[vmem] * (shares + 1),
         out_shape=[jax.ShapeDtypeStruct((seq_count, share), jnp.float32)]
         + [jax.ShapeDtypeStruct((seq_count, share), jnp.bfloat16)] * (shares - 1)
-        + [jax.ShapeDtypeStruct(state.shape, state.dtype)],
+        + [near(state)],
         scratch_shapes=[near(a) for a in arrays]
         + [
-            near(state),
             pltpu.VMEM((channels, lanes), jnp.bfloat16),
             pltpu.VMEM((channels, lanes), jnp.bfloat16),
             pltpu.VMEM((seq_count, channels), jnp.bfloat16),
-            pltpu.SemaphoreType.DMA((len(arrays) + cut + 1,)),
+            pltpu.SemaphoreType.DMA((len(arrays) + cut + shares,)),
         ],
         compiler_params=pltpu.CompilerParams(vmem_limit_bytes=16 * 1024 * 1024),
         name="mixer",

time: 140 us -> 140 us (level)
    unnamed x22 -> x25, local copies, waits for them, and re-layouts: 6.63 us -> 8.49 us
  transfers between devices with their start and end apart: 23 -> 23, of which waited for: 13 -> 14; matrix products, arithmetic and copies ran while one was open for 9% -> 8% of each run, Pallas kernels for 5% -> 5%
where the time goes in v8:
time: 140 us; the launch traced here: 139 us
  starting transfers between devices  69.1 us (49%)
  waiting for transfers between devices  36.6 us (26%)
  Pallas kernels  13.4 us (10%)
  local copies, waits for them, and re-layouts  13.2 us (9%)
  other arithmetic  5.28 us (4%)
    all_to_all x2, starting transfers between devices, exchange(): return lax.all_to_all(x, axis, 0, 0, tiled=True)  36.5 us
    ppermute x21, starting transfers between devices, shifted(): lax.ppermute(pieces[k], axis, [(i, (i + k) % size) for i in range(size)])  32.6 us
    all_to_all x2, waiting for transfers between devices, exchange(): return lax.all_to_all(x, axis, 0, 0, tiled=True)  20.7 us
    ppermute x21, waiting for transfers between devices, shifted(): lax.ppermute(pieces[k], axis, [(i, (i + k) % size) for i in range(size)])  15.9 us
    unnamed x25, local copies, waits for them, and re-layouts  8.49 us
    pallas_call x2, Pallas kernels, fetch(): pl.pallas_call(kernel, in_specs=[pl.BlockSpec(memory_space=pltpu.HBM)] *...  3.79 us
    pallas_call x1, Pallas kernels, mixer(): pl.pallas_call(kernel, in_specs=[pl.BlockSpec(memory_space=pltpu.SMEM)] +...  3.63 us
    pallas_call x2, Pallas kernels, expert(): pl.pallas_call(kernel, in_specs=[pl.BlockSpec(memory_space=pltpu.SMEM)] +...  3.17 us
  transfers between devices with their start and end apart: 23, of which 14 were waited for; matrix products, arithmetic and copies ran while one was open for 8% of the time, Pallas kernels for 5%

profile of v8, /device:TPU:40, one launch (start us, length us, event | category | flops | bytes accessed | tf_op | source)
XLA Modules:
  0.0 139.0 jit_solution(16445102870370610771)
XLA Ops:
  0.6 3.6 %mixer.1 = (f32[64,512]{1,0:T(8,128)S(1)}, bf16[64,512]{1,0:T(8,128)(2,1)S(1)}, bf16[64,512]{1,0:T(8,128)(2,1)S(1)}, bf16[64,512]{1,0:T(8,128)(2,1)S(1)}, f32[64,24,128]{2,1,0:T(8,128)S(1)}) custom-call(s32[1]{0:T(128)} %bitcast.here_ref, f32[24,64]{1,0:T(8,128)} %refs_0_.3, f32[24,64]{1,0:T(8,128)} %refs_1_.3, f32[1,24]{1,0:T(1,128)} %bitcast.33, ...), custom_call_target="tpu_custom_call" | custom-call | tf_op jit(solution)/shard_map/mixer/pallas_call | solution.py:221
  4.3 1.7 %collective-permute-start = (bf16[64,512]{1,0:T(8,128)(2,1)S(1)}, bf16[64,512]{1,0:T(8,128)(2,1)S(1)}, u32[]{:S(2)}, u32[]{:S(2)}) collective-permute-start(bf16[64,512]{1,0:T(8,128)(2,1)S(1)} %get-tuple-element.26), channel_id=1, source_target_pairs={{0,1},{1,2},{2,3},{3,0},{4,5},{5,6},{6,7},{7,4},{8,9},{9,10},{10,1... | collective-permute-start | bytes 196616 | tf_op jit(solution)/shard_map/ppermute | solution.py:19
  6.0 3.0 %collective-permute-start.1 = (bf16[64,512]{1,0:T(8,128)(2,1)S(1)}, bf16[64,512]{1,0:T(8,128)(2,1)S(1)}, u32[]{:S(2)}, u32[]{:S(2)}) collective-permute-start(bf16[64,512]{1,0:T(8,128)(2,1)S(1)} %get-tuple-element.27), channel_id=1, source_target_pairs={{0,2},{1,3},{2,0},{3,1},{4,6},{5,7},{6,4},{7,5},{8,10},{9,11},{10,... | collective-permute-start | bytes 196616 | tf_op jit(solution)/shard_map/ppermute | solution.py:19
  9.0 1.3 collective-permute-start.2
  10.7 1.6 %collective-permute-done.1.refs_1_ = bf16[64,512]{1,0:T(8,128)(2,1)S(1)} collective-permute-done((bf16[64,512]{1,0:T(8,128)(2,1)S(1)}, bf16[64,512]{1,0:T(8,128)(2,1)S(1)}, u32[]{:S(2)}, u32[]{:S(2)}) %collective-permute-start.1) | collective-permute-done | bytes 65568 | tf_op jit(solution)/shard_map/ppermute | solution.py:19
  12.3 1.0 collective-permute-done.2.refs_2_
  13.3 0.9 place_rows.1
  14.2 24.8 %all-to-all-start = ((bf16[32,8,512]{2,1,0:T(8,128)(2,1)}), bf16[32,8,512]{2,1,0:T(8,128)(2,1)S(1)}, u32[]{:S(2)}, u32[]{:S(2)}) async-start(bf16[32,8,512]{2,1,0:T(8,128)(2,1)} %bitcast.10), calls=%async_computation | async-start | bytes 524288 | tf_op jit(solution)/shard_map/all_to_all | solution.py:13
  39.0 1.9 %fetch.2 = (bf16[2048,256]{1,0:T(8,128)(2,1)S(1)}, bf16[2048,256]{1,0:T(8,128)(2,1)S(1)}, bf16[256,2048]{1,0:T(8,128)(2,1)S(1)}) custom-call(bf16[2,2048,256]{2,1,0:T(8,128)(2,1)} %refs_0_.5, bf16[2,2048,256]{2,1,0:T(8,128)(2,1)} %refs_1_.5, bf16[2,256,2048]{2,1,0:T(8,128)(2,1)} %refs_2_.3), custom_call_target="tpu_custom_call" | custom-call | tf_op jit(solution)/shard_map/fetch/pallas_call | solution.py:299
  40.9 1.0 copy-done.2
  41.9 1.0 copy-done.4
  42.8 1.0 copy-done.6
  43.8 1.9 %fetch.3 = (bf16[2048,256]{1,0:T(8,128)(2,1)S(1)}, bf16[2048,256]{1,0:T(8,128)(2,1)S(1)}, bf16[256,2048]{1,0:T(8,128)(2,1)S(1)}) custom-call(bf16[2,2048,256]{2,1,0:T(8,128)(2,1)} %refs_0_.5, bf16[2,2048,256]{2,1,0:T(8,128)(2,1)} %refs_1_.5, bf16[2,256,2048]{2,1,0:T(8,128)(2,1)} %refs_2_.3), custom_call_target="tpu_custom_call" | custom-call | tf_op jit(solution)/shard_map/fetch/pallas_call | solution.py:299
  45.7 1.0 copy-done
  46.7 1.0 pad_maximum_fusion
  47.8 0.9 reshape.143
  48.6 1.7 %copy.27 = bf16[4,512,68]{1,2,0:T(8,128)(2,1)} copy(bf16[4,512,68]{1,0,2:T(4,128)(2,1)} %reshape.143) | data formatting | bytes 557056 | tf_op jit(solution)/shard_map/reshape | solution.py:528
  50.4 2.6 %collective-permute-start.5 = (bf16[64,512]{1,0:T(8,128)(2,1)S(1)}, bf16[64,512]{1,0:T(8,128)(2,1)}, u32[]{:S(2)}, u32[]{:S(2)}) collective-permute-start(bf16[64,512]{1,0:T(8,128)(2,1)S(1)} %get-tuple-element.29), channel_id=1, source_target_pairs={{0,3},{1,0},{2,1},{3,2},{4,7},{5,4},{6,5},{7,6},{8,11},{9,8},{10,9... | collective-permute-start | bytes 196616 | tf_op jit(solution)/shard_map/ppermute | solution.py:19
  53.0 1.0 collective-permute-start.3
  54.6 1.5 %gather_fusion.1 = bf16[4,512,68]{1,2,0:T(8,128)(2,1)S(1)} fusion(bf16[4,512,68]{1,2,0:T(8,128)(2,1)} %copy.27, s32[1024]{0:T(1024)S(1)} %pad_clamp_fusion), kind=kCustom, calls=%fused_computation.1 | custom fusion | bytes 557072 | tf_op jit(solution)/shard_map/gather | solution.py:528
  56.1 2.8 %collective-permute-done.4 = bf16[64,512]{1,0:T(8,128)(2,1)} collective-permute-done((bf16[64,512]{1,0:T(8,128)(2,1)S(1)}, bf16[64,512]{1,0:T(8,128)(2,1)}, u32[]{:S(2)}, u32[]{:S(2)}) %collective-permute-start.4) | collective-permute-done | bytes 65568 | tf_op jit(solution)/shard_map/ppermute | solution.py:19
  59.3 1.0 convert_reduce_fusion
  61.5 3.7 %collective-permute-start.7 = (bf16[128,512]{1,0:T(8,128)(2,1)S(1)}, bf16[128,512]{1,0:T(8,128)(2,1)S(1)}, u32[]{:S(2)}, u32[]{:S(2)}) collective-permute-start(bf16[128,512]{1,0:T(8,128)(2,1)S(1)} %get-tuple-element.31.refs_0_), channel_id=1, source_target_pairs={{0,2},{1,3},{2,0},{3,1},{4,6},{5,7},{6,4},{7,5},{8,10},{9,11},{10,... | collective-permute-start | bytes 393224 | tf_op jit(solution)/shard_map/ppermute | solution.py:19
  65.3 1.9 %collective-permute-start.12 = (bf16[128,512]{1,0:T(8,128)(2,1)S(1)}, bf16[128,512]{1,0:T(8,128)(2,1)S(1)}, u32[]{:S(2)}, u32[]{:S(2)}) collective-permute-start(bf16[128,512]{1,0:T(8,128)(2,1)S(1)} %get-tuple-element.39.refs_0_), channel_id=1, source_target_pairs={{0,1},{1,2},{2,3},{3,0},{4,5},{5,6},{6,7},{7,4},{8,9},{9,10},{10,1... | collective-permute-start | bytes 393224 | tf_op jit(solution)/shard_map/ppermute | solution.py:19
  68.0 2.0 %collective-permute-start.14 = (bf16[128,512]{1,0:T(8,128)(2,1)S(1)}, bf16[128,512]{1,0:T(8,128)(2,1)S(1)}, u32[]{:S(2)}, u32[]{:S(2)}) collective-permute-start(bf16[128,512]{1,0:T(8,128)(2,1)S(1)} %get-tuple-element.39.refs_0_), channel_id=1, source_target_pairs={{0,3},{1,0},{2,1},{3,2},{4,7},{5,4},{6,5},{7,6},{8,11},{9,8},{10,9... | collective-permute-start | bytes 393224 | tf_op jit(solution)/shard_map/ppermute | solution.py:19
  70.0 2.2 %collective-permute-done.7.refs_2_ = bf16[128,512]{1,0:T(8,128)(2,1)S(1)} collective-permute-done((bf16[128,512]{1,0:T(8,128)(2,1)S(1)}, bf16[128,512]{1,0:T(8,128)(2,1)S(1)}, u32[]{:S(2)}, u32[]{:S(2)}) %collective-permute-start.7) | collective-permute-done | bytes 131104 | tf_op jit(solution)/shard_map/ppermute | solution.py:19
  72.3 1.2 copy-done.3
  73.5 1.2 copy-done.5
  74.7 1.2 copy-done.7
  76.0 1.6 %expert.2 = (bf16[128,512]{1,0:T(8,128)(2,1)S(1)}, bf16[128,512]{1,0:T(8,128)(2,1)S(1)}, bf16[128,512]{1,0:T(8,128)(2,1)S(1)}, bf16[128,512]{1,0:T(8,128)(2,1)S(1)}) custom-call(s32[1]{0:T(128)} %bitcast.here_ref, bf16[128,512]{1,0:T(8,128)(2,1)S(1)} %get-tuple-element.31.refs_0_, bf16[128,512]{1,0:T(8,128)(2,1)S(1)} %collective-permute-done.6.refs_1_, ...), custom_call_target="tpu_custom_call" | custom-call | tf_op jit(solution)/shard_map/expert/pallas_call | solution.py:408
  77.6 2.3 %collective-permute-start.9 = (bf16[128,512]{1,0:T(8,128)(2,1)S(1)}, bf16[128,512]{1,0:T(8,128)(2,1)S(1)}, u32[]{:S(2)}, u32[]{:S(2)}) collective-permute-start(bf16[128,512]{1,0:T(8,128)(2,1)S(1)} %get-tuple-element.36), channel_id=1, source_target_pairs={{0,1},{1,2},{2,3},{3,0},{4,5},{5,6},{6,7},{7,4},{8,9},{9,10},{10,1... | collective-permute-start | bytes 393224 | tf_op jit(solution)/shard_map/ppermute | solution.py:19
  79.8 1.1 fusion.2
  81.0 2.8 %collective-permute-start.10 = (bf16[128,512]{1,0:T(8,128)(2,1)S(1)}, bf16[128,512]{1,0:T(8,128)(2,1)S(1)}, u32[]{:S(2)}, u32[]{:S(2)}) collective-permute-start(bf16[128,512]{1,0:T(8,128)(2,1)S(1)} %get-tuple-element.37), channel_id=1, source_target_pairs={{0,2},{1,3},{2,0},{3,1},{4,6},{5,7},{6,4},{7,5},{8,10},{9,11},{10,... | collective-permute-start | bytes 393224 | tf_op jit(solution)/shard_map/ppermute | solution.py:19
  83.8 1.6 %expert.3 = (bf16[128,512]{1,0:T(8,128)(2,1)S(1)}, bf16[128,512]{1,0:T(8,128)(2,1)S(1)}, bf16[128,512]{1,0:T(8,128)(2,1)S(1)}, bf16[128,512]{1,0:T(8,128)(2,1)S(1)}) custom-call(s32[1]{0:T(128)} %bitcast.here_ref, bf16[128,512]{1,0:T(8,128)(2,1)S(1)} %get-tuple-element.39.refs_0_, bf16[128,512]{1,0:T(8,128)(2,1)S(1)} %collective-permute-done.12.refs_1_, ...), custom_call_target="tpu_custom_call" | custom-call | tf_op jit(solution)/shard_map/expert/pallas_call | solution.py:408
  85.4 2.1 %collective-permute-start.15 = (bf16[128,512]{1,0:T(8,128)(2,1)S(1)}, bf16[128,512]{1,0:T(8,128)(2,1)S(1)}, u32[]{:S(2)}, u32[]{:S(2)}) collective-permute-start(bf16[128,512]{1,0:T(8,128)(2,1)S(1)} %get-tuple-element.44), channel_id=1, source_target_pairs={{0,1},{1,2},{2,3},{3,0},{4,5},{5,6},{6,7},{7,4},{8,9},{9,10},{10,1... | collective-permute-start | bytes 393224 | tf_op jit(solution)/shard_map/ppermute | solution.py:19
  88.4 2.0 %collective-permute-start.17 = (bf16[128,512]{1,0:T(8,128)(2,1)S(1)}, bf16[128,512]{1,0:T(8,128)(2,1)S(1)}, u32[]{:S(2)}, u32[]{:S(2)}) collective-permute-start(bf16[128,512]{1,0:T(8,128)(2,1)S(1)} %get-tuple-element.46), channel_id=1, source_target_pairs={{0,3},{1,0},{2,1},{3,2},{4,7},{5,4},{6,5},{7,6},{8,11},{9,8},{10,9... | collective-permute-start | bytes 393224 | tf_op jit(solution)/shard_map/ppermute | solution.py:19
  90.4 2.2 %collective-permute-done.15.refs_5_ = bf16[128,512]{1,0:T(8,128)(2,1)S(1)} collective-permute-done((bf16[128,512]{1,0:T(8,128)(2,1)S(1)}, bf16[128,512]{1,0:T(8,128)(2,1)S(1)}, u32[]{:S(2)}, u32[]{:S(2)}) %collective-permute-start.15) | collective-permute-done | bytes 131104 | tf_op jit(solution)/shard_map/ppermute | solution.py:19
  92.6 1.4 %collective-permute-done.16.refs_6_ = bf16[128,512]{1,0:T(8,128)(2,1)S(1)} collective-permute-done((bf16[128,512]{1,0:T(8,128)(2,1)S(1)}, bf16[128,512]{1,0:T(8,128)(2,1)S(1)}, u32[]{:S(2)}, u32[]{:S(2)}) %collective-permute-start.16) | collective-permute-done | bytes 131104 | tf_op jit(solution)/shard_map/ppermute | solution.py:19
  94.6 0.9 add_up.1
  95.5 11.8 %all-to-all-start.1 = ((bf16[32,8,512]{2,1,0:T(8,128)(2,1)}), bf16[32,8,512]{2,1,0:T(8,128)(2,1)S(1)}, u32[]{:S(2)}, u32[]{:S(2)}) async-start(bf16[32,8,512]{2,1,0:T(8,128)(2,1)} %bitcast.13), calls=%async_computation.1 | async-start | bytes 524288 | tf_op jit(solution)/shard_map/all_to_all | solution.py:13
  107.2 1.0 fusion.3.hidden_ref
  109.2 20.0 %all-to-all-done.1 = bf16[32,8,512]{2,1,0:T(8,128)(2,1)S(1)} async-done(((bf16[32,8,512]{2,1,0:T(8,128)(2,1)}), bf16[32,8,512]{2,1,0:T(8,128)(2,1)S(1)}, u32[]{:S(2)}, u32[]{:S(2)}) %all-to-all-start.1) | async-done | bytes 262176 | tf_op jit(solution)/shard_map/all_to_all | solution.py:13
  129.4 1.4 collective-permute-start.18
  130.8 2.9 %collective-permute-start.19 = (bf16[64,512]{1,0:T(8,128)(2,1)S(1)}, bf16[64,512]{1,0:T(8,128)(2,1)S(1)}, u32[]{:S(2)}, u32[]{:S(2)}) collective-permute-start(bf16[64,512]{1,0:T(8,128)(2,1)S(1)} %convolution_convert_fusion.refs_0_), channel_id=1, source_target_pairs={{0,2},{1,3},{2,0},{3,1},{4,6},{5,7},{6,4},{7,5},{8,10},{9,11},{10,... | collective-permute-start | bytes 196616 | tf_op jit(solution)/shard_map/ppermute | solution.py:19
  134.0 0.9 copy.28
  135.5 1.5 %collective-permute-done.19.refs_2_ = bf16[64,512]{1,0:T(8,128)(2,1)S(1)} collective-permute-done((bf16[64,512]{1,0:T(8,128)(2,1)S(1)}, bf16[64,512]{1,0:T(8,128)(2,1)S(1)}, u32[]{:S(2)}, u32[]{:S(2)}) %collective-permute-start.19) | collective-permute-done | bytes 65568 | tf_op jit(solution)/shard_map/ppermute | solution.py:19
  136.9 1.0 collective-permute-done.20.refs_3_
  137.9 0.9 finish.1
  (60 shorter events, 7.0 us)
Async XLA Ops:
  0.6 9.7 %copy-start.11 = (s32[64,2]{0,1:T(2,128)S(1)}, s32[64,2]{0,1:T(2,128)}, u32[]{:S(2)}) copy-start(s32[64,2]{0,1:T(2,128)} %param.20) | copy-start | bytes 1540
  4.3 6.4 %collective-permute-start = (bf16[64,512]{1,0:T(8,128)(2,1)S(1)}, bf16[64,512]{1,0:T(8,128)(2,1)S(1)}, u32[]{:S(2)}, u32[]{:S(2)}) collective-permute-start(bf16[64,512]{1,0:T(8,128)(2,1)S(1)} %get-tuple-element.26), channel_id=1, source_target_pairs={{0,1},{1,2},{2,3},{3,0},{4,5},{5,6},{6,7},{7,4},{8,9},{9,10},{10,1... | collective-permute-start | bytes 196616 | tf_op jit(solution)/shard_map/ppermute | solution.py:19
  6.0 6.3 %collective-permute-start.1 = (bf16[64,512]{1,0:T(8,128)(2,1)S(1)}, bf16[64,512]{1,0:T(8,128)(2,1)S(1)}, u32[]{:S(2)}, u32[]{:S(2)}) collective-permute-start(bf16[64,512]{1,0:T(8,128)(2,1)S(1)} %get-tuple-element.27), channel_id=1, source_target_pairs={{0,2},{1,3},{2,0},{3,1},{4,6},{5,7},{6,4},{7,5},{8,10},{9,11},{10,... | collective-permute-start | bytes 196616 | tf_op jit(solution)/shard_map/ppermute | solution.py:19
  9.0 4.3 %collective-permute-start.2 = (bf16[64,512]{1,0:T(8,128)(2,1)S(1)}, bf16[64,512]{1,0:T(8,128)(2,1)S(1)}, u32[]{:S(2)}, u32[]{:S(2)}) collective-permute-start(bf16[64,512]{1,0:T(8,128)(2,1)S(1)} %get-tuple-element.28), channel_id=1, source_target_pairs={{0,3},{1,0},{2,1},{3,2},{4,7},{5,4},{6,5},{7,6},{8,11},{9,8},{10,9... | collective-permute-start | bytes 196616 | tf_op jit(solution)/shard_map/ppermute | solution.py:19
  14.2 46.8 %all-to-all-start = ((bf16[32,8,512]{2,1,0:T(8,128)(2,1)}), bf16[32,8,512]{2,1,0:T(8,128)(2,1)S(1)}, u32[]{:S(2)}, u32[]{:S(2)}) async-start(bf16[32,8,512]{2,1,0:T(8,128)(2,1)} %bitcast.10), calls=%async_computation | async-start | bytes 524288 | tf_op jit(solution)/shard_map/all_to_all | solution.py:13
  40.9 1.0 copy-start.2
  41.8 1.0 copy-start.4
  42.8 1.0 copy-start.6
  43.8 2.9 %copy-start.8 = (f32[2048]{0:T(1024)S(1)}, f32[2048]{0:T(1024)}, u32[]{:S(2)}) copy-start(f32[2048]{0:T(1024)} %param.29) | copy-start | bytes 24580
  43.8 2.9 %copy-start.10 = (bf16[2048,4]{0,1:T(4,128)(2,1)S(1)}, bf16[2048,4]{0,1:T(4,128)(2,1)}, u32[]{:S(2)}) copy-start(bf16[2048,4]{0,1:T(4,128)(2,1)} %param.30) | copy-start | bytes 49156
  45.7 1.0 copy-start
  50.4 5.7 %collective-permute-start.5 = (bf16[64,512]{1,0:T(8,128)(2,1)S(1)}, bf16[64,512]{1,0:T(8,128)(2,1)}, u32[]{:S(2)}, u32[]{:S(2)}) collective-permute-start(bf16[64,512]{1,0:T(8,128)(2,1)S(1)} %get-tuple-element.29), channel_id=1, source_target_pairs={{0,3},{1,0},{2,1},{3,2},{4,7},{5,4},{6,5},{7,6},{8,11},{9,8},{10,9... | collective-permute-start | bytes 196616 | tf_op jit(solution)/shard_map/ppermute | solution.py:19
  53.0 5.9 %collective-permute-start.4 = (bf16[64,512]{1,0:T(8,128)(2,1)S(1)}, bf16[64,512]{1,0:T(8,128)(2,1)}, u32[]{:S(2)}, u32[]{:S(2)}) collective-permute-start(bf16[64,512]{1,0:T(8,128)(2,1)S(1)} %get-tuple-element.29), channel_id=1, source_target_pairs={{0,2},{1,3},{2,0},{3,1},{4,6},{5,7},{6,4},{7,5},{8,10},{9,11},{10,... | collective-permute-start | bytes 196616 | tf_op jit(solution)/shard_map/ppermute | solution.py:19
  53.0 6.3 %collective-permute-start.3 = (bf16[64,512]{1,0:T(8,128)(2,1)S(1)}, bf16[64,512]{1,0:T(8,128)(2,1)}, u32[]{:S(2)}, u32[]{:S(2)}) collective-permute-start(bf16[64,512]{1,0:T(8,128)(2,1)S(1)} %get-tuple-element.29), channel_id=1, source_target_pairs={{0,1},{1,2},{2,3},{3,0},{4,5},{5,6},{6,7},{7,4},{8,9},{9,10},{10,1... | collective-permute-start | bytes 196616 | tf_op jit(solution)/shard_map/ppermute | solution.py:19
  61.0 22.8 %copy-start.1 = (bf16[256,2048]{1,0:T(8,128)(2,1)S(1)}, bf16[256,2048]{1,0:T(8,128)(2,1)}, u32[]{:S(2)}) copy-start(bf16[256,2048]{1,0:T(8,128)(2,1)} %copy-done) | copy-start | bytes 3145732
  61.1 7.0 %collective-permute-start.6 = (bf16[128,512]{1,0:T(8,128)(2,1)S(1)}, bf16[128,512]{1,0:T(8,128)(2,1)S(1)}, u32[]{:S(2)}, u32[]{:S(2)}) collective-permute-start(bf16[128,512]{1,0:T(8,128)(2,1)S(1)} %get-tuple-element.31.refs_0_), channel_id=1, source_target_pairs={{0,1},{1,2},{2,3},{3,0},{4,5},{5,6},{6,7},{7,4},{8,9},{9,10},{10,1... | collective-permute-start | bytes 393224 | tf_op jit(solution)/shard_map/ppermute | solution.py:19
  61.5 10.8 %collective-permute-start.7 = (bf16[128,512]{1,0:T(8,128)(2,1)S(1)}, bf16[128,512]{1,0:T(8,128)(2,1)S(1)}, u32[]{:S(2)}, u32[]{:S(2)}) collective-permute-start(bf16[128,512]{1,0:T(8,128)(2,1)S(1)} %get-tuple-element.31.refs_0_), channel_id=1, source_target_pairs={{0,2},{1,3},{2,0},{3,1},{4,6},{5,7},{6,4},{7,5},{8,10},{9,11},{10,... | collective-permute-start | bytes 393224 | tf_op jit(solution)/shard_map/ppermute | solution.py:19
  65.1 7.2 %collective-permute-start.8 = (bf16[128,512]{1,0:T(8,128)(2,1)S(1)}, bf16[128,512]{1,0:T(8,128)(2,1)S(1)}, u32[]{:S(2)}, u32[]{:S(2)}) collective-permute-start(bf16[128,512]{1,0:T(8,128)(2,1)S(1)} %get-tuple-element.31.refs_0_), channel_id=1, source_target_pairs={{0,3},{1,0},{2,1},{3,2},{4,7},{5,4},{6,5},{7,6},{8,11},{9,8},{10,9... | collective-permute-start | bytes 393224 | tf_op jit(solution)/shard_map/ppermute | solution.py:19
  65.3 18.5 %collective-permute-start.12 = (bf16[128,512]{1,0:T(8,128)(2,1)S(1)}, bf16[128,512]{1,0:T(8,128)(2,1)S(1)}, u32[]{:S(2)}, u32[]{:S(2)}) collective-permute-start(bf16[128,512]{1,0:T(8,128)(2,1)S(1)} %get-tuple-element.39.refs_0_), channel_id=1, source_target_pairs={{0,1},{1,2},{2,3},{3,0},{4,5},{5,6},{6,7},{7,4},{8,9},{9,10},{10,1... | collective-permute-start | bytes 393224 | tf_op jit(solution)/shard_map/ppermute | solution.py:19
  67.2 16.6 %collective-permute-start.13 = (bf16[128,512]{1,0:T(8,128)(2,1)S(1)}, bf16[128,512]{1,0:T(8,128)(2,1)S(1)}, u32[]{:S(2)}, u32[]{:S(2)}) collective-permute-start(bf16[128,512]{1,0:T(8,128)(2,1)S(1)} %get-tuple-element.39.refs_0_), channel_id=1, source_target_pairs={{0,2},{1,3},{2,0},{3,1},{4,6},{5,7},{6,4},{7,5},{8,10},{9,11},{10,... | collective-permute-start | bytes 393224 | tf_op jit(solution)/shard_map/ppermute | solution.py:19
  68.0 15.8 %collective-permute-start.14 = (bf16[128,512]{1,0:T(8,128)(2,1)S(1)}, bf16[128,512]{1,0:T(8,128)(2,1)S(1)}, u32[]{:S(2)}, u32[]{:S(2)}) collective-permute-start(bf16[128,512]{1,0:T(8,128)(2,1)S(1)} %get-tuple-element.39.refs_0_), channel_id=1, source_target_pairs={{0,3},{1,0},{2,1},{3,2},{4,7},{5,4},{6,5},{7,6},{8,11},{9,8},{10,9... | collective-permute-start | bytes 393224 | tf_op jit(solution)/shard_map/ppermute | solution.py:19
  72.3 1.2 copy-start.3
  73.5 1.2 copy-start.5
  74.7 1.2 copy-start.7
  77.6 10.8 %collective-permute-start.9 = (bf16[128,512]{1,0:T(8,128)(2,1)S(1)}, bf16[128,512]{1,0:T(8,128)(2,1)S(1)}, u32[]{:S(2)}, u32[]{:S(2)}) collective-permute-start(bf16[128,512]{1,0:T(8,128)(2,1)S(1)} %get-tuple-element.36), channel_id=1, source_target_pairs={{0,1},{1,2},{2,3},{3,0},{4,5},{5,6},{6,7},{7,4},{8,9},{9,10},{10,1... | collective-permute-start | bytes 393224 | tf_op jit(solution)/shard_map/ppermute | solution.py:19
  81.0 9.4 %collective-permute-start.10 = (bf16[128,512]{1,0:T(8,128)(2,1)S(1)}, bf16[128,512]{1,0:T(8,128)(2,1)S(1)}, u32[]{:S(2)}, u32[]{:S(2)}) collective-permute-start(bf16[128,512]{1,0:T(8,128)(2,1)S(1)} %get-tuple-element.37), channel_id=1, source_target_pairs={{0,2},{1,3},{2,0},{3,1},{4,6},{5,7},{6,4},{7,5},{8,10},{9,11},{10,... | collective-permute-start | bytes 393224 | tf_op jit(solution)/shard_map/ppermute | solution.py:19
  83.8 6.6 %collective-permute-start.11 = (bf16[128,512]{1,0:T(8,128)(2,1)S(1)}, bf16[128,512]{1,0:T(8,128)(2,1)S(1)}, u32[]{:S(2)}, u32[]{:S(2)}) collective-permute-start(bf16[128,512]{1,0:T(8,128)(2,1)S(1)} %get-tuple-element.38), channel_id=1, source_target_pairs={{0,3},{1,0},{2,1},{3,2},{4,7},{5,4},{6,5},{7,6},{8,11},{9,8},{10,9... | collective-permute-start | bytes 393224 | tf_op jit(solution)/shard_map/ppermute | solution.py:19
  85.4 7.2 %collective-permute-start.15 = (bf16[128,512]{1,0:T(8,128)(2,1)S(1)}, bf16[128,512]{1,0:T(8,128)(2,1)S(1)}, u32[]{:S(2)}, u32[]{:S(2)}) collective-permute-start(bf16[128,512]{1,0:T(8,128)(2,1)S(1)} %get-tuple-element.44), channel_id=1, source_target_pairs={{0,1},{1,2},{2,3},{3,0},{4,5},{5,6},{6,7},{7,4},{8,9},{9,10},{10,1... | collective-permute-start | bytes 393224 | tf_op jit(solution)/shard_map/ppermute | solution.py:19
  87.6 6.5 %collective-permute-start.16 = (bf16[128,512]{1,0:T(8,128)(2,1)S(1)}, bf16[128,512]{1,0:T(8,128)(2,1)S(1)}, u32[]{:S(2)}, u32[]{:S(2)}) collective-permute-start(bf16[128,512]{1,0:T(8,128)(2,1)S(1)} %get-tuple-element.45), channel_id=1, source_target_pairs={{0,2},{1,3},{2,0},{3,1},{4,6},{5,7},{6,4},{7,5},{8,10},{9,11},{10,... | collective-permute-start | bytes 393224 | tf_op jit(solution)/shard_map/ppermute | solution.py:19
  88.4 6.2 %collective-permute-start.17 = (bf16[128,512]{1,0:T(8,128)(2,1)S(1)}, bf16[128,512]{1,0:T(8,128)(2,1)S(1)}, u32[]{:S(2)}, u32[]{:S(2)}) collective-permute-start(bf16[128,512]{1,0:T(8,128)(2,1)S(1)} %get-tuple-element.46), channel_id=1, source_target_pairs={{0,3},{1,0},{2,1},{3,2},{4,7},{5,4},{6,5},{7,6},{8,11},{9,8},{10,9... | collective-permute-start | bytes 393224 | tf_op jit(solution)/shard_map/ppermute | solution.py:19
  95.5 42.5 %copy-start.9 = (f32[2048]{0:T(1024)S(1)}, f32[2048]{0:T(1024)}, u32[]{:S(2)}) copy-start(f32[2048]{0:T(1024)} %param.35) | copy-start | bytes 24580
  95.5 33.8 %all-to-all-start.1 = ((bf16[32,8,512]{2,1,0:T(8,128)(2,1)}), bf16[32,8,512]{2,1,0:T(8,128)(2,1)S(1)}, u32[]{:S(2)}, u32[]{:S(2)}) async-start(bf16[32,8,512]{2,1,0:T(8,128)(2,1)} %bitcast.13), calls=%async_computation.1 | async-start | bytes 524288 | tf_op jit(solution)/shard_map/all_to_all | solution.py:13
  129.4 6.1 %collective-permute-start.18 = (bf16[64,512]{1,0:T(8,128)(2,1)S(1)}, bf16[64,512]{1,0:T(8,128)(2,1)S(1)}, u32[]{:S(2)}, u32[]{:S(2)}) collective-permute-start(bf16[64,512]{1,0:T(8,128)(2,1)S(1)} %convolution_convert_fusion.refs_0_), channel_id=1, source_target_pairs={{0,1},{1,2},{2,3},{3,0},{4,5},{5,6},{6,7},{7,4},{8,9},{9,10},{10,1... | collective-permute-start | bytes 196616 | tf_op jit(solution)/shard_map/ppermute | solution.py:19
  130.8 6.2 %collective-permute-start.19 = (bf16[64,512]{1,0:T(8,128)(2,1)S(1)}, bf16[64,512]{1,0:T(8,128)(2,1)S(1)}, u32[]{:S(2)}, u32[]{:S(2)}) collective-permute-start(bf16[64,512]{1,0:T(8,128)(2,1)S(1)} %convolution_convert_fusion.refs_0_), channel_id=1, source_target_pairs={{0,2},{1,3},{2,0},{3,1},{4,6},{5,7},{6,4},{7,5},{8,10},{9,11},{10,... | collective-permute-start | bytes 196616 | tf_op jit(solution)/shard_map/ppermute | solution.py:19
  133.6 4.3 %collective-permute-start.20 = (bf16[64,512]{1,0:T(8,128)(2,1)S(1)}, bf16[64,512]{1,0:T(8,128)(2,1)S(1)}, u32[]{:S(2)}, u32[]{:S(2)}) collective-permute-start(bf16[64,512]{1,0:T(8,128)(2,1)S(1)} %convolution_convert_fusion.refs_0_), channel_id=1, source_target_pairs={{0,3},{1,0},{2,1},{3,2},{4,7},{5,4},{6,5},{7,6},{8,11},{9,8},{10,9... | collective-permute-start | bytes 196616 | tf_op jit(solution)/shard_map/ppermute | solution.py:19

commit v9 on v8

--- a/solution.py
+++ b/solution.py
@@ -107,12 +107,6 @@
                     rows = slice(q * piece, (q + 1) * piece)
                     copies[i, q] = pltpu.make_async_copy(
                         a.at[rows], b.at[rows], sems.at[len(arrays) + q]
-                    )
-            elif i == 9:
-                for k in range(shares):
-                    columns = columns_of(tos[k], share)
-                    copies[i, k] = pltpu.make_async_copy(
-                        a.at[:, columns], b.at[:, columns], sems.at[len(arrays) + cut + k]
                     )
             else:
                 copies[i] = pltpu.make_async_copy(a, b, sems.at[i])
@@ -204,8 +198,8 @@
                     lane_group == g, read[g * seq_count : (g + 1) * seq_count], 0.0
                 )
             act_ref[:, span] = jax.nn.gelu(value).astype(jnp.bfloat16)
+        copies[9].wait()
         for k in range(shares):
-            copies[9, k].wait()
             part = jnp.dot(
                 act_ref[...],
                 w_out_ref[:, columns_of(tos[k], share)],
@@ -283,12 +277,16 @@
     )(base, target.T, *arrived)
 
 
-def fetch(which, *weights):
+def fetch(*weights):
     count = len(weights)
+    local_experts = weights[0].shape[0]
 
     def kernel(*refs):
         copies = [
-            pltpu.make_async_copy(refs[i].at[which], refs[count + i], refs[-1].at[i])
+            pltpu.make_async_copy(
+                refs[i].at[j], refs[count + j * count + i], refs[-1].at[j * count + i]
+            )
+            for j in range(local_experts)
             for i in range(count)
         ]
         for copy in copies:
@@ -296,15 +294,16 @@
         for copy in copies:
             copy.wait()
 
-    return pl.pallas_call(
+    out = pl.pallas_call(
         kernel,
         in_specs=[pl.BlockSpec(memory_space=pltpu.HBM)] * count,
-        out_specs=[pl.BlockSpec(memory_space=pltpu.VMEM)] * count,
-        out_shape=[pltpu.VMEM(w.shape[1:], w.dtype) for w in weights],
-        scratch_shapes=[pltpu.SemaphoreType.DMA((count,))],
+        out_specs=[pl.BlockSpec(memory_space=pltpu.VMEM)] * (count * local_experts),
+        out_shape=[pltpu.VMEM(w.shape[1:], w.dtype) for w in weights] * local_experts,
+        scratch_shapes=[pltpu.SemaphoreType.DMA((count * local_experts,))],
         compiler_params=pltpu.CompilerParams(vmem_limit_bytes=1024 * 1024),
         name="fetch",
     )(*[pltpu.with_memory_space_constraint(w, pltpu.HBM) for w in weights])
+    return [out[j * count : (j + 1) * count] for j in range(local_experts)]
 
 
 def swap_halves(first, second):
@@ -535,10 +534,10 @@
     gathered = []
     for j in range(local_experts):
         gathered.append(shifted([rows[j]] * shares, "tp"))
+    weights = fetch(w_gate, w_up, w_down)
     arrived = []
     for j in range(local_experts):
-        weights = fetch(j, w_gate, w_up, w_down)
-        outs = expert(here_array, gathered[j], gain_mix, *weights)
+        outs = expert(here_array, gathered[j], gain_mix, *weights[j])
         arrived.append(shifted(outs, "tp"))
     summed = add_up(arrived)
     returned = exchange(summed.reshape(ep_count, local_slots, share), "ep")

time: 140 us -> 132 us (0.943)
  starting transfers between devices: 69.1 us -> 62.2 us
  waiting for transfers between devices: 36.6 us -> 41.8 us
  local copies, waits for them, and re-layouts: 13.2 us -> 9.9 us
    all_to_all x2, waiting for transfers between devices: 20.7 us -> 29 us  [exchange(): return lax.all_to_all(x, axis, 0, 0, tiled=True)]
    all_to_all x2, starting transfers between devices: 36.5 us -> 29.7 us  [exchange(): return lax.all_to_all(x, axis, 0, 0, tiled=True)]
    ppermute x21, waiting for transfers between devices: 15.9 us -> 12.9 us  [shifted(): lax.ppermute(pieces[k], axis, [(i, (i + k) % size) for i in range(size)])]
    reshape x2, local copies, waits for them, and re-layouts: 2.57 us -> 0.19 us  [layer(): jnp.concatenate([w_group, w_expert], axis=-1).reshape(shares, share, -1)]
    pallas_call x2 -> x1, Pallas kernels: 3.79 us -> 2.86 us  [fetch(): pl.pallas_call(kernel, in_specs=[pl.BlockSpec(memory_space=pltpu.HBM)] *...]
    unnamed x25 -> x27, local copies, waits for them, and re-layouts: 8.49 us -> 8.5 us
  transfers between devices with their start and end apart: 23 -> 23, of which waited for: 14 -> 12; matrix products, arithmetic and copies ran while one was open for 8% -> 5% of each run, Pallas kernels for 5% -> 5%
where the time goes in v9:
time: 132 us
  starting transfers between devices  62.2 us (47%)
  waiting for transfers between devices  41.8 us (32%)
  Pallas kernels  12.1 us (9%)
  local copies, waits for them, and re-layouts  9.9 us (8%)
  other arithmetic  4.33 us (3%)
    ppermute x21, starting transfers between devices, shifted(): lax.ppermute(pieces[k], axis, [(i, (i + k) % size) for i in range(size)])  32.5 us
    all_to_all x2, starting transfers between devices, exchange(): return lax.all_to_all(x, axis, 0, 0, tiled=True)  29.7 us
    all_to_all x2, waiting for transfers between devices, exchange(): return lax.all_to_all(x, axis, 0, 0, tiled=True)  29 us
    ppermute x21, waiting for transfers between devices, shifted(): lax.ppermute(pieces[k], axis, [(i, (i + k) % size) for i in range(size)])  12.9 us
    unnamed x27, local copies, waits for them, and re-layouts  8.5 us
    pallas_call x1, Pallas kernels, mixer(): pl.pallas_call(kernel, in_specs=[pl.BlockSpec(memory_space=pltpu.SMEM)] +...  3.3 us
    pallas_call x2, Pallas kernels, expert(): pl.pallas_call(kernel, in_specs=[pl.BlockSpec(memory_space=pltpu.SMEM)] +...  3.17 us
    pallas_call x1, Pallas kernels, fetch(): pl.pallas_call(kernel, in_specs=[pl.BlockSpec(memory_space=pltpu.HBM)] *...  2.86 us
  transfers between devices with their start and end apart: 23, of which 12 were waited for; matrix products, arithmetic and copies ran while one was open for 5% of the time, Pallas kernels for 5%

profile of v9, /device:TPU:40, one launch (start us, length us, event | category | flops | bytes accessed | tf_op | source)
XLA Modules:
  0.0 131.8 jit_solution(12132476214314114412)
XLA Ops:
  0.7 3.3 %mixer.1 = (f32[64,512]{1,0:T(8,128)S(1)}, bf16[64,512]{1,0:T(8,128)(2,1)S(1)}, bf16[64,512]{1,0:T(8,128)(2,1)S(1)}, bf16[64,512]{1,0:T(8,128)(2,1)S(1)}, f32[64,24,128]{2,1,0:T(8,128)S(1)}) custom-call(s32[1]{0:T(128)} %bitcast.here_ref, f32[24,64]{1,0:T(8,128)} %refs_0_.2, f32[24,64]{1,0:T(8,128)} %refs_1_.2, f32[1,24]{1,0:T(1,128)} %bitcast.33, ...), custom_call_target="tpu_custom_call" | custom-call | tf_op jit(solution)/shard_map/mixer/pallas_call | solution.py:215
  4.0 1.7 %collective-permute-start = (bf16[64,512]{1,0:T(8,128)(2,1)S(1)}, bf16[64,512]{1,0:T(8,128)(2,1)S(1)}, u32[]{:S(2)}, u32[]{:S(2)}) collective-permute-start(bf16[64,512]{1,0:T(8,128)(2,1)S(1)} %get-tuple-element.26), channel_id=1, source_target_pairs={{0,1},{1,2},{2,3},{3,0},{4,5},{5,6},{6,7},{7,4},{8,9},{9,10},{10,1... | collective-permute-start | bytes 196616 | tf_op jit(solution)/shard_map/ppermute | solution.py:19
  5.7 3.0 %collective-permute-start.1 = (bf16[64,512]{1,0:T(8,128)(2,1)S(1)}, bf16[64,512]{1,0:T(8,128)(2,1)S(1)}, u32[]{:S(2)}, u32[]{:S(2)}) collective-permute-start(bf16[64,512]{1,0:T(8,128)(2,1)S(1)} %get-tuple-element.27), channel_id=1, source_target_pairs={{0,2},{1,3},{2,0},{3,1},{4,6},{5,7},{6,4},{7,5},{8,10},{9,11},{10,... | collective-permute-start | bytes 196616 | tf_op jit(solution)/shard_map/ppermute | solution.py:19
  8.7 1.3 collective-permute-start.2
  10.4 1.6 %collective-permute-done.1.refs_1_ = bf16[64,512]{1,0:T(8,128)(2,1)S(1)} collective-permute-done((bf16[64,512]{1,0:T(8,128)(2,1)S(1)}, bf16[64,512]{1,0:T(8,128)(2,1)S(1)}, u32[]{:S(2)}, u32[]{:S(2)}) %collective-permute-start.1) | collective-permute-done | bytes 65568 | tf_op jit(solution)/shard_map/ppermute | solution.py:19
  12.0 1.0 collective-permute-done.2.refs_2_
  13.0 0.9 place_rows.1
  13.9 24.8 %all-to-all-start = ((bf16[32,8,512]{2,1,0:T(8,128)(2,1)}), bf16[32,8,512]{2,1,0:T(8,128)(2,1)S(1)}, u32[]{:S(2)}, u32[]{:S(2)}) async-start(bf16[32,8,512]{2,1,0:T(8,128)(2,1)} %bitcast.10), calls=%async_computation | async-start | bytes 524288 | tf_op jit(solution)/shard_map/all_to_all | solution.py:13
  39.0 2.6 %collective-permute-start.5 = (bf16[64,512]{1,0:T(8,128)(2,1)S(1)}, bf16[64,512]{1,0:T(8,128)(2,1)}, u32[]{:S(2)}, u32[]{:S(2)}) collective-permute-start(bf16[64,512]{1,0:T(8,128)(2,1)S(1)} %get-tuple-element.29), channel_id=1, source_target_pairs={{0,3},{1,0},{2,1},{3,2},{4,7},{5,4},{6,5},{7,6},{8,11},{9,8},{10,9... | collective-permute-start | bytes 196616 | tf_op jit(solution)/shard_map/ppermute | solution.py:19
  41.7 1.0 collective-permute-start.3
  43.2 0.6 gather_fusion.1
  43.8 2.9 %fetch.1 = (bf16[2048,256]{1,0:T(8,128)(2,1)S(1)}, bf16[2048,256]{1,0:T(8,128)(2,1)S(1)}, bf16[256,2048]{1,0:T(8,128)(2,1)S(1)}, bf16[2048,256]{1,0:T(8,128)(2,1...) custom-call(bf16[2,2048,256]{2,1,0:T(8,128)(2,1)} %refs_0_.3, bf16[2,2048,256]{2,1,0:T(8,128)(2,1)} %refs_1_.3, ...), custom_call_target="tpu_custom_call" | custom-call | tf_op jit(solution)/shard_map/fetch/pallas_call | solution.py:297
  46.7 1.0 copy-done
  47.7 1.0 copy-done.2
  48.7 1.0 copy-done.4
  49.6 1.0 copy-done.6
  50.6 1.0 convert_reduce_fusion
  51.7 9.0 %all-to-all-done = bf16[32,8,512]{2,1,0:T(8,128)(2,1)S(1)} async-done(((bf16[32,8,512]{2,1,0:T(8,128)(2,1)}), bf16[32,8,512]{2,1,0:T(8,128)(2,1)S(1)}, u32[]{:S(2)}, u32[]{:S(2)}) %all-to-all-start) | async-done | bytes 262176 | tf_op jit(solution)/shard_map/all_to_all | solution.py:13
  61.2 3.7 %collective-permute-start.7 = (bf16[128,512]{1,0:T(8,128)(2,1)S(1)}, bf16[128,512]{1,0:T(8,128)(2,1)S(1)}, u32[]{:S(2)}, u32[]{:S(2)}) collective-permute-start(bf16[128,512]{1,0:T(8,128)(2,1)S(1)} %get-tuple-element.31.refs_0_), channel_id=1, source_target_pairs={{0,2},{1,3},{2,0},{3,1},{4,6},{5,7},{6,4},{7,5},{8,10},{9,11},{10,... | collective-permute-start | bytes 393224 | tf_op jit(solution)/shard_map/ppermute | solution.py:19
  65.0 1.9 %collective-permute-start.12 = (bf16[128,512]{1,0:T(8,128)(2,1)S(1)}, bf16[128,512]{1,0:T(8,128)(2,1)S(1)}, u32[]{:S(2)}, u32[]{:S(2)}) collective-permute-start(bf16[128,512]{1,0:T(8,128)(2,1)S(1)} %get-tuple-element.39.refs_0_), channel_id=1, source_target_pairs={{0,1},{1,2},{2,3},{3,0},{4,5},{5,6},{6,7},{7,4},{8,9},{9,10},{10,1... | collective-permute-start | bytes 393224 | tf_op jit(solution)/shard_map/ppermute | solution.py:19
  67.0 0.7 collective-permute-done.6.refs_1_
  67.7 2.0 %collective-permute-start.14 = (bf16[128,512]{1,0:T(8,128)(2,1)S(1)}, bf16[128,512]{1,0:T(8,128)(2,1)S(1)}, u32[]{:S(2)}, u32[]{:S(2)}) collective-permute-start(bf16[128,512]{1,0:T(8,128)(2,1)S(1)} %get-tuple-element.39.refs_0_), channel_id=1, source_target_pairs={{0,3},{1,0},{2,1},{3,2},{4,7},{5,4},{6,5},{7,6},{8,11},{9,8},{10,9... | collective-permute-start | bytes 393224 | tf_op jit(solution)/shard_map/ppermute | solution.py:19
  69.7 2.2 %collective-permute-done.7.refs_2_ = bf16[128,512]{1,0:T(8,128)(2,1)S(1)} collective-permute-done((bf16[128,512]{1,0:T(8,128)(2,1)S(1)}, bf16[128,512]{1,0:T(8,128)(2,1)S(1)}, u32[]{:S(2)}, u32[]{:S(2)}) %collective-permute-start.7) | collective-permute-done | bytes 131104 | tf_op jit(solution)/shard_map/ppermute | solution.py:19
  72.0 1.2 copy-done.3
  73.2 1.2 copy-done.5
  74.4 1.2 copy-done.7
  75.7 1.6 %expert.2 = (bf16[128,512]{1,0:T(8,128)(2,1)S(1)}, bf16[128,512]{1,0:T(8,128)(2,1)S(1)}, bf16[128,512]{1,0:T(8,128)(2,1)S(1)}, bf16[128,512]{1,0:T(8,128)(2,1)S(1)}) custom-call(s32[1]{0:T(128)} %bitcast.here_ref, bf16[128,512]{1,0:T(8,128)(2,1)S(1)} %get-tuple-element.31.refs_0_, bf16[128,512]{1,0:T(8,128)(2,1)S(1)} %collective-permute-done.6.refs_1_, ...), custom_call_target="tpu_custom_call" | custom-call | tf_op jit(solution)/shard_map/expert/pallas_call | solution.py:407
  77.3 2.2 %collective-permute-start.9 = (bf16[128,512]{1,0:T(8,128)(2,1)S(1)}, bf16[128,512]{1,0:T(8,128)(2,1)S(1)}, u32[]{:S(2)}, u32[]{:S(2)}) collective-permute-start(bf16[128,512]{1,0:T(8,128)(2,1)S(1)} %get-tuple-element.36), channel_id=1, source_target_pairs={{0,1},{1,2},{2,3},{3,0},{4,5},{5,6},{6,7},{7,4},{8,9},{9,10},{10,1... | collective-permute-start | bytes 393224 | tf_op jit(solution)/shard_map/ppermute | solution.py:19
  79.5 1.1 fusion.2
  80.7 2.9 %collective-permute-start.10 = (bf16[128,512]{1,0:T(8,128)(2,1)S(1)}, bf16[128,512]{1,0:T(8,128)(2,1)S(1)}, u32[]{:S(2)}, u32[]{:S(2)}) collective-permute-start(bf16[128,512]{1,0:T(8,128)(2,1)S(1)} %get-tuple-element.37), channel_id=1, source_target_pairs={{0,2},{1,3},{2,0},{3,1},{4,6},{5,7},{6,4},{7,5},{8,10},{9,11},{10,... | collective-permute-start | bytes 393224 | tf_op jit(solution)/shard_map/ppermute | solution.py:19
  83.5 1.6 %expert.3 = (bf16[128,512]{1,0:T(8,128)(2,1)S(1)}, bf16[128,512]{1,0:T(8,128)(2,1)S(1)}, bf16[128,512]{1,0:T(8,128)(2,1)S(1)}, bf16[128,512]{1,0:T(8,128)(2,1)S(1)}) custom-call(s32[1]{0:T(128)} %bitcast.here_ref, bf16[128,512]{1,0:T(8,128)(2,1)S(1)} %get-tuple-element.39.refs_0_, bf16[128,512]{1,0:T(8,128)(2,1)S(1)} %collective-permute-done.12.refs_1_, ...), custom_call_target="tpu_custom_call" | custom-call | tf_op jit(solution)/shard_map/expert/pallas_call | solution.py:407
  85.1 2.1 %collective-permute-start.15 = (bf16[128,512]{1,0:T(8,128)(2,1)S(1)}, bf16[128,512]{1,0:T(8,128)(2,1)S(1)}, u32[]{:S(2)}, u32[]{:S(2)}) collective-permute-start(bf16[128,512]{1,0:T(8,128)(2,1)S(1)} %get-tuple-element.44), channel_id=1, source_target_pairs={{0,1},{1,2},{2,3},{3,0},{4,5},{5,6},{6,7},{7,4},{8,9},{9,10},{10,1... | collective-permute-start | bytes 393224 | tf_op jit(solution)/shard_map/ppermute | solution.py:19
  87.3 0.8 collective-permute-start.16
  88.1 2.0 %collective-permute-start.17 = (bf16[128,512]{1,0:T(8,128)(2,1)S(1)}, bf16[128,512]{1,0:T(8,128)(2,1)S(1)}, u32[]{:S(2)}, u32[]{:S(2)}) collective-permute-start(bf16[128,512]{1,0:T(8,128)(2,1)S(1)} %get-tuple-element.46), channel_id=1, source_target_pairs={{0,3},{1,0},{2,1},{3,2},{4,7},{5,4},{6,5},{7,6},{8,11},{9,8},{10,9... | collective-permute-start | bytes 393224 | tf_op jit(solution)/shard_map/ppermute | solution.py:19
  90.1 2.2 %collective-permute-done.15.refs_5_ = bf16[128,512]{1,0:T(8,128)(2,1)S(1)} collective-permute-done((bf16[128,512]{1,0:T(8,128)(2,1)S(1)}, bf16[128,512]{1,0:T(8,128)(2,1)S(1)}, u32[]{:S(2)}, u32[]{:S(2)}) %collective-permute-start.15) | collective-permute-done | bytes 131104 | tf_op jit(solution)/shard_map/ppermute | solution.py:19
  92.3 1.4 %collective-permute-done.16.refs_6_ = bf16[128,512]{1,0:T(8,128)(2,1)S(1)} collective-permute-done((bf16[128,512]{1,0:T(8,128)(2,1)S(1)}, bf16[128,512]{1,0:T(8,128)(2,1)S(1)}, u32[]{:S(2)}, u32[]{:S(2)}) %collective-permute-start.16) | collective-permute-done | bytes 131104 | tf_op jit(solution)/shard_map/ppermute | solution.py:19
  93.7 0.6 collective-permute-done.17.refs_7_
  94.3 0.9 add_up.1
  95.2 4.9 %all-to-all-start.1 = ((bf16[32,8,512]{2,1,0:T(8,128)(2,1)}), bf16[32,8,512]{2,1,0:T(8,128)(2,1)S(1)}, u32[]{:S(2)}, u32[]{:S(2)}) async-start(bf16[32,8,512]{2,1,0:T(8,128)(2,1)} %bitcast.13), calls=%async_computation.1 | async-start | bytes 524288 | tf_op jit(solution)/shard_map/all_to_all | solution.py:13
  100.1 1.0 fusion.3.hidden_ref
  102.1 19.9 %all-to-all-done.1 = bf16[32,8,512]{2,1,0:T(8,128)(2,1)S(1)} async-done(((bf16[32,8,512]{2,1,0:T(8,128)(2,1)}), bf16[32,8,512]{2,1,0:T(8,128)(2,1)S(1)}, u32[]{:S(2)}, u32[]{:S(2)}) %all-to-all-start.1) | async-done | bytes 262176 | tf_op jit(solution)/shard_map/all_to_all | solution.py:13
  122.2 1.2 collective-permute-start.18
  123.5 3.0 %collective-permute-start.19 = (bf16[64,512]{1,0:T(8,128)(2,1)S(1)}, bf16[64,512]{1,0:T(8,128)(2,1)S(1)}, u32[]{:S(2)}, u32[]{:S(2)}) collective-permute-start(bf16[64,512]{1,0:T(8,128)(2,1)S(1)} %convolution_convert_fusion.refs_0_), channel_id=1, source_target_pairs={{0,2},{1,3},{2,0},{3,1},{4,6},{5,7},{6,4},{7,5},{8,10},{9,11},{10,... | collective-permute-start | bytes 196616 | tf_op jit(solution)/shard_map/ppermute | solution.py:19
  126.7 0.9 copy.28
  127.6 0.9 collective-permute-done.18.refs_1_
  128.5 0.9 collective-permute-done.19.refs_2_
  129.4 1.3 %collective-permute-done.20.refs_3_ = bf16[64,512]{1,0:T(8,128)(2,1)S(1)} collective-permute-done((bf16[64,512]{1,0:T(8,128)(2,1)S(1)}, bf16[64,512]{1,0:T(8,128)(2,1)S(1)}, u32[]{:S(2)}, u32[]{:S(2)}) %collective-permute-start.20) | collective-permute-done | bytes 65568 | tf_op jit(solution)/shard_map/ppermute | solution.py:19
  130.7 0.9 finish.1
  (61 shorter events, 3.5 us)
Async XLA Ops:
  0.6 9.4 %copy-start.12 = (s32[64,2]{0,1:T(2,128)S(1)}, s32[64,2]{0,1:T(2,128)}, u32[]{:S(2)}) copy-start(s32[64,2]{0,1:T(2,128)} %param.20) | copy-start | bytes 1540
  0.6 38.0 %copy-start.8 = (f32[2048]{0:T(1024)S(1)}, f32[2048]{0:T(1024)}, u32[]{:S(2)}) copy-start(f32[2048]{0:T(1024)} %param.29) | copy-start | bytes 24580
  0.7 38.0 %copy-start.10 = (bf16[2048,64]{0,1:T(8,128)(2,1)S(1)}, bf16[2048,64]{0,1:T(8,128)(2,1)}, u32[]{:S(2)}) copy-start(bf16[2048,64]{0,1:T(8,128)(2,1)} %param.31) | copy-start | bytes 786436
  0.7 38.0 %copy-start.11 = (bf16[2048,4]{0,1:T(4,128)(2,1)S(1)}, bf16[2048,4]{0,1:T(4,128)(2,1)}, u32[]{:S(2)}) copy-start(bf16[2048,4]{0,1:T(4,128)(2,1)} %param.30) | copy-start | bytes 49156
  4.0 6.4 %collective-permute-start = (bf16[64,512]{1,0:T(8,128)(2,1)S(1)}, bf16[64,512]{1,0:T(8,128)(2,1)S(1)}, u32[]{:S(2)}, u32[]{:S(2)}) collective-permute-start(bf16[64,512]{1,0:T(8,128)(2,1)S(1)} %get-tuple-element.26), channel_id=1, source_target_pairs={{0,1},{1,2},{2,3},{3,0},{4,5},{5,6},{6,7},{7,4},{8,9},{9,10},{10,1... | collective-permute-start | bytes 196616 | tf_op jit(solution)/shard_map/ppermute | solution.py:19
  5.7 6.3 %collective-permute-start.1 = (bf16[64,512]{1,0:T(8,128)(2,1)S(1)}, bf16[64,512]{1,0:T(8,128)(2,1)S(1)}, u32[]{:S(2)}, u32[]{:S(2)}) collective-permute-start(bf16[64,512]{1,0:T(8,128)(2,1)S(1)} %get-tuple-element.27), channel_id=1, source_target_pairs={{0,2},{1,3},{2,0},{3,1},{4,6},{5,7},{6,4},{7,5},{8,10},{9,11},{10,... | collective-permute-start | bytes 196616 | tf_op jit(solution)/shard_map/ppermute | solution.py:19
  8.7 4.3 %collective-permute-start.2 = (bf16[64,512]{1,0:T(8,128)(2,1)S(1)}, bf16[64,512]{1,0:T(8,128)(2,1)S(1)}, u32[]{:S(2)}, u32[]{:S(2)}) collective-permute-start(bf16[64,512]{1,0:T(8,128)(2,1)S(1)} %get-tuple-element.28), channel_id=1, source_target_pairs={{0,3},{1,0},{2,1},{3,2},{4,7},{5,4},{6,5},{7,6},{8,11},{9,8},{10,9... | collective-permute-start | bytes 196616 | tf_op jit(solution)/shard_map/ppermute | solution.py:19
  13.9 46.8 %all-to-all-start = ((bf16[32,8,512]{2,1,0:T(8,128)(2,1)}), bf16[32,8,512]{2,1,0:T(8,128)(2,1)S(1)}, u32[]{:S(2)}, u32[]{:S(2)}) async-start(bf16[32,8,512]{2,1,0:T(8,128)(2,1)} %bitcast.10), calls=%async_computation | async-start | bytes 524288 | tf_op jit(solution)/shard_map/all_to_all | solution.py:13
  39.0 11.6 %collective-permute-start.5 = (bf16[64,512]{1,0:T(8,128)(2,1)S(1)}, bf16[64,512]{1,0:T(8,128)(2,1)}, u32[]{:S(2)}, u32[]{:S(2)}) collective-permute-start(bf16[64,512]{1,0:T(8,128)(2,1)S(1)} %get-tuple-element.29), channel_id=1, source_target_pairs={{0,3},{1,0},{2,1},{3,2},{4,7},{5,4},{6,5},{7,6},{8,11},{9,8},{10,9... | collective-permute-start | bytes 196616 | tf_op jit(solution)/shard_map/ppermute | solution.py:19
  41.7 9.0 %collective-permute-start.4 = (bf16[64,512]{1,0:T(8,128)(2,1)S(1)}, bf16[64,512]{1,0:T(8,128)(2,1)}, u32[]{:S(2)}, u32[]{:S(2)}) collective-permute-start(bf16[64,512]{1,0:T(8,128)(2,1)S(1)} %get-tuple-element.29), channel_id=1, source_target_pairs={{0,2},{1,3},{2,0},{3,1},{4,6},{5,7},{6,4},{7,5},{8,10},{9,11},{10,... | collective-permute-start | bytes 196616 | tf_op jit(solution)/shard_map/ppermute | solution.py:19
  41.7 9.0 %collective-permute-start.3 = (bf16[64,512]{1,0:T(8,128)(2,1)S(1)}, bf16[64,512]{1,0:T(8,128)(2,1)}, u32[]{:S(2)}, u32[]{:S(2)}) collective-permute-start(bf16[64,512]{1,0:T(8,128)(2,1)S(1)} %get-tuple-element.29), channel_id=1, source_target_pairs={{0,1},{1,2},{2,3},{3,0},{4,5},{5,6},{6,7},{7,4},{8,9},{9,10},{10,1... | collective-permute-start | bytes 196616 | tf_op jit(solution)/shard_map/ppermute | solution.py:19
  46.7 1.0 copy-start
  47.7 1.0 copy-start.2
  48.7 1.0 copy-start.4
  49.6 1.0 copy-start.6
  60.7 22.9 %copy-start.1 = (bf16[256,2048]{1,0:T(8,128)(2,1)S(1)}, bf16[256,2048]{1,0:T(8,128)(2,1)}, u32[]{:S(2)}) copy-start(bf16[256,2048]{1,0:T(8,128)(2,1)} %copy-done) | copy-start | bytes 3145732
  60.8 7.0 %collective-permute-start.6 = (bf16[128,512]{1,0:T(8,128)(2,1)S(1)}, bf16[128,512]{1,0:T(8,128)(2,1)S(1)}, u32[]{:S(2)}, u32[]{:S(2)}) collective-permute-start(bf16[128,512]{1,0:T(8,128)(2,1)S(1)} %get-tuple-element.31.refs_0_), channel_id=1, source_target_pairs={{0,1},{1,2},{2,3},{3,0},{4,5},{5,6},{6,7},{7,4},{8,9},{9,10},{10,1... | collective-permute-start | bytes 393224 | tf_op jit(solution)/shard_map/ppermute | solution.py:19
  61.2 10.8 %collective-permute-start.7 = (bf16[128,512]{1,0:T(8,128)(2,1)S(1)}, bf16[128,512]{1,0:T(8,128)(2,1)S(1)}, u32[]{:S(2)}, u32[]{:S(2)}) collective-permute-start(bf16[128,512]{1,0:T(8,128)(2,1)S(1)} %get-tuple-element.31.refs_0_), channel_id=1, source_target_pairs={{0,2},{1,3},{2,0},{3,1},{4,6},{5,7},{6,4},{7,5},{8,10},{9,11},{10,... | collective-permute-start | bytes 393224 | tf_op jit(solution)/shard_map/ppermute | solution.py:19
  64.8 7.2 %collective-permute-start.8 = (bf16[128,512]{1,0:T(8,128)(2,1)S(1)}, bf16[128,512]{1,0:T(8,128)(2,1)S(1)}, u32[]{:S(2)}, u32[]{:S(2)}) collective-permute-start(bf16[128,512]{1,0:T(8,128)(2,1)S(1)} %get-tuple-element.31.refs_0_), channel_id=1, source_target_pairs={{0,3},{1,0},{2,1},{3,2},{4,7},{5,4},{6,5},{7,6},{8,11},{9,8},{10,9... | collective-permute-start | bytes 393224 | tf_op jit(solution)/shard_map/ppermute | solution.py:19
  65.0 18.5 %collective-permute-start.12 = (bf16[128,512]{1,0:T(8,128)(2,1)S(1)}, bf16[128,512]{1,0:T(8,128)(2,1)S(1)}, u32[]{:S(2)}, u32[]{:S(2)}) collective-permute-start(bf16[128,512]{1,0:T(8,128)(2,1)S(1)} %get-tuple-element.39.refs_0_), channel_id=1, source_target_pairs={{0,1},{1,2},{2,3},{3,0},{4,5},{5,6},{6,7},{7,4},{8,9},{9,10},{10,1... | collective-permute-start | bytes 393224 | tf_op jit(solution)/shard_map/ppermute | solution.py:19
  66.9 16.6 %collective-permute-start.13 = (bf16[128,512]{1,0:T(8,128)(2,1)S(1)}, bf16[128,512]{1,0:T(8,128)(2,1)S(1)}, u32[]{:S(2)}, u32[]{:S(2)}) collective-permute-start(bf16[128,512]{1,0:T(8,128)(2,1)S(1)} %get-tuple-element.39.refs_0_), channel_id=1, source_target_pairs={{0,2},{1,3},{2,0},{3,1},{4,6},{5,7},{6,4},{7,5},{8,10},{9,11},{10,... | collective-permute-start | bytes 393224 | tf_op jit(solution)/shard_map/ppermute | solution.py:19
  67.7 15.8 %collective-permute-start.14 = (bf16[128,512]{1,0:T(8,128)(2,1)S(1)}, bf16[128,512]{1,0:T(8,128)(2,1)S(1)}, u32[]{:S(2)}, u32[]{:S(2)}) collective-permute-start(bf16[128,512]{1,0:T(8,128)(2,1)S(1)} %get-tuple-element.39.refs_0_), channel_id=1, source_target_pairs={{0,3},{1,0},{2,1},{3,2},{4,7},{5,4},{6,5},{7,6},{8,11},{9,8},{10,9... | collective-permute-start | bytes 393224 | tf_op jit(solution)/shard_map/ppermute | solution.py:19
  72.0 1.2 copy-start.3
  73.2 1.2 copy-start.5
  74.4 1.2 copy-start.7
  77.3 10.8 %collective-permute-start.9 = (bf16[128,512]{1,0:T(8,128)(2,1)S(1)}, bf16[128,512]{1,0:T(8,128)(2,1)S(1)}, u32[]{:S(2)}, u32[]{:S(2)}) collective-permute-start(bf16[128,512]{1,0:T(8,128)(2,1)S(1)} %get-tuple-element.36), channel_id=1, source_target_pairs={{0,1},{1,2},{2,3},{3,0},{4,5},{5,6},{6,7},{7,4},{8,9},{9,10},{10,1... | collective-permute-start | bytes 393224 | tf_op jit(solution)/shard_map/ppermute | solution.py:19
  80.7 9.4 %collective-permute-start.10 = (bf16[128,512]{1,0:T(8,128)(2,1)S(1)}, bf16[128,512]{1,0:T(8,128)(2,1)S(1)}, u32[]{:S(2)}, u32[]{:S(2)}) collective-permute-start(bf16[128,512]{1,0:T(8,128)(2,1)S(1)} %get-tuple-element.37), channel_id=1, source_target_pairs={{0,2},{1,3},{2,0},{3,1},{4,6},{5,7},{6,4},{7,5},{8,10},{9,11},{10,... | collective-permute-start | bytes 393224 | tf_op jit(solution)/shard_map/ppermute | solution.py:19
  83.5 6.6 %collective-permute-start.11 = (bf16[128,512]{1,0:T(8,128)(2,1)S(1)}, bf16[128,512]{1,0:T(8,128)(2,1)S(1)}, u32[]{:S(2)}, u32[]{:S(2)}) collective-permute-start(bf16[128,512]{1,0:T(8,128)(2,1)S(1)} %get-tuple-element.38), channel_id=1, source_target_pairs={{0,3},{1,0},{2,1},{3,2},{4,7},{5,4},{6,5},{7,6},{8,11},{9,8},{10,9... | collective-permute-start | bytes 393224 | tf_op jit(solution)/shard_map/ppermute | solution.py:19
  85.1 7.2 %collective-permute-start.15 = (bf16[128,512]{1,0:T(8,128)(2,1)S(1)}, bf16[128,512]{1,0:T(8,128)(2,1)S(1)}, u32[]{:S(2)}, u32[]{:S(2)}) collective-permute-start(bf16[128,512]{1,0:T(8,128)(2,1)S(1)} %get-tuple-element.44), channel_id=1, source_target_pairs={{0,1},{1,2},{2,3},{3,0},{4,5},{5,6},{6,7},{7,4},{8,9},{9,10},{10,1... | collective-permute-start | bytes 393224 | tf_op jit(solution)/shard_map/ppermute | solution.py:19
  87.3 6.5 %collective-permute-start.16 = (bf16[128,512]{1,0:T(8,128)(2,1)S(1)}, bf16[128,512]{1,0:T(8,128)(2,1)S(1)}, u32[]{:S(2)}, u32[]{:S(2)}) collective-permute-start(bf16[128,512]{1,0:T(8,128)(2,1)S(1)} %get-tuple-element.45), channel_id=1, source_target_pairs={{0,2},{1,3},{2,0},{3,1},{4,6},{5,7},{6,4},{7,5},{8,10},{9,11},{10,... | collective-permute-start | bytes 393224 | tf_op jit(solution)/shard_map/ppermute | solution.py:19
  88.1 6.2 %collective-permute-start.17 = (bf16[128,512]{1,0:T(8,128)(2,1)S(1)}, bf16[128,512]{1,0:T(8,128)(2,1)S(1)}, u32[]{:S(2)}, u32[]{:S(2)}) collective-permute-start(bf16[128,512]{1,0:T(8,128)(2,1)S(1)} %get-tuple-element.46), channel_id=1, source_target_pairs={{0,3},{1,0},{2,1},{3,2},{4,7},{5,4},{6,5},{7,6},{8,11},{9,8},{10,9... | collective-permute-start | bytes 393224 | tf_op jit(solution)/shard_map/ppermute | solution.py:19
  95.2 35.6 %copy-start.9 = (f32[2048]{0:T(1024)S(1)}, f32[2048]{0:T(1024)}, u32[]{:S(2)}) copy-start(f32[2048]{0:T(1024)} %param.35) | copy-start | bytes 24580
  95.2 26.9 %all-to-all-start.1 = ((bf16[32,8,512]{2,1,0:T(8,128)(2,1)}), bf16[32,8,512]{2,1,0:T(8,128)(2,1)S(1)}, u32[]{:S(2)}, u32[]{:S(2)}) async-start(bf16[32,8,512]{2,1,0:T(8,128)(2,1)} %bitcast.13), calls=%async_computation.1 | async-start | bytes 524288 | tf_op jit(solution)/shard_map/all_to_all | solution.py:13
  122.2 6.3 %collective-permute-start.18 = (bf16[64,512]{1,0:T(8,128)(2,1)S(1)}, bf16[64,512]{1,0:T(8,128)(2,1)S(1)}, u32[]{:S(2)}, u32[]{:S(2)}) collective-permute-start(bf16[64,512]{1,0:T(8,128)(2,1)S(1)} %convolution_convert_fusion.refs_0_), channel_id=1, source_target_pairs={{0,1},{1,2},{2,3},{3,0},{4,5},{5,6},{6,7},{7,4},{8,9},{9,10},{10,1... | collective-permute-start | bytes 196616 | tf_op jit(solution)/shard_map/ppermute | solution.py:19
  123.5 5.9 %collective-permute-start.19 = (bf16[64,512]{1,0:T(8,128)(2,1)S(1)}, bf16[64,512]{1,0:T(8,128)(2,1)S(1)}, u32[]{:S(2)}, u32[]{:S(2)}) collective-permute-start(bf16[64,512]{1,0:T(8,128)(2,1)S(1)} %convolution_convert_fusion.refs_0_), channel_id=1, source_target_pairs={{0,2},{1,3},{2,0},{3,1},{4,6},{5,7},{6,4},{7,5},{8,10},{9,11},{10,... | collective-permute-start | bytes 196616 | tf_op jit(solution)/shard_map/ppermute | solution.py:19
  126.5 4.3 %collective-permute-start.20 = (bf16[64,512]{1,0:T(8,128)(2,1)S(1)}, bf16[64,512]{1,0:T(8,128)(2,1)S(1)}, u32[]{:S(2)}, u32[]{:S(2)}) collective-permute-start(bf16[64,512]{1,0:T(8,128)(2,1)S(1)} %convolution_convert_fusion.refs_0_), channel_id=1, source_target_pairs={{0,3},{1,0},{2,1},{3,2},{4,7},{5,4},{6,5},{7,6},{8,11},{9,8},{10,9... | collective-permute-start | bytes 196616 | tf_op jit(solution)/shard_map/ppermute | solution.py:19

commit v10 on v9

--- a/solution.py
+++ b/solution.py
@@ -277,11 +277,12 @@
     )(base, target.T, *arrived)
 
 
-def fetch(*weights):
+def fetch(new_state, *weights):
     count = len(weights)
     local_experts = weights[0].shape[0]
 
-    def kernel(*refs):
+    def kernel(new_ref, *refs):
+        new_far, refs = refs[count], refs[:count] + refs[count + 1 :]
         copies = [
             pltpu.make_async_copy(
                 refs[i].at[j], refs[count + j * count + i], refs[-1].at[j * count + i]
@@ -289,6 +290,9 @@
             for j in range(local_experts)
             for i in range(count)
         ]
+        copies.append(
+            pltpu.make_async_copy(new_ref, new_far, refs[-1].at[count * local_experts])
+        )
         for copy in copies:
             copy.start()
         for copy in copies:
@@ -296,14 +300,18 @@
 
     out = pl.pallas_call(
         kernel,
-        in_specs=[pl.BlockSpec(memory_space=pltpu.HBM)] * count,
-        out_specs=[pl.BlockSpec(memory_space=pltpu.VMEM)] * (count * local_experts),
-        out_shape=[pltpu.VMEM(w.shape[1:], w.dtype) for w in weights] * local_experts,
-        scratch_shapes=[pltpu.SemaphoreType.DMA((count * local_experts,))],
-        compiler_params=pltpu.CompilerParams(vmem_limit_bytes=1024 * 1024),
+        in_specs=[pl.BlockSpec(memory_space=pltpu.VMEM)]
+        + [pl.BlockSpec(memory_space=pltpu.HBM)] * count,
+        out_specs=[pl.BlockSpec(memory_space=pltpu.HBM)]
+        + [pl.BlockSpec(memory_space=pltpu.VMEM)] * (count * local_experts),
+        out_shape=[jax.ShapeDtypeStruct(new_state.shape, new_state.dtype)]
+        + [pltpu.VMEM(w.shape[1:], w.dtype) for w in weights] * local_experts,
+        scratch_shapes=[pltpu.SemaphoreType.DMA((count * local_experts + 1,))],
+        compiler_params=pltpu.CompilerParams(vmem_limit_bytes=2 * 1024 * 1024),
         name="fetch",
-    )(*[pltpu.with_memory_space_constraint(w, pltpu.HBM) for w in weights])
-    return [out[j * count : (j + 1) * count] for j in range(local_experts)]
+    )(new_state, *[pltpu.with_memory_space_constraint(w, pltpu.HBM) for w in weights])
+    new_state, *out = out
+    return new_state, [out[j * count : (j + 1) * count] for j in range(local_experts)]
 
 
 def swap_halves(first, second):
@@ -534,7 +542,7 @@
     gathered = []
     for j in range(local_experts):
         gathered.append(shifted([rows[j]] * shares, "tp"))
-    weights = fetch(w_gate, w_up, w_down)
+    new_state, weights = fetch(new_state, w_gate, w_up, w_down)
     arrived = []
     for j in range(local_experts):
         outs = expert(here_array, gathered[j], gain_mix, *weights[j])

time: 132 us -> 134 us (1.015)
  waiting for transfers between devices: 41.8 us -> 38.6 us
  other arithmetic: 4.33 us -> 6.07 us
  starting transfers between devices: 62.2 us -> 63.9 us
  local copies, waits for them, and re-layouts: 9.9 us -> 11.4 us
    all_to_all x2, waiting for transfers between devices: 29 us -> 26.4 us  [exchange(): return lax.all_to_all(x, axis, 0, 0, tiled=True)]
    unnamed x27 -> x32, local copies, waits for them, and re-layouts: 8.5 us -> 8.66 us
  transfers between devices with their start and end apart: 23 -> 23, of which waited for: 12 -> 11; matrix products, arithmetic and copies ran while one was open for 5% -> 7% of each run, Pallas kernels for 5% -> 5%
where the time goes in v10:
time: 134 us
  starting transfers between devices  63.9 us (48%)
  waiting for transfers between devices  38.6 us (29%)
  Pallas kernels  12.4 us (9%)
  local copies, waits for them, and re-layouts  11.4 us (9%)
  other arithmetic  6.07 us (5%)
    ppermute x21, starting transfers between devices, shifted(): lax.ppermute(pieces[k], axis, [(i, (i + k) % size) for i in range(size)])  33 us
    all_to_all x2, starting transfers between devices, exchange(): return lax.all_to_all(x, axis, 0, 0, tiled=True)  30.9 us
    all_to_all x2, waiting for transfers between devices, exchange(): return lax.all_to_all(x, axis, 0, 0, tiled=True)  26.4 us
    ppermute x21, waiting for transfers between devices, shifted(): lax.ppermute(pieces[k], axis, [(i, (i + k) % size) for i in range(size)])  12.2 us
    unnamed x32, local copies, waits for them, and re-layouts  8.66 us
    pallas_call x1, Pallas kernels, mixer(): pl.pallas_call(kernel, in_specs=[pl.BlockSpec(memory_space=pltpu.SMEM)] +...  3.3 us
    pallas_call x2, Pallas kernels, expert(): pl.pallas_call(kernel, in_specs=[pl.BlockSpec(memory_space=pltpu.SMEM)] +...  3.19 us
    pallas_call x1, Pallas kernels, fetch(): pl.pallas_call(kernel, in_specs=[pl.BlockSpec(memory_space=pltpu.VMEM)] +...  3.15 us
  transfers between devices with their start and end apart: 23, of which 11 were waited for; matrix products, arithmetic and copies ran while one was open for 7% of the time, Pallas kernels for 5%

profile of v10, /device:TPU:40, one launch (start us, length us, event | category | flops | bytes accessed | tf_op | source)
XLA Modules:
  0.0 133.8 jit_solution(1235964045138401571)
XLA Ops:
  0.7 3.3 %mixer.1 = (f32[64,512]{1,0:T(8,128)S(1)}, bf16[64,512]{1,0:T(8,128)(2,1)S(1)}, bf16[64,512]{1,0:T(8,128)(2,1)S(1)}, bf16[64,512]{1,0:T(8,128)(2,1)S(1)}, f32[64,24,128]{2,1,0:T(8,128)S(1)}) custom-call(s32[1]{0:T(128)} %bitcast.here_ref, f32[24,64]{1,0:T(8,128)} %refs_0_.2, f32[24,64]{1,0:T(8,128)} %refs_1_.2, f32[1,24]{1,0:T(1,128)} %bitcast.36, ...), custom_call_target="tpu_custom_call" | custom-call | tf_op jit(solution)/shard_map/mixer/pallas_call | solution.py:215
  4.0 0.9 copy-done.6
  4.9 1.6 %collective-permute-start = (bf16[64,512]{1,0:T(8,128)(2,1)S(1)}, bf16[64,512]{1,0:T(8,128)(2,1)S(1)}, u32[]{:S(2)}, u32[]{:S(2)}) collective-permute-start(bf16[64,512]{1,0:T(8,128)(2,1)S(1)} %get-tuple-element.27), channel_id=1, source_target_pairs={{0,1},{1,2},{2,3},{3,0},{4,5},{5,6},{6,7},{7,4},{8,9},{9,10},{10,1... | collective-permute-start | bytes 196616 | tf_op jit(solution)/shard_map/ppermute | solution.py:19
  6.5 3.0 %collective-permute-start.1 = (bf16[64,512]{1,0:T(8,128)(2,1)S(1)}, bf16[64,512]{1,0:T(8,128)(2,1)S(1)}, u32[]{:S(2)}, u32[]{:S(2)}) collective-permute-start(bf16[64,512]{1,0:T(8,128)(2,1)S(1)} %get-tuple-element.28), channel_id=1, source_target_pairs={{0,2},{1,3},{2,0},{3,1},{4,6},{5,7},{6,4},{7,5},{8,10},{9,11},{10,... | collective-permute-start | bytes 196616 | tf_op jit(solution)/shard_map/ppermute | solution.py:19
  9.5 1.3 collective-permute-start.2
  11.2 1.6 %collective-permute-done.1.refs_1_ = bf16[64,512]{1,0:T(8,128)(2,1)S(1)} collective-permute-done((bf16[64,512]{1,0:T(8,128)(2,1)S(1)}, bf16[64,512]{1,0:T(8,128)(2,1)S(1)}, u32[]{:S(2)}, u32[]{:S(2)}) %collective-permute-start.1) | collective-permute-done | bytes 65568 | tf_op jit(solution)/shard_map/ppermute | solution.py:19
  12.8 1.0 collective-permute-done.2.refs_2_
  13.8 0.9 place_rows.1
  14.7 24.8 %all-to-all-start = ((bf16[32,8,512]{2,1,0:T(8,128)(2,1)}), bf16[32,8,512]{2,1,0:T(8,128)(2,1)S(1)}, u32[]{:S(2)}, u32[]{:S(2)}) async-start(bf16[32,8,512]{2,1,0:T(8,128)(2,1)} %bitcast.10), calls=%async_computation | async-start | bytes 524288 | tf_op jit(solution)/shard_map/all_to_all | solution.py:13
  40.4 2.5 %collective-permute-start.5 = (bf16[64,512]{1,0:T(8,128)(2,1)S(1)}, bf16[64,512]{1,0:T(8,128)(2,1)S(1)}, u32[]{:S(2)}, u32[]{:S(2)}) collective-permute-start(bf16[64,512]{1,0:T(8,128)(2,1)S(1)} %get-tuple-element.30), channel_id=1, source_target_pairs={{0,3},{1,0},{2,1},{3,2},{4,7},{5,4},{6,5},{7,6},{8,11},{9,8},{10,9... | collective-permute-start | bytes 196616 | tf_op jit(solution)/shard_map/ppermute | solution.py:19
  42.9 0.9 collective-permute-start.3
  43.7 1.1 gather_fusion
  44.9 1.3 gather_fusion.1
  46.2 1.1 copy-done.7
  47.3 3.1 %fetch.1 = (f32[64,24,128]{2,1,0:T(8,128)}, bf16[2048,256]{1,0:T(8,128)(2,1)S(1)}, bf16[2048,256]{1,0:T(8,128)(2,1)S(1)}, bf16[256,2048]{1,0:T(8,128)(2,1)S(1)},...) custom-call(f32[64,24,128]{2,1,0:T(8,128)S(1)} %copy-done.7, ...), custom_call_target="tpu_custom_call" | custom-call | tf_op jit(solution)/shard_map/fetch/pallas_call | solution.py:301
  50.5 1.0 copy-done
  51.5 1.0 copy-done.2
  52.5 1.0 copy-done.4
  53.4 1.6 %convert_reduce_fusion = f32[64]{0:T(128)} fusion(bf16[1,64,512]{2,1,0:T(8,128)(2,1)S(1)} %bitcast.33, bf16[1,64,512]{2,1,0:T(8,128)(2,1)} %bitcast.5, bf16[1,64,512]{2,1,0:T(8,128)(2,1)} %bitcast.4, bf16[1,64,512]{2,1,0:T(8,128)(2,1)S(1)} %bitcast.26), kind=kLoop, calls=%fused_computation.5 | loop fusion | flops 655296 | bytes 262400 | tf_op jit(solution)/shard_map/reduce_sum | solution.py:25
  55.0 6.4 %all-to-all-done = bf16[32,8,512]{2,1,0:T(8,128)(2,1)S(1)} async-done(((bf16[32,8,512]{2,1,0:T(8,128)(2,1)}), bf16[32,8,512]{2,1,0:T(8,128)(2,1)S(1)}, u32[]{:S(2)}, u32[]{:S(2)}) %all-to-all-start) | async-done | bytes 262176 | tf_op jit(solution)/shard_map/all_to_all | solution.py:13
  61.8 3.8 %collective-permute-start.7 = (bf16[128,512]{1,0:T(8,128)(2,1)S(1)}, bf16[128,512]{1,0:T(8,128)(2,1)S(1)}, u32[]{:S(2)}, u32[]{:S(2)}) collective-permute-start(bf16[128,512]{1,0:T(8,128)(2,1)S(1)} %get-tuple-element.32.refs_0_), channel_id=1, source_target_pairs={{0,2},{1,3},{2,0},{3,1},{4,6},{5,7},{6,4},{7,5},{8,10},{9,11},{10,... | collective-permute-start | bytes 393224 | tf_op jit(solution)/shard_map/ppermute | solution.py:19
  65.8 0.7 broadcast_multiply_fusion
  66.5 1.9 %collective-permute-start.12 = (bf16[128,512]{1,0:T(8,128)(2,1)S(1)}, bf16[128,512]{1,0:T(8,128)(2,1)S(1)}, u32[]{:S(2)}, u32[]{:S(2)}) collective-permute-start(bf16[128,512]{1,0:T(8,128)(2,1)S(1)} %get-tuple-element.41.refs_0_), channel_id=1, source_target_pairs={{0,1},{1,2},{2,3},{3,0},{4,5},{5,6},{6,7},{7,4},{8,9},{9,10},{10,1... | collective-permute-start | bytes 393224 | tf_op jit(solution)/shard_map/ppermute | solution.py:19
  68.5 2.6 %collective-permute-start.14 = (bf16[128,512]{1,0:T(8,128)(2,1)S(1)}, bf16[128,512]{1,0:T(8,128)(2,1)S(1)}, u32[]{:S(2)}, u32[]{:S(2)}) collective-permute-start(bf16[128,512]{1,0:T(8,128)(2,1)S(1)} %get-tuple-element.41.refs_0_), channel_id=1, source_target_pairs={{0,3},{1,0},{2,1},{3,2},{4,7},{5,4},{6,5},{7,6},{8,11},{9,8},{10,9... | collective-permute-start | bytes 393224 | tf_op jit(solution)/shard_map/ppermute | solution.py:19
  71.1 1.6 %collective-permute-done.7.refs_2_ = bf16[128,512]{1,0:T(8,128)(2,1)S(1)} collective-permute-done((bf16[128,512]{1,0:T(8,128)(2,1)S(1)}, bf16[128,512]{1,0:T(8,128)(2,1)S(1)}, u32[]{:S(2)}, u32[]{:S(2)}) %collective-permute-start.7) | collective-permute-done | bytes 131104 | tf_op jit(solution)/shard_map/ppermute | solution.py:19
  72.8 1.2 copy-done.1
  74.0 1.2 copy-done.3
  75.2 1.2 copy-done.5
  76.4 1.6 %expert.2 = (bf16[128,512]{1,0:T(8,128)(2,1)S(1)}, bf16[128,512]{1,0:T(8,128)(2,1)S(1)}, bf16[128,512]{1,0:T(8,128)(2,1)S(1)}, bf16[128,512]{1,0:T(8,128)(2,1)S(1)}) custom-call(s32[1]{0:T(128)} %bitcast.here_ref, bf16[128,512]{1,0:T(8,128)(2,1)S(1)} %get-tuple-element.32.refs_0_, bf16[128,512]{1,0:T(8,128)(2,1)S(1)} %collective-permute-done.6.refs_1_, ...), custom_call_target="tpu_custom_call" | custom-call | tf_op jit(solution)/shard_map/expert/pallas_call | solution.py:415
  78.0 2.5 %collective-permute-start.9 = (bf16[128,512]{1,0:T(8,128)(2,1)S(1)}, bf16[128,512]{1,0:T(8,128)(2,1)S(1)}, u32[]{:S(2)}, u32[]{:S(2)}) collective-permute-start(bf16[128,512]{1,0:T(8,128)(2,1)S(1)} %get-tuple-element.38), channel_id=1, source_target_pairs={{0,1},{1,2},{2,3},{3,0},{4,5},{5,6},{6,7},{7,4},{8,9},{9,10},{10,1... | collective-permute-start | bytes 393224 | tf_op jit(solution)/shard_map/ppermute | solution.py:19
  80.6 1.1 fusion.2
  81.7 2.6 %collective-permute-start.10 = (bf16[128,512]{1,0:T(8,128)(2,1)S(1)}, bf16[128,512]{1,0:T(8,128)(2,1)S(1)}, u32[]{:S(2)}, u32[]{:S(2)}) collective-permute-start(bf16[128,512]{1,0:T(8,128)(2,1)S(1)} %get-tuple-element.39), channel_id=1, source_target_pairs={{0,2},{1,3},{2,0},{3,1},{4,6},{5,7},{6,4},{7,5},{8,10},{9,11},{10,... | collective-permute-start | bytes 393224 | tf_op jit(solution)/shard_map/ppermute | solution.py:19
  84.5 1.6 %expert.3 = (bf16[128,512]{1,0:T(8,128)(2,1)S(1)}, bf16[128,512]{1,0:T(8,128)(2,1)S(1)}, bf16[128,512]{1,0:T(8,128)(2,1)S(1)}, bf16[128,512]{1,0:T(8,128)(2,1)S(1)}) custom-call(s32[1]{0:T(128)} %bitcast.here_ref, bf16[128,512]{1,0:T(8,128)(2,1)S(1)} %get-tuple-element.41.refs_0_, bf16[128,512]{1,0:T(8,128)(2,1)S(1)} %collective-permute-done.12.refs_1_, ...), custom_call_target="tpu_custom_call" | custom-call | tf_op jit(solution)/shard_map/expert/pallas_call | solution.py:415
  86.2 1.9 %collective-permute-start.15 = (bf16[128,512]{1,0:T(8,128)(2,1)S(1)}, bf16[128,512]{1,0:T(8,128)(2,1)S(1)}, u32[]{:S(2)}, u32[]{:S(2)}) collective-permute-start(bf16[128,512]{1,0:T(8,128)(2,1)S(1)} %get-tuple-element.46), channel_id=1, source_target_pairs={{0,1},{1,2},{2,3},{3,0},{4,5},{5,6},{6,7},{7,4},{8,9},{9,10},{10,1... | collective-permute-start | bytes 393224 | tf_op jit(solution)/shard_map/ppermute | solution.py:19
  88.0 1.1 collective-permute-start.16
  89.1 1.7 %collective-permute-start.17 = (bf16[128,512]{1,0:T(8,128)(2,1)S(1)}, bf16[128,512]{1,0:T(8,128)(2,1)S(1)}, u32[]{:S(2)}, u32[]{:S(2)}) collective-permute-start(bf16[128,512]{1,0:T(8,128)(2,1)S(1)} %get-tuple-element.48), channel_id=1, source_target_pairs={{0,3},{1,0},{2,1},{3,2},{4,7},{5,4},{6,5},{7,6},{8,11},{9,8},{10,9... | collective-permute-start | bytes 393224 | tf_op jit(solution)/shard_map/ppermute | solution.py:19
  90.9 2.2 %collective-permute-done.15.refs_5_ = bf16[128,512]{1,0:T(8,128)(2,1)S(1)} collective-permute-done((bf16[128,512]{1,0:T(8,128)(2,1)S(1)}, bf16[128,512]{1,0:T(8,128)(2,1)S(1)}, u32[]{:S(2)}, u32[]{:S(2)}) %collective-permute-start.15) | collective-permute-done | bytes 131104 | tf_op jit(solution)/shard_map/ppermute | solution.py:19
  93.1 1.4 %collective-permute-done.16.refs_6_ = bf16[128,512]{1,0:T(8,128)(2,1)S(1)} collective-permute-done((bf16[128,512]{1,0:T(8,128)(2,1)S(1)}, bf16[128,512]{1,0:T(8,128)(2,1)S(1)}, u32[]{:S(2)}, u32[]{:S(2)}) %collective-permute-start.16) | collective-permute-done | bytes 131104 | tf_op jit(solution)/shard_map/ppermute | solution.py:19
  95.0 0.9 add_up.1
  95.9 6.1 %all-to-all-start.1 = ((bf16[32,8,512]{2,1,0:T(8,128)(2,1)}), bf16[32,8,512]{2,1,0:T(8,128)(2,1)S(1)}, u32[]{:S(2)}, u32[]{:S(2)}) async-start(bf16[32,8,512]{2,1,0:T(8,128)(2,1)} %bitcast.13), calls=%async_computation.1 | async-start | bytes 524288 | tf_op jit(solution)/shard_map/all_to_all | solution.py:13
  102.1 1.0 fusion.3.hidden_ref
  104.0 20.0 %all-to-all-done.1 = bf16[32,8,512]{2,1,0:T(8,128)(2,1)S(1)} async-done(((bf16[32,8,512]{2,1,0:T(8,128)(2,1)}), bf16[32,8,512]{2,1,0:T(8,128)(2,1)S(1)}, u32[]{:S(2)}, u32[]{:S(2)}) %all-to-all-start.1) | async-done | bytes 262176 | tf_op jit(solution)/shard_map/all_to_all | solution.py:13
  124.2 1.5 %collective-permute-start.18 = (bf16[64,512]{1,0:T(8,128)(2,1)S(1)}, bf16[64,512]{1,0:T(8,128)(2,1)S(1)}, u32[]{:S(2)}, u32[]{:S(2)}) collective-permute-start(bf16[64,512]{1,0:T(8,128)(2,1)S(1)} %convolution_convert_fusion.refs_0_), channel_id=1, source_target_pairs={{0,1},{1,2},{2,3},{3,0},{4,5},{5,6},{6,7},{7,4},{8,9},{9,10},{10,1... | collective-permute-start | bytes 196616 | tf_op jit(solution)/shard_map/ppermute | solution.py:19
  125.7 2.8 %collective-permute-start.19 = (bf16[64,512]{1,0:T(8,128)(2,1)S(1)}, bf16[64,512]{1,0:T(8,128)(2,1)S(1)}, u32[]{:S(2)}, u32[]{:S(2)}) collective-permute-start(bf16[64,512]{1,0:T(8,128)(2,1)S(1)} %convolution_convert_fusion.refs_0_), channel_id=1, source_target_pairs={{0,2},{1,3},{2,0},{3,1},{4,6},{5,7},{6,4},{7,5},{8,10},{9,11},{10,... | collective-permute-start | bytes 196616 | tf_op jit(solution)/shard_map/ppermute | solution.py:19
  128.9 1.4 %collective-permute-done.18.refs_1_ = bf16[64,512]{1,0:T(8,128)(2,1)S(1)} collective-permute-done((bf16[64,512]{1,0:T(8,128)(2,1)S(1)}, bf16[64,512]{1,0:T(8,128)(2,1)S(1)}, u32[]{:S(2)}, u32[]{:S(2)}) %collective-permute-start.18) | collective-permute-done | bytes 65568 | tf_op jit(solution)/shard_map/ppermute | solution.py:19
  130.3 1.5 %collective-permute-done.19.refs_2_ = bf16[64,512]{1,0:T(8,128)(2,1)S(1)} collective-permute-done((bf16[64,512]{1,0:T(8,128)(2,1)S(1)}, bf16[64,512]{1,0:T(8,128)(2,1)S(1)}, u32[]{:S(2)}, u32[]{:S(2)}) %collective-permute-start.19) | collective-permute-done | bytes 65568 | tf_op jit(solution)/shard_map/ppermute | solution.py:19
  131.7 1.0 collective-permute-done.20.refs_3_
  132.7 0.9 finish.1
  (66 shorter events, 4.4 us)
Async XLA Ops:
  0.6 10.2 %copy-start.14 = (s32[64,2]{0,1:T(2,128)S(1)}, s32[64,2]{0,1:T(2,128)}, u32[]{:S(2)}) copy-start(s32[64,2]{0,1:T(2,128)} %param.20) | copy-start | bytes 1540
  0.7 38.8 %copy-start.8 = (f32[2048]{0:T(1024)S(1)}, f32[2048]{0:T(1024)}, u32[]{:S(2)}) copy-start(f32[2048]{0:T(1024)} %param.29) | copy-start | bytes 24580
  0.7 38.8 %copy-start.11 = (bf16[2048,64]{0,1:T(8,128)(2,1)S(1)}, bf16[2048,64]{0,1:T(8,128)(2,1)}, u32[]{:S(2)}) copy-start(bf16[2048,64]{0,1:T(8,128)(2,1)} %param.31) | copy-start | bytes 786436
  0.7 38.8 %copy-start.13 = (bf16[2048,4]{0,1:T(4,128)(2,1)S(1)}, bf16[2048,4]{0,1:T(4,128)(2,1)}, u32[]{:S(2)}) copy-start(bf16[2048,4]{0,1:T(4,128)(2,1)} %param.30) | copy-start | bytes 49156
  4.0 0.9 copy-start.6
  4.9 6.3 %collective-permute-start = (bf16[64,512]{1,0:T(8,128)(2,1)S(1)}, bf16[64,512]{1,0:T(8,128)(2,1)S(1)}, u32[]{:S(2)}, u32[]{:S(2)}) collective-permute-start(bf16[64,512]{1,0:T(8,128)(2,1)S(1)} %get-tuple-element.27), channel_id=1, source_target_pairs={{0,1},{1,2},{2,3},{3,0},{4,5},{5,6},{6,7},{7,4},{8,9},{9,10},{10,1... | collective-permute-start | bytes 196616 | tf_op jit(solution)/shard_map/ppermute | solution.py:19
  6.5 6.3 %collective-permute-start.1 = (bf16[64,512]{1,0:T(8,128)(2,1)S(1)}, bf16[64,512]{1,0:T(8,128)(2,1)S(1)}, u32[]{:S(2)}, u32[]{:S(2)}) collective-permute-start(bf16[64,512]{1,0:T(8,128)(2,1)S(1)} %get-tuple-element.28), channel_id=1, source_target_pairs={{0,2},{1,3},{2,0},{3,1},{4,6},{5,7},{6,4},{7,5},{8,10},{9,11},{10,... | collective-permute-start | bytes 196616 | tf_op jit(solution)/shard_map/ppermute | solution.py:19
  9.5 4.3 %collective-permute-start.2 = (bf16[64,512]{1,0:T(8,128)(2,1)S(1)}, bf16[64,512]{1,0:T(8,128)(2,1)S(1)}, u32[]{:S(2)}, u32[]{:S(2)}) collective-permute-start(bf16[64,512]{1,0:T(8,128)(2,1)S(1)} %get-tuple-element.29), channel_id=1, source_target_pairs={{0,3},{1,0},{2,1},{3,2},{4,7},{5,4},{6,5},{7,6},{8,11},{9,8},{10,9... | collective-permute-start | bytes 196616 | tf_op jit(solution)/shard_map/ppermute | solution.py:19
  14.7 46.8 %all-to-all-start = ((bf16[32,8,512]{2,1,0:T(8,128)(2,1)}), bf16[32,8,512]{2,1,0:T(8,128)(2,1)S(1)}, u32[]{:S(2)}, u32[]{:S(2)}) async-start(bf16[32,8,512]{2,1,0:T(8,128)(2,1)} %bitcast.10), calls=%async_computation | async-start | bytes 524288 | tf_op jit(solution)/shard_map/all_to_all | solution.py:13
  40.4 13.0 %collective-permute-start.5 = (bf16[64,512]{1,0:T(8,128)(2,1)S(1)}, bf16[64,512]{1,0:T(8,128)(2,1)S(1)}, u32[]{:S(2)}, u32[]{:S(2)}) collective-permute-start(bf16[64,512]{1,0:T(8,128)(2,1)S(1)} %get-tuple-element.30), channel_id=1, source_target_pairs={{0,3},{1,0},{2,1},{3,2},{4,7},{5,4},{6,5},{7,6},{8,11},{9,8},{10,9... | collective-permute-start | bytes 196616 | tf_op jit(solution)/shard_map/ppermute | solution.py:19
  42.9 10.5 %collective-permute-start.4 = (bf16[64,512]{1,0:T(8,128)(2,1)S(1)}, bf16[64,512]{1,0:T(8,128)(2,1)}, u32[]{:S(2)}, u32[]{:S(2)}) collective-permute-start(bf16[64,512]{1,0:T(8,128)(2,1)S(1)} %get-tuple-element.30), channel_id=1, source_target_pairs={{0,2},{1,3},{2,0},{3,1},{4,6},{5,7},{6,4},{7,5},{8,10},{9,11},{10,... | collective-permute-start | bytes 196616 | tf_op jit(solution)/shard_map/ppermute | solution.py:19
  42.9 10.5 %collective-permute-start.3 = (bf16[64,512]{1,0:T(8,128)(2,1)S(1)}, bf16[64,512]{1,0:T(8,128)(2,1)}, u32[]{:S(2)}, u32[]{:S(2)}) collective-permute-start(bf16[64,512]{1,0:T(8,128)(2,1)S(1)} %get-tuple-element.30), channel_id=1, source_target_pairs={{0,1},{1,2},{2,3},{3,0},{4,5},{5,6},{6,7},{7,4},{8,9},{9,10},{10,1... | collective-permute-start | bytes 196616 | tf_op jit(solution)/shard_map/ppermute | solution.py:19
  46.2 1.1 copy-start.7
  50.5 1.0 copy-start
  51.5 1.0 copy-start.2
  52.5 1.0 copy-start.4
  61.5 7.0 %collective-permute-start.6 = (bf16[128,512]{1,0:T(8,128)(2,1)S(1)}, bf16[128,512]{1,0:T(8,128)(2,1)S(1)}, u32[]{:S(2)}, u32[]{:S(2)}) collective-permute-start(bf16[128,512]{1,0:T(8,128)(2,1)S(1)} %get-tuple-element.32.refs_0_), channel_id=1, source_target_pairs={{0,1},{1,2},{2,3},{3,0},{4,5},{5,6},{6,7},{7,4},{8,9},{9,10},{10,1... | collective-permute-start | bytes 393224 | tf_op jit(solution)/shard_map/ppermute | solution.py:19
  61.8 10.9 %collective-permute-start.7 = (bf16[128,512]{1,0:T(8,128)(2,1)S(1)}, bf16[128,512]{1,0:T(8,128)(2,1)S(1)}, u32[]{:S(2)}, u32[]{:S(2)}) collective-permute-start(bf16[128,512]{1,0:T(8,128)(2,1)S(1)} %get-tuple-element.32.refs_0_), channel_id=1, source_target_pairs={{0,2},{1,3},{2,0},{3,1},{4,6},{5,7},{6,4},{7,5},{8,10},{9,11},{10,... | collective-permute-start | bytes 393224 | tf_op jit(solution)/shard_map/ppermute | solution.py:19
  65.6 7.2 %collective-permute-start.8 = (bf16[128,512]{1,0:T(8,128)(2,1)S(1)}, bf16[128,512]{1,0:T(8,128)(2,1)S(1)}, u32[]{:S(2)}, u32[]{:S(2)}) collective-permute-start(bf16[128,512]{1,0:T(8,128)(2,1)S(1)} %get-tuple-element.32.refs_0_), channel_id=1, source_target_pairs={{0,3},{1,0},{2,1},{3,2},{4,7},{5,4},{6,5},{7,6},{8,11},{9,8},{10,9... | collective-permute-start | bytes 393224 | tf_op jit(solution)/shard_map/ppermute | solution.py:19
  66.5 17.8 %collective-permute-start.12 = (bf16[128,512]{1,0:T(8,128)(2,1)S(1)}, bf16[128,512]{1,0:T(8,128)(2,1)S(1)}, u32[]{:S(2)}, u32[]{:S(2)}) collective-permute-start(bf16[128,512]{1,0:T(8,128)(2,1)S(1)} %get-tuple-element.41.refs_0_), channel_id=1, source_target_pairs={{0,1},{1,2},{2,3},{3,0},{4,5},{5,6},{6,7},{7,4},{8,9},{9,10},{10,1... | collective-permute-start | bytes 393224 | tf_op jit(solution)/shard_map/ppermute | solution.py:19
  68.3 16.2 %collective-permute-start.13 = (bf16[128,512]{1,0:T(8,128)(2,1)S(1)}, bf16[128,512]{1,0:T(8,128)(2,1)S(1)}, u32[]{:S(2)}, u32[]{:S(2)}) collective-permute-start(bf16[128,512]{1,0:T(8,128)(2,1)S(1)} %get-tuple-element.41.refs_0_), channel_id=1, source_target_pairs={{0,2},{1,3},{2,0},{3,1},{4,6},{5,7},{6,4},{7,5},{8,10},{9,11},{10,... | collective-permute-start | bytes 393224 | tf_op jit(solution)/shard_map/ppermute | solution.py:19
  68.5 16.0 %collective-permute-start.14 = (bf16[128,512]{1,0:T(8,128)(2,1)S(1)}, bf16[128,512]{1,0:T(8,128)(2,1)S(1)}, u32[]{:S(2)}, u32[]{:S(2)}) collective-permute-start(bf16[128,512]{1,0:T(8,128)(2,1)S(1)} %get-tuple-element.41.refs_0_), channel_id=1, source_target_pairs={{0,3},{1,0},{2,1},{3,2},{4,7},{5,4},{6,5},{7,6},{8,11},{9,8},{10,9... | collective-permute-start | bytes 393224 | tf_op jit(solution)/shard_map/ppermute | solution.py:19
  72.8 1.2 copy-start.1
  74.0 1.2 copy-start.3
  75.2 1.2 copy-start.5
  78.0 11.1 %collective-permute-start.9 = (bf16[128,512]{1,0:T(8,128)(2,1)S(1)}, bf16[128,512]{1,0:T(8,128)(2,1)S(1)}, u32[]{:S(2)}, u32[]{:S(2)}) collective-permute-start(bf16[128,512]{1,0:T(8,128)(2,1)S(1)} %get-tuple-element.38), channel_id=1, source_target_pairs={{0,1},{1,2},{2,3},{3,0},{4,5},{5,6},{6,7},{7,4},{8,9},{9,10},{10,1... | collective-permute-start | bytes 393224 | tf_op jit(solution)/shard_map/ppermute | solution.py:19
  81.7 9.2 %collective-permute-start.10 = (bf16[128,512]{1,0:T(8,128)(2,1)S(1)}, bf16[128,512]{1,0:T(8,128)(2,1)S(1)}, u32[]{:S(2)}, u32[]{:S(2)}) collective-permute-start(bf16[128,512]{1,0:T(8,128)(2,1)S(1)} %get-tuple-element.39), channel_id=1, source_target_pairs={{0,2},{1,3},{2,0},{3,1},{4,6},{5,7},{6,4},{7,5},{8,10},{9,11},{10,... | collective-permute-start | bytes 393224 | tf_op jit(solution)/shard_map/ppermute | solution.py:19
  84.2 6.6 %collective-permute-start.11 = (bf16[128,512]{1,0:T(8,128)(2,1)S(1)}, bf16[128,512]{1,0:T(8,128)(2,1)S(1)}, u32[]{:S(2)}, u32[]{:S(2)}) collective-permute-start(bf16[128,512]{1,0:T(8,128)(2,1)S(1)} %get-tuple-element.40), channel_id=1, source_target_pairs={{0,3},{1,0},{2,1},{3,2},{4,7},{5,4},{6,5},{7,6},{8,11},{9,8},{10,9... | collective-permute-start | bytes 393224 | tf_op jit(solution)/shard_map/ppermute | solution.py:19
  84.5 17.5 %copy-start.12 = (f32[4,512]{1,0:T(4,128)S(1)}, f32[4,512]{1,0:T(4,128)}, u32[]{:S(2)}) copy-start(f32[4,512]{1,0:T(4,128)} %gather_fusion) | copy-start | bytes 24580
  86.1 16.9 %copy-start.10 = (bf16[4,512,68]{1,2,0:T(8,128)(2,1)S(1)}, bf16[4,512,68]{1,2,0:T(8,128)(2,1)}, u32[]{:S(2)}) copy-start(bf16[4,512,68]{1,2,0:T(8,128)(2,1)} %gather_fusion.1) | copy-start | bytes 835588
  86.1 17.6 %copy-start.15 = (s32[64]{0:T(128)S(1)}, s32[64]{0:T(128)}, u32[]{:S(2)}) copy-start(s32[64]{0:T(128)} %fusion.10) | copy-start | bytes 772
  86.2 46.6 %copy-start.9 = (f32[2048]{0:T(1024)S(1)}, f32[2048]{0:T(1024)}, u32[]{:S(2)}) copy-start(f32[2048]{0:T(1024)} %param.35) | copy-start | bytes 24580
  86.2 6.9 %collective-permute-start.15 = (bf16[128,512]{1,0:T(8,128)(2,1)S(1)}, bf16[128,512]{1,0:T(8,128)(2,1)S(1)}, u32[]{:S(2)}, u32[]{:S(2)}) collective-permute-start(bf16[128,512]{1,0:T(8,128)(2,1)S(1)} %get-tuple-element.46), channel_id=1, source_target_pairs={{0,1},{1,2},{2,3},{3,0},{4,5},{5,6},{6,7},{7,4},{8,9},{9,10},{10,1... | collective-permute-start | bytes 393224 | tf_op jit(solution)/shard_map/ppermute | solution.py:19
  88.0 6.5 %collective-permute-start.16 = (bf16[128,512]{1,0:T(8,128)(2,1)S(1)}, bf16[128,512]{1,0:T(8,128)(2,1)S(1)}, u32[]{:S(2)}, u32[]{:S(2)}) collective-permute-start(bf16[128,512]{1,0:T(8,128)(2,1)S(1)} %get-tuple-element.47), channel_id=1, source_target_pairs={{0,2},{1,3},{2,0},{3,1},{4,6},{5,7},{6,4},{7,5},{8,10},{9,11},{10,... | collective-permute-start | bytes 393224 | tf_op jit(solution)/shard_map/ppermute | solution.py:19
  89.1 5.9 %collective-permute-start.17 = (bf16[128,512]{1,0:T(8,128)(2,1)S(1)}, bf16[128,512]{1,0:T(8,128)(2,1)S(1)}, u32[]{:S(2)}, u32[]{:S(2)}) collective-permute-start(bf16[128,512]{1,0:T(8,128)(2,1)S(1)} %get-tuple-element.48), channel_id=1, source_target_pairs={{0,3},{1,0},{2,1},{3,2},{4,7},{5,4},{6,5},{7,6},{8,11},{9,8},{10,9... | collective-permute-start | bytes 393224 | tf_op jit(solution)/shard_map/ppermute | solution.py:19
  95.9 28.1 %all-to-all-start.1 = ((bf16[32,8,512]{2,1,0:T(8,128)(2,1)}), bf16[32,8,512]{2,1,0:T(8,128)(2,1)S(1)}, u32[]{:S(2)}, u32[]{:S(2)}) async-start(bf16[32,8,512]{2,1,0:T(8,128)(2,1)} %bitcast.13), calls=%async_computation.1 | async-start | bytes 524288 | tf_op jit(solution)/shard_map/all_to_all | solution.py:13
  124.2 6.1 %collective-permute-start.18 = (bf16[64,512]{1,0:T(8,128)(2,1)S(1)}, bf16[64,512]{1,0:T(8,128)(2,1)S(1)}, u32[]{:S(2)}, u32[]{:S(2)}) collective-permute-start(bf16[64,512]{1,0:T(8,128)(2,1)S(1)} %convolution_convert_fusion.refs_0_), channel_id=1, source_target_pairs={{0,1},{1,2},{2,3},{3,0},{4,5},{5,6},{6,7},{7,4},{8,9},{9,10},{10,1... | collective-permute-start | bytes 196616 | tf_op jit(solution)/shard_map/ppermute | solution.py:19
  125.7 6.0 %collective-permute-start.19 = (bf16[64,512]{1,0:T(8,128)(2,1)S(1)}, bf16[64,512]{1,0:T(8,128)(2,1)S(1)}, u32[]{:S(2)}, u32[]{:S(2)}) collective-permute-start(bf16[64,512]{1,0:T(8,128)(2,1)S(1)} %convolution_convert_fusion.refs_0_), channel_id=1, source_target_pairs={{0,2},{1,3},{2,0},{3,1},{4,6},{5,7},{6,4},{7,5},{8,10},{9,11},{10,... | collective-permute-start | bytes 196616 | tf_op jit(solution)/shard_map/ppermute | solution.py:19
  128.5 4.3 %collective-permute-start.20 = (bf16[64,512]{1,0:T(8,128)(2,1)S(1)}, bf16[64,512]{1,0:T(8,128)(2,1)S(1)}, u32[]{:S(2)}, u32[]{:S(2)}) collective-permute-start(bf16[64,512]{1,0:T(8,128)(2,1)S(1)} %convolution_convert_fusion.refs_0_), channel_id=1, source_target_pairs={{0,3},{1,0},{2,1},{3,2},{4,7},{5,4},{6,5},{7,6},{8,11},{9,8},{10,9... | collective-permute-start | bytes 196616 | tf_op jit(solution)/shard_map/ppermute | solution.py:19
